TPU v7x, 256 devices: a whole 4x4x8 slice. The times are simulated.
256 devices in a mesh: kv: 32 (over z, y), tp: 8 (over x, core).
Axes of the slice: x: 4, y: 4, z: 8, core: 2. Of those that a mesh axis runs over, the one named last changes fastest.
Arguments:
- tokens: bfloat16 [64, 4096], P(None, ('kv', 'tp')), may hold values from -8 to 8
- gate_weights: bfloat16 [2, 4096, 11264], P(None, None, ('kv', 'tp')), may hold values from -0.09375 to 0.09375
- up_weights: bfloat16 [2, 4096, 11264], P(None, None, ('kv', 'tp')), may hold values from -0.09375 to 0.09375
- down_weights: bfloat16 [2, 11264, 4096], P(None, ('kv', 'tp')), may hold values from -1 to 1
- norm_gain: bfloat16 [3, 4096], P(None, ('kv', 'tp')), may hold values from 0.25 to 4.5
- norm_bias: bfloat16 [3, 4096], P(None, ('kv', 'tp')), may hold values from -3 to 3
- query_weight: bfloat16 [4096, 4096], P('kv', 'tp'), may hold values from -0.09375 to 0.09375
- forget_weight: bfloat16 [4096, 4096], P('kv', 'tp'), may hold values from -0.09375 to 0.09375
- input_weight: bfloat16 [4096, 4096], P('kv', 'tp'), may hold values from -0.09375 to 0.09375
- outgate_weight: bfloat16 [4096, 4096], P('kv', 'tp'), may hold values from -0.09375 to 0.09375
- lower_bound: float32 [4096], P('tp'), may hold values from 0.05 to 0.9
- head_gain: float32 [4096], P('tp'), may hold values from 0.1 to 1.9
- out_weight: bfloat16 [4096, 4096], P('tp'), may hold values from -0.25 to 0.25
- state: float32 [64, 32, 128, 128], P('kv', 'tp'), may hold values from -3 to 3
Outputs:
- mixed: bfloat16 [64, 4096], P(None, ('kv', 'tp'))
- new_state: float32 [64, 32, 128, 128], P('kv', 'tp')
All inputs are finite; a program needn't handle non-finite values.
Results may differ from a plain program's by a relative error of at most 0.022.
Values may be sent and summed in bfloat16 or wider, within the bound.
No kernel may reach another device: no remote copies, remote signals or barrier semaphores. Data moves between devices by JAX's collectives and lax.ppermute only.
A program may use at most 64 MiB of HBM per device.

v0:
```python
import jax
import jax.numpy as jnp
from jax import lax
from jax.sharding import Mesh
from jax.sharding import PartitionSpec as P

HEAD = 128
KV_TP = ("kv_0", "kv_1", "tp_0", "tp_1")
KV = ("kv_0", "kv_1")
TP = ("tp_0", "tp_1")


residual_scale = 8.0**0.25
norm_eps = 1e-05
head_eps = 1e-06


def turned_gather(arrays, axis, dims):
    turned = [jnp.moveaxis(a, dim, 0) for a, dim in zip(arrays, dims)]
    both = jnp.concatenate([t.reshape(len(t), -1) for t in turned], axis=1)
    whole, at, gathered = (lax.all_gather(both, axis, axis=0, tiled=True), 0, [])
    for t, dim in zip(turned, dims):
        section = whole[:, at : at + t[0].size].reshape(-1, *t.shape[1:])
        gathered.append(jnp.moveaxis(section, 0, dim))
        at += t[0].size
    return tuple(gathered)


def rows_for(lines, count):
    spare = -lines.shape[0] % count
    if not spare:
        return lines
    return jnp.concatenate([lines, jnp.zeros((spare, *lines.shape[1:]), lines.dtype)])


def from_everyone(x, axis):
    copies = jnp.broadcast_to(x, (lax.axis_size(axis), *x.shape))
    return lax.all_to_all(copies, axis, split_axis=0, concat_axis=0, tiled=True)


def laid_out(blocks, dim):
    blocks = jnp.moveaxis(blocks, 0, dim)
    shape = blocks.shape
    return blocks.reshape(*shape[:dim], shape[dim] * shape[dim + 1], *shape[dim + 2 :])


def whole_of(x, axes, dim):
    far, near = axes
    leading = from_everyone(x, far)
    blocks = jnp.swapaxes(from_everyone(leading, near), 0, 1)
    return laid_out(blocks.reshape(-1, *x.shape), dim)


def in_blocks(x, dim, count):
    before, after = (x.shape[:dim], x.shape[dim + 1 :])
    return jnp.moveaxis(x.reshape(*before, count, -1, *after), dim, 0)


def sum_at_owner(x, axis, dim):
    blocks = in_blocks(x, dim, lax.axis_size(axis))
    arrived = lax.all_to_all(blocks, axis, split_axis=0, concat_axis=0, tiled=True)
    return arrived.sum(axis=0)


def sum_by_axis(x, axes, dim):
    far, near = axes
    blocks = in_blocks(x, dim, lax.axis_size(far))
    nearer = sum_at_owner(blocks, near, dim + 1)
    arrived = lax.all_to_all(nearer, far, split_axis=0, concat_axis=0, tiled=True)
    return arrived.sum(axis=0)


def nested_sum(x, axes):
    lines = x.reshape(-1)
    padded = rows_for(lines, lax.axis_size(axes[0]) * lax.axis_size(axes[1]))
    whole = whole_of(sum_by_axis(padded, axes, 0), axes, 0)
    return lax.slice_in_dim(whole, 0, len(lines)).reshape(x.shape)


def sum_at_owner_2(x, axis, dim):
    blocks = in_blocks(x, dim, lax.axis_size(axis))
    arrived = lax.all_to_all(blocks, axis, split_axis=0, concat_axis=0, tiled=True)
    return arrived.astype(jnp.float32).sum(axis=0)


def gathered_copies(x, axis, dim):
    blocks = from_everyone(x, axis)
    return laid_out(blocks, dim)


def whole_norm(stream, gain_row, bias_row):
    row_mean = jnp.mean(stream, axis=-1, keepdims=True)
    centred = stream - row_mean
    spread = jnp.mean(centred * centred, axis=-1, keepdims=True)
    return centred * lax.rsqrt(spread + norm_eps) * gain_row.astype(jnp.float32) + bias_row.astype(
        jnp.float32
    )


def ffn_partial(whole_rows, gate_w, up_w, down_w):
    gate_proj = jnp.dot(whole_rows, gate_w, preferred_element_type=jnp.float32)
    up_proj = jnp.dot(whole_rows, up_w, preferred_element_type=jnp.float32)
    hidden = (jax.nn.silu(gate_proj) * up_proj).astype(jnp.bfloat16)
    return jnp.dot(hidden, down_w, preferred_element_type=jnp.float32)


def local(
    tokens,
    gate_weights,
    up_weights,
    down_weights,
    norm_gain,
    norm_bias,
    query_weight,
    forget_weight,
    input_weight,
    outgate_weight,
    lower_bound,
    head_gain,
    out_weight,
    state,
):
    own_cols = tokens.shape[1]
    col_offset = lax.axis_index(KV_TP) * own_cols
    whole_tokens, whole_gain, whole_bias = turned_gather(
        (tokens, norm_gain, norm_bias), KV_TP, (1, 1, 1)
    )

    def finish(partial_value, residual_whole, index, want_whole):
        total = nested_sum(partial_value, (("kv_0", "kv_1"), ("tp_0", "tp_1")))
        stream = residual_scale * residual_whole + 0.5 * total
        normed = whole_norm(stream, whole_gain[index], whole_bias[index]).astype(jnp.bfloat16)
        if want_whole:
            return normed
        return lax.dynamic_slice_in_dim(normed, col_offset, own_cols, 1)

    partial_one = ffn_partial(whole_tokens, gate_weights[0], up_weights[0], down_weights[0])
    normed_one = finish(partial_one, whole_tokens.astype(jnp.float32), 0, True)
    seq_count = state.shape[0]
    head_count = state.shape[1]
    head_cols = query_weight.shape[1]
    weight_rows = query_weight.shape[0]
    seq_offset = lax.axis_index(KV) * seq_count
    block_rows = lax.dynamic_slice_in_dim(
        normed_one, lax.axis_index(KV) * weight_rows, weight_rows, 1
    )
    weights = (query_weight, forget_weight, input_weight, outgate_weight)
    projected = sum_at_owner_2(
        jnp.concatenate(
            [jnp.dot(block_rows, weight, preferred_element_type=jnp.float32) for weight in weights],
            axis=1,
        ).astype(jnp.bfloat16),
        KV,
        0,
    ).astype(jnp.bfloat16)
    query_pre = projected[:, :head_cols].astype(jnp.float32).reshape(seq_count, head_count, HEAD)
    forget_pre = (
        projected[:, head_cols : 2 * head_cols]
        .astype(jnp.float32)
        .reshape(seq_count, head_count, HEAD)
    )
    input_pre = (
        projected[:, 2 * head_cols : 3 * head_cols]
        .astype(jnp.float32)
        .reshape(seq_count, head_count, HEAD)
    )
    outgate_pre = projected[:, 3 * head_cols :].astype(jnp.float32)
    low_bound = lower_bound.reshape(head_count, HEAD)
    forget = low_bound + (1.0 - low_bound) * jax.nn.sigmoid(forget_pre)
    key_part = (1.0 - low_bound) * jax.nn.sigmoid(-forget_pre)
    updated = forget[..., None] * state + key_part[..., None] * input_pre[:, :, None, :]
    readout = jnp.einsum(
        "shd,shde->she", jax.nn.silu(query_pre), updated, precision=lax.Precision.HIGHEST
    )
    readout = readout * lax.rsqrt(jnp.mean(readout * readout, axis=-1, keepdims=True) + head_eps)
    gated_out = (
        readout.reshape(seq_count, head_cols) * head_gain * jax.nn.silu(outgate_pre)
    ).astype(jnp.bfloat16)
    mixer_part = jnp.dot(gated_out, out_weight, preferred_element_type=jnp.float32)
    head_sum = sum_at_owner_2(mixer_part.astype(jnp.bfloat16), TP, 1)
    piece_cols = head_sum.shape[1]
    own_normed = lax.dynamic_slice_in_dim(normed_one, seq_offset, seq_count, 0)
    own_normed = lax.dynamic_slice_in_dim(
        own_normed, lax.axis_index(TP) * piece_cols, piece_cols, 1
    )
    stream_own = (residual_scale * own_normed.astype(jnp.float32) + head_sum).astype(jnp.bfloat16)
    seq_rows = gathered_copies(stream_own, TP, 1)
    stream_two = gathered_copies(seq_rows, KV, 0)
    normed_two = whole_norm(stream_two.astype(jnp.float32), whole_gain[1], whole_bias[1]).astype(
        jnp.bfloat16
    )
    partial_two = ffn_partial(normed_two, gate_weights[1], up_weights[1], down_weights[1])
    mixed = finish(partial_two, normed_two.astype(jnp.float32), 2, False)
    return (mixed, updated)


def solution(mesh):
    finer = Mesh(mesh.devices.reshape(8, 4, 4, 2), ("kv_0", "kv_1", "tp_0", "tp_1"))
    in_specs = (
        P(None, KV_TP),
        P(None, None, KV_TP),
        P(None, None, KV_TP),
        P(None, KV_TP, None),
        P(None, KV_TP),
        P(None, KV_TP),
        P(KV, TP),
        P(KV, TP),
        P(KV, TP),
        P(KV, TP),
        P(TP),
        P(TP),
        P(TP, None),
        P(KV, TP, None, None),
    )
    out_specs = (P(None, KV_TP), P(KV, TP, None, None))
    return jax.shard_map(local, mesh=finer, in_specs=in_specs, out_specs=out_specs, check_vma=False)
```

profile of v0, /device:TPU:1, one launch (start us, length us, event | category | flops | bytes accessed | tf_op | source)
XLA Modules:
  0.0 302.1 jit_solution(11334063490553480618)
XLA Ops:
  0.7 0.8 copy.27
  1.5 0.8 copy.26
  2.3 0.8 pad_maximum_fusion.1
  3.0 67.7 %all_gather.3 = bf16[4096,70]{1,0:T(8,128)(2,1)S(1)} all-gather(bf16[16,70]{1,0:T(8,128)(2,1)S(1)} %pad_maximum_fusion.1), channel_id=1, replica_groups=mesh['kv_0'=8,'kv_1'=4,'tp_0'=4,'tp_1'=2] {'kv_0','kv_1','tp_0','tp_1'}, dimensions={0}, use_global_device_ids=true | all-gather | bytes 575680 | tf_op jit(solution)/shard_map/all_gather | solution.py:21
  70.8 4.6 %fusion.54 = (bf16[1,44,4096]{2,0,1:T(2,128)(2,1)}, bf16[1,44,4096]{2,0,1:T(2,128)(2,1)}) fusion(bf16[2,44,4096]{2,0,1:T(2,128)(2,1)} %param.17), kind=kLoop, calls=%fused_computation.115 | loop fusion | bytes 1441792 | tf_op jit(solution)/shard_map/slice | solution.py:192
  75.3 2.8 fusion.53
  78.1 1.9 fusion.52
  80.6 2.2 fusion.2
  83.1 0.6 copy.77
  83.7 18.4 %all_to_all.76 = f32[8,32,1024]{2,1,0:T(8,128)S(1)} all-to-all(f32[8,32,1024]{2,1,0:T(8,128)S(1)} %bitcast.90), channel_id=1, replica_groups=mesh['kv_0'=8,'kv_1'=4,'tp_0'=4,'tp_1'=2] {'tp_0','tp_1'}, dimensions={0} | all-to-all | bytes 2097152 | tf_op jit(solution)/shard_map/all_to_all | solution.py:61
  102.2 14.2 %all_to_all.77 = f32[32,1,1024]{2,1,0:T(1,128)S(1)} all-to-all(f32[32,1,1024]{2,1,0:T(1,128)S(1)} %all_to_all.49), channel_id=1, replica_groups=mesh['kv_0'=8,'kv_1'=4,'tp_0'=4,'tp_1'=2] {'kv_0','kv_1'}, dimensions={0} | all-to-all | bytes 262144 | tf_op jit(solution)/shard_map/all_to_all | solution.py:69
  116.6 0.7 broadcast_in_dim.12
  117.3 3.9 %all-to-all-start.2 = ((f32[32,1,1024]{2,1,0:T(1,128)}), f32[32,1,1024]{2,1,0:T(1,128)S(1)}, u32[]{:S(2)}, u32[]{:S(2)}) async-start(f32[32,1,1024]{2,1,0:T(1,128)} %broadcast_in_dim.12), calls=%async_computation.2 | async-start | bytes 262144 | tf_op jit(solution)/shard_map/all_to_all | solution.py:38
  121.5 9.1 %all-to-all-done.2 = f32[32,1,1024]{2,1,0:T(1,128)S(1)} async-done(((f32[32,1,1024]{2,1,0:T(1,128)}), f32[32,1,1024]{2,1,0:T(1,128)S(1)}, u32[]{:S(2)}, u32[]{:S(2)}) %all-to-all-start.2) | async-done | bytes 131104 | tf_op jit(solution)/shard_map/all_to_all | solution.py:38
  130.6 1.1 broadcast_in_dim.13
  131.7 7.1 %all-to-all-start.3 = ((f32[8,32,1024]{2,1,0:T(8,128)}), f32[8,32,1024]{2,1,0:T(8,128)S(1)}, u32[]{:S(2)}, u32[]{:S(2)}) async-start(f32[8,32,1024]{2,1,0:T(8,128)} %broadcast_in_dim.13), calls=%async_computation.3 | async-start | bytes 2097152 | tf_op jit(solution)/shard_map/all_to_all | solution.py:38
  139.5 3.4 %convert_reduce_fusion = (f32[4096]{0:T(1024)S(1)}, f32[4096]{0:T(1024)S(1)}, f32[4096]{0:T(1024)S(1)}, f32[4096]{0:T(1024)S(1)}, f32[4096]{0:T(1024)S(1)}, /*index=5*/f32[4096]{0:T(1024)S(1)}) fusion(bf16[3,4096]{0,1:T(8,128)(2,1)S(1)} %get-tuple-element.13, bf16[3,4096]{0,1:T(8,128)(2,1)S(1)} %get-tuple-element.12), kind=kLoop, calls=%fused_computation.1 | loop fusion | flops 24576 | bytes 147456 | tf_op jit(solution)/shard_map/add | solution.py:95
  142.8 11.0 %all-to-all-done.3 = f32[8,32,1024]{2,1,0:T(8,128)S(1)} async-done(((f32[8,32,1024]{2,1,0:T(8,128)}), f32[8,32,1024]{2,1,0:T(8,128)S(1)}, u32[]{:S(2)}, u32[]{:S(2)}) %all-to-all-start.3) | async-done | bytes 1048608 | tf_op jit(solution)/shard_map/all_to_all | solution.py:38
  153.9 0.6 copy.33
  156.8 0.9 pad_maximum_fusion
  157.7 3.9 %all-to-all-start.4 = ((bf16[32,2,2048]{2,1,0:T(2,128)(2,1)}), bf16[32,2,2048]{2,1,0:T(2,128)(2,1)S(1)}, u32[]{:S(2)}, u32[]{:S(2)}) async-start(bf16[32,2,2048]{2,1,0:T(2,128)(2,1)} %pad_maximum_fusion), calls=%async_computation.4 | async-start | bytes 524288 | tf_op jit(solution)/shard_map/all_to_all | solution.py:82
  161.6 11.4 %all-to-all-done.4 = bf16[32,2,2048]{2,1,0:T(2,128)(2,1)S(1)} async-done(((bf16[32,2,2048]{2,1,0:T(2,128)(2,1)}), bf16[32,2,2048]{2,1,0:T(2,128)(2,1)S(1)}, u32[]{:S(2)}, u32[]{:S(2)}) %all-to-all-start.4) | async-done | bytes 262176 | tf_op jit(solution)/shard_map/all_to_all | solution.py:82
  173.7 0.8 copy-done.3
  175.2 3.5 %convolution_convert_fusion = bf16[2,4096]{1,0:T(2,128)(2,1)} fusion(bf16[512,4096]{1,0:T(8,128)(2,1)} %param.26, f32[1,2,4,128]{3,2,1,0:T(4,128)S(1)} %multiply_bitcast_fusion.2, bf16[2,2048]{1,0:T(2,128)(2,1)S(1)} %reduce_sum.124, f32[512]{0:T(512)S(1)} %copy-done.12), kind=kOutput, calls=%fused_computation | convolution fusion | flops 8404992 | bytes 4218880 | tf_op jit(solution)/shard_map/dot_general | solution.py:179
  178.7 5.9 %all-to-all-start.5 = ((bf16[8,2,512]{2,1,0:T(2,128)(2,1)}), bf16[8,2,512]{2,1,0:T(2,128)(2,1)S(1)}, u32[]{:S(2)}, u32[]{:S(2)}) async-start(bf16[8,2,512]{2,1,0:T(2,128)(2,1)} %bitcast.17), calls=%async_computation.5 | async-start | bytes 32768 | tf_op jit(solution)/shard_map/all_to_all | solution.py:82
  184.6 4.7 %all-to-all-done.5 = bf16[8,2,512]{2,1,0:T(2,128)(2,1)S(1)} async-done(((bf16[8,2,512]{2,1,0:T(2,128)(2,1)}), bf16[8,2,512]{2,1,0:T(2,128)(2,1)S(1)}, u32[]{:S(2)}, u32[]{:S(2)}) %all-to-all-start.5) | async-done | bytes 16416 | tf_op jit(solution)/shard_map/all_to_all | solution.py:82
  189.4 7.7 %all_to_all.78 = bf16[8,2,512]{2,1,0:T(2,128)(2,1)S(1)} all-to-all(bf16[8,2,512]{2,1,0:T(2,128)(2,1)S(1)} %broadcast_in_dim.14), channel_id=1, replica_groups=mesh['kv_0'=8,'kv_1'=4,'tp_0'=4,'tp_1'=2] {'tp_0','tp_1'}, dimensions={0} | all-to-all | bytes 32768 | tf_op jit(solution)/shard_map/all_to_all | solution.py:38
  197.6 19.6 %all_to_all.79 = bf16[32,2,4096]{2,1,0:T(2,128)(2,1)S(1)} all-to-all(bf16[32,2,4096]{2,1,0:T(2,128)(2,1)S(1)} %broadcast_in_dim.15), channel_id=1, replica_groups=mesh['kv_0'=8,'kv_1'=4,'tp_0'=4,'tp_1'=2] {'kv_0','kv_1'}, dimensions={0} | all-to-all | bytes 1048576 | tf_op jit(solution)/shard_map/all_to_all | solution.py:38
  217.7 0.8 multiply_reduce_fusion.1
  218.5 0.9 add_convert_fusion
  220.2 2.2 fusion.3
  222.8 0.6 copy.76
  223.4 19.7 %all_to_all.80 = f32[8,32,1024]{2,1,0:T(8,128)S(1)} all-to-all(f32[8,32,1024]{2,1,0:T(8,128)S(1)} %bitcast.91), channel_id=1, replica_groups=mesh['kv_0'=8,'kv_1'=4,'tp_0'=4,'tp_1'=2] {'tp_0','tp_1'}, dimensions={0} | all-to-all | bytes 2097152 | tf_op jit(solution)/shard_map/all_to_all | solution.py:61
  243.3 13.5 %all_to_all.81 = f32[32,1,1024]{2,1,0:T(1,128)S(1)} all-to-all(f32[32,1,1024]{2,1,0:T(1,128)S(1)} %all_to_all.59), channel_id=1, replica_groups=mesh['kv_0'=8,'kv_1'=4,'tp_0'=4,'tp_1'=2] {'kv_0','kv_1'}, dimensions={0} | all-to-all | bytes 262144 | tf_op jit(solution)/shard_map/all_to_all | solution.py:69
  256.9 0.7 broadcast_in_dim.16
  257.6 3.9 %all-to-all-start.10 = ((f32[32,1,1024]{2,1,0:T(1,128)}), f32[32,1,1024]{2,1,0:T(1,128)S(1)}, u32[]{:S(2)}, u32[]{:S(2)}) async-start(f32[32,1,1024]{2,1,0:T(1,128)} %broadcast_in_dim.16), calls=%async_computation.10 | async-start | bytes 262144 | tf_op jit(solution)/shard_map/all_to_all | solution.py:38
  262.0 8.9 %all-to-all-done.10 = f32[32,1,1024]{2,1,0:T(1,128)S(1)} async-done(((f32[32,1,1024]{2,1,0:T(1,128)}), f32[32,1,1024]{2,1,0:T(1,128)S(1)}, u32[]{:S(2)}, u32[]{:S(2)}) %all-to-all-start.10) | async-done | bytes 131104 | tf_op jit(solution)/shard_map/all_to_all | solution.py:38
  270.9 1.2 broadcast_in_dim.17
  272.1 7.1 %all-to-all-start.11 = ((f32[8,32,1024]{2,1,0:T(8,128)}), f32[8,32,1024]{2,1,0:T(8,128)S(1)}, u32[]{:S(2)}, u32[]{:S(2)}) async-start(f32[8,32,1024]{2,1,0:T(8,128)} %broadcast_in_dim.17), calls=%async_computation.11 | async-start | bytes 2097152 | tf_op jit(solution)/shard_map/all_to_all | solution.py:38
  279.2 1.2 convert_multiply_fusion
  280.4 13.8 %all-to-all-done.11 = f32[8,32,1024]{2,1,0:T(8,128)S(1)} async-done(((f32[8,32,1024]{2,1,0:T(8,128)}), f32[8,32,1024]{2,1,0:T(8,128)S(1)}, u32[]{:S(2)}, u32[]{:S(2)}) %all-to-all-start.11) | async-done | bytes 1048608 | tf_op jit(solution)/shard_map/all_to_all | solution.py:38
  294.3 0.6 copy.39
  294.9 1.5 mul.305
  296.4 0.8 mul.307
  297.2 1.4 fusion.6
  298.8 1.7 multiply_reduce_fusion
  300.6 0.9 fusion.12
  301.5 0.7 copy.41
  (89 shorter events, 8.9 us)
Async XLA Ops:
  0.6 155.3 %copy-start = (bf16[128,512]{1,0:T(8,128)(2,1)S(1)}, bf16[128,512]{1,0:T(8,128)(2,1)}, u32[]{:S(2)}) copy-start(bf16[128,512]{1,0:T(8,128)(2,1)} %param.23) | copy-start | bytes 393220
  0.6 74.7 %copy-start.1 = (bf16[2,4096,44]{1,0,2:T(2,128)(2,1)S(1)}, bf16[2,4096,44]{1,0,2:T(2,128)(2,1)}, u32[]{:S(2)}) copy-start(bf16[2,4096,44]{1,0,2:T(2,128)(2,1)} %param.16) | copy-start | bytes 2162692
  75.3 2.8 copy-start.2
  78.1 2.4 copy-start.6
  117.3 13.3 %all-to-all-start.2 = ((f32[32,1,1024]{2,1,0:T(1,128)}), f32[32,1,1024]{2,1,0:T(1,128)S(1)}, u32[]{:S(2)}, u32[]{:S(2)}) async-start(f32[32,1,1024]{2,1,0:T(1,128)} %broadcast_in_dim.12), calls=%async_computation.2 | async-start | bytes 262144 | tf_op jit(solution)/shard_map/all_to_all | solution.py:38
  131.7 22.1 %all-to-all-start.3 = ((f32[8,32,1024]{2,1,0:T(8,128)}), f32[8,32,1024]{2,1,0:T(8,128)S(1)}, u32[]{:S(2)}, u32[]{:S(2)}) async-start(f32[8,32,1024]{2,1,0:T(8,128)} %broadcast_in_dim.13), calls=%async_computation.3 | async-start | bytes 2097152 | tf_op jit(solution)/shard_map/all_to_all | solution.py:38
  155.3 0.9 copy-start.8
  155.3 1.1 copy-start.9
  155.3 1.3 copy-start.10
  155.6 6.0 %copy-start.11 = (f32[512]{0:T(512)S(1)}, f32[512]{0:T(512)}, u32[]{:S(2)}) copy-start(f32[512]{0:T(512)} %param.24) | copy-start | bytes 6148
  155.6 17.7 %copy-start.7 = (f32[2,4,128,128]{3,2,1,0:T(8,128)S(1)}, f32[2,4,128,128]{3,2,1,0:T(8,128)}, u32[]{:S(2)}) copy-start(f32[2,4,128,128]{3,2,1,0:T(8,128)} %param.27) | copy-start | bytes 1572868
  156.1 19.1 %copy-start.12 = (f32[512]{0:T(512)S(1)}, f32[512]{0:T(512)}, u32[]{:S(2)}) copy-start(f32[512]{0:T(512)} %param.25) | copy-start | bytes 6148
  157.7 15.3 %all-to-all-start.4 = ((bf16[32,2,2048]{2,1,0:T(2,128)(2,1)}), bf16[32,2,2048]{2,1,0:T(2,128)(2,1)S(1)}, u32[]{:S(2)}, u32[]{:S(2)}) async-start(bf16[32,2,2048]{2,1,0:T(2,128)(2,1)} %pad_maximum_fusion), calls=%async_computation.4 | async-start | bytes 524288 | tf_op jit(solution)/shard_map/all_to_all | solution.py:82
  173.7 0.8 copy-start.3
  178.7 10.6 %all-to-all-start.5 = ((bf16[8,2,512]{2,1,0:T(2,128)(2,1)}), bf16[8,2,512]{2,1,0:T(2,128)(2,1)S(1)}, u32[]{:S(2)}, u32[]{:S(2)}) async-start(bf16[8,2,512]{2,1,0:T(2,128)(2,1)} %bitcast.17), calls=%async_computation.5 | async-start | bytes 32768 | tf_op jit(solution)/shard_map/all_to_all | solution.py:82
  197.6 22.1 %copy-start.5 = (bf16[1,4096,44]{1,0,2:T(2,128)(2,1)S(1)}, bf16[1,4096,44]{1,0,2:T(2,128)(2,1)}, u32[]{:S(2)}) copy-start(bf16[1,4096,44]{1,0,2:T(2,128)(2,1)} %get-tuple-element.14) | copy-start | bytes 1081348
  217.2 3.1 %copy-start.4 = (bf16[1,44,4096]{2,0,1:T(2,128)(2,1)S(1)}, bf16[1,44,4096]{2,0,1:T(2,128)(2,1)}, u32[]{:S(2)}) copy-start(bf16[1,44,4096]{2,0,1:T(2,128)(2,1)} %get-tuple-element.18) | copy-start | bytes 1081348
  257.6 13.3 %all-to-all-start.10 = ((f32[32,1,1024]{2,1,0:T(1,128)}), f32[32,1,1024]{2,1,0:T(1,128)S(1)}, u32[]{:S(2)}, u32[]{:S(2)}) async-start(f32[32,1,1024]{2,1,0:T(1,128)} %broadcast_in_dim.16), calls=%async_computation.10 | async-start | bytes 262144 | tf_op jit(solution)/shard_map/all_to_all | solution.py:38
  272.1 22.1 %all-to-all-start.11 = ((f32[8,32,1024]{2,1,0:T(8,128)}), f32[8,32,1024]{2,1,0:T(8,128)S(1)}, u32[]{:S(2)}, u32[]{:S(2)}) async-start(f32[8,32,1024]{2,1,0:T(8,128)} %broadcast_in_dim.17), calls=%async_computation.11 | async-start | bytes 2097152 | tf_op jit(solution)/shard_map/all_to_all | solution.py:38
where the time goes:
time: 303 us; the launch traced here: 302 us
  blocking collectives  161 us (53%)
  waiting for transfers between devices  58.8 us (19%)
  starting transfers between devices  31.7 us (10%)
  local copies, waits for them, and re-layouts  24.7 us (8%)
  other arithmetic  14.9 us (5%)
  matrix products  10 us (3%)
    all_gather x1, blocking collectives, turned_gather(): lax.all_gather(both, axis, axis=0, tiled=True)  67.7 us
    all_to_all x4, waiting for transfers between devices, from_everyone(): return lax.all_to_all(copies, axis, split_axis=0, concat_axis=0, tiled=True)  42.7 us
    all_to_all x2, blocking collectives, sum_at_owner(): lax.all_to_all(blocks, axis, split_axis=0, concat_axis=0, tiled=True)  38.1 us
    all_to_all x2, blocking collectives, sum_by_axis(): lax.all_to_all(nearer, far, split_axis=0, concat_axis=0, tiled=True)  27.8 us
    all_to_all x2, blocking collectives, from_everyone(): return lax.all_to_all(copies, axis, split_axis=0, concat_axis=0, tiled=True)  27.3 us
    all_to_all x4, starting transfers between devices, from_everyone(): return lax.all_to_all(copies, axis, split_axis=0, concat_axis=0, tiled=True)  22 us
    all_to_all x2, waiting for transfers between devices, sum_at_owner_2(): lax.all_to_all(blocks, axis, split_axis=0, concat_axis=0, tiled=True)  16.1 us
    all_to_all x2, starting transfers between devices, sum_at_owner_2(): lax.all_to_all(blocks, axis, split_axis=0, concat_axis=0, tiled=True)  9.75 us
  transfers between devices with their start and end apart: 6, of which 6 were waited for; matrix products, arithmetic and copies ran while one was open for 2% of the time, Pallas kernels for 0%

commit v1 on v0

v1 whole, which is shorter than its diff:
```python
import jax
import jax.numpy as jnp
from jax import lax
from jax.sharding import Mesh
from jax.sharding import PartitionSpec as P

HEAD = 128
LANES = 128
KV_TP = ("kv_0", "kv_1", "tp_0", "tp_1")
KV = ("kv_0", "kv_1")
TP = ("tp_0", "tp_1")
CHIPS = ("kv_0", "kv_1", "tp_0")
CORE = "tp_1"
SWAP = [(0, 1), (1, 0)]

residual_scale = 8.0**0.25
norm_eps = 1e-05
head_eps = 1e-06
bf16 = jnp.bfloat16
f32 = jnp.float32


def exchange(blocks, axes):
    return lax.all_to_all(blocks, axes, split_axis=0, concat_axis=0, tiled=True)


def to_everyone(block, axes, count):
    return exchange(jnp.broadcast_to(block[None], (count, *block.shape)), axes)


def rows_of(lines, count):
    return jnp.pad(lines, ((0, count - lines.shape[0]), (0, LANES - lines.shape[1])))


def ffn_partial(whole_rows, gate_w, up_w, down_w):
    gate_proj = jnp.dot(whole_rows, gate_w, preferred_element_type=f32)
    up_proj = jnp.dot(whole_rows, up_w, preferred_element_type=f32)
    hidden = (jax.nn.silu(gate_proj) * up_proj).astype(bf16)
    return jnp.dot(hidden, down_w, preferred_element_type=f32)


def local(
    tokens,
    gate_weights,
    up_weights,
    down_weights,
    norm_gain,
    norm_bias,
    query_weight,
    forget_weight,
    input_weight,
    outgate_weight,
    lower_bound,
    head_gain,
    out_weight,
    state,
):
    batch, own_cols = tokens.shape
    seqs, heads = state.shape[:2]
    kv_count, tp_count = lax.axis_size(KV), lax.axis_size(TP)
    x_count = tp_count // 2
    chip_count = kv_count * x_count
    half = batch // 2
    width = own_cols * kv_count * tp_count
    kv, tp, core = lax.axis_index(KV), lax.axis_index(TP), lax.axis_index(CORE)

    turned = tokens.reshape(kv_count, 2, own_cols).swapaxes(0, 1).reshape(batch, own_cols)
    lines = jnp.concatenate([turned, norm_gain, norm_bias, jnp.zeros((2, own_cols), bf16)])
    place = (
        lax.broadcasted_iota(jnp.int32, (own_cols, LANES), 1)
        == lax.broadcasted_iota(jnp.int32, (own_cols, LANES), 0) + tp * own_cols
    ).astype(bf16)
    placed = jnp.dot(lines, place, preferred_element_type=f32).astype(bf16)
    block = lax.all_gather(placed, TP, axis=0).astype(f32).sum(axis=0).astype(bf16)
    own_half = lax.dynamic_slice_in_dim(block, core * half, half, 0)
    arrived = to_everyone(jnp.concatenate([own_half, block[batch:]]), KV, kv_count)
    both = lax.all_gather(arrived, CORE, axis=0)
    whole_tokens = both[:, :, :half].swapaxes(1, 2).reshape(batch, width)
    params = both[0, :, half:].astype(f32)

    def sum_over_kv(partial_value, extra):
        pieces = partial_value.astype(bf16).reshape(2, half, kv_count, LANES).swapaxes(1, 2)
        kept = lax.dynamic_index_in_dim(pieces, core, 0, keepdims=False)
        sent = lax.dynamic_index_in_dim(pieces, 1 - core, 0, keepdims=False)
        paired = (kept.astype(f32) + lax.ppermute(sent, CORE, SWAP).astype(f32)).astype(bf16)
        if extra is not None:
            paired = jnp.concatenate([paired, extra], axis=1)
        return exchange(paired, KV).astype(f32).sum(axis=0)

    def over_tp(lines):
        gathered = lax.all_gather(lines, TP, axis=0)
        return gathered.reshape(x_count, 2, *lines.shape)

    partial_one = ffn_partial(whole_tokens, gate_weights[0], up_weights[0], down_weights[0])
    weights = (query_weight, forget_weight, input_weight, outgate_weight)
    all_weights = jnp.concatenate(weights, axis=1)
    chunk_count = all_weights.shape[1] // LANES
    share = kv_count // chunk_count
    gain_one, bias_one = block[batch : batch + 1], block[batch + 3 : batch + 4]
    bias_part = jnp.dot(bias_one, all_weights, preferred_element_type=f32)
    bias_rows = jnp.repeat(bias_part.reshape(chunk_count, 1, LANES), share, axis=0).astype(bf16)
    row_sum = partial_one.sum(axis=1)
    high = row_sum.astype(bf16)
    low = (row_sum - high.astype(f32)).astype(bf16)
    sum_row = jnp.broadcast_to(jnp.concatenate([high, low])[None, None], (kv_count, 1, LANES))
    extra = jnp.concatenate([sum_row, bias_rows, jnp.zeros((kv_count, 6, LANES), bf16)], axis=1)
    arrived = sum_over_kv(partial_one, extra)
    bias_own = arrived[half + 1 : half + 2] / share
    gathered = over_tp(arrived[: half + 8])
    total = gathered[:, :, :half].sum(axis=0).reshape(batch, LANES)
    total_row = gathered[:, :, half].sum(axis=(0, 1))
    stream_one = residual_scale * block[:batch].astype(f32) + 0.5 * total
    row_mean = (
        residual_scale * whole_tokens.astype(f32).sum(axis=1)
        + 0.5 * (total_row[:batch] + total_row[batch:])
    ) / width
    centred = stream_one - row_mean[:, None]

    scaled = (centred * gain_one.astype(f32)).astype(bf16)
    projected = jnp.dot(scaled, all_weights, preferred_element_type=f32).astype(bf16)
    projected = projected.reshape(2, half, chunk_count, LANES).transpose(1, 2, 0, 3)
    blocks = jnp.concatenate(
        [
            projected.reshape(kv_count, 2 * chunk_count, LANES),
            centred.astype(bf16).reshape(2, half, LANES).swapaxes(0, 1),
            jnp.broadcast_to(bias_own.astype(bf16)[None], (kv_count, 1, LANES)),
            jnp.zeros((kv_count, 5, LANES), bf16),
        ],
        axis=1,
    )
    arrived = exchange(blocks, KV).astype(f32)
    proj_sum = arrived[:, : 2 * chunk_count].sum(axis=0).reshape(chunk_count, 2, LANES)
    own_rows = arrived[:, 2 * chunk_count : 2 * chunk_count + 2]
    bias_sum = arrived[:, 2 * chunk_count + 2].reshape(chunk_count, share, LANES).sum(axis=1)
    own_rows = own_rows - jnp.mean(own_rows, axis=(0, 2), keepdims=True)
    row_scale = lax.rsqrt(jnp.mean(own_rows * own_rows, axis=(0, 2), keepdims=True) + norm_eps)
    pre = (proj_sum * row_scale + bias_sum[:, None]).astype(bf16).astype(f32)
    pre = pre.reshape(4, heads, 2, HEAD).swapaxes(1, 2)
    query_pre, forget_pre, input_pre, outgate_pre = pre[0], pre[1], pre[2], pre[3]

    low_bound = lower_bound.reshape(heads, HEAD)
    forget = low_bound + (1.0 - low_bound) * jax.nn.sigmoid(forget_pre)
    key_part = (1.0 - low_bound) * jax.nn.sigmoid(-forget_pre)
    updated = forget[..., None] * state + key_part[..., None] * input_pre[:, :, None, :]
    readout = jnp.einsum(
        "shd,shde->she", jax.nn.silu(query_pre), updated, precision=lax.Precision.HIGHEST
    )
    readout = readout * lax.rsqrt(jnp.mean(readout * readout, axis=-1, keepdims=True) + head_eps)
    gated_out = (readout * head_gain.reshape(heads, HEAD) * jax.nn.silu(outgate_pre)).astype(bf16)
    mixer_part = jnp.dot(
        gated_out.reshape(seqs, heads * HEAD), out_weight, preferred_element_type=f32
    )
    piece_chunks = kv_count // tp_count
    mixer_part = mixer_part.reshape(2, tp_count, piece_chunks, LANES).transpose(1, 2, 0, 3)
    mixer_sum = exchange(mixer_part, TP).reshape(tp_count, piece_chunks, 2, LANES).sum(axis=0)
    at = tp * piece_chunks
    piece = lax.dynamic_slice_in_dim(own_rows, at, piece_chunks, 0)
    piece_gain = lax.dynamic_slice_in_dim(params[:, 0:1], at, piece_chunks, 0)
    piece_bias = lax.dynamic_slice_in_dim(params[:, 3:4], at, piece_chunks, 0)
    piece = (piece * row_scale * piece_gain + piece_bias).astype(bf16).astype(f32)
    stream_own = (residual_scale * piece + mixer_sum).astype(bf16)
    stream_own = stream_own.reshape(2 * piece_chunks, LANES)
    arrived = lax.all_gather(to_everyone(stream_own, CHIPS, chip_count), CORE, axis=0)
    arrived = arrived.reshape(2, kv_count, x_count, piece_chunks, 2, LANES)
    stream_two = arrived.transpose(4, 1, 2, 0, 3, 5).reshape(batch, width).astype(f32)
    row_mean = jnp.mean(stream_two, axis=-1, keepdims=True)
    centred = stream_two - row_mean
    spread = jnp.mean(centred * centred, axis=-1, keepdims=True)
    normed_two = (
        centred * lax.rsqrt(spread + norm_eps) * params[:, 1].reshape(1, width)
        + params[:, 4].reshape(1, width)
    ).astype(bf16)

    partial_two = ffn_partial(normed_two, gate_weights[1], up_weights[1], down_weights[1])
    total = over_tp(sum_over_kv(partial_two, None)).sum(axis=0).reshape(batch, LANES)
    own_normed = lax.dynamic_slice_in_dim(normed_two, kv * LANES, LANES, 1)
    stream_three = residual_scale * own_normed.astype(f32) + 0.5 * total
    block_sum = stream_three.sum(axis=1)
    block_mean = block_sum / LANES
    off = stream_three - block_mean[:, None]
    stats = jnp.concatenate([block_mean, (off * off).sum(axis=1)])[None]
    stats = to_everyone(stats, KV, kv_count)[:, 0]
    means, squares = stats[:, :batch], stats[:, batch:]
    row_mean = means.mean(axis=0)
    spread = (squares.sum(axis=0) + LANES * ((means - row_mean) ** 2).sum(axis=0)) / width
    own = lax.dynamic_slice_in_dim(stream_three, tp * own_cols, own_cols, 1)
    mixed = (own - row_mean[:, None]) * lax.rsqrt(spread + norm_eps)[:, None] * norm_gain[
        2
    ].astype(f32) + norm_bias[2].astype(f32)
    mixed = mixed.reshape(2, half, own_cols).swapaxes(0, 1).reshape(batch, own_cols)
    return (mixed.astype(bf16), updated)


def solution(mesh):
    finer = Mesh(mesh.devices.reshape(8, 4, 4, 2), KV_TP)
    in_specs = (
        P(None, KV_TP),
        P(None, None, KV_TP),
        P(None, None, KV_TP),
        P(None, KV_TP, None),
        P(None, KV_TP),
        P(None, KV_TP),
        P(KV, TP),
        P(KV, TP),
        P(KV, TP),
        P(KV, TP),
        P(TP),
        P(TP),
        P(TP, None),
        P(KV, TP, None, None),
    )
    out_specs = (P(None, KV_TP), P(KV, TP, None, None))
    return jax.shard_map(local, mesh=finer, in_specs=in_specs, out_specs=out_specs, check_vma=False)
```

time: 303 us -> 205 us (0.68)
  blocking collectives: 161 us -> 73.2 us
  waiting for transfers between devices: 58.8 us -> 43.2 us
  other arithmetic: 14.9 us -> 6.53 us
  local copies, waits for them, and re-layouts: 24.7 us -> 30.7 us
  starting transfers between devices: 31.7 us -> 36.5 us
    all_to_all x6 -> x1, blocking collectives: 93.2 us -> 19.3 us  [exchange(): return lax.all_to_all(blocks, axes, split_axis=0, concat_axis=0, tiled=True)]
    all_to_all x6, waiting for transfers between devices: 58.8 us -> 40.9 us  [exchange(): return lax.all_to_all(blocks, axes, split_axis=0, concat_axis=0, tiled=True)]
    all_gather x1 -> x5, blocking collectives: 67.7 us -> 53.9 us  [the longest x2 29.7 us: over_tp(): gathered = lax.all_gather(lines, TP, axis=0)]
    dot_general x0 -> x1, local copies, waits for them, and re-layouts: none -> 6.48 us  [local(): jnp.dot(gated_out.reshape(seqs, heads * HEAD), out_weight, preferred_elem...]
    all_to_all x6, starting transfers between devices: 31.7 us -> 35.6 us  [exchange(): return lax.all_to_all(blocks, axes, split_axis=0, concat_axis=0, tiled=True)]
    mul x5 -> x4, local copies, waits for them, and re-layouts: 4.03 us -> 0.27 us  [the longest x1 0.09 us: local(): stream_one = residual_scale * block[:batch].astype(f32) + 0.5 * total]
    unnamed x34 -> x42, local copies, waits for them, and re-layouts: 3.54 us -> 7.25 us
    add x1 -> x2, other arithmetic: 3.39 us -> 0.01 us  [the longest x1 0.01 us: local(): (own - row_mean[:, None]) * lax.rsqrt(spread + norm_eps)[:, None]]
  transfers between devices with their start and end apart: 6 -> 8, of which waited for: 6 -> 7; matrix products, arithmetic and copies ran while one was open for 2% -> 11% of each run, Pallas kernels for 0% -> 0%
where the time goes in v1:
time: 205 us; the launch traced here: 204 us
  blocking collectives  73.2 us (36%)
  waiting for transfers between devices  43.2 us (21%)
  starting transfers between devices  36.5 us (18%)
  local copies, waits for them, and re-layouts  30.7 us (15%)
  matrix products  12.4 us (6%)
  other arithmetic  6.53 us (3%)
    all_to_all x6, waiting for transfers between devices, exchange(): return lax.all_to_all(blocks, axes, split_axis=0, concat_axis=0, tiled=True)  40.9 us
    all_to_all x6, starting transfers between devices, exchange(): return lax.all_to_all(blocks, axes, split_axis=0, concat_axis=0, tiled=True)  35.6 us
    all_gather x2, blocking collectives, over_tp(): gathered = lax.all_gather(lines, TP, axis=0)  29.7 us
    all_to_all x1, blocking collectives, exchange(): return lax.all_to_all(blocks, axes, split_axis=0, concat_axis=0, tiled=True)  19.3 us
    all_gather x1, blocking collectives, local(): lax.all_gather(placed, TP, axis=0).astype(f32).sum(axis=0).astype(bf16)  15.8 us
    unnamed x42, local copies, waits for them, and re-layouts  7.25 us
    dot_general x1, local copies, waits for them, and re-layouts, local(): jnp.dot(gated_out.reshape(seqs, heads * HEAD), out_weight, preferred_elem...  6.48 us
    dot_general x2, matrix products, ffn_partial(): return jnp.dot(hidden, down_w, preferred_element_type=f32)  4.8 us
  transfers between devices with their start and end apart: 8, of which 7 were waited for; matrix products, arithmetic and copies ran while one was open for 11% of the time, Pallas kernels for 0%

profile of v1, /device:TPU:1, one launch (start us, length us, event | category | flops | bytes accessed | tf_op | source)
XLA Modules:
  0.0 203.8 jit_solution(8800877866191311839)
XLA Ops:
  0.7 0.8 copy.264
  1.5 0.8 copy.265
  2.3 0.8 copy.262
  3.6 15.8 %all-gather = bf16[576,128]{1,0:T(8,128)(2,1)S(1)} all-gather(bf16[72,128]{1,0:T(8,128)(2,1)S(1)} %convolution_convert_fusion.2), channel_id=2, replica_groups=mesh['kv_0'=8,'kv_1'=4,'tp_0'=4,'tp_1'=2] {'tp_0','tp_1'}, dimensions={0}, use_global_device_ids=true | all-gather | bytes 165888 | tf_op jit(solution)/shard_map/all_gather | solution.py:74
  19.5 0.8 broadcast_in_dim.23
  20.2 9.8 %all-to-all-start = ((bf16[32,40,128]{2,1,0:T(8,128)(2,1)}), bf16[32,40,128]{2,1,0:T(8,128)(2,1)S(1)}, u32[]{:S(2)}, u32[]{:S(2)}) async-start(bf16[32,40,128]{2,1,0:T(8,128)(2,1)} %broadcast_in_dim.23), calls=%async_computation | async-start | bytes 655360 | tf_op jit(solution)/shard_map/all_to_all | solution.py:24
  30.2 0.9 constant_dynamic-update-slice_fusion.3
  31.1 0.9 constant_dynamic-update-slice_fusion.2
  32.0 0.9 constant_dynamic-update-slice_fusion.1
  32.9 0.9 constant_dynamic-update-slice_fusion
  34.1 3.8 %fusion.64 = (bf16[1,4096,44]{1,0,2:T(2,128)(2,1)S(1)}, bf16[1,4096,44]{1,0,2:T(2,128)(2,1)}) fusion(bf16[2,4096,44]{1,0,2:T(2,128)(2,1)} %param.15), kind=kLoop, calls=%fused_computation.153 | loop fusion | bytes 1441792 | tf_op jit(solution)/shard_map/slice | solution.py:174
  37.9 2.8 %fusion.65 = (bf16[1,4096,44]{1,0,2:T(2,128)(2,1)}, bf16[1,4096,44]{1,0,2:T(2,128)(2,1)}) fusion(bf16[2,4096,44]{1,0,2:T(2,128)(2,1)S(1)} %copy-done), kind=kLoop, calls=%fused_computation.154 | loop fusion | bytes 1441792 | tf_op jit(solution)/shard_map/slice | solution.py:174
  40.7 2.8 %fusion.66 = (bf16[1,44,4096]{2,0,1:T(2,128)(2,1)}, bf16[1,44,4096]{2,0,1:T(2,128)(2,1)}) fusion(bf16[2,44,4096]{2,0,1:T(2,128)(2,1)S(1)} %copy-done.1), kind=kLoop, calls=%fused_computation.155 | loop fusion | bytes 1441792 | tf_op jit(solution)/shard_map/slice | solution.py:174
  43.5 3.7 %all-gather.1 = bf16[64,40,128]{2,1,0:T(8,128)(2,1)S(1)} all-gather(bf16[32,40,128]{2,1,0:T(8,128)(2,1)S(1)} %all-to-all-done), channel_id=3, replica_groups=mesh['kv_0'=8,'kv_1'=4,'tp_0'=4,'tp_1'=2] {'tp_1'}, dimensions={0}, use_global_device_ids=true | all-gather | bytes 983040 | tf_op jit(solution)/shard_map/all_gather | solution.py:77
  47.5 1.7 fusion.7
  49.2 2.6 %convert_bitcast_fusion = (bf16[8,8,32,128]{3,1,2,0:T(8,128)(2,1)S(1)}, f32[64]{0:T(128)S(1)}) fusion(bf16[1,44,4096]{2,0,1:T(2,128)(2,1)} %get-tuple-element.35, bf16[8,8,32,128]{3,2,1,0:T(8,128)(2,1)S(1)} %bitcast.216, bf16[1,4096,44]{1,0,2:T(2,128)(2,1)} %get-tuple-element.33, f32[64,44]{0,1:T(8,128)S(1)} %fusion.7), kind=kOutput, calls=%fused_computation.29 | convolution fusion | flops 46678464 | bytes 1780992 | tf_op jit(solution)/shard_map/dot_general | solution.py:39
  52.6 1.1 collective-permute-done
  53.8 0.9 maximum_maximum_fusion
  54.7 8.1 %all-to-all-start.1 = ((bf16[32,40,128]{2,1,0:T(8,128)(2,1)}), bf16[32,40,128]{2,1,0:T(8,128)(2,1)S(1)}, u32[]{:S(2)}, u32[]{:S(2)}) async-start(bf16[32,40,128]{2,1,0:T(8,128)(2,1)} %maximum_maximum_fusion), calls=%async_computation.1 | async-start | bytes 655360 | tf_op jit(solution)/shard_map/all_to_all | solution.py:24
  63.1 6.5 %copy.304 = bf16[4096,512]{1,0:T(8,128)(2,1)} copy(bf16[4096,512]{0,1:T(8,128)(2,1)} %bitcast.211) | data formatting | bytes 8388608 | tf_op jit(solution)/shard_map/dot_general | solution.py:150
  69.8 5.8 %all-to-all-done.1 = bf16[32,40,128]{2,1,0:T(8,128)(2,1)S(1)} async-done(((bf16[32,40,128]{2,1,0:T(8,128)(2,1)}), bf16[32,40,128]{2,1,0:T(8,128)(2,1)S(1)}, u32[]{:S(2)}, u32[]{:S(2)}) %all-to-all-start.1) | async-done | bytes 327712 | tf_op jit(solution)/shard_map/all_to_all | solution.py:24
  75.7 15.0 %all-gather.2 = f32[320,128]{1,0:T(8,128)S(1)} all-gather(f32[40,128]{1,0:T(8,128)S(1)} %convert_reduce_fusion.1), channel_id=4, replica_groups=mesh['kv_0'=8,'kv_1'=4,'tp_0'=4,'tp_1'=2] {'tp_0','tp_1'}, dimensions={0}, use_global_device_ids=true | all-gather | bytes 184320 | tf_op jit(solution)/shard_map/all_gather | solution.py:91
  91.6 0.9 copy.277
  92.5 4.1 %all-to-all-start.2 = ((bf16[32,40,128]{2,1,0:T(8,128)(2,1)}), bf16[32,40,128]{2,1,0:T(8,128)(2,1)S(1)}, u32[]{:S(2)}, u32[]{:S(2)}) async-start(bf16[32,40,128]{2,1,0:T(8,128)(2,1)} %copy.277), calls=%async_computation.2 | async-start | bytes 655360 | tf_op jit(solution)/shard_map/all_to_all | solution.py:24
  96.6 12.7 %all-to-all-done.2 = bf16[32,40,128]{2,1,0:T(8,128)(2,1)S(1)} async-done(((bf16[32,40,128]{2,1,0:T(8,128)(2,1)}), bf16[32,40,128]{2,1,0:T(8,128)(2,1)S(1)}, u32[]{:S(2)}, u32[]{:S(2)}) %all-to-all-start.2) | async-done | bytes 327712 | tf_op jit(solution)/shard_map/all_to_all | solution.py:24
  110.4 0.5 fusion.45
  111.0 4.0 %convolution_bitcast_fusion = f32[8,4,2,128]{3,2,1,0:T(2,128)} fusion(bf16[8,4,128,512]{3,2,1,0:T(8,128)(2,1)} %bitcast.206, f32[4,2,4,128]{3,1,2,0:T(2,128)S(1)} %convert_bitcast_fusion.1, f32[2,4,1,128]{3,2,1,0:T(1,128)S(1)} %fusion.45, f32[4,128]{1,0:T(4,128)S(1)} %bitcast.246, f32[2,4]{0,1:T(4,128)S(1)} %add_rsqrt_fusion.1), kind=kOutput, calls=%fused_computation.4 | convolution fusion | flops 8396800 | bytes 4239360 | tf_op jit(solution)/shard_map/dot_general | solution.py:150
  115.0 5.8 %all-to-all-start.3 = ((f32[8,4,2,128]{3,2,1,0:T(2,128)}), f32[8,4,2,128]{3,2,1,0:T(2,128)S(1)}, u32[]{:S(2)}, u32[]{:S(2)}) async-start(f32[8,4,2,128]{3,2,1,0:T(2,128)} %convolution_bitcast_fusion), calls=%async_computation.3 | async-start | bytes 65536 | tf_op jit(solution)/shard_map/all_to_all | solution.py:24
  120.8 4.7 %all-to-all-done.3 = f32[8,4,2,128]{3,2,1,0:T(2,128)S(1)} async-done(((f32[8,4,2,128]{3,2,1,0:T(2,128)}), f32[8,4,2,128]{3,2,1,0:T(2,128)S(1)}, u32[]{:S(2)}, u32[]{:S(2)}) %all-to-all-start.3) | async-done | bytes 32800 | tf_op jit(solution)/shard_map/all_to_all | solution.py:24
  125.7 19.3 %all_to_all.35 = bf16[128,8,128]{2,1,0:T(8,128)(2,1)S(1)} all-to-all(bf16[128,8,128]{2,1,0:T(8,128)(2,1)S(1)} %broadcast_in_dim.31), channel_id=1, replica_groups=mesh['kv_0'=8,'kv_1'=4,'tp_0'=4,'tp_1'=2] {'kv_0','kv_1','tp_0'}, dimensions={0} | all-to-all | bytes 524288 | tf_op jit(solution)/shard_map/all_to_all | solution.py:24
  145.0 4.7 %all-gather.3 = bf16[256,8,128]{2,1,0:T(8,128)(2,1)S(1)} all-gather(bf16[128,8,128]{2,1,0:T(8,128)(2,1)S(1)} %all_to_all.35), channel_id=5, replica_groups=mesh['kv_0'=8,'kv_1'=4,'tp_0'=4,'tp_1'=2] {'tp_1'}, dimensions={0}, use_global_device_ids=true | all-gather | bytes 786432 | tf_op jit(solution)/shard_map/all_gather | solution.py:163
  149.7 0.9 bitcast_reduce_fusion
  150.6 0.7 multiply_reduce_fusion
  151.4 0.6 copy-done.5
  152.0 0.8 add_convert_fusion
  153.4 0.5 fusion.17
  153.9 2.2 %fusion = bf16[8,8,32,128]{3,1,2,0:T(8,128)(2,1)S(1)} fusion(bf16[64,4096]{1,0:T(8,128)(2,1)S(1)} %convert_element_type.209, bf16[1,44,4096]{2,0,1:T(2,128)(2,1)} %get-tuple-element.34, bf16[1,4096,44]{1,0,2:T(2,128)(2,1)S(1)} %copy-done.3, f32[64,44]{0,1:T(8,128)S(1)} %fusion.17), kind=kOutput, calls=%fused_computation.2 | convolution fusion | flops 46416384 | bytes 1780736 | tf_op jit(solution)/shard_map/dot_general | solution.py:39
  156.9 1.2 collective-permute-done.1
  158.0 0.8 fusion.12
  158.8 3.9 %all-to-all-start.5 = ((bf16[32,32,128]{2,1,0:T(8,128)(2,1)}), bf16[32,32,128]{2,1,0:T(8,128)(2,1)S(1)}, u32[]{:S(2)}, u32[]{:S(2)}) async-start(bf16[32,32,128]{2,1,0:T(8,128)(2,1)} %fusion.12), calls=%async_computation.5 | async-start | bytes 524288 | tf_op jit(solution)/shard_map/all_to_all | solution.py:24
  162.7 0.8 dynamic-slice.10
  163.5 0.7 dynamic-slice.11
  165.4 9.1 %all-to-all-done.5 = bf16[32,32,128]{2,1,0:T(8,128)(2,1)S(1)} async-done(((bf16[32,32,128]{2,1,0:T(8,128)(2,1)}), bf16[32,32,128]{2,1,0:T(8,128)(2,1)S(1)}, u32[]{:S(2)}, u32[]{:S(2)}) %all-to-all-start.5) | async-done | bytes 262176 | tf_op jit(solution)/shard_map/all_to_all | solution.py:24
  174.5 14.7 %all-gather.4 = f32[256,128]{1,0:T(8,128)S(1)} all-gather(f32[32,128]{1,0:T(8,128)S(1)} %convert_reduce_fusion.2), channel_id=6, replica_groups=mesh['kv_0'=8,'kv_1'=4,'tp_0'=4,'tp_1'=2] {'tp_0','tp_1'}, dimensions={0}, use_global_device_ids=true | all-gather | bytes 147456 | tf_op jit(solution)/shard_map/all_gather | solution.py:91
  189.6 0.6 broadcast_in_dim.32
  190.2 3.9 %all-to-all-start.6 = ((f32[32,1,128]{2,1,0:T(1,128)}), f32[32,1,128]{2,1,0:T(1,128)S(1)}, u32[]{:S(2)}, u32[]{:S(2)}) async-start(f32[32,1,128]{2,1,0:T(1,128)} %broadcast_in_dim.32), calls=%async_computation.6 | async-start | bytes 32768 | tf_op jit(solution)/shard_map/all_to_all | solution.py:24
  194.1 8.6 %all-to-all-done.6 = f32[32,1,128]{2,1,0:T(1,128)S(1)} async-done(((f32[32,1,128]{2,1,0:T(1,128)}), f32[32,1,128]{2,1,0:T(1,128)S(1)}, u32[]{:S(2)}, u32[]{:S(2)}) %all-to-all-start.6) | async-done | bytes 16416 | tf_op jit(solution)/shard_map/all_to_all | solution.py:24
  203.1 0.7 copy.298
  (130 shorter events, 7.9 us)
Async XLA Ops:
  0.6 37.3 %copy-start = (bf16[2,4096,44]{1,0,2:T(2,128)(2,1)S(1)}, bf16[2,4096,44]{1,0,2:T(2,128)(2,1)}, u32[]{:S(2)}) copy-start(bf16[2,4096,44]{1,0,2:T(2,128)(2,1)} %param.16) | copy-start | bytes 2162692
  19.4 21.2 %copy-start.1 = (bf16[2,44,4096]{2,0,1:T(2,128)(2,1)S(1)}, bf16[2,44,4096]{2,0,1:T(2,128)(2,1)}, u32[]{:S(2)}) copy-start(bf16[2,44,4096]{2,0,1:T(2,128)(2,1)} %param.17) | copy-start | bytes 2162692
  20.2 23.3 %all-to-all-start = ((bf16[32,40,128]{2,1,0:T(8,128)(2,1)}), bf16[32,40,128]{2,1,0:T(8,128)(2,1)S(1)}, u32[]{:S(2)}, u32[]{:S(2)}) async-start(bf16[32,40,128]{2,1,0:T(8,128)(2,1)} %broadcast_in_dim.23), calls=%async_computation | async-start | bytes 655360 | tf_op jit(solution)/shard_map/all_to_all | solution.py:24
  52.1 1.6 collective-permute-start
  54.7 20.9 %all-to-all-start.1 = ((bf16[32,40,128]{2,1,0:T(8,128)(2,1)}), bf16[32,40,128]{2,1,0:T(8,128)(2,1)S(1)}, u32[]{:S(2)}, u32[]{:S(2)}) async-start(bf16[32,40,128]{2,1,0:T(8,128)(2,1)} %maximum_maximum_fusion), calls=%async_computation.1 | async-start | bytes 655360 | tf_op jit(solution)/shard_map/all_to_all | solution.py:24
  69.5 27.0 %copy-start.9 = (f32[512]{0:T(512)S(1)}, f32[512]{0:T(512)}, u32[]{:S(2)}) copy-start(f32[512]{0:T(512)} %param.24) | copy-start | bytes 6148
  69.5 40.5 %copy-start.4 = (f32[2,4,128,128]{3,2,1,0:T(8,128)S(1)}, f32[2,4,128,128]{3,2,1,0:T(8,128)}, u32[]{:S(2)}) copy-start(f32[2,4,128,128]{3,2,1,0:T(8,128)} %param.27) | copy-start | bytes 1572868
  75.7 35.4 %copy-start.12 = (f32[512]{0:T(512)S(1)}, f32[512]{0:T(512)}, u32[]{:S(2)}) copy-start(f32[512]{0:T(512)} %param.25) | copy-start | bytes 6148
  92.5 16.9 %all-to-all-start.2 = ((bf16[32,40,128]{2,1,0:T(8,128)(2,1)}), bf16[32,40,128]{2,1,0:T(8,128)(2,1)S(1)}, u32[]{:S(2)}, u32[]{:S(2)}) async-start(bf16[32,40,128]{2,1,0:T(8,128)(2,1)} %copy.277), calls=%async_computation.2 | async-start | bytes 655360 | tf_op jit(solution)/shard_map/all_to_all | solution.py:24
  96.6 54.8 %copy-start.7 = (f32[32,1,128]{2,1,0:T(1,128)}, f32[32,1,128]{2,1,0:T(1,128)S(1)}, u32[]{:S(2)}) copy-start(f32[32,1,128]{2,1,0:T(1,128)S(1)} %get-tuple-element.41) | copy-start | bytes 49156
  96.6 54.8 %copy-start.8 = (f32[32,1,128]{2,1,0:T(1,128)}, f32[32,1,128]{2,1,0:T(1,128)S(1)}, u32[]{:S(2)}) copy-start(f32[32,1,128]{2,1,0:T(1,128)S(1)} %get-tuple-element.42) | copy-start | bytes 49156
  110.4 41.0 %copy-start.2 = (f32[2,4,128,128]{3,2,1,0:T(8,128)}, f32[2,4,128,128]{3,2,1,0:T(8,128)S(1)}, u32[]{:S(2)}) copy-start(f32[2,4,128,128]{3,2,1,0:T(8,128)S(1)} %multiply_add_fusion) | copy-start | bytes 1572868
  115.0 10.5 %all-to-all-start.3 = ((f32[8,4,2,128]{3,2,1,0:T(2,128)}), f32[8,4,2,128]{3,2,1,0:T(2,128)S(1)}, u32[]{:S(2)}, u32[]{:S(2)}) async-start(f32[8,4,2,128]{3,2,1,0:T(2,128)} %convolution_bitcast_fusion), calls=%async_computation.3 | async-start | bytes 65536 | tf_op jit(solution)/shard_map/all_to_all | solution.py:24
  145.0 8.9 %copy-start.3 = (bf16[1,4096,44]{1,0,2:T(2,128)(2,1)S(1)}, bf16[1,4096,44]{1,0,2:T(2,128)(2,1)}, u32[]{:S(2)}) copy-start(bf16[1,4096,44]{1,0,2:T(2,128)(2,1)} %get-tuple-element.32) | copy-start | bytes 1081348
  151.4 0.6 copy-start.5
  153.3 11.0 %copy-start.6 = (f32[2,32]{0,1:T(8,128)S(1)}, f32[2,32]{0,1:T(8,128)}, u32[]{:S(2)}) copy-start(f32[2,32]{0,1:T(8,128)} %copy-done.5) | copy-start | bytes 772
  156.2 37.9 %copy-start.10 = (bf16[3,16]{1,0:T(4,128)(2,1)S(1)}, bf16[3,16]{1,0:T(4,128)(2,1)}, u32[]{:S(2)}) copy-start(bf16[3,16]{1,0:T(4,128)(2,1)} %param.19) | copy-start | bytes 292
  156.2 37.9 %copy-start.11 = (bf16[3,16]{1,0:T(4,128)(2,1)S(1)}, bf16[3,16]{1,0:T(4,128)(2,1)}, u32[]{:S(2)}) copy-start(bf16[3,16]{1,0:T(4,128)(2,1)} %param.18) | copy-start | bytes 292
  156.4 1.6 collective-permute-start.1
  158.8 15.7 %all-to-all-start.5 = ((bf16[32,32,128]{2,1,0:T(8,128)(2,1)}), bf16[32,32,128]{2,1,0:T(8,128)(2,1)S(1)}, u32[]{:S(2)}, u32[]{:S(2)}) async-start(bf16[32,32,128]{2,1,0:T(8,128)(2,1)} %fusion.12), calls=%async_computation.5 | async-start | bytes 524288 | tf_op jit(solution)/shard_map/all_to_all | solution.py:24
  190.2 12.5 %all-to-all-start.6 = ((f32[32,1,128]{2,1,0:T(1,128)}), f32[32,1,128]{2,1,0:T(1,128)S(1)}, u32[]{:S(2)}, u32[]{:S(2)}) async-start(f32[32,1,128]{2,1,0:T(1,128)} %broadcast_in_dim.32), calls=%async_computation.6 | async-start | bytes 32768 | tf_op jit(solution)/shard_map/all_to_all | solution.py:24

commit v2 on v1

--- a/solution.py
+++ b/solution.py
@@ -1,6 +1,7 @@
 import jax
 import jax.numpy as jnp
 from jax import lax
+from jax.experimental import pallas as pl
 from jax.sharding import Mesh
 from jax.sharding import PartitionSpec as P
 
@@ -32,11 +33,33 @@
     return jnp.pad(lines, ((0, count - lines.shape[0]), (0, LANES - lines.shape[1])))
 
 
-def ffn_partial(whole_rows, gate_w, up_w, down_w):
-    gate_proj = jnp.dot(whole_rows, gate_w, preferred_element_type=f32)
-    up_proj = jnp.dot(whole_rows, up_w, preferred_element_type=f32)
+def ffn_partial(whole_rows, gate_ws, up_ws, down_ws, layer):
+    gate_proj = jnp.einsum("sf,lfh->shl", whole_rows, gate_ws, preferred_element_type=f32)
+    up_proj = jnp.einsum("sf,lfh->shl", whole_rows, up_ws, preferred_element_type=f32)
     hidden = (jax.nn.silu(gate_proj) * up_proj).astype(bf16)
-    return jnp.dot(hidden, down_w, preferred_element_type=f32)
+    other = lax.broadcasted_iota(jnp.int32, hidden.shape, 2) != layer
+    hidden = jnp.where(other, 0, hidden)
+    return jnp.einsum("shl,lhf->sf", hidden, down_ws, preferred_element_type=f32)
+
+
+def out_kernel(gated_ref, weight_ref, result_ref):
+    result_ref[...] = jnp.dot(gated_ref[...], weight_ref[...], preferred_element_type=f32)
+
+
+def out_projection(gated, weight):
+    rows, depth = gated.shape
+    width = weight.shape[1]
+    step = 1024
+    return pl.pallas_call(
+        out_kernel,
+        grid=(width // step,),
+        in_specs=[
+            pl.BlockSpec((rows, depth), lambda i: (0, 0)),
+            pl.BlockSpec((depth, step), lambda i: (0, i)),
+        ],
+        out_specs=pl.BlockSpec((rows, step), lambda i: (0, i)),
+        out_shape=jax.ShapeDtypeStruct((rows, width), f32),
+    )(gated, weight)
 
 
 def local(
@@ -71,7 +94,7 @@
         == lax.broadcasted_iota(jnp.int32, (own_cols, LANES), 0) + tp * own_cols
     ).astype(bf16)
     placed = jnp.dot(lines, place, preferred_element_type=f32).astype(bf16)
-    block = lax.all_gather(placed, TP, axis=0).astype(f32).sum(axis=0).astype(bf16)
+    block = to_everyone(placed, TP, tp_count).astype(f32).sum(axis=0).astype(bf16)
     own_half = lax.dynamic_slice_in_dim(block, core * half, half, 0)
     arrived = to_everyone(jnp.concatenate([own_half, block[batch:]]), KV, kv_count)
     both = lax.all_gather(arrived, CORE, axis=0)
@@ -88,16 +111,21 @@
         return exchange(paired, KV).astype(f32).sum(axis=0)
 
     def over_tp(lines):
-        gathered = lax.all_gather(lines, TP, axis=0)
+        gathered = to_everyone(lines, TP, tp_count)
         return gathered.reshape(x_count, 2, *lines.shape)
 
-    partial_one = ffn_partial(whole_tokens, gate_weights[0], up_weights[0], down_weights[0])
+    partial_one = ffn_partial(whole_tokens, gate_weights, up_weights, down_weights, 0)
     weights = (query_weight, forget_weight, input_weight, outgate_weight)
-    all_weights = jnp.concatenate(weights, axis=1)
-    chunk_count = all_weights.shape[1] // LANES
+    chunk_count = 4 * heads
+
+    def project(lines):
+        return jnp.concatenate(
+            [jnp.dot(lines, w, preferred_element_type=f32) for w in weights], axis=1
+        )
+
     share = kv_count // chunk_count
     gain_one, bias_one = block[batch : batch + 1], block[batch + 3 : batch + 4]
-    bias_part = jnp.dot(bias_one, all_weights, preferred_element_type=f32)
+    bias_part = project(bias_one)
     bias_rows = jnp.repeat(bias_part.reshape(chunk_count, 1, LANES), share, axis=0).astype(bf16)
     row_sum = partial_one.sum(axis=1)
     high = row_sum.astype(bf16)
@@ -117,7 +145,7 @@
     centred = stream_one - row_mean[:, None]
 
     scaled = (centred * gain_one.astype(f32)).astype(bf16)
-    projected = jnp.dot(scaled, all_weights, preferred_element_type=f32).astype(bf16)
+    projected = project(scaled).astype(bf16)
     projected = projected.reshape(2, half, chunk_count, LANES).transpose(1, 2, 0, 3)
     blocks = jnp.concatenate(
         [
@@ -147,9 +175,8 @@
     )
     readout = readout * lax.rsqrt(jnp.mean(readout * readout, axis=-1, keepdims=True) + head_eps)
     gated_out = (readout * head_gain.reshape(heads, HEAD) * jax.nn.silu(outgate_pre)).astype(bf16)
-    mixer_part = jnp.dot(
-        gated_out.reshape(seqs, heads * HEAD), out_weight, preferred_element_type=f32
-    )
+    gated_rows = jnp.pad(gated_out.reshape(seqs, heads * HEAD), ((0, 8 - seqs), (0, 0)))
+    mixer_part = out_projection(gated_rows, out_weight)[:seqs]
     piece_chunks = kv_count // tp_count
     mixer_part = mixer_part.reshape(2, tp_count, piece_chunks, LANES).transpose(1, 2, 0, 3)
     mixer_sum = exchange(mixer_part, TP).reshape(tp_count, piece_chunks, 2, LANES).sum(axis=0)
@@ -171,7 +198,7 @@
         + params[:, 4].reshape(1, width)
     ).astype(bf16)
 
-    partial_two = ffn_partial(normed_two, gate_weights[1], up_weights[1], down_weights[1])
+    partial_two = ffn_partial(normed_two, gate_weights, up_weights, down_weights, 1)
     total = over_tp(sum_over_kv(partial_two, None)).sum(axis=0).reshape(batch, LANES)
     own_normed = lax.dynamic_slice_in_dim(normed_two, kv * LANES, LANES, 1)
     stream_three = residual_scale * own_normed.astype(f32) + 0.5 * total

time: 205 us -> 199 us (0.971)
  blocking collectives: 73.2 us -> 23.2 us
  waiting for transfers between devices: 43.2 us -> 80.3 us
  starting transfers between devices: 36.5 us -> 53 us
  local copies, waits for them, and re-layouts: 30.7 us -> 18 us
  Pallas kernels: 0 us -> 4.23 us
  matrix products: 12.4 us -> 8.5 us
  other arithmetic: 6.53 us -> 9.47 us
    all_gather x3 -> x0, blocking collectives: 45.5 us -> none  [the longest x2 29.7 us: over_tp(): gathered = lax.all_gather(lines, TP, axis=0)]
    all_to_all x6 -> x9, waiting for transfers between devices: 40.9 us -> 78 us  [exchange(): return lax.all_to_all(blocks, axes, split_axis=0, concat_axis=0, tiled=True)]
    all_to_all x6 -> x9, starting transfers between devices: 35.6 us -> 52.1 us  [exchange(): return lax.all_to_all(blocks, axes, split_axis=0, concat_axis=0, tiled=True)]
    slice x4 -> x2, local copies, waits for them, and re-layouts: 9.49 us -> 1.55 us  [the longest x1 0.91 us: local(): mixer_part = out_projection(gated_rows, out_weight)[:seqs]]
    dot_general x1 -> x4, local copies, waits for them, and re-layouts: 6.48 us -> 0.03 us  [project(): jnp.dot(lines, w, preferred_element_type=f32)]
    all_to_all x1, blocking collectives: 19.3 us -> 14.8 us  [exchange(): return lax.all_to_all(blocks, axes, split_axis=0, concat_axis=0, tiled=True)]
    pallas_call x0 -> x1, Pallas kernels: none -> 4.23 us  [out_projection(): pl.pallas_call(out_kernel, grid=(width // step,), in_specs=[pl.BlockSpec(...]
    dot_general x7 -> x12, matrix products: 11.6 us -> 7.72 us  [the longest x8 3.05 us: project(): jnp.dot(lines, w, preferred_element_type=f32)]
  transfers between devices with their start and end apart: 8 -> 11, of which waited for: 7 -> 11; matrix products, arithmetic and copies ran while one was open for 11% -> 2% of each run, Pallas kernels for 0% -> 0%
where the time goes in v2:
time: 199 us; the launch traced here: 198 us
  waiting for transfers between devices  80.3 us (40%)
  starting transfers between devices  53 us (27%)
  blocking collectives  23.2 us (12%)
  local copies, waits for them, and re-layouts  18 us (9%)
  other arithmetic  9.47 us (5%)
  matrix products  8.5 us (4%)
  Pallas kernels  4.23 us (2%)
    all_to_all x9, waiting for transfers between devices, exchange(): return lax.all_to_all(blocks, axes, split_axis=0, concat_axis=0, tiled=True)  78 us
    all_to_all x9, starting transfers between devices, exchange(): return lax.all_to_all(blocks, axes, split_axis=0, concat_axis=0, tiled=True)  52.1 us
    all_to_all x1, blocking collectives, exchange(): return lax.all_to_all(blocks, axes, split_axis=0, concat_axis=0, tiled=True)  14.8 us
    unnamed x46, local copies, waits for them, and re-layouts  4.65 us
    all_gather x1, blocking collectives, local(): lax.all_gather(to_everyone(stream_own, CHIPS, chip_count), CORE, axis=0)  4.41 us
    pallas_call x1, Pallas kernels, out_projection(): pl.pallas_call(out_kernel, grid=(width // step,), in_specs=[pl.BlockSpec(...  4.23 us
    broadcast_in_dim x6, local copies, waits for them, and re-layouts, to_everyone(): return exchange(jnp.broadcast_to(block[None], (count, *block.shape)), axes)  4.12 us
    all_gather x1, blocking collectives, local(): both = lax.all_gather(arrived, CORE, axis=0)  4.07 us
  transfers between devices with their start and end apart: 11, of which 11 were waited for; matrix products, arithmetic and copies ran while one was open for 2% of the time, Pallas kernels for 0%

profile of v2, /device:TPU:1, one launch (start us, length us, event | category | flops | bytes accessed | tf_op | source)
XLA Modules:
  0.0 198.0 jit_solution(9890076662077135908)
XLA Ops:
  0.7 0.8 copy.276
  1.5 0.8 copy.277
  2.3 0.8 copy.274
  3.6 0.7 broadcast_in_dim.34
  4.3 6.5 %all-to-all-start = ((bf16[8,72,128]{2,1,0:T(8,128)(2,1)}), bf16[8,72,128]{2,1,0:T(8,128)(2,1)S(1)}, u32[]{:S(2)}, u32[]{:S(2)}) async-start(bf16[8,72,128]{2,1,0:T(8,128)(2,1)} %broadcast_in_dim.34), calls=%async_computation | async-start | bytes 294912 | tf_op jit(solution)/shard_map/all_to_all | solution.py:25
  10.9 5.3 %all-to-all-done = bf16[8,72,128]{2,1,0:T(8,128)(2,1)S(1)} async-done(((bf16[8,72,128]{2,1,0:T(8,128)(2,1)}), bf16[8,72,128]{2,1,0:T(8,128)(2,1)S(1)}, u32[]{:S(2)}, u32[]{:S(2)}) %all-to-all-start) | async-done | bytes 147488 | tf_op jit(solution)/shard_map/all_to_all | solution.py:25
  16.2 1.0 fusion.67
  17.3 0.8 broadcast_in_dim.36
  18.1 10.5 %all-to-all-start.1 = ((bf16[32,40,128]{2,1,0:T(8,128)(2,1)}), bf16[32,40,128]{2,1,0:T(8,128)(2,1)S(1)}, u32[]{:S(2)}, u32[]{:S(2)}) async-start(bf16[32,40,128]{2,1,0:T(8,128)(2,1)} %broadcast_in_dim.36), calls=%async_computation.1 | async-start | bytes 655360 | tf_op jit(solution)/shard_map/all_to_all | solution.py:25
  28.6 1.0 fusion.66
  30.0 11.2 %all-to-all-done.1 = bf16[32,40,128]{2,1,0:T(8,128)(2,1)S(1)} async-done(((bf16[32,40,128]{2,1,0:T(8,128)(2,1)}), bf16[32,40,128]{2,1,0:T(8,128)(2,1)S(1)}, u32[]{:S(2)}, u32[]{:S(2)}) %all-to-all-start.1) | async-done | bytes 327712 | tf_op jit(solution)/shard_map/all_to_all | solution.py:25
  41.2 4.1 %all-gather = bf16[64,40,128]{2,1,0:T(8,128)(2,1)S(1)} all-gather(bf16[32,40,128]{2,1,0:T(8,128)(2,1)S(1)} %all-to-all-done.1), channel_id=2, replica_groups=mesh['kv_0'=8,'kv_1'=4,'tp_0'=4,'tp_1'=2] {'tp_1'}, dimensions={0}, use_global_device_ids=true | all-gather | bytes 983040 | tf_op jit(solution)/shard_map/all_gather | solution.py:100
  45.7 1.7 convolution_bitcast_fusion.5
  47.5 1.2 convert_bitcast_fusion
  49.5 1.1 collective-permute-done
  50.7 0.9 maximum_maximum_fusion
  51.6 4.1 %all-to-all-start.2 = ((bf16[32,40,128]{2,1,0:T(8,128)(2,1)}), bf16[32,40,128]{2,1,0:T(8,128)(2,1)S(1)}, u32[]{:S(2)}, u32[]{:S(2)}) async-start(bf16[32,40,128]{2,1,0:T(8,128)(2,1)} %maximum_maximum_fusion), calls=%async_computation.2 | async-start | bytes 655360 | tf_op jit(solution)/shard_map/all_to_all | solution.py:25
  56.1 12.3 %all-to-all-done.2 = bf16[32,40,128]{2,1,0:T(8,128)(2,1)S(1)} async-done(((bf16[32,40,128]{2,1,0:T(8,128)(2,1)}), bf16[32,40,128]{2,1,0:T(8,128)(2,1)S(1)}, u32[]{:S(2)}, u32[]{:S(2)}) %all-to-all-start.2) | async-done | bytes 327712 | tf_op jit(solution)/shard_map/all_to_all | solution.py:25
  68.5 0.7 broadcast_in_dim.40
  69.2 5.7 %all-to-all-start.3 = ((f32[8,40,128]{2,1,0:T(8,128)}), f32[8,40,128]{2,1,0:T(8,128)S(1)}, u32[]{:S(2)}, u32[]{:S(2)}) async-start(f32[8,40,128]{2,1,0:T(8,128)} %broadcast_in_dim.40), calls=%async_computation.3 | async-start | bytes 327680 | tf_op jit(solution)/shard_map/all_to_all | solution.py:25
  74.8 5.6 %all-to-all-done.3 = f32[8,40,128]{2,1,0:T(8,128)S(1)} async-done(((f32[8,40,128]{2,1,0:T(8,128)}), f32[8,40,128]{2,1,0:T(8,128)S(1)}, u32[]{:S(2)}, u32[]{:S(2)}) %all-to-all-start.3) | async-done | bytes 163872 | tf_op jit(solution)/shard_map/all_to_all | solution.py:25
  81.9 0.9 copy.290
  82.8 4.0 %all-to-all-start.4 = ((bf16[32,40,128]{2,1,0:T(8,128)(2,1)}), bf16[32,40,128]{2,1,0:T(8,128)(2,1)S(1)}, u32[]{:S(2)}, u32[]{:S(2)}) async-start(bf16[32,40,128]{2,1,0:T(8,128)(2,1)} %copy.290), calls=%async_computation.4 | async-start | bytes 655360 | tf_op jit(solution)/shard_map/all_to_all | solution.py:25
  86.8 0.6 fusion.70
  87.5 11.9 %all-to-all-done.4 = bf16[32,40,128]{2,1,0:T(8,128)(2,1)S(1)} async-done(((bf16[32,40,128]{2,1,0:T(8,128)(2,1)}), bf16[32,40,128]{2,1,0:T(8,128)(2,1)S(1)}, u32[]{:S(2)}, u32[]{:S(2)}) %all-to-all-start.4) | async-done | bytes 327712 | tf_op jit(solution)/shard_map/all_to_all | solution.py:25
  100.4 0.8 copy-done.2
  101.9 0.6 pad.4.gated_ref
  102.5 4.2 %shard_map.149 = f32[8,4096]{1,0:T(8,128)} custom-call(bf16[8,512]{1,0:T(8,128)(2,1)} %pad.4.gated_ref, bf16[512,4096]{1,0:T(8,128)(2,1)} %weight_ref.1), custom_call_target="tpu_custom_call" | custom-call | tf_op jit(solution)/shard_map/pallas_call | solution.py:53
  106.7 0.9 slice.126
  108.3 6.0 %all-to-all-start.5 = ((f32[8,4,2,128]{3,1,2,0:T(4,128)}), f32[8,4,2,128]{3,1,2,0:T(4,128)S(1)}, u32[]{:S(2)}, u32[]{:S(2)}) async-start(f32[8,4,2,128]{3,1,2,0:T(4,128)} %bitcast.215), calls=%async_computation.5 | async-start | bytes 65536 | tf_op jit(solution)/shard_map/all_to_all | solution.py:25
  114.3 4.7 %all-to-all-done.5 = f32[8,4,2,128]{3,1,2,0:T(4,128)S(1)} async-done(((f32[8,4,2,128]{3,1,2,0:T(4,128)}), f32[8,4,2,128]{3,1,2,0:T(4,128)S(1)}, u32[]{:S(2)}, u32[]{:S(2)}) %all-to-all-start.5) | async-done | bytes 32800 | tf_op jit(solution)/shard_map/all_to_all | solution.py:25
  119.1 0.7 broadcast_in_dim.45
  119.9 6.2 %all-to-all-start.6 = ((bf16[128,8,128]{2,1,0:T(8,128)(2,1)}), bf16[128,8,128]{2,1,0:T(8,128)(2,1)S(1)}, u32[]{:S(2)}, u32[]{:S(2)}) async-start(bf16[128,8,128]{2,1,0:T(8,128)(2,1)} %broadcast_in_dim.45), calls=%async_computation.6 | async-start | bytes 524288 | tf_op jit(solution)/shard_map/all_to_all | solution.py:25
  126.6 13.1 %all-to-all-done.6 = bf16[128,8,128]{2,1,0:T(8,128)(2,1)S(1)} async-done(((bf16[128,8,128]{2,1,0:T(8,128)(2,1)}), bf16[128,8,128]{2,1,0:T(8,128)(2,1)S(1)}, u32[]{:S(2)}, u32[]{:S(2)}) %all-to-all-start.6) | async-done | bytes 262176 | tf_op jit(solution)/shard_map/all_to_all | solution.py:25
  139.7 4.4 %all-gather.1 = bf16[256,8,128]{2,1,0:T(8,128)(2,1)S(1)} all-gather(bf16[128,8,128]{2,1,0:T(8,128)(2,1)S(1)} %all-to-all-done.6), channel_id=3, replica_groups=mesh['kv_0'=8,'kv_1'=4,'tp_0'=4,'tp_1'=2] {'tp_1'}, dimensions={0}, use_global_device_ids=true | all-gather | bytes 786432 | tf_op jit(solution)/shard_map/all_gather | solution.py:190
  144.1 0.9 bitcast_reduce_fusion
  145.8 0.7 multiply_reduce_fusion
  147.9 2.0 copy.299
  149.9 3.8 %add_convert_fusion = bf16[64,4096]{0,1:T(8,128)(2,1)S(1)} fusion(f32[64,4096]{0,1:T(8,128)} %copy.299, f32[4096]{0:T(1024)S(1)} %bitcast.235, f32[4096]{0:T(1024)S(1)} %bitcast.234, f32[64]{0:T(128)S(1)} %copy-done.15, f32[64]{0:T(128)S(1)} %copy-done.14), kind=kLoop, calls=%fused_computation.3 | loop fusion | flops 1310720 | bytes 1606144 | tf_op jit(solution)/shard_map/convert_element_type | solution.py:199
  154.3 1.1 fusion.1
  156.2 1.2 collective-permute-done.1
  157.5 14.8 %all_to_all.50 = bf16[32,32,128]{2,1,0:T(8,128)(2,1)S(1)} all-to-all(bf16[32,32,128]{2,1,0:T(8,128)(2,1)S(1)} %fusion.20), channel_id=1, replica_groups=mesh['kv_0'=8,'kv_1'=4,'tp_0'=4,'tp_1'=2] {'kv_0','kv_1'}, dimensions={0} | all-to-all | bytes 524288 | tf_op jit(solution)/shard_map/all_to_all | solution.py:25
  172.3 0.6 broadcast_in_dim.46
  172.9 5.4 %all-to-all-start.8 = ((f32[8,32,128]{2,1,0:T(8,128)}), f32[8,32,128]{2,1,0:T(8,128)S(1)}, u32[]{:S(2)}, u32[]{:S(2)}) async-start(f32[8,32,128]{2,1,0:T(8,128)} %broadcast_in_dim.46), calls=%async_computation.8 | async-start | bytes 262144 | tf_op jit(solution)/shard_map/all_to_all | solution.py:25
  178.3 5.3 %all-to-all-done.8 = f32[8,32,128]{2,1,0:T(8,128)S(1)} async-done(((f32[8,32,128]{2,1,0:T(8,128)}), f32[8,32,128]{2,1,0:T(8,128)S(1)}, u32[]{:S(2)}, u32[]{:S(2)}) %all-to-all-start.8) | async-done | bytes 131104 | tf_op jit(solution)/shard_map/all_to_all | solution.py:25
  184.5 3.9 %all-to-all-start.9 = ((f32[32,1,128]{2,1,0:T(1,128)}), f32[32,1,128]{2,1,0:T(1,128)S(1)}, u32[]{:S(2)}, u32[]{:S(2)}) async-start(f32[32,1,128]{2,1,0:T(1,128)} %broadcast_in_dim.47), calls=%async_computation.9 | async-start | bytes 32768 | tf_op jit(solution)/shard_map/all_to_all | solution.py:25
  188.4 8.6 %all-to-all-done.9 = f32[32,1,128]{2,1,0:T(1,128)S(1)} async-done(((f32[32,1,128]{2,1,0:T(1,128)}), f32[32,1,128]{2,1,0:T(1,128)S(1)}, u32[]{:S(2)}, u32[]{:S(2)}) %all-to-all-start.9) | async-done | bytes 16416 | tf_op jit(solution)/shard_map/all_to_all | solution.py:25
  197.4 0.7 copy.311
  (155 shorter events, 12.1 us)
Async XLA Ops:
  0.6 46.8 %copy-start = (bf16[2,44,4096]{2,0,1:T(2,128)(2,1)S(1)}, bf16[2,44,4096]{2,0,1:T(2,128)(2,1)}, u32[]{:S(2)}) copy-start(bf16[2,44,4096]{2,0,1:T(2,128)(2,1)} %param.17) | copy-start | bytes 2162692
  0.6 29.0 %copy-start.4 = (bf16[128,512]{1,0:T(8,128)(2,1)S(1)}, bf16[128,512]{1,0:T(8,128)(2,1)}, u32[]{:S(2)}) copy-start(bf16[128,512]{1,0:T(8,128)(2,1)} %param.23) | copy-start | bytes 393220
  0.7 29.1 %copy-start.7 = (bf16[128,512]{1,0:T(8,128)(2,1)S(1)}, bf16[128,512]{1,0:T(8,128)(2,1)}, u32[]{:S(2)}) copy-start(bf16[128,512]{1,0:T(8,128)(2,1)} %param.20) | copy-start | bytes 393220
  4.3 11.9 %all-to-all-start = ((bf16[8,72,128]{2,1,0:T(8,128)(2,1)}), bf16[8,72,128]{2,1,0:T(8,128)(2,1)S(1)}, u32[]{:S(2)}, u32[]{:S(2)}) async-start(bf16[8,72,128]{2,1,0:T(8,128)(2,1)} %broadcast_in_dim.34), calls=%async_computation | async-start | bytes 294912 | tf_op jit(solution)/shard_map/all_to_all | solution.py:25
  18.1 23.1 %all-to-all-start.1 = ((bf16[32,40,128]{2,1,0:T(8,128)(2,1)}), bf16[32,40,128]{2,1,0:T(8,128)(2,1)S(1)}, u32[]{:S(2)}, u32[]{:S(2)}) async-start(bf16[32,40,128]{2,1,0:T(8,128)(2,1)} %broadcast_in_dim.36), calls=%async_computation.1 | async-start | bytes 655360 | tf_op jit(solution)/shard_map/all_to_all | solution.py:25
  45.2 2.2 %copy-start.1 = (bf16[2,4096,44]{1,0,2:T(2,128)(2,1)S(1)}, bf16[2,4096,44]{1,0,2:T(2,128)(2,1)}, u32[]{:S(2)}) copy-start(bf16[2,4096,44]{1,0,2:T(2,128)(2,1)} %param.16) | copy-start | bytes 2162692
  49.0 1.6 collective-permute-start
  50.6 30.3 %copy-start.5 = (bf16[128,512]{1,0:T(8,128)(2,1)S(1)}, bf16[128,512]{1,0:T(8,128)(2,1)}, u32[]{:S(2)}) copy-start(bf16[128,512]{1,0:T(8,128)(2,1)} %param.22) | copy-start | bytes 393220
  50.6 30.5 %copy-start.6 = (bf16[128,512]{1,0:T(8,128)(2,1)S(1)}, bf16[128,512]{1,0:T(8,128)(2,1)}, u32[]{:S(2)}) copy-start(bf16[128,512]{1,0:T(8,128)(2,1)} %param.21) | copy-start | bytes 393220
  51.6 16.8 %all-to-all-start.2 = ((bf16[32,40,128]{2,1,0:T(8,128)(2,1)}), bf16[32,40,128]{2,1,0:T(8,128)(2,1)S(1)}, u32[]{:S(2)}, u32[]{:S(2)}) async-start(bf16[32,40,128]{2,1,0:T(8,128)(2,1)} %maximum_maximum_fusion), calls=%async_computation.2 | async-start | bytes 655360 | tf_op jit(solution)/shard_map/all_to_all | solution.py:25
  69.2 11.2 %all-to-all-start.3 = ((f32[8,40,128]{2,1,0:T(8,128)}), f32[8,40,128]{2,1,0:T(8,128)S(1)}, u32[]{:S(2)}, u32[]{:S(2)}) async-start(f32[8,40,128]{2,1,0:T(8,128)} %broadcast_in_dim.40), calls=%async_computation.3 | async-start | bytes 327680 | tf_op jit(solution)/shard_map/all_to_all | solution.py:25
  80.9 5.9 %copy-start.10 = (f32[512]{0:T(512)S(1)}, f32[512]{0:T(512)}, u32[]{:S(2)}) copy-start(f32[512]{0:T(512)} %param.24) | copy-start | bytes 6148
  81.8 18.3 %copy-start.8 = (f32[2,4,128,128]{3,2,1,0:T(8,128)S(1)}, f32[2,4,128,128]{3,2,1,0:T(8,128)}, u32[]{:S(2)}) copy-start(f32[2,4,128,128]{3,2,1,0:T(8,128)} %param.27) | copy-start | bytes 1572868
  82.8 19.0 %copy-start.13 = (f32[512]{0:T(512)S(1)}, f32[512]{0:T(512)}, u32[]{:S(2)}) copy-start(f32[512]{0:T(512)} %param.25) | copy-start | bytes 6148
  82.8 16.6 %all-to-all-start.4 = ((bf16[32,40,128]{2,1,0:T(8,128)(2,1)}), bf16[32,40,128]{2,1,0:T(8,128)(2,1)S(1)}, u32[]{:S(2)}, u32[]{:S(2)}) async-start(bf16[32,40,128]{2,1,0:T(8,128)(2,1)} %copy.290), calls=%async_computation.4 | async-start | bytes 655360 | tf_op jit(solution)/shard_map/all_to_all | solution.py:25
  100.4 0.8 copy-start.2
  108.3 10.7 %all-to-all-start.5 = ((f32[8,4,2,128]{3,1,2,0:T(4,128)}), f32[8,4,2,128]{3,1,2,0:T(4,128)S(1)}, u32[]{:S(2)}, u32[]{:S(2)}) async-start(f32[8,4,2,128]{3,1,2,0:T(4,128)} %bitcast.215), calls=%async_computation.5 | async-start | bytes 65536 | tf_op jit(solution)/shard_map/all_to_all | solution.py:25
  119.9 19.9 %all-to-all-start.6 = ((bf16[128,8,128]{2,1,0:T(8,128)(2,1)}), bf16[128,8,128]{2,1,0:T(8,128)(2,1)S(1)}, u32[]{:S(2)}, u32[]{:S(2)}) async-start(bf16[128,8,128]{2,1,0:T(8,128)(2,1)} %broadcast_in_dim.45), calls=%async_computation.6 | async-start | bytes 524288 | tf_op jit(solution)/shard_map/all_to_all | solution.py:25
  147.9 2.0 %copy-start.9 = (f32[32,1,128]{2,1,0:T(1,128)S(1)}, f32[32,1,128]{2,1,0:T(1,128)}, u32[]{:S(2)}) copy-start(f32[32,1,128]{2,1,0:T(1,128)} %get-tuple-element.37) | copy-start | bytes 49156
  147.9 2.0 %copy-start.14 = (f32[64]{0:T(128)S(1)}, f32[64]{0:T(128)}, u32[]{:S(2)}) copy-start(f32[64]{0:T(128)} %div.86) | copy-start | bytes 772
  147.9 2.0 %copy-start.15 = (f32[64]{0:T(128)S(1)}, f32[64]{0:T(128)}, u32[]{:S(2)}) copy-start(f32[64]{0:T(128)} %rsqrt.37) | copy-start | bytes 772
  149.9 3.8 %copy-start.3 = (bf16[2,4096,44]{1,0,2:T(2,128)(2,1)S(1)}, bf16[2,4096,44]{1,0,2:T(2,128)(2,1)}, u32[]{:S(2)}) copy-start(bf16[2,4096,44]{1,0,2:T(2,128)(2,1)} %param.15) | copy-start | bytes 2162692
  149.9 4.4 %copy-start.16 = (pred[2]{0:T(512)(128)(4,1)S(1)}, pred[2]{0:T(512)(128)(4,1)}, u32[]{:S(2)}) copy-start(pred[2]{0:T(512)(128)(4,1)} %iota_compare_fusion.2) | copy-start | bytes 10
  155.5 32.8 %copy-start.11 = (bf16[3,16]{1,0:T(4,128)(2,1)S(1)}, bf16[3,16]{1,0:T(4,128)(2,1)}, u32[]{:S(2)}) copy-start(bf16[3,16]{1,0:T(4,128)(2,1)} %param.19) | copy-start | bytes 292
  155.5 32.8 %copy-start.12 = (bf16[3,16]{1,0:T(4,128)(2,1)S(1)}, bf16[3,16]{1,0:T(4,128)(2,1)}, u32[]{:S(2)}) copy-start(bf16[3,16]{1,0:T(4,128)(2,1)} %param.18) | copy-start | bytes 292
  155.7 1.6 collective-permute-start.1
  172.9 10.7 %all-to-all-start.8 = ((f32[8,32,128]{2,1,0:T(8,128)}), f32[8,32,128]{2,1,0:T(8,128)S(1)}, u32[]{:S(2)}, u32[]{:S(2)}) async-start(f32[8,32,128]{2,1,0:T(8,128)} %broadcast_in_dim.46), calls=%async_computation.8 | async-start | bytes 262144 | tf_op jit(solution)/shard_map/all_to_all | solution.py:25
  184.5 12.5 %all-to-all-start.9 = ((f32[32,1,128]{2,1,0:T(1,128)}), f32[32,1,128]{2,1,0:T(1,128)S(1)}, u32[]{:S(2)}, u32[]{:S(2)}) async-start(f32[32,1,128]{2,1,0:T(1,128)} %broadcast_in_dim.47), calls=%async_computation.9 | async-start | bytes 32768 | tf_op jit(solution)/shard_map/all_to_all | solution.py:25

commit v3 on v2

--- a/solution.py
+++ b/solution.py
@@ -2,6 +2,7 @@
 import jax.numpy as jnp
 from jax import lax
 from jax.experimental import pallas as pl
+from jax.experimental.pallas import tpu as pltpu
 from jax.sharding import Mesh
 from jax.sharding import PartitionSpec as P
 
@@ -42,24 +43,192 @@
     return jnp.einsum("shl,lhf->sf", hidden, down_ws, preferred_element_type=f32)
 
 
-def out_kernel(gated_ref, weight_ref, result_ref):
-    result_ref[...] = jnp.dot(gated_ref[...], weight_ref[...], preferred_element_type=f32)
-
-
-def out_projection(gated, weight):
-    rows, depth = gated.shape
-    width = weight.shape[1]
-    step = 1024
+def norm_kernel(arrived_ref, params_ref, result_ref, raw_ref):
+    cores, kv_count, x_count, rows, _ = arrived_ref.shape
+    pieces = rows // 2
+    chunks = cores * x_count * pieces
+    for x in range(x_count):
+        for core in range(cores):
+            tiles = arrived_ref[core, :, x].astype(f32)
+            raw_ref[x * cores + core] = tiles.reshape(kv_count * rows, LANES)
+
+    def lines(chunk, seq):
+        at = (chunk % pieces) * 2 + seq
+        return raw_ref[chunk // pieces, pl.ds(at, kv_count, stride=rows), :]
+
+    width = chunks * LANES
+    for seq in range(2):
+        total = sum(lines(chunk, seq) for chunk in range(chunks))
+        mean = jnp.sum(total, axis=1, keepdims=True) / width
+        squares = jnp.zeros((kv_count, LANES), f32)
+        for chunk in range(chunks):
+            off = lines(chunk, seq) - mean
+            squares = squares + off * off
+        spread = jnp.sum(squares, axis=1, keepdims=True) / width
+        scale = lax.rsqrt(spread + norm_eps)
+        for chunk in range(chunks):
+            params = params_ref[chunk].astype(f32)
+            normed = (lines(chunk, seq) - mean) * scale * params[1:2] + params[4:5]
+            result_ref[
+                seq * kv_count : (seq + 1) * kv_count, chunk * LANES : (chunk + 1) * LANES
+            ] = normed.astype(bf16)
+
+
+def norm_of_tiles(arrived, params):
+    cores, kv_count, x_count, rows, lanes = arrived.shape
     return pl.pallas_call(
-        out_kernel,
-        grid=(width // step,),
-        in_specs=[
-            pl.BlockSpec((rows, depth), lambda i: (0, 0)),
-            pl.BlockSpec((depth, step), lambda i: (0, i)),
+        norm_kernel,
+        out_shape=jax.ShapeDtypeStruct((2 * kv_count, cores * x_count * rows // 2 * lanes), bf16),
+        scratch_shapes=[pltpu.VMEM((cores * x_count, kv_count * rows, lanes), f32)],
+        name="norm_two",
+    )(arrived, params)
+
+
+def mixer_kernel(
+    tp_ref,
+    arrived_ref,
+    params_ref,
+    low_ref,
+    head_gain_ref,
+    state_hbm,
+    weight_hbm,
+    sent_ref,
+    piece_ref,
+    updated_hbm,
+    state_ref,
+    weight_ref,
+    rows_ref,
+    low_rows_ref,
+    gain_rows_ref,
+    readout_ref,
+    gated_ref,
+    state_sem,
+    weight_sem,
+    updated_sem,
+):
+    seqs, heads = state_ref.shape[:2]
+    kv_count = arrived_ref.shape[0]
+    chunks = 4 * heads
+    share = kv_count // chunks
+    parts = weight_ref.shape[0]
+    piece_chunks = kv_count // parts
+
+    state_copy = pltpu.make_async_copy(state_hbm, state_ref, state_sem)
+    state_copy.start()
+    step = weight_ref.shape[2]
+    weight_copies = [
+        pltpu.make_async_copy(
+            weight_hbm.at[:, pl.ds(part * step, step)], weight_ref.at[part], weight_sem.at[part]
+        )
+        for part in range(parts)
+    ]
+    for copy in weight_copies:
+        copy.start()
+
+    total = arrived_ref[0].astype(f32)
+    for block in range(1, kv_count):
+        total = total + arrived_ref[block].astype(f32)
+    tail = seqs * chunks
+    width = kv_count * LANES
+    mean = jnp.sum(total[tail : tail + 8], axis=1, keepdims=True) / width
+    squares = jnp.zeros((8, LANES), f32)
+    for block in range(kv_count):
+        off = arrived_ref[block, tail : tail + 8, :].astype(f32) - mean
+        squares = squares + off * off
+    scale = lax.rsqrt(jnp.sum(squares, axis=1, keepdims=True) / width + norm_eps)
+    for chunk in range(chunks):
+        bias = arrived_ref[chunk * share, tail : tail + 8, :].astype(f32)
+        for other in range(1, share):
+            bias = bias + arrived_ref[chunk * share + other, tail : tail + 8, :].astype(f32)
+        rows_ref[2 * chunk : 2 * chunk + 2, :] = jnp.broadcast_to(bias[2:3], (2, LANES))
+    odd = lax.broadcasted_iota(jnp.int32, (tail, LANES), 0) % 2 == 1
+    row_scale = jnp.where(odd, scale[1:2], scale[0:1])
+    pre = (total[:tail] * row_scale + rows_ref[...]).astype(bf16).astype(f32)
+    size = 2 * heads
+    query_pre, forget_pre = pre[:size], pre[size : 2 * size]
+    input_pre, outgate_pre = pre[2 * size : 3 * size], pre[3 * size :]
+
+    tp = tp_ref[0]
+    for chunk in range(piece_chunks):
+        at = tp * piece_chunks + chunk
+        rows = arrived_ref[at, tail : tail + 8, :].astype(f32)
+        params = params_ref[at].astype(f32)
+        rows = ((rows - mean) * scale * params[0:1] + params[3:4]).astype(bf16).astype(f32)
+        piece_ref[2 * chunk : 2 * chunk + 2, :] = residual_scale * rows[0:2]
+
+    for head in range(heads):
+        at = slice(2 * head, 2 * head + 2)
+        low_rows_ref[at, :] = jnp.broadcast_to(low_ref[head : head + 1, :], (2, LANES))
+        gain_rows_ref[at, :] = jnp.broadcast_to(head_gain_ref[head : head + 1, :], (2, LANES))
+    low = low_rows_ref[...]
+    forget = (low + (1.0 - low) * jax.nn.sigmoid(forget_pre)).T
+    key = ((1.0 - low) * jax.nn.sigmoid(-forget_pre)).T
+    query = jax.nn.silu(query_pre).T
+    state_copy.wait()
+    updated_copies = []
+    for head in range(heads):
+        for seq in range(seqs):
+            row = head * 2 + seq
+            new = (
+                forget[:, row : row + 1] * state_ref[seq, head]
+                + key[:, row : row + 1] * input_pre[row : row + 1, :]
+            )
+            state_ref[seq, head] = new
+            updated_copies.append(
+                pltpu.make_async_copy(
+                    state_ref.at[seq, head], updated_hbm.at[seq, head], updated_sem.at[row]
+                )
+            )
+            updated_copies[-1].start()
+            readout_ref[row : row + 1, :] = jnp.sum(
+                query[:, row : row + 1] * new, axis=0, keepdims=True
+            )
+    readout = readout_ref[...]
+    readout = readout * lax.rsqrt(jnp.mean(readout * readout, axis=1, keepdims=True) + head_eps)
+    gated = readout * gain_rows_ref[...] * jax.nn.silu(outgate_pre)
+    gated_ref[...] = jnp.zeros(gated_ref.shape, f32)
+    for head in range(heads):
+        gated_ref[0:2, head * HEAD : (head + 1) * HEAD] = gated[2 * head : 2 * head + 2]
+    lhs = gated_ref[...].astype(bf16)
+    for part in range(parts):
+        weight_copies[part].wait()
+        mixed = jnp.dot(lhs, weight_ref[part], preferred_element_type=f32)
+        for chunk in range(piece_chunks):
+            sent_ref[part, 2 * chunk : 2 * chunk + 2, :] = mixed[
+                0:2, chunk * LANES : (chunk + 1) * LANES
+            ]
+    for copy in updated_copies:
+        copy.wait()
+
+
+def mixer(tp, arrived, params, lower_bound, head_gain, state, weight, parts):
+    seqs, heads = state.shape[:2]
+    depth, width = weight.shape
+    rows = 2 * width // parts // LANES
+    vmem, anywhere = pl.BlockSpec(memory_space=pltpu.VMEM), pl.BlockSpec(memory_space=pl.ANY)
+    return pl.pallas_call(
+        mixer_kernel,
+        in_specs=[pl.BlockSpec(memory_space=pltpu.SMEM)] + [vmem] * 4 + [anywhere] * 2,
+        out_specs=[vmem, vmem, anywhere],
+        out_shape=[
+            jax.ShapeDtypeStruct((parts, rows, LANES), f32),
+            jax.ShapeDtypeStruct((rows, LANES), f32),
+            jax.ShapeDtypeStruct(state.shape, f32),
         ],
-        out_specs=pl.BlockSpec((rows, step), lambda i: (0, i)),
-        out_shape=jax.ShapeDtypeStruct((rows, width), f32),
-    )(gated, weight)
+        scratch_shapes=[
+            pltpu.VMEM(state.shape, f32),
+            pltpu.VMEM((parts, depth, width // parts), bf16),
+            pltpu.VMEM((seqs * 4 * heads, LANES), f32),
+            pltpu.VMEM((2 * heads, LANES), f32),
+            pltpu.VMEM((2 * heads, LANES), f32),
+            pltpu.VMEM((2 * heads, LANES), f32),
+            pltpu.VMEM((8, heads * HEAD), f32),
+            pltpu.SemaphoreType.DMA,
+            pltpu.SemaphoreType.DMA((parts,)),
+            pltpu.SemaphoreType.DMA((seqs * heads,)),
+        ],
+        name="mixer",
+    )(tp.reshape(1), arrived, params, lower_bound, head_gain, state, weight)
 
 
 def local(
@@ -79,7 +248,7 @@
     state,
 ):
     batch, own_cols = tokens.shape
-    seqs, heads = state.shape[:2]
+    heads = state.shape[1]
     kv_count, tp_count = lax.axis_size(KV), lax.axis_size(TP)
     x_count = tp_count // 2
     chip_count = kv_count * x_count
@@ -99,7 +268,7 @@
     arrived = to_everyone(jnp.concatenate([own_half, block[batch:]]), KV, kv_count)
     both = lax.all_gather(arrived, CORE, axis=0)
     whole_tokens = both[:, :, :half].swapaxes(1, 2).reshape(batch, width)
-    params = both[0, :, half:].astype(f32)
+    params = both[0, :, half:]
 
     def sum_over_kv(partial_value, extra):
         pieces = partial_value.astype(bf16).reshape(2, half, kv_count, LANES).swapaxes(1, 2)
@@ -156,47 +325,22 @@
         ],
         axis=1,
     )
-    arrived = exchange(blocks, KV).astype(f32)
-    proj_sum = arrived[:, : 2 * chunk_count].sum(axis=0).reshape(chunk_count, 2, LANES)
-    own_rows = arrived[:, 2 * chunk_count : 2 * chunk_count + 2]
-    bias_sum = arrived[:, 2 * chunk_count + 2].reshape(chunk_count, share, LANES).sum(axis=1)
-    own_rows = own_rows - jnp.mean(own_rows, axis=(0, 2), keepdims=True)
-    row_scale = lax.rsqrt(jnp.mean(own_rows * own_rows, axis=(0, 2), keepdims=True) + norm_eps)
-    pre = (proj_sum * row_scale + bias_sum[:, None]).astype(bf16).astype(f32)
-    pre = pre.reshape(4, heads, 2, HEAD).swapaxes(1, 2)
-    query_pre, forget_pre, input_pre, outgate_pre = pre[0], pre[1], pre[2], pre[3]
-
-    low_bound = lower_bound.reshape(heads, HEAD)
-    forget = low_bound + (1.0 - low_bound) * jax.nn.sigmoid(forget_pre)
-    key_part = (1.0 - low_bound) * jax.nn.sigmoid(-forget_pre)
-    updated = forget[..., None] * state + key_part[..., None] * input_pre[:, :, None, :]
-    readout = jnp.einsum(
-        "shd,shde->she", jax.nn.silu(query_pre), updated, precision=lax.Precision.HIGHEST
+    arrived = exchange(blocks, KV)
+    mixer_part, piece, updated = mixer(
+        tp,
+        arrived,
+        params,
+        lower_bound.reshape(heads, HEAD),
+        head_gain.reshape(heads, HEAD),
+        state,
+        out_weight,
+        tp_count,
     )
-    readout = readout * lax.rsqrt(jnp.mean(readout * readout, axis=-1, keepdims=True) + head_eps)
-    gated_out = (readout * head_gain.reshape(heads, HEAD) * jax.nn.silu(outgate_pre)).astype(bf16)
-    gated_rows = jnp.pad(gated_out.reshape(seqs, heads * HEAD), ((0, 8 - seqs), (0, 0)))
-    mixer_part = out_projection(gated_rows, out_weight)[:seqs]
-    piece_chunks = kv_count // tp_count
-    mixer_part = mixer_part.reshape(2, tp_count, piece_chunks, LANES).transpose(1, 2, 0, 3)
-    mixer_sum = exchange(mixer_part, TP).reshape(tp_count, piece_chunks, 2, LANES).sum(axis=0)
-    at = tp * piece_chunks
-    piece = lax.dynamic_slice_in_dim(own_rows, at, piece_chunks, 0)
-    piece_gain = lax.dynamic_slice_in_dim(params[:, 0:1], at, piece_chunks, 0)
-    piece_bias = lax.dynamic_slice_in_dim(params[:, 3:4], at, piece_chunks, 0)
-    piece = (piece * row_scale * piece_gain + piece_bias).astype(bf16).astype(f32)
-    stream_own = (residual_scale * piece + mixer_sum).astype(bf16)
-    stream_own = stream_own.reshape(2 * piece_chunks, LANES)
+    mixer_sum = exchange(mixer_part, TP).sum(axis=0)
+    stream_own = (piece + mixer_sum).astype(bf16)
     arrived = lax.all_gather(to_everyone(stream_own, CHIPS, chip_count), CORE, axis=0)
-    arrived = arrived.reshape(2, kv_count, x_count, piece_chunks, 2, LANES)
-    stream_two = arrived.transpose(4, 1, 2, 0, 3, 5).reshape(batch, width).astype(f32)
-    row_mean = jnp.mean(stream_two, axis=-1, keepdims=True)
-    centred = stream_two - row_mean
-    spread = jnp.mean(centred * centred, axis=-1, keepdims=True)
-    normed_two = (
-        centred * lax.rsqrt(spread + norm_eps) * params[:, 1].reshape(1, width)
-        + params[:, 4].reshape(1, width)
-    ).astype(bf16)
+    arrived = arrived.reshape(2, kv_count, x_count, *stream_own.shape)
+    normed_two = norm_of_tiles(arrived, params)
 
     partial_two = ffn_partial(normed_two, gate_weights, up_weights, down_weights, 1)
     total = over_tp(sum_over_kv(partial_two, None)).sum(axis=0).reshape(batch, LANES)

time: 199 us -> 194 us (0.975)
  blocking collectives: 23.2 us -> 34.1 us
  waiting for transfers between devices: 80.3 us -> 71.6 us
  local copies, waits for them, and re-layouts: 18 us -> 11 us
  starting transfers between devices: 53 us -> 46.9 us
  matrix products: 8.5 us -> 13.8 us
  Pallas kernels: 4.23 us -> 8 us
  other arithmetic: 9.47 us -> 6.56 us
    all_to_all x1 -> x2, blocking collectives: 14.8 us -> 25.5 us  [exchange(): return lax.all_to_all(blocks, axes, split_axis=0, concat_axis=0, tiled=True)]
    all_to_all x9 -> x8, waiting for transfers between devices: 78 us -> 70.1 us  [exchange(): return lax.all_to_all(blocks, axes, split_axis=0, concat_axis=0, tiled=True)]
    all_to_all x9 -> x8, starting transfers between devices: 52.1 us -> 46 us  [exchange(): return lax.all_to_all(blocks, axes, split_axis=0, concat_axis=0, tiled=True)]
    pallas_call x1 -> x2, Pallas kernels: 4.23 us -> 8 us  [the longest x1 5.54 us: mixer(): pl.pallas_call(mixer_kernel, in_specs=[pl.BlockSpec(memory_space=pltpu.SM...]
    convert_element_type x4 -> x1, other arithmetic: 3.95 us -> 0.69 us  [local(): stream_own = (piece + mixer_sum).astype(bf16)]
    convert_element_type x5 -> x0, local copies, waits for them, and re-layouts: 2.75 us -> none  [the longest x3 2.66 us: local(): arrived.transpose(4, 1, 2, 0, 3, 5).reshape(batch, width).astype(f32)]
    dot_general x2, matrix products: 2.36 us -> 4.82 us  [ffn_partial(): jnp.einsum('shl,lhf->sf', hidden, down_ws, preferred_element_type=f32)]
    reduce_sum x8 -> x1, other arithmetic: 2.11 us -> 0.01 us  [local(): mixer_sum = exchange(mixer_part, TP).sum(axis=0)]
  transfers between devices with their start and end apart: 11 -> 10, of which waited for: 11 -> 10; matrix products, arithmetic and copies ran while one was open for 2% -> 4% of each run, Pallas kernels for 0% -> 0%
where the time goes in v3:
time: 194 us; the launch traced here: 193 us
  waiting for transfers between devices  71.6 us (37%)
  starting transfers between devices  46.9 us (24%)
  blocking collectives  34.1 us (18%)
  matrix products  13.8 us (7%)
  local copies, waits for them, and re-layouts  11 us (6%)
  Pallas kernels  8 us (4%)
  other arithmetic  6.56 us (3%)
    all_to_all x8, waiting for transfers between devices, exchange(): return lax.all_to_all(blocks, axes, split_axis=0, concat_axis=0, tiled=True)  70.1 us
    all_to_all x8, starting transfers between devices, exchange(): return lax.all_to_all(blocks, axes, split_axis=0, concat_axis=0, tiled=True)  46 us
    all_to_all x2, blocking collectives, exchange(): return lax.all_to_all(blocks, axes, split_axis=0, concat_axis=0, tiled=True)  25.5 us
    pallas_call x1, Pallas kernels, mixer(): pl.pallas_call(mixer_kernel, in_specs=[pl.BlockSpec(memory_space=pltpu.SM...  5.54 us
    dot_general x2, matrix products, ffn_partial(): jnp.einsum('shl,lhf->sf', hidden, down_ws, preferred_element_type=f32)  4.82 us
    dot_general x8, matrix products, project(): jnp.dot(lines, w, preferred_element_type=f32)  4.7 us
    all_gather x1, blocking collectives, local(): lax.all_gather(to_everyone(stream_own, CHIPS, chip_count), CORE, axis=0)  4.54 us
    unnamed x33, local copies, waits for them, and re-layouts  4.3 us
  transfers between devices with their start and end apart: 10, of which 10 were waited for; matrix products, arithmetic and copies ran while one was open for 4% of the time, Pallas kernels for 0%

profile of v3, /device:TPU:1, one launch (start us, length us, event | category | flops | bytes accessed | tf_op | source)
XLA Modules:
  0.0 193.1 jit_solution(802671742479714586)
XLA Ops:
  0.7 0.9 copy.117
  1.7 0.8 copy.119
  2.5 0.8 copy.120
  3.6 0.7 broadcast_in_dim.32
  4.3 6.5 %all-to-all-start = ((bf16[8,72,128]{2,1,0:T(8,128)(2,1)}), bf16[8,72,128]{2,1,0:T(8,128)(2,1)S(1)}, u32[]{:S(2)}, u32[]{:S(2)}) async-start(bf16[8,72,128]{2,1,0:T(8,128)(2,1)} %broadcast_in_dim.32), calls=%async_computation | async-start | bytes 294912 | tf_op jit(solution)/shard_map/all_to_all | solution.py:26
  11.9 4.3 %all-to-all-done = bf16[8,72,128]{2,1,0:T(8,128)(2,1)S(1)} async-done(((bf16[8,72,128]{2,1,0:T(8,128)(2,1)}), bf16[8,72,128]{2,1,0:T(8,128)(2,1)S(1)}, u32[]{:S(2)}, u32[]{:S(2)}) %all-to-all-start) | async-done | bytes 147488 | tf_op jit(solution)/shard_map/all_to_all | solution.py:26
  16.3 0.8 broadcast_in_dim.34
  17.1 10.5 %all-to-all-start.1 = ((bf16[32,40,128]{2,1,0:T(8,128)(2,1)}), bf16[32,40,128]{2,1,0:T(8,128)(2,1)S(1)}, u32[]{:S(2)}, u32[]{:S(2)}) async-start(bf16[32,40,128]{2,1,0:T(8,128)(2,1)} %broadcast_in_dim.34), calls=%async_computation.1 | async-start | bytes 655360 | tf_op jit(solution)/shard_map/all_to_all | solution.py:26
  27.6 1.0 fusion.58
  28.6 1.0 fusion.57
  29.6 1.0 fusion.56
  30.7 1.0 fusion.55
  31.8 8.3 %all-to-all-done.1 = bf16[32,40,128]{2,1,0:T(8,128)(2,1)S(1)} async-done(((bf16[32,40,128]{2,1,0:T(8,128)(2,1)}), bf16[32,40,128]{2,1,0:T(8,128)(2,1)S(1)}, u32[]{:S(2)}, u32[]{:S(2)}) %all-to-all-start.1) | async-done | bytes 327712 | tf_op jit(solution)/shard_map/all_to_all | solution.py:26
  40.2 4.1 %all-gather = bf16[64,40,128]{2,1,0:T(8,128)(2,1)S(1)} all-gather(bf16[32,40,128]{2,1,0:T(8,128)(2,1)S(1)} %all-to-all-done.1), channel_id=2, replica_groups=mesh['kv_0'=8,'kv_1'=4,'tp_0'=4,'tp_1'=2] {'tp_1'}, dimensions={0}, use_global_device_ids=true | all-gather | bytes 983040 | tf_op jit(solution)/shard_map/all_gather | solution.py:269
  44.7 2.4 %convolution_bitcast_fusion.5 = f32[64,44,2]{0,1,2:T(8,128)} fusion(bf16[64,4096,1]{1,0,2:T(8,128)(2,1)S(1)} %reshape.153, bf16[2,4096,44]{1,0,2:T(2,128)(2,1)} %param.15), kind=kOutput, calls=%fused_computation.11 | convolution fusion | flops 46137344 | bytes 1267712 | tf_op jit(solution)/shard_map/sf,lfh->shl/dot_general | solution.py:38
  47.1 2.7 %convert_bitcast_fusion = (bf16[8,8,32,128]{3,1,2,0:T(8,128)(2,1)S(1)}, f32[64]{0:T(128)}) fusion(bf16[2,44,4096]{2,0,1:T(2,128)(2,1)S(1)} %copy-done, bf16[64,4096,1]{1,0,2:T(8,128)(2,1)S(1)} %reshape.153, bf16[2,4096,44]{1,0,2:T(2,128)(2,1)S(1)} %copy-done.1, f32[64,44,2]{0,1,2:T(8,128)} %convolution_bitcast_fusion.5, pred[2]{0:T(512)(128)(4,1)} %iota_compare_fusion.3), kind=kOutput, calls=%fused_computation.35 | convolution fusion | flops 92838336 | bytes 2513154 | tf_op jit(solution)/shard_map/shl,lhf->sf/dot_general | solution.py:43
  50.5 0.7 fusion.60
  51.8 1.5 maximum_maximum_fusion
  53.3 4.1 %all-to-all-start.2 = ((bf16[32,40,128]{2,1,0:T(8,128)(2,1)}), bf16[32,40,128]{2,1,0:T(8,128)(2,1)S(1)}, u32[]{:S(2)}, u32[]{:S(2)}) async-start(bf16[32,40,128]{2,1,0:T(8,128)(2,1)} %maximum_maximum_fusion), calls=%async_computation.2 | async-start | bytes 655360 | tf_op jit(solution)/shard_map/all_to_all | solution.py:26
  57.7 12.4 %all-to-all-done.2 = bf16[32,40,128]{2,1,0:T(8,128)(2,1)S(1)} async-done(((bf16[32,40,128]{2,1,0:T(8,128)(2,1)}), bf16[32,40,128]{2,1,0:T(8,128)(2,1)S(1)}, u32[]{:S(2)}, u32[]{:S(2)}) %all-to-all-start.2) | async-done | bytes 327712 | tf_op jit(solution)/shard_map/all_to_all | solution.py:26
  70.2 0.7 broadcast_in_dim.38
  70.9 5.7 %all-to-all-start.3 = ((f32[8,40,128]{2,1,0:T(8,128)}), f32[8,40,128]{2,1,0:T(8,128)S(1)}, u32[]{:S(2)}, u32[]{:S(2)}) async-start(f32[8,40,128]{2,1,0:T(8,128)} %broadcast_in_dim.38), calls=%async_computation.3 | async-start | bytes 327680 | tf_op jit(solution)/shard_map/all_to_all | solution.py:26
  76.5 5.6 %all-to-all-done.3 = f32[8,40,128]{2,1,0:T(8,128)S(1)} async-done(((f32[8,40,128]{2,1,0:T(8,128)}), f32[8,40,128]{2,1,0:T(8,128)S(1)}, u32[]{:S(2)}, u32[]{:S(2)}) %all-to-all-start.3) | async-done | bytes 163872 | tf_op jit(solution)/shard_map/all_to_all | solution.py:26
  83.4 0.9 maximum_maximum_fusion.1
  84.2 3.9 %all-to-all-start.4 = ((bf16[32,40,128]{2,1,0:T(8,128)(2,1)}), bf16[32,40,128]{2,1,0:T(8,128)(2,1)S(1)}, u32[]{:S(2)}, u32[]{:S(2)}) async-start(bf16[32,40,128]{2,1,0:T(8,128)(2,1)} %maximum_maximum_fusion.1), calls=%async_computation.4 | async-start | bytes 655360 | tf_op jit(solution)/shard_map/all_to_all | solution.py:26
  88.1 0.6 slice_bitcast_fusion.1.params_ref
  88.7 12.0 %all-to-all-done.4.arrived_ref = bf16[32,40,128]{2,1,0:T(8,128)(2,1)S(1)} async-done(((bf16[32,40,128]{2,1,0:T(8,128)(2,1)}), bf16[32,40,128]{2,1,0:T(8,128)(2,1)S(1)}, u32[]{:S(2)}, u32[]{:S(2)}) %all-to-all-start.4) | async-done | bytes 327712 | tf_op jit(solution)/shard_map/all_to_all | solution.py:26
  100.7 0.7 copy-done.2
  101.4 5.5 %mixer.1 = (f32[8,8,128]{2,1,0:T(8,128)}, f32[8,128]{1,0:T(8,128)}, f32[2,4,128,128]{3,2,1,0:T(8,128)}) custom-call(s32[1]{0:T(128)} %bitcast.tp_ref, bf16[32,40,128]{2,1,0:T(8,128)(2,1)} %copy-done.2, bf16[32,8,128]{2,1,0:T(8,128)(2,1)} %slice_bitcast_fusion.1.params_ref, f32[4,128]{1,0:T(4,128)} %bitcast.188, f32[4,128]{1,0:T(4,128)} %bitcast.189, ...), custom_call_target="tpu_custom_call" | custom-call | tf_op jit(solution)/shard_map/mixer/pallas_call | solution.py:209
  107.0 10.7 %all_to_all.50 = f32[8,8,128]{2,1,0:T(8,128)S(1)} all-to-all(f32[8,8,128]{2,1,0:T(8,128)} %get-tuple-element.6), channel_id=1, replica_groups=mesh['kv_0'=8,'kv_1'=4,'tp_0'=4,'tp_1'=2] {'tp_0','tp_1'}, dimensions={0} | all-to-all | bytes 65536 | tf_op jit(solution)/shard_map/all_to_all | solution.py:26
  117.7 0.7 add_convert_fusion.1
  118.4 0.7 broadcast_in_dim.42
  119.1 6.2 %all-to-all-start.6 = ((bf16[128,8,128]{2,1,0:T(8,128)(2,1)}), bf16[128,8,128]{2,1,0:T(8,128)(2,1)S(1)}, u32[]{:S(2)}, u32[]{:S(2)}) async-start(bf16[128,8,128]{2,1,0:T(8,128)(2,1)} %broadcast_in_dim.42), calls=%async_computation.6 | async-start | bytes 524288 | tf_op jit(solution)/shard_map/all_to_all | solution.py:26
  125.3 13.7 %all-to-all-done.6 = bf16[128,8,128]{2,1,0:T(8,128)(2,1)S(1)} async-done(((bf16[128,8,128]{2,1,0:T(8,128)(2,1)}), bf16[128,8,128]{2,1,0:T(8,128)(2,1)S(1)}, u32[]{:S(2)}, u32[]{:S(2)}) %all-to-all-start.6) | async-done | bytes 262176 | tf_op jit(solution)/shard_map/all_to_all | solution.py:26
  139.0 4.5 %all-gather.1 = bf16[256,8,128]{2,1,0:T(8,128)(2,1)} all-gather(bf16[128,8,128]{2,1,0:T(8,128)(2,1)S(1)} %all-to-all-done.6), channel_id=3, replica_groups=mesh['kv_0'=8,'kv_1'=4,'tp_0'=4,'tp_1'=2] {'tp_1'}, dimensions={0}, use_global_device_ids=true | all-gather | bytes 786432 | tf_op jit(solution)/shard_map/all_gather | solution.py:341
  143.5 2.5 %norm_two.1 = bf16[64,4096]{1,0:T(8,128)(2,1)} custom-call(bf16[2,32,4,8,128]{4,3,2,1,0:T(8,128)(2,1)} %bitcast.167, bf16[32,8,128]{2,1,0:T(8,128)(2,1)} %slice_bitcast_fusion.1.params_ref), custom_call_target="tpu_custom_call" | custom-call | tf_op jit(solution)/shard_map/norm_two/pallas_call | solution.py:79
  146.0 1.7 convolution_bitcast_fusion.3
  147.7 2.2 %fusion.1 = bf16[8,8,32,128]{3,1,2,0:T(8,128)(2,1)S(1)} fusion(bf16[2,44,4096]{2,0,1:T(2,128)(2,1)S(1)} %copy-done, bf16[2,4096,44]{1,0,2:T(2,128)(2,1)S(1)} %copy-done.1, bf16[64,4096]{1,0:T(8,128)(2,1)} %norm_two.1, f32[64,44,2]{0,1,2:T(8,128)S(1)} %convolution_bitcast_fusion.3, pred[2]{0:T(512)(128)(4,1)S(1)} %iota_compare_fusion.2), kind=kOutput, calls=%fused_computation.3 | convolution fusion | flops 92576256 | bytes 2512898 | tf_op jit(solution)/shard_map/shl,lhf->sf/dot_general | solution.py:43
  150.6 1.2 collective-permute-done.1
  151.8 14.8 %all_to_all.51 = bf16[32,32,128]{2,1,0:T(8,128)(2,1)S(1)} all-to-all(bf16[32,32,128]{2,1,0:T(8,128)(2,1)S(1)} %fusion.16), channel_id=1, replica_groups=mesh['kv_0'=8,'kv_1'=4,'tp_0'=4,'tp_1'=2] {'kv_0','kv_1'}, dimensions={0} | all-to-all | bytes 524288 | tf_op jit(solution)/shard_map/all_to_all | solution.py:26
  166.6 0.7 broadcast_in_dim.43
  167.3 5.4 %all-to-all-start.8 = ((f32[8,32,128]{2,1,0:T(8,128)}), f32[8,32,128]{2,1,0:T(8,128)S(1)}, u32[]{:S(2)}, u32[]{:S(2)}) async-start(f32[8,32,128]{2,1,0:T(8,128)} %broadcast_in_dim.43), calls=%async_computation.8 | async-start | bytes 262144 | tf_op jit(solution)/shard_map/all_to_all | solution.py:26
  172.7 5.3 %all-to-all-done.8 = f32[8,32,128]{2,1,0:T(8,128)S(1)} async-done(((f32[8,32,128]{2,1,0:T(8,128)}), f32[8,32,128]{2,1,0:T(8,128)S(1)}, u32[]{:S(2)}, u32[]{:S(2)}) %all-to-all-start.8) | async-done | bytes 131104 | tf_op jit(solution)/shard_map/all_to_all | solution.py:26
  178.0 0.8 fusion.59
  179.1 0.6 broadcast_in_dim.86
  179.7 3.9 %all-to-all-start.9 = ((f32[32,1,128]{2,1,0:T(1,128)}), f32[32,1,128]{2,1,0:T(1,128)S(1)}, u32[]{:S(2)}, u32[]{:S(2)}) async-start(f32[32,1,128]{2,1,0:T(1,128)} %broadcast_in_dim.86), calls=%async_computation.9 | async-start | bytes 32768 | tf_op jit(solution)/shard_map/all_to_all | solution.py:26
  183.6 8.6 %all-to-all-done.9 = f32[32,1,128]{2,1,0:T(1,128)S(1)} async-done(((f32[32,1,128]{2,1,0:T(1,128)}), f32[32,1,128]{2,1,0:T(1,128)S(1)}, u32[]{:S(2)}, u32[]{:S(2)}) %all-to-all-start.9) | async-done | bytes 16416 | tf_op jit(solution)/shard_map/all_to_all | solution.py:26
  192.5 0.7 copy.137
  (100 shorter events, 6.5 us)
Async XLA Ops:
  0.6 46.5 %copy-start = (bf16[2,44,4096]{2,0,1:T(2,128)(2,1)S(1)}, bf16[2,44,4096]{2,0,1:T(2,128)(2,1)}, u32[]{:S(2)}) copy-start(bf16[2,44,4096]{2,0,1:T(2,128)(2,1)} %param.17) | copy-start | bytes 2162692
  0.6 46.5 %copy-start.1 = (bf16[2,4096,44]{1,0,2:T(2,128)(2,1)S(1)}, bf16[2,4096,44]{1,0,2:T(2,128)(2,1)}, u32[]{:S(2)}) copy-start(bf16[2,4096,44]{1,0,2:T(2,128)(2,1)} %param.16) | copy-start | bytes 2162692
  4.3 11.9 %all-to-all-start = ((bf16[8,72,128]{2,1,0:T(8,128)(2,1)}), bf16[8,72,128]{2,1,0:T(8,128)(2,1)S(1)}, u32[]{:S(2)}, u32[]{:S(2)}) async-start(bf16[8,72,128]{2,1,0:T(8,128)(2,1)} %broadcast_in_dim.32), calls=%async_computation | async-start | bytes 294912 | tf_op jit(solution)/shard_map/all_to_all | solution.py:26
  16.2 15.6 %copy-start.7 = (bf16[72,128]{1,0:T(8,128)(2,1)}, bf16[72,128]{1,0:T(8,128)(2,1)S(1)}, u32[]{:S(2)}) copy-start(bf16[72,128]{1,0:T(8,128)(2,1)S(1)} %reduce_sum.129) | copy-start | bytes 55300
  17.1 23.1 %all-to-all-start.1 = ((bf16[32,40,128]{2,1,0:T(8,128)(2,1)}), bf16[32,40,128]{2,1,0:T(8,128)(2,1)S(1)}, u32[]{:S(2)}, u32[]{:S(2)}) async-start(bf16[32,40,128]{2,1,0:T(8,128)(2,1)} %broadcast_in_dim.34), calls=%async_computation.1 | async-start | bytes 655360 | tf_op jit(solution)/shard_map/all_to_all | solution.py:26
  47.1 35.2 %copy-start.3 = (bf16[128,512]{1,0:T(8,128)(2,1)S(1)}, bf16[128,512]{1,0:T(8,128)(2,1)}, u32[]{:S(2)}) copy-start(bf16[128,512]{1,0:T(8,128)(2,1)} %param.23) | copy-start | bytes 393220
  47.1 35.4 %copy-start.4 = (bf16[128,512]{1,0:T(8,128)(2,1)S(1)}, bf16[128,512]{1,0:T(8,128)(2,1)}, u32[]{:S(2)}) copy-start(bf16[128,512]{1,0:T(8,128)(2,1)} %param.22) | copy-start | bytes 393220
  47.1 35.5 %copy-start.5 = (bf16[128,512]{1,0:T(8,128)(2,1)S(1)}, bf16[128,512]{1,0:T(8,128)(2,1)}, u32[]{:S(2)}) copy-start(bf16[128,512]{1,0:T(8,128)(2,1)} %param.21) | copy-start | bytes 393220
  49.8 7.7 %copy-start.8 = (bf16[72,128]{1,0:T(8,128)(2,1)S(1)}, bf16[72,128]{1,0:T(8,128)(2,1)}, u32[]{:S(2)}) copy-start(bf16[72,128]{1,0:T(8,128)(2,1)} %copy-done.7) | copy-start | bytes 55300
  49.9 32.9 %copy-start.6 = (bf16[128,512]{1,0:T(8,128)(2,1)S(1)}, bf16[128,512]{1,0:T(8,128)(2,1)}, u32[]{:S(2)}) copy-start(bf16[128,512]{1,0:T(8,128)(2,1)} %param.20) | copy-start | bytes 393220
  50.1 1.6 collective-permute-start
  53.3 16.8 %all-to-all-start.2 = ((bf16[32,40,128]{2,1,0:T(8,128)(2,1)}), bf16[32,40,128]{2,1,0:T(8,128)(2,1)S(1)}, u32[]{:S(2)}, u32[]{:S(2)}) async-start(bf16[32,40,128]{2,1,0:T(8,128)(2,1)} %maximum_maximum_fusion), calls=%async_computation.2 | async-start | bytes 655360 | tf_op jit(solution)/shard_map/all_to_all | solution.py:26
  70.9 11.2 %all-to-all-start.3 = ((f32[8,40,128]{2,1,0:T(8,128)}), f32[8,40,128]{2,1,0:T(8,128)S(1)}, u32[]{:S(2)}, u32[]{:S(2)}) async-start(f32[8,40,128]{2,1,0:T(8,128)} %broadcast_in_dim.38), calls=%async_computation.3 | async-start | bytes 327680 | tf_op jit(solution)/shard_map/all_to_all | solution.py:26
  84.2 16.5 %all-to-all-start.4 = ((bf16[32,40,128]{2,1,0:T(8,128)(2,1)}), bf16[32,40,128]{2,1,0:T(8,128)(2,1)S(1)}, u32[]{:S(2)}, u32[]{:S(2)}) async-start(bf16[32,40,128]{2,1,0:T(8,128)(2,1)} %maximum_maximum_fusion.1), calls=%async_computation.4 | async-start | bytes 655360 | tf_op jit(solution)/shard_map/all_to_all | solution.py:26
  88.1 57.9 %copy-start.11 = (bf16[2,4096,44]{1,0,2:T(2,128)(2,1)S(1)}, bf16[2,4096,44]{1,0,2:T(2,128)(2,1)}, u32[]{:S(2)}) copy-start(bf16[2,4096,44]{1,0,2:T(2,128)(2,1)} %param.15) | copy-start | bytes 2162692
  100.7 0.7 copy-start.2
  119.1 19.9 %all-to-all-start.6 = ((bf16[128,8,128]{2,1,0:T(8,128)(2,1)}), bf16[128,8,128]{2,1,0:T(8,128)(2,1)S(1)}, u32[]{:S(2)}, u32[]{:S(2)}) async-start(bf16[128,8,128]{2,1,0:T(8,128)(2,1)} %broadcast_in_dim.42), calls=%async_computation.6 | async-start | bytes 524288 | tf_op jit(solution)/shard_map/all_to_all | solution.py:26
  147.6 35.9 %copy-start.9 = (bf16[3,16]{1,0:T(4,128)(2,1)S(1)}, bf16[3,16]{1,0:T(4,128)(2,1)}, u32[]{:S(2)}) copy-start(bf16[3,16]{1,0:T(4,128)(2,1)} %param.19) | copy-start | bytes 292
  147.6 35.9 %copy-start.10 = (bf16[3,16]{1,0:T(4,128)(2,1)S(1)}, bf16[3,16]{1,0:T(4,128)(2,1)}, u32[]{:S(2)}) copy-start(bf16[3,16]{1,0:T(4,128)(2,1)} %param.18) | copy-start | bytes 292
  150.1 1.6 collective-permute-start.1
  167.3 10.7 %all-to-all-start.8 = ((f32[8,32,128]{2,1,0:T(8,128)}), f32[8,32,128]{2,1,0:T(8,128)S(1)}, u32[]{:S(2)}, u32[]{:S(2)}) async-start(f32[8,32,128]{2,1,0:T(8,128)} %broadcast_in_dim.43), calls=%async_computation.8 | async-start | bytes 262144 | tf_op jit(solution)/shard_map/all_to_all | solution.py:26
  179.7 12.5 %all-to-all-start.9 = ((f32[32,1,128]{2,1,0:T(1,128)}), f32[32,1,128]{2,1,0:T(1,128)S(1)}, u32[]{:S(2)}, u32[]{:S(2)}) async-start(f32[32,1,128]{2,1,0:T(1,128)} %broadcast_in_dim.86), calls=%async_computation.9 | async-start | bytes 32768 | tf_op jit(solution)/shard_map/all_to_all | solution.py:26

commit v4 on v3

--- a/solution.py
+++ b/solution.py
@@ -80,6 +80,7 @@
         norm_kernel,
         out_shape=jax.ShapeDtypeStruct((2 * kv_count, cores * x_count * rows // 2 * lanes), bf16),
         scratch_shapes=[pltpu.VMEM((cores * x_count, kv_count * rows, lanes), f32)],
+        compiler_params=pltpu.CompilerParams(vmem_limit_bytes=8 * 2**20),
         name="norm_two",
     )(arrived, params)
 
@@ -90,40 +91,26 @@
     params_ref,
     low_ref,
     head_gain_ref,
-    state_hbm,
-    weight_hbm,
+    state_ref,
+    weight_ref,
     sent_ref,
     piece_ref,
     updated_hbm,
-    state_ref,
-    weight_ref,
+    updated_ref,
     rows_ref,
     low_rows_ref,
     gain_rows_ref,
     readout_ref,
     gated_ref,
-    state_sem,
-    weight_sem,
     updated_sem,
 ):
     seqs, heads = state_ref.shape[:2]
     kv_count = arrived_ref.shape[0]
     chunks = 4 * heads
     share = kv_count // chunks
-    parts = weight_ref.shape[0]
+    parts = sent_ref.shape[0]
     piece_chunks = kv_count // parts
-
-    state_copy = pltpu.make_async_copy(state_hbm, state_ref, state_sem)
-    state_copy.start()
-    step = weight_ref.shape[2]
-    weight_copies = [
-        pltpu.make_async_copy(
-            weight_hbm.at[:, pl.ds(part * step, step)], weight_ref.at[part], weight_sem.at[part]
-        )
-        for part in range(parts)
-    ]
-    for copy in weight_copies:
-        copy.start()
+    step = weight_ref.shape[1] // parts
 
     total = arrived_ref[0].astype(f32)
     for block in range(1, kv_count):
@@ -164,7 +151,6 @@
     forget = (low + (1.0 - low) * jax.nn.sigmoid(forget_pre)).T
     key = ((1.0 - low) * jax.nn.sigmoid(-forget_pre)).T
     query = jax.nn.silu(query_pre).T
-    state_copy.wait()
     updated_copies = []
     for head in range(heads):
         for seq in range(seqs):
@@ -173,10 +159,10 @@
                 forget[:, row : row + 1] * state_ref[seq, head]
                 + key[:, row : row + 1] * input_pre[row : row + 1, :]
             )
-            state_ref[seq, head] = new
+            updated_ref[seq, head] = new
             updated_copies.append(
                 pltpu.make_async_copy(
-                    state_ref.at[seq, head], updated_hbm.at[seq, head], updated_sem.at[row]
+                    updated_ref.at[seq, head], updated_hbm.at[seq, head], updated_sem.at[row]
                 )
             )
             updated_copies[-1].start()
@@ -191,8 +177,8 @@
         gated_ref[0:2, head * HEAD : (head + 1) * HEAD] = gated[2 * head : 2 * head + 2]
     lhs = gated_ref[...].astype(bf16)
     for part in range(parts):
-        weight_copies[part].wait()
-        mixed = jnp.dot(lhs, weight_ref[part], preferred_element_type=f32)
+        weight = weight_ref[:, part * step : (part + 1) * step]
+        mixed = jnp.dot(lhs, weight, preferred_element_type=f32)
         for chunk in range(piece_chunks):
             sent_ref[part, 2 * chunk : 2 * chunk + 2, :] = mixed[
                 0:2, chunk * LANES : (chunk + 1) * LANES
@@ -203,12 +189,12 @@
 
 def mixer(tp, arrived, params, lower_bound, head_gain, state, weight, parts):
     seqs, heads = state.shape[:2]
-    depth, width = weight.shape
+    width = weight.shape[1]
     rows = 2 * width // parts // LANES
     vmem, anywhere = pl.BlockSpec(memory_space=pltpu.VMEM), pl.BlockSpec(memory_space=pl.ANY)
     return pl.pallas_call(
         mixer_kernel,
-        in_specs=[pl.BlockSpec(memory_space=pltpu.SMEM)] + [vmem] * 4 + [anywhere] * 2,
+        in_specs=[pl.BlockSpec(memory_space=pltpu.SMEM)] + [vmem] * 6,
         out_specs=[vmem, vmem, anywhere],
         out_shape=[
             jax.ShapeDtypeStruct((parts, rows, LANES), f32),
@@ -217,16 +203,14 @@
         ],
         scratch_shapes=[
             pltpu.VMEM(state.shape, f32),
-            pltpu.VMEM((parts, depth, width // parts), bf16),
             pltpu.VMEM((seqs * 4 * heads, LANES), f32),
             pltpu.VMEM((2 * heads, LANES), f32),
             pltpu.VMEM((2 * heads, LANES), f32),
             pltpu.VMEM((2 * heads, LANES), f32),
             pltpu.VMEM((8, heads * HEAD), f32),
-            pltpu.SemaphoreType.DMA,
-            pltpu.SemaphoreType.DMA((parts,)),
             pltpu.SemaphoreType.DMA((seqs * heads,)),
         ],
+        compiler_params=pltpu.CompilerParams(vmem_limit_bytes=8 * 2**20),
         name="mixer",
     )(tp.reshape(1), arrived, params, lower_bound, head_gain, state, weight)
 

time: 194 us -> 186 us (0.959)
  Pallas kernels: 8 us -> 2.48 us
    pallas_call x1, Pallas kernels: 5.54 us -> 1.86 us  [mixer(): pl.pallas_call(mixer_kernel, in_specs=[pl.BlockSpec(memory_space=pltpu.SM...]
    unnamed x33 -> x37, local copies, waits for them, and re-layouts: 4.3 us -> 5.79 us
where the time goes in v4:
time: 186 us; the launch traced here: 185 us
  waiting for transfers between devices  72.2 us (39%)
  starting transfers between devices  46.9 us (25%)
  blocking collectives  33.1 us (18%)
  local copies, waits for them, and re-layouts  12.5 us (7%)
  matrix products  12.2 us (7%)
  other arithmetic  4.68 us (3%)
  Pallas kernels  2.48 us (1%)
    all_to_all x8, waiting for transfers between devices, exchange(): return lax.all_to_all(blocks, axes, split_axis=0, concat_axis=0, tiled=True)  70 us
    all_to_all x8, starting transfers between devices, exchange(): return lax.all_to_all(blocks, axes, split_axis=0, concat_axis=0, tiled=True)  46 us
    all_to_all x2, blocking collectives, exchange(): return lax.all_to_all(blocks, axes, split_axis=0, concat_axis=0, tiled=True)  24.6 us
    unnamed x37, local copies, waits for them, and re-layouts  5.79 us
    dot_general x8, matrix products, project(): jnp.dot(lines, w, preferred_element_type=f32)  4.7 us
    all_gather x1, blocking collectives, local(): lax.all_gather(to_everyone(stream_own, CHIPS, chip_count), CORE, axis=0)  4.41 us
    broadcast_in_dim x6, local copies, waits for them, and re-layouts, to_everyone(): return exchange(jnp.broadcast_to(block[None], (count, *block.shape)), axes)  4.13 us
    dot_general x2, matrix products, ffn_partial(): jnp.einsum('sf,lfh->shl', whole_rows, gate_ws, preferred_element_type=f32)  4.08 us
  transfers between devices with their start and end apart: 10, of which 10 were waited for; matrix products, arithmetic and copies ran while one was open for 4% of the time, Pallas kernels for 0%

profile of v4, /device:TPU:1, one launch (start us, length us, event | category | flops | bytes accessed | tf_op | source)
XLA Modules:
  0.0 185.3 jit_solution(8916576216621824974)
XLA Ops:
  0.7 0.9 copy.117
  1.7 0.8 copy.119
  2.5 0.8 copy.120
  3.6 0.7 broadcast_in_dim.32
  4.3 6.5 %all-to-all-start = ((bf16[8,72,128]{2,1,0:T(8,128)(2,1)}), bf16[8,72,128]{2,1,0:T(8,128)(2,1)S(1)}, u32[]{:S(2)}, u32[]{:S(2)}) async-start(bf16[8,72,128]{2,1,0:T(8,128)(2,1)} %broadcast_in_dim.32), calls=%async_computation | async-start | bytes 294912 | tf_op jit(solution)/shard_map/all_to_all | solution.py:26
  10.8 0.7 pad.13.clone
  11.4 4.8 %all-to-all-done = bf16[8,72,128]{2,1,0:T(8,128)(2,1)S(1)} async-done(((bf16[8,72,128]{2,1,0:T(8,128)(2,1)}), bf16[8,72,128]{2,1,0:T(8,128)(2,1)S(1)}, u32[]{:S(2)}, u32[]{:S(2)}) %all-to-all-start) | async-done | bytes 147488 | tf_op jit(solution)/shard_map/all_to_all | solution.py:26
  16.3 0.8 broadcast_in_dim.34
  17.1 10.5 %all-to-all-start.1 = ((bf16[32,40,128]{2,1,0:T(8,128)(2,1)}), bf16[32,40,128]{2,1,0:T(8,128)(2,1)S(1)}, u32[]{:S(2)}, u32[]{:S(2)}) async-start(bf16[32,40,128]{2,1,0:T(8,128)(2,1)} %broadcast_in_dim.34), calls=%async_computation.1 | async-start | bytes 655360 | tf_op jit(solution)/shard_map/all_to_all | solution.py:26
  27.6 1.0 fusion.58
  28.6 1.0 fusion.57
  29.7 1.0 fusion.56
  30.7 1.0 fusion.55
  31.8 0.6 copy.127
  32.4 7.8 %all-to-all-done.1 = bf16[32,40,128]{2,1,0:T(8,128)(2,1)S(1)} async-done(((bf16[32,40,128]{2,1,0:T(8,128)(2,1)}), bf16[32,40,128]{2,1,0:T(8,128)(2,1)S(1)}, u32[]{:S(2)}, u32[]{:S(2)}) %all-to-all-start.1) | async-done | bytes 327712 | tf_op jit(solution)/shard_map/all_to_all | solution.py:26
  40.2 4.1 %all-gather = bf16[64,40,128]{2,1,0:T(8,128)(2,1)S(1)} all-gather(bf16[32,40,128]{2,1,0:T(8,128)(2,1)S(1)} %all-to-all-done.1), channel_id=2, replica_groups=mesh['kv_0'=8,'kv_1'=4,'tp_0'=4,'tp_1'=2] {'tp_1'}, dimensions={0}, use_global_device_ids=true | all-gather | bytes 983040 | tf_op jit(solution)/shard_map/all_gather | solution.py:253
  44.7 2.4 %convolution_bitcast_fusion.5 = f32[64,44,2]{0,1,2:T(8,128)} fusion(bf16[64,4096,1]{1,0,2:T(8,128)(2,1)S(1)} %reshape.153, bf16[2,4096,44]{1,0,2:T(2,128)(2,1)} %param.15), kind=kOutput, calls=%fused_computation.11 | convolution fusion | flops 46137344 | bytes 1267712 | tf_op jit(solution)/shard_map/sf,lfh->shl/dot_general | solution.py:38
  47.1 2.1 %convert_bitcast_fusion = (bf16[8,8,32,128]{3,1,2,0:T(8,128)(2,1)S(1)}, f32[64]{0:T(128)S(1)}) fusion(bf16[2,44,4096]{2,0,1:T(2,128)(2,1)S(1)} %copy-done, bf16[64,4096,1]{1,0,2:T(8,128)(2,1)S(1)} %reshape.153, bf16[2,4096,44]{1,0,2:T(2,128)(2,1)S(1)} %copy-done.5, f32[64,44,2]{0,1,2:T(8,128)} %convolution_bitcast_fusion.5, ...), kind=kOutput, calls=%fused_computation.35 | convolution fusion | flops 92838336 | bytes 2513154 | tf_op jit(solution)/shard_map/shl,lhf->sf/dot_general | solution.py:43
  50.1 1.1 collective-permute-done
  51.3 1.6 maximum_maximum_fusion
  52.9 4.1 %all-to-all-start.2 = ((bf16[32,40,128]{2,1,0:T(8,128)(2,1)}), bf16[32,40,128]{2,1,0:T(8,128)(2,1)S(1)}, u32[]{:S(2)}, u32[]{:S(2)}) async-start(bf16[32,40,128]{2,1,0:T(8,128)(2,1)} %maximum_maximum_fusion), calls=%async_computation.2 | async-start | bytes 655360 | tf_op jit(solution)/shard_map/all_to_all | solution.py:26
  57.0 0.7 fusion.49
  57.9 11.8 %all-to-all-done.2 = bf16[32,40,128]{2,1,0:T(8,128)(2,1)S(1)} async-done(((bf16[32,40,128]{2,1,0:T(8,128)(2,1)}), bf16[32,40,128]{2,1,0:T(8,128)(2,1)S(1)}, u32[]{:S(2)}, u32[]{:S(2)}) %all-to-all-start.2) | async-done | bytes 327712 | tf_op jit(solution)/shard_map/all_to_all | solution.py:26
  69.8 0.7 broadcast_in_dim.38
  70.4 5.7 %all-to-all-start.3 = ((f32[8,40,128]{2,1,0:T(8,128)}), f32[8,40,128]{2,1,0:T(8,128)S(1)}, u32[]{:S(2)}, u32[]{:S(2)}) async-start(f32[8,40,128]{2,1,0:T(8,128)} %broadcast_in_dim.38), calls=%async_computation.3 | async-start | bytes 327680 | tf_op jit(solution)/shard_map/all_to_all | solution.py:26
  76.1 5.6 %all-to-all-done.3 = f32[8,40,128]{2,1,0:T(8,128)S(1)} async-done(((f32[8,40,128]{2,1,0:T(8,128)}), f32[8,40,128]{2,1,0:T(8,128)S(1)}, u32[]{:S(2)}, u32[]{:S(2)}) %all-to-all-start.3) | async-done | bytes 163872 | tf_op jit(solution)/shard_map/all_to_all | solution.py:26
  82.9 0.9 maximum_maximum_fusion.1
  83.8 3.9 %all-to-all-start.4 = ((bf16[32,40,128]{2,1,0:T(8,128)(2,1)}), bf16[32,40,128]{2,1,0:T(8,128)(2,1)S(1)}, u32[]{:S(2)}, u32[]{:S(2)}) async-start(bf16[32,40,128]{2,1,0:T(8,128)(2,1)} %maximum_maximum_fusion.1), calls=%async_computation.4 | async-start | bytes 655360 | tf_op jit(solution)/shard_map/all_to_all | solution.py:26
  87.7 12.6 %all-to-all-done.4.arrived_ref = bf16[32,40,128]{2,1,0:T(8,128)(2,1)S(1)} async-done(((bf16[32,40,128]{2,1,0:T(8,128)(2,1)}), bf16[32,40,128]{2,1,0:T(8,128)(2,1)S(1)}, u32[]{:S(2)}, u32[]{:S(2)}) %all-to-all-start.4) | async-done | bytes 327712 | tf_op jit(solution)/shard_map/all_to_all | solution.py:26
  100.3 2.2 %copy-done.1 = bf16[512,4096]{1,0:T(8,128)(2,1)S(1)} copy-done((bf16[512,4096]{1,0:T(8,128)(2,1)S(1)}, bf16[512,4096]{1,0:T(8,128)(2,1)}, u32[]{:S(2)}) %copy-start.1) | copy-done | bytes 4194328
  102.5 1.9 %mixer.1 = (f32[8,8,128]{2,1,0:T(8,128)S(1)}, f32[8,128]{1,0:T(8,128)S(1)}, f32[2,4,128,128]{3,2,1,0:T(8,128)}) custom-call(s32[1]{0:T(128)} %bitcast.tp_ref, bf16[32,40,128]{2,1,0:T(8,128)(2,1)S(1)} %all-to-all-done.4.arrived_ref, bf16[32,8,128]{2,1,0:T(8,128)(2,1)S(1)} %slice_bitcast_fusion.1.params_ref, f32[4,128]{1,0:T(4,128)S(1)} %bitcast.163, ...), custom_call_target="tpu_custom_call" | custom-call | tf_op jit(solution)/shard_map/mixer/pallas_call | solution.py:195
  104.4 9.8 %all_to_all.50 = f32[8,8,128]{2,1,0:T(8,128)S(1)} all-to-all(f32[8,8,128]{2,1,0:T(8,128)S(1)} %get-tuple-element.6), channel_id=1, replica_groups=mesh['kv_0'=8,'kv_1'=4,'tp_0'=4,'tp_1'=2] {'tp_0','tp_1'}, dimensions={0} | all-to-all | bytes 65536 | tf_op jit(solution)/shard_map/all_to_all | solution.py:26
  114.2 0.7 broadcast_in_dim.42
  114.9 6.2 %all-to-all-start.6 = ((bf16[128,8,128]{2,1,0:T(8,128)(2,1)}), bf16[128,8,128]{2,1,0:T(8,128)(2,1)S(1)}, u32[]{:S(2)}, u32[]{:S(2)}) async-start(bf16[128,8,128]{2,1,0:T(8,128)(2,1)} %broadcast_in_dim.42), calls=%async_computation.6 | async-start | bytes 524288 | tf_op jit(solution)/shard_map/all_to_all | solution.py:26
  121.1 13.7 %all-to-all-done.6 = bf16[128,8,128]{2,1,0:T(8,128)(2,1)S(1)} async-done(((bf16[128,8,128]{2,1,0:T(8,128)(2,1)}), bf16[128,8,128]{2,1,0:T(8,128)(2,1)S(1)}, u32[]{:S(2)}, u32[]{:S(2)}) %all-to-all-start.6) | async-done | bytes 262176 | tf_op jit(solution)/shard_map/all_to_all | solution.py:26
  134.8 4.4 %all-gather.1 = bf16[256,8,128]{2,1,0:T(8,128)(2,1)S(1)} all-gather(bf16[128,8,128]{2,1,0:T(8,128)(2,1)S(1)} %all-to-all-done.6), channel_id=3, replica_groups=mesh['kv_0'=8,'kv_1'=4,'tp_0'=4,'tp_1'=2] {'tp_1'}, dimensions={0}, use_global_device_ids=true | all-gather | bytes 786432 | tf_op jit(solution)/shard_map/all_gather | solution.py:325
  139.2 0.6 norm_two.1
  139.8 1.7 convolution_bitcast_fusion.3
  141.6 1.1 fusion.1
  143.4 1.2 collective-permute-done.1
  144.7 14.8 %all_to_all.51 = bf16[32,32,128]{2,1,0:T(8,128)(2,1)S(1)} all-to-all(bf16[32,32,128]{2,1,0:T(8,128)(2,1)S(1)} %fusion.16), channel_id=1, replica_groups=mesh['kv_0'=8,'kv_1'=4,'tp_0'=4,'tp_1'=2] {'kv_0','kv_1'}, dimensions={0} | all-to-all | bytes 524288 | tf_op jit(solution)/shard_map/all_to_all | solution.py:26
  159.5 0.6 broadcast_in_dim.43
  160.2 5.4 %all-to-all-start.8 = ((f32[8,32,128]{2,1,0:T(8,128)}), f32[8,32,128]{2,1,0:T(8,128)S(1)}, u32[]{:S(2)}, u32[]{:S(2)}) async-start(f32[8,32,128]{2,1,0:T(8,128)} %broadcast_in_dim.43), calls=%async_computation.8 | async-start | bytes 262144 | tf_op jit(solution)/shard_map/all_to_all | solution.py:26
  165.6 5.3 %all-to-all-done.8 = f32[8,32,128]{2,1,0:T(8,128)S(1)} async-done(((f32[8,32,128]{2,1,0:T(8,128)}), f32[8,32,128]{2,1,0:T(8,128)S(1)}, u32[]{:S(2)}, u32[]{:S(2)}) %all-to-all-start.8) | async-done | bytes 131104 | tf_op jit(solution)/shard_map/all_to_all | solution.py:26
  171.2 0.6 broadcast_in_dim.86
  171.9 3.9 %all-to-all-start.9 = ((f32[32,1,128]{2,1,0:T(1,128)}), f32[32,1,128]{2,1,0:T(1,128)S(1)}, u32[]{:S(2)}, u32[]{:S(2)}) async-start(f32[32,1,128]{2,1,0:T(1,128)} %broadcast_in_dim.86), calls=%async_computation.9 | async-start | bytes 32768 | tf_op jit(solution)/shard_map/all_to_all | solution.py:26
  175.8 8.6 %all-to-all-done.9 = f32[32,1,128]{2,1,0:T(1,128)S(1)} async-done(((f32[32,1,128]{2,1,0:T(1,128)}), f32[32,1,128]{2,1,0:T(1,128)S(1)}, u32[]{:S(2)}, u32[]{:S(2)}) %all-to-all-start.9) | async-done | bytes 16416 | tf_op jit(solution)/shard_map/all_to_all | solution.py:26
  184.6 0.7 copy.137
  (104 shorter events, 5.2 us)
Async XLA Ops:
  0.6 46.5 %copy-start = (bf16[2,44,4096]{2,0,1:T(2,128)(2,1)S(1)}, bf16[2,44,4096]{2,0,1:T(2,128)(2,1)}, u32[]{:S(2)}) copy-start(bf16[2,44,4096]{2,0,1:T(2,128)(2,1)} %param.17) | copy-start | bytes 2162692
  0.6 46.5 %copy-start.5 = (bf16[2,4096,44]{1,0,2:T(2,128)(2,1)S(1)}, bf16[2,4096,44]{1,0,2:T(2,128)(2,1)}, u32[]{:S(2)}) copy-start(bf16[2,4096,44]{1,0,2:T(2,128)(2,1)} %param.16) | copy-start | bytes 2162692
  4.3 11.9 %all-to-all-start = ((bf16[8,72,128]{2,1,0:T(8,128)(2,1)}), bf16[8,72,128]{2,1,0:T(8,128)(2,1)S(1)}, u32[]{:S(2)}, u32[]{:S(2)}) async-start(bf16[8,72,128]{2,1,0:T(8,128)(2,1)} %broadcast_in_dim.32), calls=%async_computation | async-start | bytes 294912 | tf_op jit(solution)/shard_map/all_to_all | solution.py:26
  16.2 16.2 %copy-start.10 = (bf16[72,128]{1,0:T(8,128)(2,1)}, bf16[72,128]{1,0:T(8,128)(2,1)S(1)}, u32[]{:S(2)}) copy-start(bf16[72,128]{1,0:T(8,128)(2,1)S(1)} %reduce_sum.129) | copy-start | bytes 55300
  17.1 23.1 %all-to-all-start.1 = ((bf16[32,40,128]{2,1,0:T(8,128)(2,1)}), bf16[32,40,128]{2,1,0:T(8,128)(2,1)S(1)}, u32[]{:S(2)}, u32[]{:S(2)}) async-start(bf16[32,40,128]{2,1,0:T(8,128)(2,1)} %broadcast_in_dim.34), calls=%async_computation.1 | async-start | bytes 655360 | tf_op jit(solution)/shard_map/all_to_all | solution.py:26
  47.1 34.8 %copy-start.6 = (bf16[128,512]{1,0:T(8,128)(2,1)S(1)}, bf16[128,512]{1,0:T(8,128)(2,1)}, u32[]{:S(2)}) copy-start(bf16[128,512]{1,0:T(8,128)(2,1)} %param.23) | copy-start | bytes 393220
  47.1 34.9 %copy-start.7 = (bf16[128,512]{1,0:T(8,128)(2,1)S(1)}, bf16[128,512]{1,0:T(8,128)(2,1)}, u32[]{:S(2)}) copy-start(bf16[128,512]{1,0:T(8,128)(2,1)} %param.22) | copy-start | bytes 393220
  47.1 35.1 %copy-start.8 = (bf16[128,512]{1,0:T(8,128)(2,1)S(1)}, bf16[128,512]{1,0:T(8,128)(2,1)}, u32[]{:S(2)}) copy-start(bf16[128,512]{1,0:T(8,128)(2,1)} %param.21) | copy-start | bytes 393220
  49.3 32.5 %copy-start.11 = (bf16[72,128]{1,0:T(8,128)(2,1)S(1)}, bf16[72,128]{1,0:T(8,128)(2,1)}, u32[]{:S(2)}) copy-start(bf16[72,128]{1,0:T(8,128)(2,1)} %copy-done.10) | copy-start | bytes 55300
  49.3 33.1 %copy-start.9 = (bf16[128,512]{1,0:T(8,128)(2,1)S(1)}, bf16[128,512]{1,0:T(8,128)(2,1)}, u32[]{:S(2)}) copy-start(bf16[128,512]{1,0:T(8,128)(2,1)} %param.20) | copy-start | bytes 393220
  49.4 50.9 %copy-start.2 = (f32[2,4,128,128]{3,2,1,0:T(8,128)S(1)}, f32[2,4,128,128]{3,2,1,0:T(8,128)}, u32[]{:S(2)}) copy-start(f32[2,4,128,128]{3,2,1,0:T(8,128)} %state_ref.1) | copy-start | bytes 1572868
  49.4 50.9 %copy-start.3 = (f32[512]{0:T(512)S(1)}, f32[512]{0:T(512)}, u32[]{:S(2)}) copy-start(f32[512]{0:T(512)} %param.24) | copy-start | bytes 6148
  49.4 50.9 %copy-start.4 = (f32[512]{0:T(512)S(1)}, f32[512]{0:T(512)}, u32[]{:S(2)}) copy-start(f32[512]{0:T(512)} %param.25) | copy-start | bytes 6148
  49.5 1.6 collective-permute-start
  52.9 16.8 %all-to-all-start.2 = ((bf16[32,40,128]{2,1,0:T(8,128)(2,1)}), bf16[32,40,128]{2,1,0:T(8,128)(2,1)S(1)}, u32[]{:S(2)}, u32[]{:S(2)}) async-start(bf16[32,40,128]{2,1,0:T(8,128)(2,1)} %maximum_maximum_fusion), calls=%async_computation.2 | async-start | bytes 655360 | tf_op jit(solution)/shard_map/all_to_all | solution.py:26
  70.4 11.2 %all-to-all-start.3 = ((f32[8,40,128]{2,1,0:T(8,128)}), f32[8,40,128]{2,1,0:T(8,128)S(1)}, u32[]{:S(2)}, u32[]{:S(2)}) async-start(f32[8,40,128]{2,1,0:T(8,128)} %broadcast_in_dim.38), calls=%async_computation.3 | async-start | bytes 327680 | tf_op jit(solution)/shard_map/all_to_all | solution.py:26
  83.8 16.5 %all-to-all-start.4 = ((bf16[32,40,128]{2,1,0:T(8,128)(2,1)}), bf16[32,40,128]{2,1,0:T(8,128)(2,1)S(1)}, u32[]{:S(2)}, u32[]{:S(2)}) async-start(bf16[32,40,128]{2,1,0:T(8,128)(2,1)} %maximum_maximum_fusion.1), calls=%async_computation.4 | async-start | bytes 655360 | tf_op jit(solution)/shard_map/all_to_all | solution.py:26
  100.3 2.2 %copy-start.1 = (bf16[512,4096]{1,0:T(8,128)(2,1)S(1)}, bf16[512,4096]{1,0:T(8,128)(2,1)}, u32[]{:S(2)}) copy-start(bf16[512,4096]{1,0:T(8,128)(2,1)} %weight_ref.1) | copy-start | bytes 12582916
  114.9 19.9 %all-to-all-start.6 = ((bf16[128,8,128]{2,1,0:T(8,128)(2,1)}), bf16[128,8,128]{2,1,0:T(8,128)(2,1)S(1)}, u32[]{:S(2)}, u32[]{:S(2)}) async-start(bf16[128,8,128]{2,1,0:T(8,128)(2,1)} %broadcast_in_dim.42), calls=%async_computation.6 | async-start | bytes 524288 | tf_op jit(solution)/shard_map/all_to_all | solution.py:26
  141.6 34.2 %copy-start.12 = (bf16[3,16]{1,0:T(4,128)(2,1)S(1)}, bf16[3,16]{1,0:T(4,128)(2,1)}, u32[]{:S(2)}) copy-start(bf16[3,16]{1,0:T(4,128)(2,1)} %param.19) | copy-start | bytes 292
  141.6 34.2 %copy-start.13 = (bf16[3,16]{1,0:T(4,128)(2,1)S(1)}, bf16[3,16]{1,0:T(4,128)(2,1)}, u32[]{:S(2)}) copy-start(bf16[3,16]{1,0:T(4,128)(2,1)} %param.18) | copy-start | bytes 292
  143.0 1.6 collective-permute-start.1
  160.2 10.7 %all-to-all-start.8 = ((f32[8,32,128]{2,1,0:T(8,128)}), f32[8,32,128]{2,1,0:T(8,128)S(1)}, u32[]{:S(2)}, u32[]{:S(2)}) async-start(f32[8,32,128]{2,1,0:T(8,128)} %broadcast_in_dim.43), calls=%async_computation.8 | async-start | bytes 262144 | tf_op jit(solution)/shard_map/all_to_all | solution.py:26
  171.9 12.5 %all-to-all-start.9 = ((f32[32,1,128]{2,1,0:T(1,128)}), f32[32,1,128]{2,1,0:T(1,128)S(1)}, u32[]{:S(2)}, u32[]{:S(2)}) async-start(f32[32,1,128]{2,1,0:T(1,128)} %broadcast_in_dim.86), calls=%async_computation.9 | async-start | bytes 32768 | tf_op jit(solution)/shard_map/all_to_all | solution.py:26

commit v5 on v3

--- a/solution.py
+++ b/solution.py
@@ -30,16 +30,21 @@
     return exchange(jnp.broadcast_to(block[None], (count, *block.shape)), axes)
 
 
-def rows_of(lines, count):
-    return jnp.pad(lines, ((0, count - lines.shape[0]), (0, LANES - lines.shape[1])))
+def alone(blocks, axes, *held):
+    blocks, *held = lax.optimization_barrier((blocks, *held))
+    return lax.optimization_barrier((exchange(blocks, axes), *held))
+
+
+def copies(block, count):
+    return jnp.broadcast_to(block[None], (count, *block.shape))
 
 
 def ffn_partial(whole_rows, gate_ws, up_ws, down_ws, layer):
     gate_proj = jnp.einsum("sf,lfh->shl", whole_rows, gate_ws, preferred_element_type=f32)
     up_proj = jnp.einsum("sf,lfh->shl", whole_rows, up_ws, preferred_element_type=f32)
     hidden = (jax.nn.silu(gate_proj) * up_proj).astype(bf16)
-    other = lax.broadcasted_iota(jnp.int32, hidden.shape, 2) != layer
-    hidden = jnp.where(other, 0, hidden)
+    own = lax.broadcasted_iota(jnp.int32, hidden.shape, 2) == layer
+    hidden = jnp.where(own, hidden, 0)
     return jnp.einsum("shl,lhf->sf", hidden, down_ws, preferred_element_type=f32)
 
 
@@ -80,6 +85,7 @@
         norm_kernel,
         out_shape=jax.ShapeDtypeStruct((2 * kv_count, cores * x_count * rows // 2 * lanes), bf16),
         scratch_shapes=[pltpu.VMEM((cores * x_count, kv_count * rows, lanes), f32)],
+        compiler_params=pltpu.CompilerParams(vmem_limit_bytes=8 * 2**20),
         name="norm_two",
     )(arrived, params)
 
@@ -90,31 +96,27 @@
     params_ref,
     low_ref,
     head_gain_ref,
-    state_hbm,
+    state_ref,
     weight_hbm,
     sent_ref,
     piece_ref,
     updated_hbm,
-    state_ref,
+    updated_ref,
     weight_ref,
     rows_ref,
     low_rows_ref,
     gain_rows_ref,
     readout_ref,
     gated_ref,
-    state_sem,
+    updated_sem,
     weight_sem,
-    updated_sem,
 ):
     seqs, heads = state_ref.shape[:2]
     kv_count = arrived_ref.shape[0]
     chunks = 4 * heads
     share = kv_count // chunks
-    parts = weight_ref.shape[0]
+    parts = sent_ref.shape[0]
     piece_chunks = kv_count // parts
-
-    state_copy = pltpu.make_async_copy(state_hbm, state_ref, state_sem)
-    state_copy.start()
     step = weight_ref.shape[2]
     weight_copies = [
         pltpu.make_async_copy(
@@ -164,7 +166,6 @@
     forget = (low + (1.0 - low) * jax.nn.sigmoid(forget_pre)).T
     key = ((1.0 - low) * jax.nn.sigmoid(-forget_pre)).T
     query = jax.nn.silu(query_pre).T
-    state_copy.wait()
     updated_copies = []
     for head in range(heads):
         for seq in range(seqs):
@@ -173,10 +174,10 @@
                 forget[:, row : row + 1] * state_ref[seq, head]
                 + key[:, row : row + 1] * input_pre[row : row + 1, :]
             )
-            state_ref[seq, head] = new
+            updated_ref[seq, head] = new
             updated_copies.append(
                 pltpu.make_async_copy(
-                    state_ref.at[seq, head], updated_hbm.at[seq, head], updated_sem.at[row]
+                    updated_ref.at[seq, head], updated_hbm.at[seq, head], updated_sem.at[row]
                 )
             )
             updated_copies[-1].start()
@@ -208,7 +209,7 @@
     vmem, anywhere = pl.BlockSpec(memory_space=pltpu.VMEM), pl.BlockSpec(memory_space=pl.ANY)
     return pl.pallas_call(
         mixer_kernel,
-        in_specs=[pl.BlockSpec(memory_space=pltpu.SMEM)] + [vmem] * 4 + [anywhere] * 2,
+        in_specs=[pl.BlockSpec(memory_space=pltpu.SMEM)] + [vmem] * 5 + [anywhere],
         out_specs=[vmem, vmem, anywhere],
         out_shape=[
             jax.ShapeDtypeStruct((parts, rows, LANES), f32),
@@ -223,12 +224,20 @@
             pltpu.VMEM((2 * heads, LANES), f32),
             pltpu.VMEM((2 * heads, LANES), f32),
             pltpu.VMEM((8, heads * HEAD), f32),
-            pltpu.SemaphoreType.DMA,
+            pltpu.SemaphoreType.DMA((seqs * heads,)),
             pltpu.SemaphoreType.DMA((parts,)),
-            pltpu.SemaphoreType.DMA((seqs * heads,)),
         ],
+        compiler_params=pltpu.CompilerParams(vmem_limit_bytes=8 * 2**20),
         name="mixer",
-    )(tp.reshape(1), arrived, params, lower_bound, head_gain, state, weight)
+    )(
+        tp.reshape(1),
+        arrived,
+        params,
+        lower_bound,
+        head_gain,
+        state,
+        pltpu.with_memory_space_constraint(weight, pltpu.HBM),
+    )
 
 
 def local(
@@ -257,33 +266,38 @@
     kv, tp, core = lax.axis_index(KV), lax.axis_index(TP), lax.axis_index(CORE)
 
     turned = tokens.reshape(kv_count, 2, own_cols).swapaxes(0, 1).reshape(batch, own_cols)
-    lines = jnp.concatenate([turned, norm_gain, norm_bias, jnp.zeros((2, own_cols), bf16)])
+    lines = jnp.concatenate([turned, norm_gain, norm_bias, norm_gain[:2]])
     place = (
         lax.broadcasted_iota(jnp.int32, (own_cols, LANES), 1)
         == lax.broadcasted_iota(jnp.int32, (own_cols, LANES), 0) + tp * own_cols
     ).astype(bf16)
     placed = jnp.dot(lines, place, preferred_element_type=f32).astype(bf16)
-    block = to_everyone(placed, TP, tp_count).astype(f32).sum(axis=0).astype(bf16)
+    first, second = jnp.int32(0), jnp.int32(1)
+    arrived, kv, tp, core, first, second, norm_gain, norm_bias = alone(
+        copies(placed, tp_count), TP, kv, tp, core, first, second, norm_gain, norm_bias
+    )
+    block = arrived.astype(f32).sum(axis=0).astype(bf16)
     own_half = lax.dynamic_slice_in_dim(block, core * half, half, 0)
     arrived = to_everyone(jnp.concatenate([own_half, block[batch:]]), KV, kv_count)
     both = lax.all_gather(arrived, CORE, axis=0)
     whole_tokens = both[:, :, :half].swapaxes(1, 2).reshape(batch, width)
     params = both[0, :, half:]
 
-    def sum_over_kv(partial_value, extra):
+    def sum_over_kv(partial_value, extra, *held):
         pieces = partial_value.astype(bf16).reshape(2, half, kv_count, LANES).swapaxes(1, 2)
         kept = lax.dynamic_index_in_dim(pieces, core, 0, keepdims=False)
         sent = lax.dynamic_index_in_dim(pieces, 1 - core, 0, keepdims=False)
         paired = (kept.astype(f32) + lax.ppermute(sent, CORE, SWAP).astype(f32)).astype(bf16)
         if extra is not None:
             paired = jnp.concatenate([paired, extra], axis=1)
-        return exchange(paired, KV).astype(f32).sum(axis=0)
-
-    def over_tp(lines):
-        gathered = to_everyone(lines, TP, tp_count)
-        return gathered.reshape(x_count, 2, *lines.shape)
-
-    partial_one = ffn_partial(whole_tokens, gate_weights, up_weights, down_weights, 0)
+        arrived, *held = alone(paired, KV, *held)
+        return arrived.astype(f32).sum(axis=0), *held
+
+    def over_tp(lines, *held):
+        gathered, *held = alone(copies(lines, tp_count), TP, *held)
+        return gathered.reshape(x_count, 2, *lines.shape), *held
+
+    partial_one = ffn_partial(whole_tokens, gate_weights, up_weights, down_weights, first)
     weights = (query_weight, forget_weight, input_weight, outgate_weight)
     chunk_count = 4 * heads
 
@@ -293,22 +307,28 @@
         )
 
     share = kv_count // chunk_count
-    gain_one, bias_one = block[batch : batch + 1], block[batch + 3 : batch + 4]
+    bias_one = block[batch + 3 : batch + 4]
     bias_part = project(bias_one)
     bias_rows = jnp.repeat(bias_part.reshape(chunk_count, 1, LANES), share, axis=0).astype(bf16)
     row_sum = partial_one.sum(axis=1)
     high = row_sum.astype(bf16)
     low = (row_sum - high.astype(f32)).astype(bf16)
     sum_row = jnp.broadcast_to(jnp.concatenate([high, low])[None, None], (kv_count, 1, LANES))
-    extra = jnp.concatenate([sum_row, bias_rows, jnp.zeros((kv_count, 6, LANES), bf16)], axis=1)
-    arrived = sum_over_kv(partial_one, extra)
-    bias_own = arrived[half + 1 : half + 2] / share
-    gathered = over_tp(arrived[: half + 8])
+    extra = jnp.concatenate([sum_row] + [bias_rows] * 7, axis=1)
+    token_sum = whole_tokens.astype(f32).sum(axis=1)
+    arrived, kv, tp, core, second, norm_gain, norm_bias, block, params, token_sum = sum_over_kv(
+        partial_one, extra, kv, tp, core, second, norm_gain, norm_bias, block, params, token_sum
+    )
+    gathered, kv, tp, core, second, norm_gain, norm_bias, block, params, token_sum, arrived = over_tp(
+        arrived, kv, tp, core, second, norm_gain, norm_bias, block, params, token_sum, arrived
+    )
+    bias_own = (arrived[half + 1 : half + 2] / share).astype(bf16)
+    gain_one = block[batch : batch + 1]
     total = gathered[:, :, :half].sum(axis=0).reshape(batch, LANES)
     total_row = gathered[:, :, half].sum(axis=(0, 1))
     stream_one = residual_scale * block[:batch].astype(f32) + 0.5 * total
     row_mean = (
-        residual_scale * whole_tokens.astype(f32).sum(axis=1)
+        residual_scale * token_sum
         + 0.5 * (total_row[:batch] + total_row[batch:])
     ) / width
     centred = stream_one - row_mean[:, None]
@@ -320,12 +340,13 @@
         [
             projected.reshape(kv_count, 2 * chunk_count, LANES),
             centred.astype(bf16).reshape(2, half, LANES).swapaxes(0, 1),
-            jnp.broadcast_to(bias_own.astype(bf16)[None], (kv_count, 1, LANES)),
-            jnp.zeros((kv_count, 5, LANES), bf16),
+            jnp.broadcast_to(bias_own[None], (kv_count, 6, LANES)),
         ],
         axis=1,
     )
-    arrived = exchange(blocks, KV)
+    arrived, kv, tp, core, second, norm_gain, norm_bias, params = alone(
+        blocks, KV, kv, tp, core, second, norm_gain, norm_bias, params
+    )
     mixer_part, piece, updated = mixer(
         tp,
         arrived,
@@ -336,21 +357,36 @@
         out_weight,
         tp_count,
     )
-    mixer_sum = exchange(mixer_part, TP).sum(axis=0)
-    stream_own = (piece + mixer_sum).astype(bf16)
-    arrived = lax.all_gather(to_everyone(stream_own, CHIPS, chip_count), CORE, axis=0)
+    arrived, kv, tp, core, second, norm_gain, norm_bias, params, piece = alone(
+        mixer_part, TP, kv, tp, core, second, norm_gain, norm_bias, params, piece
+    )
+    stream_own = (piece + arrived.sum(axis=0)).astype(bf16)
+    arrived, kv, tp, core, second, norm_gain, norm_bias, params = alone(
+        copies(stream_own, chip_count), CHIPS, kv, tp, core, second, norm_gain, norm_bias, params
+    )
+    arrived = lax.all_gather(arrived, CORE, axis=0)
     arrived = arrived.reshape(2, kv_count, x_count, *stream_own.shape)
     normed_two = norm_of_tiles(arrived, params)
 
-    partial_two = ffn_partial(normed_two, gate_weights, up_weights, down_weights, 1)
-    total = over_tp(sum_over_kv(partial_two, None)).sum(axis=0).reshape(batch, LANES)
-    own_normed = lax.dynamic_slice_in_dim(normed_two, kv * LANES, LANES, 1)
+    partial_two = ffn_partial(normed_two, gate_weights, up_weights, down_weights, second)
+    own_normed = normed_two
+    arrived, kv, tp, norm_gain, norm_bias, own_normed = sum_over_kv(
+        partial_two, None, kv, tp, norm_gain, norm_bias, own_normed
+    )
+    gathered, kv, tp, norm_gain, norm_bias, own_normed = over_tp(
+        arrived, kv, tp, norm_gain, norm_bias, own_normed
+    )
+    total = gathered.sum(axis=0).reshape(batch, LANES)
+    own_normed = lax.dynamic_slice_in_dim(own_normed, kv * LANES, LANES, 1)
     stream_three = residual_scale * own_normed.astype(f32) + 0.5 * total
     block_sum = stream_three.sum(axis=1)
     block_mean = block_sum / LANES
     off = stream_three - block_mean[:, None]
     stats = jnp.concatenate([block_mean, (off * off).sum(axis=1)])[None]
-    stats = to_everyone(stats, KV, kv_count)[:, 0]
+    stats, tp, norm_gain, norm_bias, stream_three = alone(
+        copies(stats, kv_count), KV, tp, norm_gain, norm_bias, stream_three
+    )
+    stats = stats[:, 0]
     means, squares = stats[:, :batch], stats[:, batch:]
     row_mean = means.mean(axis=0)
     spread = (squares.sum(axis=0) + LANES * ((means - row_mean) ** 2).sum(axis=0)) / width

time: 194 us -> 178 us (0.918)
  blocking collectives: 34.1 us -> 128 us
  waiting for transfers between devices: 71.6 us -> 11.9 us
  starting transfers between devices: 46.9 us -> 12 us
  matrix products: 13.8 us -> 9.67 us
  other arithmetic: 6.56 us -> 2.57 us
  Pallas kernels: 8 us -> 4.2 us
  local copies, waits for them, and re-layouts: 11 us -> 7.43 us
    all_to_all x2 -> x9, blocking collectives: 25.5 us -> 120 us  [exchange(): return lax.all_to_all(blocks, axes, split_axis=0, concat_axis=0, tiled=True)]
    all_to_all x8 -> x1, waiting for transfers between devices: 70.1 us -> 9.38 us  [exchange(): return lax.all_to_all(blocks, axes, split_axis=0, concat_axis=0, tiled=True)]
    all_to_all x8 -> x1, starting transfers between devices: 46 us -> 11.2 us  [exchange(): return lax.all_to_all(blocks, axes, split_axis=0, concat_axis=0, tiled=True)]
    broadcast_in_dim x6 -> x1, local copies, waits for them, and re-layouts: 4.14 us -> 0.77 us  [to_everyone(): return exchange(jnp.broadcast_to(block[None], (count, *block.shape)), axes)]
    dot_general x2, matrix products: 4.82 us -> 2.34 us  [ffn_partial(): jnp.einsum('shl,lhf->sf', hidden, down_ws, preferred_element_type=f32)]
    pallas_call x1, Pallas kernels: 5.54 us -> 3.58 us  [mixer(): pl.pallas_call(mixer_kernel, in_specs=[pl.BlockSpec(memory_space=pltpu.SM...]
  transfers between devices with their start and end apart: 10 -> 3, of which waited for: 10 -> 3; matrix products, arithmetic and copies ran while one was open for 4% -> 2% of each run, Pallas kernels for 0% -> 0%
where the time goes in v5:
time: 178 us; the launch traced here: 177 us
  blocking collectives  128 us (72%)
  starting transfers between devices  12 us (7%)
  waiting for transfers between devices  11.9 us (7%)
  matrix products  9.67 us (5%)
  local copies, waits for them, and re-layouts  7.43 us (4%)
  Pallas kernels  4.2 us (2%)
  other arithmetic  2.57 us (1%)
    all_to_all x9, blocking collectives, exchange(): return lax.all_to_all(blocks, axes, split_axis=0, concat_axis=0, tiled=True)  120 us
    all_to_all x1, starting transfers between devices, exchange(): return lax.all_to_all(blocks, axes, split_axis=0, concat_axis=0, tiled=True)  11.2 us
    all_to_all x1, waiting for transfers between devices, exchange(): return lax.all_to_all(blocks, axes, split_axis=0, concat_axis=0, tiled=True)  9.38 us
    all_gather x1, blocking collectives, local(): arrived = lax.all_gather(arrived, CORE, axis=0)  4.77 us
    dot_general x8, matrix products, project(): jnp.dot(lines, w, preferred_element_type=f32)  4.7 us
    unnamed x33, local copies, waits for them, and re-layouts  4.2 us
    all_gather x1, blocking collectives, local(): both = lax.all_gather(arrived, CORE, axis=0)  4.07 us
    pallas_call x1, Pallas kernels, mixer(): pl.pallas_call(mixer_kernel, in_specs=[pl.BlockSpec(memory_space=pltpu.SM...  3.58 us
  transfers between devices with their start and end apart: 3, of which 3 were waited for; matrix products, arithmetic and copies ran while one was open for 2% of the time, Pallas kernels for 0%

profile of v5, /device:TPU:1, one launch (start us, length us, event | category | flops | bytes accessed | tf_op | source)
XLA Modules:
  0.0 177.5 jit_solution(13585856063063185193)
XLA Ops:
  0.6 0.7 slice.48
  1.4 0.8 copy.142
  2.3 0.8 copy.143
  3.0 0.8 copy.140
  4.0 0.3 convolution_convert_fusion.4
  4.3 11.1 %all_to_all.50 = bf16[8,72,128]{2,1,0:T(8,128)(2,1)S(1)} all-to-all(bf16[8,72,128]{2,1,0:T(8,128)(2,1)S(1)} %broadcast_in_dim.25), channel_id=1, replica_groups=mesh['kv_0'=8,'kv_1'=4,'tp_0'=4,'tp_1'=2] {'tp_0','tp_1'}, dimensions={0} | all-to-all | bytes 294912 | tf_op jit(solution)/shard_map/all_to_all | solution.py:26
  15.5 1.0 fusion.54
  16.5 0.8 broadcast_in_dim.26
  17.3 11.2 %all-to-all-start.1 = ((bf16[32,40,128]{2,1,0:T(8,128)(2,1)}), bf16[32,40,128]{2,1,0:T(8,128)(2,1)S(1)}, u32[]{:S(2)}, u32[]{:S(2)}) async-start(bf16[32,40,128]{2,1,0:T(8,128)(2,1)} %broadcast_in_dim.26), calls=%async_computation.1 | async-start | bytes 655360 | tf_op jit(solution)/shard_map/all_to_all | solution.py:26
  28.5 1.0 fusion.53
  29.5 1.0 fusion.52
  30.6 1.0 fusion.55
  31.7 9.4 %all-to-all-done.1 = bf16[32,40,128]{2,1,0:T(8,128)(2,1)S(1)} async-done(((bf16[32,40,128]{2,1,0:T(8,128)(2,1)}), bf16[32,40,128]{2,1,0:T(8,128)(2,1)S(1)}, u32[]{:S(2)}, u32[]{:S(2)}) %all-to-all-start.1) | async-done | bytes 327712 | tf_op jit(solution)/shard_map/all_to_all | solution.py:26
  41.1 4.1 %all-gather = bf16[64,40,128]{2,1,0:T(8,128)(2,1)S(1)} all-gather(bf16[32,40,128]{2,1,0:T(8,128)(2,1)S(1)} %all-to-all-done.1), channel_id=2, replica_groups=mesh['kv_0'=8,'kv_1'=4,'tp_0'=4,'tp_1'=2] {'tp_1'}, dimensions={0}, use_global_device_ids=true | all-gather | bytes 983040 | tf_op jit(solution)/shard_map/all_gather | solution.py:282
  45.2 0.2 convert_reduce_fusion
  45.4 0.2 copy.145
  45.6 0.2 reshape.149
  45.8 1.7 convolution_bitcast_fusion.5
  47.6 1.2 fusion.57
  49.1 0.8 copy.202
  49.9 0.4 collective-permute-start
  50.4 1.3 collective-permute-done
  51.8 1.1 fusion.17
  52.9 0.3 concatenate.30
  53.2 16.6 %all_to_all.51 = bf16[32,40,128]{2,1,0:T(8,128)(2,1)S(1)} all-to-all(bf16[32,40,128]{2,1,0:T(8,128)(2,1)S(1)} %concatenate.30), channel_id=1, replica_groups=mesh['kv_0'=8,'kv_1'=4,'tp_0'=4,'tp_1'=2] {'kv_0','kv_1'}, dimensions={0} | all-to-all | bytes 655360 | tf_op jit(solution)/shard_map/all_to_all | solution.py:26
  69.9 10.3 %all_to_all.52 = f32[8,40,128]{2,1,0:T(8,128)S(1)} all-to-all(f32[8,40,128]{2,1,0:T(8,128)S(1)} %broadcast_in_dim.30), channel_id=1, replica_groups=mesh['kv_0'=8,'kv_1'=4,'tp_0'=4,'tp_1'=2] {'tp_0','tp_1'}, dimensions={0} | all-to-all | bytes 327680 | tf_op jit(solution)/shard_map/all_to_all | solution.py:26
  80.4 0.1 convolution_convert_fusion
  80.6 0.1 convolution_convert_fusion.1
  80.8 0.1 convolution_convert_fusion.2
  80.9 0.1 convolution_convert_fusion.3
  81.2 0.3 copy.159
  81.5 16.2 %all_to_all.53.arrived_ref = bf16[32,40,128]{2,1,0:T(8,128)(2,1)S(1)} all-to-all(bf16[32,40,128]{2,1,0:T(8,128)(2,1)S(1)} %pad_maximum_fusion), channel_id=1, replica_groups=mesh['kv_0'=8,'kv_1'=4,'tp_0'=4,'tp_1'=2] {'kv_0','kv_1'}, dimensions={0} | all-to-all | bytes 655360 | tf_op jit(solution)/shard_map/all_to_all | solution.py:26
  97.8 3.6 %mixer.1 = (f32[8,8,128]{2,1,0:T(8,128)S(1)}, f32[8,128]{1,0:T(8,128)S(1)}, f32[2,4,128,128]{3,2,1,0:T(8,128)}) custom-call(s32[1]{0:T(128)} %bitcast.30.tp_ref, bf16[32,40,128]{2,1,0:T(8,128)(2,1)S(1)} %all_to_all.53.arrived_ref, bf16[32,8,128]{2,1,0:T(8,128)(2,1)S(1)} %slice_bitcast_fusion.1.params_ref, f32[4,128]{1,0:T(4,128)S(1)} %bitcast.161, ...), custom_call_target="tpu_custom_call" | custom-call | tf_op jit(solution)/shard_map/mixer/pallas_call | solution.py:210
  101.4 9.3 %all_to_all.54 = f32[8,8,128]{2,1,0:T(8,128)S(1)} all-to-all(f32[8,8,128]{2,1,0:T(8,128)S(1)} %get-tuple-element.223), channel_id=1, replica_groups=mesh['kv_0'=8,'kv_1'=4,'tp_0'=4,'tp_1'=2] {'tp_0','tp_1'}, dimensions={0} | all-to-all | bytes 65536 | tf_op jit(solution)/shard_map/all_to_all | solution.py:26
  110.7 19.6 %all_to_all.55 = bf16[128,8,128]{2,1,0:T(8,128)(2,1)S(1)} all-to-all(bf16[128,8,128]{2,1,0:T(8,128)(2,1)S(1)} %broadcast_in_dim.33), channel_id=1, replica_groups=mesh['kv_0'=8,'kv_1'=4,'tp_0'=4,'tp_1'=2] {'kv_0','kv_1','tp_0'}, dimensions={0} | all-to-all | bytes 524288 | tf_op jit(solution)/shard_map/all_to_all | solution.py:26
  130.3 4.8 %all-gather.1 = bf16[256,8,128]{2,1,0:T(8,128)(2,1)S(1)} all-gather(bf16[128,8,128]{2,1,0:T(8,128)(2,1)S(1)} %all_to_all.55), channel_id=3, replica_groups=mesh['kv_0'=8,'kv_1'=4,'tp_0'=4,'tp_1'=2] {'tp_1'}, dimensions={0}, use_global_device_ids=true | all-gather | bytes 786432 | tf_op jit(solution)/shard_map/all_gather | solution.py:367
  135.1 0.6 norm_two.1
  135.7 0.6 convolution_bitcast_fusion.3
  136.4 1.1 fusion.1
  137.8 0.5 collective-permute-start.1
  138.2 1.2 collective-permute-done.1
  139.4 0.1 fusion.16
  139.5 14.8 %all_to_all.56 = bf16[32,32,128]{2,1,0:T(8,128)(2,1)S(1)} all-to-all(bf16[32,32,128]{2,1,0:T(8,128)(2,1)S(1)} %fusion.16), channel_id=1, replica_groups=mesh['kv_0'=8,'kv_1'=4,'tp_0'=4,'tp_1'=2] {'kv_0','kv_1'}, dimensions={0} | all-to-all | bytes 524288 | tf_op jit(solution)/shard_map/all_to_all | solution.py:26
  154.4 9.7 %all_to_all.57 = f32[8,32,128]{2,1,0:T(8,128)S(1)} all-to-all(f32[8,32,128]{2,1,0:T(8,128)S(1)} %broadcast_in_dim.34), channel_id=1, replica_groups=mesh['kv_0'=8,'kv_1'=4,'tp_0'=4,'tp_1'=2] {'tp_0','tp_1'}, dimensions={0} | all-to-all | bytes 262144 | tf_op jit(solution)/shard_map/all_to_all | solution.py:26
  164.1 0.1 fusion.56
  164.3 0.2 multiply_reduce_fusion
  164.5 11.9 %all_to_all.58 = f32[32,1,128]{2,1,0:T(1,128)S(1)} all-to-all(f32[32,1,128]{2,1,0:T(1,128)S(1)} %broadcast_in_dim.35), channel_id=1, replica_groups=mesh['kv_0'=8,'kv_1'=4,'tp_0'=4,'tp_1'=2] {'kv_0','kv_1'}, dimensions={0} | all-to-all | bytes 32768 | tf_op jit(solution)/shard_map/all_to_all | solution.py:26
  176.8 0.7 copy.167
  (88 shorter events, 2.0 us)
Async XLA Ops:
  0.6 47.0 %copy-start = (bf16[2,44,4096]{2,0,1:T(2,128)(2,1)S(1)}, bf16[2,44,4096]{2,0,1:T(2,128)(2,1)}, u32[]{:S(2)}) copy-start(bf16[2,44,4096]{2,0,1:T(2,128)(2,1)} %param.17) | copy-start | bytes 2162692
  4.3 43.3 %copy-start.4 = (bf16[2,4096,44]{1,0,2:T(2,128)(2,1)S(1)}, bf16[2,4096,44]{1,0,2:T(2,128)(2,1)}, u32[]{:S(2)}) copy-start(bf16[2,4096,44]{1,0,2:T(2,128)(2,1)} %param.16) | copy-start | bytes 2162692
  17.3 23.8 %all-to-all-start.1 = ((bf16[32,40,128]{2,1,0:T(8,128)(2,1)}), bf16[32,40,128]{2,1,0:T(8,128)(2,1)S(1)}, u32[]{:S(2)}, u32[]{:S(2)}) async-start(bf16[32,40,128]{2,1,0:T(8,128)(2,1)} %broadcast_in_dim.26), calls=%async_computation.1 | async-start | bytes 655360 | tf_op jit(solution)/shard_map/all_to_all | solution.py:26
  47.6 32.8 %copy-start.5 = (bf16[128,512]{1,0:T(8,128)(2,1)S(1)}, bf16[128,512]{1,0:T(8,128)(2,1)}, u32[]{:S(2)}) copy-start(bf16[128,512]{1,0:T(8,128)(2,1)} %param.23) | copy-start | bytes 393220
  47.6 33.0 %copy-start.6 = (bf16[128,512]{1,0:T(8,128)(2,1)S(1)}, bf16[128,512]{1,0:T(8,128)(2,1)}, u32[]{:S(2)}) copy-start(bf16[128,512]{1,0:T(8,128)(2,1)} %param.22) | copy-start | bytes 393220
  48.9 31.9 %copy-start.7 = (bf16[128,512]{1,0:T(8,128)(2,1)S(1)}, bf16[128,512]{1,0:T(8,128)(2,1)}, u32[]{:S(2)}) copy-start(bf16[128,512]{1,0:T(8,128)(2,1)} %param.21) | copy-start | bytes 393220
  48.9 32.0 %copy-start.8 = (bf16[128,512]{1,0:T(8,128)(2,1)S(1)}, bf16[128,512]{1,0:T(8,128)(2,1)}, u32[]{:S(2)}) copy-start(bf16[128,512]{1,0:T(8,128)(2,1)} %param.20) | copy-start | bytes 393220
  49.0 48.7 %copy-start.1 = (f32[2,4,128,128]{3,2,1,0:T(8,128)S(1)}, f32[2,4,128,128]{3,2,1,0:T(8,128)}, u32[]{:S(2)}) copy-start(f32[2,4,128,128]{3,2,1,0:T(8,128)} %state_ref.1) | copy-start | bytes 1572868
  49.1 48.7 %copy-start.2 = (f32[512]{0:T(512)S(1)}, f32[512]{0:T(512)}, u32[]{:S(2)}) copy-start(f32[512]{0:T(512)} %param.24) | copy-start | bytes 6148
  49.1 48.7 %copy-start.3 = (f32[512]{0:T(512)S(1)}, f32[512]{0:T(512)}, u32[]{:S(2)}) copy-start(f32[512]{0:T(512)} %param.25) | copy-start | bytes 6148
  49.9 1.9 %collective-permute-start = (bf16[32,32,128]{2,1,0:T(8,128)(2,1)}, bf16[32,32,128]{2,1,0:T(8,128)(2,1)}, u32[]{:S(2)}, u32[]{:S(2)}) collective-permute-start(bf16[32,32,128]{2,1,0:T(8,128)(2,1)} %bitcast.158), channel_id=1, source_target_pairs={{0,1},{1,0},{2,3},{3,2},{4,5},{5,4},{6,7},{7,6},{8,9},{9,8},{10,11... | collective-permute-start | bytes 786440 | tf_op jit(solution)/shard_map/ppermute | solution.py:290
  81.5 54.2 %copy-start.11 = (bf16[2,4096,44]{1,0,2:T(2,128)(2,1)S(1)}, bf16[2,4096,44]{1,0,2:T(2,128)(2,1)}, u32[]{:S(2)}) copy-start(bf16[2,4096,44]{1,0,2:T(2,128)(2,1)} %param.15) | copy-start | bytes 2162692
  136.4 40.3 %copy-start.9 = (bf16[3,16]{1,0:T(4,128)(2,1)S(1)}, bf16[3,16]{1,0:T(4,128)(2,1)}, u32[]{:S(2)}) copy-start(bf16[3,16]{1,0:T(4,128)(2,1)} %param.18) | copy-start | bytes 292
  136.4 40.2 %copy-start.10 = (bf16[3,16]{1,0:T(4,128)(2,1)S(1)}, bf16[3,16]{1,0:T(4,128)(2,1)}, u32[]{:S(2)}) copy-start(bf16[3,16]{1,0:T(4,128)(2,1)} %param.19) | copy-start | bytes 292
  137.8 1.6 collective-permute-start.1

commit v6 on v5

--- a/solution.py
+++ b/solution.py
@@ -39,16 +39,194 @@
     return jnp.broadcast_to(block[None], (count, *block.shape))
 
 
-def ffn_partial(whole_rows, gate_ws, up_ws, down_ws, layer):
-    gate_proj = jnp.einsum("sf,lfh->shl", whole_rows, gate_ws, preferred_element_type=f32)
-    up_proj = jnp.einsum("sf,lfh->shl", whole_rows, up_ws, preferred_element_type=f32)
-    hidden = (jax.nn.silu(gate_proj) * up_proj).astype(bf16)
-    own = lax.broadcasted_iota(jnp.int32, hidden.shape, 2) == layer
-    hidden = jnp.where(own, hidden, 0)
-    return jnp.einsum("shl,lhf->sf", hidden, down_ws, preferred_element_type=f32)
-
-
-def norm_kernel(arrived_ref, params_ref, result_ref, raw_ref):
+def small(grant=8):
+    return pltpu.CompilerParams(vmem_limit_bytes=grant * 2**20)
+
+
+VMEM = pl.BlockSpec(memory_space=pltpu.VMEM)
+SMEM = pl.BlockSpec(memory_space=pltpu.SMEM)
+ANYWHERE = pl.BlockSpec(memory_space=pl.ANY)
+
+
+def place_kernel(at_ref, tokens_ref, gain_ref, bias_ref, result_ref, lines_ref):
+    own_cols, batch = tokens_ref.shape
+    half = batch // 2
+    shape = (own_cols, LANES)
+    spot = lax.broadcasted_iota(jnp.int32, shape, 0) + at_ref[1] * own_cols
+    place = (lax.broadcasted_iota(jnp.int32, shape, 1) == spot).astype(f32).astype(bf16)
+    row = lax.broadcasted_iota(jnp.int32, (batch, batch), 0)
+    source = 2 * (row % half) + row // half
+    order = (lax.broadcasted_iota(jnp.int32, (batch, batch), 1) == source).astype(f32)
+    turned = lax.dot_general(
+        order.astype(bf16), tokens_ref[...], (((1,), (1,)), ((), ())), preferred_element_type=f32
+    ).astype(bf16)
+    lines_ref[batch:, :] = jnp.zeros((8, LANES), f32)
+    lines_ref[:batch, :] = jnp.dot(turned, place, preferred_element_type=f32)
+    lines_ref[batch : batch + 3, :] = jnp.dot(gain_ref[...], place, preferred_element_type=f32)
+    lines_ref[batch + 3 : batch + 6, :] = jnp.dot(bias_ref[...], place, preferred_element_type=f32)
+    lines = lines_ref[...].astype(bf16)
+    for copy in range(result_ref.shape[0]):
+        result_ref[copy] = lines
+
+
+def placed_copies(at, tokens, gain, bias, count):
+    batch, own_cols = tokens.shape
+    return pl.pallas_call(
+        place_kernel,
+        in_specs=[SMEM, VMEM, VMEM, VMEM],
+        out_specs=VMEM,
+        out_shape=jax.ShapeDtypeStruct((count, batch + 8, LANES), bf16),
+        scratch_shapes=[pltpu.VMEM((batch + 8, LANES), f32)],
+        compiler_params=small(),
+        name="place",
+    )(at, tokens.T, gain, bias)
+
+
+def prepare_kernel(lines_ref, w0, w1, w2, w3, weight_hbm, bias_ref, weight_ref, weight_sem):
+    parts, _, step = weight_ref.shape
+    weight_copies = [
+        pltpu.make_async_copy(
+            weight_hbm.at[:, pl.ds(part * step, step)], weight_ref.at[part], weight_sem.at[part]
+        )
+        for part in range(parts)
+    ]
+    for copy in weight_copies:
+        copy.start()
+    lines = lines_ref[...]
+    for index, w_ref in enumerate((w0, w1, w2, w3)):
+        sums = jnp.dot(lines, w_ref[...], preferred_element_type=f32)
+        heads = sums.shape[1] // LANES
+        for head in range(heads):
+            chunk = index * heads + head
+            bias_ref[chunk : chunk + 1, :] = sums[3:4, head * LANES : (head + 1) * LANES]
+    for copy in weight_copies:
+        copy.wait()
+
+
+def prepare(lines, weights, weight, parts):
+    depth, width = weight.shape
+    return pl.pallas_call(
+        prepare_kernel,
+        in_specs=[VMEM] * 5 + [ANYWHERE],
+        out_specs=[VMEM, VMEM],
+        out_shape=[
+            jax.ShapeDtypeStruct((4 * weights[0].shape[1] // LANES, LANES), f32),
+            jax.ShapeDtypeStruct((parts, depth, width // parts), bf16),
+        ],
+        scratch_shapes=[pltpu.SemaphoreType.DMA((parts,))],
+        compiler_params=small(),
+        name="prepare",
+    )(lines, *weights, pltpu.with_memory_space_constraint(weight, pltpu.HBM))
+
+
+def feed_forward(rows, core, layer, gate_ref, up_ref, down_ref):
+    def stored(ref):
+        return ref[...].reshape(ref.shape[0] * ref.shape[1], ref.shape[2])
+
+    dims = (((1,), (1,)), ((), ()))
+    gate = lax.dot_general(rows, stored(gate_ref), dims, preferred_element_type=f32)
+    up = lax.dot_general(rows, stored(up_ref), dims, preferred_element_type=f32)
+    hidden = jax.nn.silu(gate) * up
+    unit = lax.broadcasted_iota(jnp.int32, hidden.shape, 1)
+    hidden = jnp.where(unit % 2 == layer, hidden, 0.0)
+    half = hidden.shape[0] // 2
+    low, high = hidden[:half], hidden[half:]
+    first = core == 0
+    hidden = jnp.concatenate([jnp.where(first, low, high), jnp.where(first, high, low)])
+    return jnp.dot(hidden.astype(bf16), stored(down_ref), preferred_element_type=f32)
+
+
+def write_halves(part, kept_ref, sent_ref):
+    chunks, half, _ = kept_ref.shape
+    for chunk in range(chunks):
+        at = slice(chunk * LANES, (chunk + 1) * LANES)
+        kept_ref[chunk] = part[:half, at].astype(bf16)
+        sent_ref[chunk] = part[half:, at].astype(bf16)
+
+
+def first_kernel(
+    at_ref, rows_ref, gate_ref, up_ref, down_ref, kept_ref, sent_ref, tail_ref, total_ref, x_ref
+):
+    chunks, half, _ = kept_ref.shape
+    core = at_ref[2]
+    for seq in range(2):
+        at = slice(seq * half, (seq + 1) * half)
+        total = jnp.zeros((half, LANES), f32)
+        for chunk in range(chunks):
+            lines = rows_ref[seq, chunk, :half, :]
+            x_ref[at, chunk * LANES : (chunk + 1) * LANES] = lines
+            total = total + lines.astype(f32)
+        total_ref[at, :] = jnp.broadcast_to(jnp.sum(total, axis=1, keepdims=True), (half, LANES))
+    part = feed_forward(x_ref[...], core, 0, gate_ref, up_ref, down_ref)
+    write_halves(part, kept_ref, sent_ref)
+    batch = 2 * half
+    sums = jnp.broadcast_to(jnp.sum(part, axis=1, keepdims=True), (batch, LANES))
+    row = (lax.broadcasted_iota(jnp.int32, (batch, LANES), 0) + core * half) % batch
+    lane = lax.broadcasted_iota(jnp.int32, (batch, LANES), 1)
+    line = jnp.sum(jnp.where(lane % batch == row, sums, 0.0), axis=0, keepdims=True)
+    high = line.astype(bf16).astype(f32)
+    line = jnp.where(lane[:1] < batch, high, line - high)
+    tail_ref[...] = jnp.broadcast_to(line, tail_ref.shape)
+
+
+def stored_order(gate, up, down):
+    return gate.transpose(2, 0, 1), up.transpose(2, 0, 1), down.transpose(1, 0, 2)
+
+
+def first_block(at, rows, gate, up, down, half):
+    chunks = rows.shape[1]
+    return pl.pallas_call(
+        first_kernel,
+        in_specs=[SMEM] + [VMEM] * 4,
+        out_specs=[VMEM] * 4,
+        out_shape=[
+            jax.ShapeDtypeStruct((chunks, half, LANES), bf16),
+            jax.ShapeDtypeStruct((chunks, half, LANES), bf16),
+            jax.ShapeDtypeStruct((8, LANES), f32),
+            jax.ShapeDtypeStruct((2 * half, LANES), f32),
+        ],
+        scratch_shapes=[pltpu.VMEM((2 * half, chunks * LANES), bf16)],
+        compiler_params=small(12),
+        name="first_block",
+    )(at, rows, *stored_order(gate, up, down))
+
+
+def blocks_kernel(kept_ref, came_ref, tail_ref, bias_ref, result_ref):
+    chunks, half, _ = kept_ref.shape
+    share = chunks // bias_ref.shape[0]
+    top = lax.broadcasted_iota(jnp.int32, (8, LANES), 0) == 0
+    for chunk in range(chunks):
+        both = kept_ref[chunk].astype(f32) + came_ref[chunk].astype(f32)
+        result_ref[chunk, :half, :] = both.astype(bf16)
+        bias = bias_ref[chunk // share : chunk // share + 1, :]
+        result_ref[chunk, half:, :] = jnp.where(top, tail_ref[...], bias).astype(bf16)
+
+
+def first_blocks(kept, came, tail, bias):
+    chunks, half, lanes = kept.shape
+    return pl.pallas_call(
+        blocks_kernel,
+        in_specs=[VMEM] * 4,
+        out_specs=VMEM,
+        out_shape=jax.ShapeDtypeStruct((chunks, half + 8, lanes), bf16),
+        compiler_params=small(),
+        name="first_blocks",
+    )(kept, came, tail, bias)
+
+
+def second_kernel(
+    at_ref,
+    arrived_ref,
+    params_ref,
+    gate_ref,
+    up_ref,
+    down_ref,
+    kept_ref,
+    sent_ref,
+    own_ref,
+    raw_ref,
+    result_ref,
+):
     cores, kv_count, x_count, rows, _ = arrived_ref.shape
     pieces = rows // 2
     chunks = cores * x_count * pieces
@@ -77,39 +255,50 @@
             result_ref[
                 seq * kv_count : (seq + 1) * kv_count, chunk * LANES : (chunk + 1) * LANES
             ] = normed.astype(bf16)
-
-
-def norm_of_tiles(arrived, params):
+    own_ref[...] = result_ref[:, pl.ds(pl.multiple_of(at_ref[0] * LANES, LANES), LANES)]
+    part = feed_forward(result_ref[...], at_ref[2], 1, gate_ref, up_ref, down_ref)
+    write_halves(part, kept_ref, sent_ref)
+
+
+def second_block(at, arrived, params, gate, up, down):
     cores, kv_count, x_count, rows, lanes = arrived.shape
+    chunks = cores * x_count * rows // 2
     return pl.pallas_call(
-        norm_kernel,
-        out_shape=jax.ShapeDtypeStruct((2 * kv_count, cores * x_count * rows // 2 * lanes), bf16),
-        scratch_shapes=[pltpu.VMEM((cores * x_count, kv_count * rows, lanes), f32)],
-        compiler_params=pltpu.CompilerParams(vmem_limit_bytes=8 * 2**20),
-        name="norm_two",
-    )(arrived, params)
+        second_kernel,
+        in_specs=[SMEM] + [VMEM] * 5,
+        out_specs=[VMEM] * 3,
+        out_shape=[
+            jax.ShapeDtypeStruct((chunks, kv_count, lanes), bf16),
+            jax.ShapeDtypeStruct((chunks, kv_count, lanes), bf16),
+            jax.ShapeDtypeStruct((2 * kv_count, lanes), bf16),
+        ],
+        scratch_shapes=[
+            pltpu.VMEM((cores * x_count, kv_count * rows, lanes), f32),
+            pltpu.VMEM((2 * kv_count, chunks * lanes), bf16),
+        ],
+        compiler_params=small(12),
+        name="second_block",
+    )(at, arrived, params, *stored_order(gate, up, down))
 
 
 def mixer_kernel(
-    tp_ref,
+    at_ref,
     arrived_ref,
     params_ref,
     low_ref,
     head_gain_ref,
     state_ref,
-    weight_hbm,
+    weight_ref,
     sent_ref,
     piece_ref,
     updated_hbm,
     updated_ref,
-    weight_ref,
     rows_ref,
     low_rows_ref,
     gain_rows_ref,
     readout_ref,
     gated_ref,
     updated_sem,
-    weight_sem,
 ):
     seqs, heads = state_ref.shape[:2]
     kv_count = arrived_ref.shape[0]
@@ -117,16 +306,6 @@
     share = kv_count // chunks
     parts = sent_ref.shape[0]
     piece_chunks = kv_count // parts
-    step = weight_ref.shape[2]
-    weight_copies = [
-        pltpu.make_async_copy(
-            weight_hbm.at[:, pl.ds(part * step, step)], weight_ref.at[part], weight_sem.at[part]
-        )
-        for part in range(parts)
-    ]
-    for copy in weight_copies:
-        copy.start()
-
     total = arrived_ref[0].astype(f32)
     for block in range(1, kv_count):
         total = total + arrived_ref[block].astype(f32)
@@ -150,7 +329,7 @@
     query_pre, forget_pre = pre[:size], pre[size : 2 * size]
     input_pre, outgate_pre = pre[2 * size : 3 * size], pre[3 * size :]
 
-    tp = tp_ref[0]
+    tp = at_ref[1]
     for chunk in range(piece_chunks):
         at = tp * piece_chunks + chunk
         rows = arrived_ref[at, tail : tail + 8, :].astype(f32)
@@ -192,7 +371,6 @@
         gated_ref[0:2, head * HEAD : (head + 1) * HEAD] = gated[2 * head : 2 * head + 2]
     lhs = gated_ref[...].astype(bf16)
     for part in range(parts):
-        weight_copies[part].wait()
         mixed = jnp.dot(lhs, weight_ref[part], preferred_element_type=f32)
         for chunk in range(piece_chunks):
             sent_ref[part, 2 * chunk : 2 * chunk + 2, :] = mixed[
@@ -202,15 +380,14 @@
         copy.wait()
 
 
-def mixer(tp, arrived, params, lower_bound, head_gain, state, weight, parts):
+def mixer(at, arrived, params, lower_bound, head_gain, state, weight):
     seqs, heads = state.shape[:2]
-    depth, width = weight.shape
-    rows = 2 * width // parts // LANES
-    vmem, anywhere = pl.BlockSpec(memory_space=pltpu.VMEM), pl.BlockSpec(memory_space=pl.ANY)
+    parts, _, step = weight.shape
+    rows = 2 * step // LANES
     return pl.pallas_call(
         mixer_kernel,
-        in_specs=[pl.BlockSpec(memory_space=pltpu.SMEM)] + [vmem] * 5 + [anywhere],
-        out_specs=[vmem, vmem, anywhere],
+        in_specs=[SMEM] + [VMEM] * 6,
+        out_specs=[VMEM, VMEM, ANYWHERE],
         out_shape=[
             jax.ShapeDtypeStruct((parts, rows, LANES), f32),
             jax.ShapeDtypeStruct((rows, LANES), f32),
@@ -218,26 +395,16 @@
         ],
         scratch_shapes=[
             pltpu.VMEM(state.shape, f32),
-            pltpu.VMEM((parts, depth, width // parts), bf16),
             pltpu.VMEM((seqs * 4 * heads, LANES), f32),
             pltpu.VMEM((2 * heads, LANES), f32),
             pltpu.VMEM((2 * heads, LANES), f32),
             pltpu.VMEM((2 * heads, LANES), f32),
             pltpu.VMEM((8, heads * HEAD), f32),
             pltpu.SemaphoreType.DMA((seqs * heads,)),
-            pltpu.SemaphoreType.DMA((parts,)),
-        ],
-        compiler_params=pltpu.CompilerParams(vmem_limit_bytes=8 * 2**20),
+        ],
+        compiler_params=small(),
         name="mixer",
-    )(
-        tp.reshape(1),
-        arrived,
-        params,
-        lower_bound,
-        head_gain,
-        state,
-        pltpu.with_memory_space_constraint(weight, pltpu.HBM),
-    )
+    )(at, arrived, params, lower_bound, head_gain, state, weight)
 
 
 def local(
@@ -265,62 +432,35 @@
     width = own_cols * kv_count * tp_count
     kv, tp, core = lax.axis_index(KV), lax.axis_index(TP), lax.axis_index(CORE)
 
-    turned = tokens.reshape(kv_count, 2, own_cols).swapaxes(0, 1).reshape(batch, own_cols)
-    lines = jnp.concatenate([turned, norm_gain, norm_bias, norm_gain[:2]])
-    place = (
-        lax.broadcasted_iota(jnp.int32, (own_cols, LANES), 1)
-        == lax.broadcasted_iota(jnp.int32, (own_cols, LANES), 0) + tp * own_cols
-    ).astype(bf16)
-    placed = jnp.dot(lines, place, preferred_element_type=f32).astype(bf16)
-    first, second = jnp.int32(0), jnp.int32(1)
-    arrived, kv, tp, core, first, second, norm_gain, norm_bias = alone(
-        copies(placed, tp_count), TP, kv, tp, core, first, second, norm_gain, norm_bias
+    at = jnp.stack([kv, tp, core])
+    blocks = placed_copies(at, tokens, norm_gain, norm_bias, tp_count)
+    arrived, at, kv, tp, core, norm_gain, norm_bias = alone(
+        blocks, TP, at, kv, tp, core, norm_gain, norm_bias
     )
     block = arrived.astype(f32).sum(axis=0).astype(bf16)
     own_half = lax.dynamic_slice_in_dim(block, core * half, half, 0)
     arrived = to_everyone(jnp.concatenate([own_half, block[batch:]]), KV, kv_count)
     both = lax.all_gather(arrived, CORE, axis=0)
-    whole_tokens = both[:, :, :half].swapaxes(1, 2).reshape(batch, width)
     params = both[0, :, half:]
-
-    def sum_over_kv(partial_value, extra, *held):
-        pieces = partial_value.astype(bf16).reshape(2, half, kv_count, LANES).swapaxes(1, 2)
-        kept = lax.dynamic_index_in_dim(pieces, core, 0, keepdims=False)
-        sent = lax.dynamic_index_in_dim(pieces, 1 - core, 0, keepdims=False)
-        paired = (kept.astype(f32) + lax.ppermute(sent, CORE, SWAP).astype(f32)).astype(bf16)
-        if extra is not None:
-            paired = jnp.concatenate([paired, extra], axis=1)
-        arrived, *held = alone(paired, KV, *held)
-        return arrived.astype(f32).sum(axis=0), *held
 
     def over_tp(lines, *held):
         gathered, *held = alone(copies(lines, tp_count), TP, *held)
         return gathered.reshape(x_count, 2, *lines.shape), *held
 
-    partial_one = ffn_partial(whole_tokens, gate_weights, up_weights, down_weights, first)
     weights = (query_weight, forget_weight, input_weight, outgate_weight)
     chunk_count = 4 * heads
-
-    def project(lines):
-        return jnp.concatenate(
-            [jnp.dot(lines, w, preferred_element_type=f32) for w in weights], axis=1
-        )
-
     share = kv_count // chunk_count
-    bias_one = block[batch + 3 : batch + 4]
-    bias_part = project(bias_one)
-    bias_rows = jnp.repeat(bias_part.reshape(chunk_count, 1, LANES), share, axis=0).astype(bf16)
-    row_sum = partial_one.sum(axis=1)
-    high = row_sum.astype(bf16)
-    low = (row_sum - high.astype(f32)).astype(bf16)
-    sum_row = jnp.broadcast_to(jnp.concatenate([high, low])[None, None], (kv_count, 1, LANES))
-    extra = jnp.concatenate([sum_row] + [bias_rows] * 7, axis=1)
-    token_sum = whole_tokens.astype(f32).sum(axis=1)
-    arrived, kv, tp, core, second, norm_gain, norm_bias, block, params, token_sum = sum_over_kv(
-        partial_one, extra, kv, tp, core, second, norm_gain, norm_bias, block, params, token_sum
-    )
-    gathered, kv, tp, core, second, norm_gain, norm_bias, block, params, token_sum, arrived = over_tp(
-        arrived, kv, tp, core, second, norm_gain, norm_bias, block, params, token_sum, arrived
+    bias_rows, mixer_weight = prepare(block[batch:], weights, out_weight, tp_count)
+    kept, sent, tail, token_sum = first_block(
+        at, both, gate_weights, up_weights, down_weights, half
+    )
+    blocks = first_blocks(kept, lax.ppermute(sent, CORE, SWAP), tail, bias_rows)
+    arrived, at, kv, tp, norm_gain, norm_bias, block, params, token_sum = alone(
+        blocks, KV, at, kv, tp, norm_gain, norm_bias, block, params, token_sum
+    )
+    arrived = arrived.astype(f32).sum(axis=0)
+    gathered, at, kv, tp, norm_gain, norm_bias, block, params, token_sum, arrived = over_tp(
+        arrived, at, kv, tp, norm_gain, norm_bias, block, params, token_sum, arrived
     )
     bias_own = (arrived[half + 1 : half + 2] / share).astype(bf16)
     gain_one = block[batch : batch + 1]
@@ -328,13 +468,15 @@
     total_row = gathered[:, :, half].sum(axis=(0, 1))
     stream_one = residual_scale * block[:batch].astype(f32) + 0.5 * total
     row_mean = (
-        residual_scale * token_sum
+        residual_scale * token_sum[:, 0]
         + 0.5 * (total_row[:batch] + total_row[batch:])
     ) / width
     centred = stream_one - row_mean[:, None]
 
     scaled = (centred * gain_one.astype(f32)).astype(bf16)
-    projected = project(scaled).astype(bf16)
+    projected = jnp.concatenate(
+        [jnp.dot(scaled, w, preferred_element_type=f32) for w in weights], axis=1
+    ).astype(bf16)
     projected = projected.reshape(2, half, chunk_count, LANES).transpose(1, 2, 0, 3)
     blocks = jnp.concatenate(
         [
@@ -344,40 +486,40 @@
         ],
         axis=1,
     )
-    arrived, kv, tp, core, second, norm_gain, norm_bias, params = alone(
-        blocks, KV, kv, tp, core, second, norm_gain, norm_bias, params
+    arrived, at, kv, tp, norm_gain, norm_bias, params = alone(
+        blocks, KV, at, kv, tp, norm_gain, norm_bias, params
     )
     mixer_part, piece, updated = mixer(
-        tp,
+        at,
         arrived,
         params,
         lower_bound.reshape(heads, HEAD),
         head_gain.reshape(heads, HEAD),
         state,
-        out_weight,
-        tp_count,
-    )
-    arrived, kv, tp, core, second, norm_gain, norm_bias, params, piece = alone(
-        mixer_part, TP, kv, tp, core, second, norm_gain, norm_bias, params, piece
+        mixer_weight,
+    )
+    arrived, at, tp, norm_gain, norm_bias, params, piece = alone(
+        mixer_part, TP, at, tp, norm_gain, norm_bias, params, piece
     )
     stream_own = (piece + arrived.sum(axis=0)).astype(bf16)
-    arrived, kv, tp, core, second, norm_gain, norm_bias, params = alone(
-        copies(stream_own, chip_count), CHIPS, kv, tp, core, second, norm_gain, norm_bias, params
+    arrived, at, tp, norm_gain, norm_bias, params = alone(
+        copies(stream_own, chip_count), CHIPS, at, tp, norm_gain, norm_bias, params
     )
     arrived = lax.all_gather(arrived, CORE, axis=0)
     arrived = arrived.reshape(2, kv_count, x_count, *stream_own.shape)
-    normed_two = norm_of_tiles(arrived, params)
-
-    partial_two = ffn_partial(normed_two, gate_weights, up_weights, down_weights, second)
-    own_normed = normed_two
-    arrived, kv, tp, norm_gain, norm_bias, own_normed = sum_over_kv(
-        partial_two, None, kv, tp, norm_gain, norm_bias, own_normed
-    )
-    gathered, kv, tp, norm_gain, norm_bias, own_normed = over_tp(
-        arrived, kv, tp, norm_gain, norm_bias, own_normed
+
+    kept, sent, own_normed = second_block(
+        at, arrived, params, gate_weights, up_weights, down_weights
+    )
+    came = lax.ppermute(sent, CORE, SWAP)
+    blocks = (kept.astype(f32) + came.astype(f32)).astype(bf16)
+    arrived, tp, norm_gain, norm_bias, own_normed = alone(
+        blocks, KV, tp, norm_gain, norm_bias, own_normed
+    )
+    gathered, tp, norm_gain, norm_bias, own_normed = over_tp(
+        arrived.astype(f32).sum(axis=0), tp, norm_gain, norm_bias, own_normed
     )
     total = gathered.sum(axis=0).reshape(batch, LANES)
-    own_normed = lax.dynamic_slice_in_dim(own_normed, kv * LANES, LANES, 1)
     stream_three = residual_scale * own_normed.astype(f32) + 0.5 * total
     block_sum = stream_three.sum(axis=1)
     block_mean = block_sum / LANES

time: 178 us -> 174 us (0.978)
  blocking collectives: 128 us -> 152 us
  starting transfers between devices: 12 us -> 0.92 us
  waiting for transfers between devices: 11.9 us -> 1.16 us
  matrix products: 9.67 us -> 0.57 us
  Pallas kernels: 4.2 us -> 9.37 us
    all_to_all x9 -> x10, blocking collectives: 120 us -> 143 us  [exchange(): return lax.all_to_all(blocks, axes, split_axis=0, concat_axis=0, tiled=True)]
    all_to_all x1 -> x0, starting transfers between devices: 11.2 us -> none  [exchange(): return lax.all_to_all(blocks, axes, split_axis=0, concat_axis=0, tiled=True)]
    all_to_all x1 -> x0, waiting for transfers between devices: 9.38 us -> none  [exchange(): return lax.all_to_all(blocks, axes, split_axis=0, concat_axis=0, tiled=True)]
    dot_general x13 -> x4, matrix products: 9.67 us -> 0.57 us  [local(): jnp.dot(scaled, w, preferred_element_type=f32)]
    pallas_call x2 -> x6, Pallas kernels: 4.2 us -> 9.37 us  [the longest x1 2.4 us: mixer(): pl.pallas_call(mixer_kernel, in_specs=[SMEM] + [VMEM] * 6, out_specs=[VME...]
    unnamed x33 -> x38, local copies, waits for them, and re-layouts: 4.2 us -> 6.27 us
  transfers between devices with their start and end apart: 3 -> 2, of which waited for: 3 -> 1; matrix products, arithmetic and copies ran while one was open for 2% -> 0% of each run, Pallas kernels for 0% -> 1%
where the time goes in v6:
time: 174 us; the launch traced here: 173 us
  blocking collectives  152 us (87%)
  Pallas kernels  9.37 us (5%)
  local copies, waits for them, and re-layouts  6.73 us (4%)
    all_to_all x10, blocking collectives, exchange(): return lax.all_to_all(blocks, axes, split_axis=0, concat_axis=0, tiled=True)  143 us
    unnamed x38, local copies, waits for them, and re-layouts  6.27 us
    all_gather x1, blocking collectives, local(): arrived = lax.all_gather(arrived, CORE, axis=0)  4.59 us
    all_gather x1, blocking collectives, local(): both = lax.all_gather(arrived, CORE, axis=0)  4.07 us
  transfers between devices with their start and end apart: 2, of which 1 were waited for; matrix products, arithmetic and copies ran while one was open for 0% of the time, Pallas kernels for 1%

profile of v6, /device:TPU:1, one launch (start us, length us, event | category | flops | bytes accessed | tf_op | source)
XLA Modules:
  0.0 173.0 jit_solution(5650864896941594738)
XLA Ops:
  0.7 0.1 pad_add_fusion.at_ref
  0.8 0.8 copy-done.11
  1.6 0.7 copy-done.12
  2.3 0.7 copy-done.14
  2.9 0.8 place.1
  3.7 11.0 %all_to_all.50 = bf16[8,72,128]{2,1,0:T(8,128)(2,1)S(1)} all-to-all(bf16[8,72,128]{2,1,0:T(8,128)(2,1)S(1)} %place.1), channel_id=1, replica_groups=mesh['kv_0'=8,'kv_1'=4,'tp_0'=4,'tp_1'=2] {'tp_0','tp_1'}, dimensions={0} | all-to-all | bytes 294912 | tf_op jit(solution)/shard_map/all_to_all | solution.py:26
  14.8 23.6 %all_to_all.51 = bf16[32,40,128]{2,1,0:T(8,128)(2,1)S(1)} all-to-all(bf16[32,40,128]{2,1,0:T(8,128)(2,1)S(1)} %broadcast_in_dim.14), channel_id=1, replica_groups=mesh['kv_0'=8,'kv_1'=4,'tp_0'=4,'tp_1'=2] {'kv_0','kv_1'}, dimensions={0} | all-to-all | bytes 655360 | tf_op jit(solution)/shard_map/all_to_all | solution.py:26
  38.5 4.1 %all-gather = bf16[64,40,128]{2,1,0:T(8,128)(2,1)S(1)} all-gather(bf16[32,40,128]{2,1,0:T(8,128)(2,1)S(1)} %all_to_all.51), channel_id=2, replica_groups=mesh['kv_0'=8,'kv_1'=4,'tp_0'=4,'tp_1'=2] {'tp_1'}, dimensions={0}, use_global_device_ids=true | all-gather | bytes 983040 | tf_op jit(solution)/shard_map/all_gather | solution.py:443
  42.5 1.1 copy-done
  43.6 1.1 copy-done.2
  44.8 1.1 copy-done.4
  45.9 1.7 first_block.1
  47.5 0.5 collective-permute-start
  48.0 2.3 %prepare.1 = (f32[16,128]{1,0:T(8,128)S(1)}, bf16[8,512,512]{2,1,0:T(8,128)(2,1)S(1)}) custom-call(bf16[8,128]{1,0:T(8,128)(2,1)S(1)} %slice.57.lines_ref, bf16[128,512]{1,0:T(8,128)(2,1)S(1)} %copy-done.10, bf16[128,512]{1,0:T(8,128)(2,1)S(1)} %copy-done.9, bf16[128,512]{1,0:T(8,128)(2,1)S(1)} %copy-done.8, bf16[128,512]{1,0:T(8,128)(2,1)S(1)} %copy-done.7, ...), custom_call_target="tpu_custom_call" | custom-call | tf_op jit(solution)/shard_map/prepare/pallas_call | solution.py:108
  50.3 0.0 copy-start.6
  50.3 0.0 copy-start.16
  50.4 0.1 first_blocks.1
  50.4 16.9 %all_to_all.52 = bf16[32,40,128]{2,1,0:T(8,128)(2,1)S(1)} all-to-all(bf16[32,40,128]{2,1,0:T(8,128)(2,1)S(1)} %first_blocks.1), channel_id=1, replica_groups=mesh['kv_0'=8,'kv_1'=4,'tp_0'=4,'tp_1'=2] {'kv_0','kv_1'}, dimensions={0} | all-to-all | bytes 655360 | tf_op jit(solution)/shard_map/all_to_all | solution.py:26
  67.4 0.1 convert_reduce_fusion
  67.5 10.2 %all_to_all.53 = f32[8,40,128]{2,1,0:T(8,128)S(1)} all-to-all(f32[8,40,128]{2,1,0:T(8,128)S(1)} %broadcast_in_dim.15), channel_id=1, replica_groups=mesh['kv_0'=8,'kv_1'=4,'tp_0'=4,'tp_1'=2] {'tp_0','tp_1'}, dimensions={0} | all-to-all | bytes 327680 | tf_op jit(solution)/shard_map/all_to_all | solution.py:26
  77.7 0.1 multiply_reduce_fusion.1
  77.8 0.1 add_multiply_fusion
  77.9 0.1 multiply_convert_fusion
  78.0 0.1 convolution_convert_fusion
  78.2 0.1 convolution_convert_fusion.1
  78.3 0.1 convolution_convert_fusion.2
  78.5 0.1 convolution_convert_fusion.3
  78.7 0.3 copy.38
  79.0 0.0 copy-start.3
  79.0 0.0 copy-start.5
  79.1 16.1 %all_to_all.54.arrived_ref = bf16[32,40,128]{2,1,0:T(8,128)(2,1)S(1)} all-to-all(bf16[32,40,128]{2,1,0:T(8,128)(2,1)S(1)} %pad_maximum_fusion), channel_id=1, replica_groups=mesh['kv_0'=8,'kv_1'=4,'tp_0'=4,'tp_1'=2] {'kv_0','kv_1'}, dimensions={0} | all-to-all | bytes 655360 | tf_op jit(solution)/shard_map/all_to_all | solution.py:26
  95.3 2.4 %mixer.1 = (f32[8,8,128]{2,1,0:T(8,128)S(1)}, f32[8,128]{1,0:T(8,128)S(1)}, f32[2,4,128,128]{3,2,1,0:T(8,128)}) custom-call(s32[3]{0:T(128)S(1)} %pad_add_fusion.at_ref, bf16[32,40,128]{2,1,0:T(8,128)(2,1)S(1)} %all_to_all.54.arrived_ref, bf16[32,8,128]{2,1,0:T(8,128)(2,1)S(1)} %slice_bitcast_fusion.params_ref, f32[4,128]{1,0:T(4,128)S(1)} %bitcast.71, ...), custom_call_target="tpu_custom_call" | custom-call | tf_op jit(solution)/shard_map/mixer/pallas_call | solution.py:387
  97.7 9.3 %all_to_all.55 = f32[8,8,128]{2,1,0:T(8,128)S(1)} all-to-all(f32[8,8,128]{2,1,0:T(8,128)S(1)} %get-tuple-element.194), channel_id=1, replica_groups=mesh['kv_0'=8,'kv_1'=4,'tp_0'=4,'tp_1'=2] {'tp_0','tp_1'}, dimensions={0} | all-to-all | bytes 65536 | tf_op jit(solution)/shard_map/all_to_all | solution.py:26
  107.1 19.6 %all_to_all.56 = bf16[128,8,128]{2,1,0:T(8,128)(2,1)S(1)} all-to-all(bf16[128,8,128]{2,1,0:T(8,128)(2,1)S(1)} %broadcast_in_dim.18), channel_id=1, replica_groups=mesh['kv_0'=8,'kv_1'=4,'tp_0'=4,'tp_1'=2] {'kv_0','kv_1','tp_0'}, dimensions={0} | all-to-all | bytes 524288 | tf_op jit(solution)/shard_map/all_to_all | solution.py:26
  126.7 4.6 %all-gather.1 = bf16[256,8,128]{2,1,0:T(8,128)(2,1)S(1)} all-gather(bf16[128,8,128]{2,1,0:T(8,128)(2,1)S(1)} %all_to_all.56), channel_id=3, replica_groups=mesh['kv_0'=8,'kv_1'=4,'tp_0'=4,'tp_1'=2] {'tp_1'}, dimensions={0}, use_global_device_ids=true | all-gather | bytes 786432 | tf_op jit(solution)/shard_map/all_gather | solution.py:508
  131.3 2.2 %second_block.1 = (bf16[32,32,128]{2,1,0:T(8,128)(2,1)S(1)}, bf16[32,32,128]{2,1,0:T(8,128)(2,1)S(1)}, bf16[64,128]{1,0:T(8,128)(2,1)S(1)}) custom-call(s32[3]{0:T(128)S(1)} %pad_add_fusion.at_ref, bf16[2,32,4,8,128]{4,3,2,1,0:T(8,128)(2,1)S(1)} %bitcast.69, bf16[32,8,128]{2,1,0:T(8,128)(2,1)S(1)} %slice_bitcast_fusion.params_ref, ...), custom_call_target="tpu_custom_call" | custom-call | tf_op jit(solution)/shard_map/second_block/pallas_call | solution.py:266
  133.4 0.5 collective-permute-start.1
  133.9 1.2 collective-permute-done.1
  135.1 0.1 add_convert_fusion
  135.1 14.8 %all_to_all.57 = bf16[32,32,128]{2,1,0:T(8,128)(2,1)S(1)} all-to-all(bf16[32,32,128]{2,1,0:T(8,128)(2,1)S(1)} %add_convert_fusion), channel_id=1, replica_groups=mesh['kv_0'=8,'kv_1'=4,'tp_0'=4,'tp_1'=2] {'kv_0','kv_1'}, dimensions={0} | all-to-all | bytes 524288 | tf_op jit(solution)/shard_map/all_to_all | solution.py:26
  150.0 9.7 %all_to_all.58 = f32[8,32,128]{2,1,0:T(8,128)S(1)} all-to-all(f32[8,32,128]{2,1,0:T(8,128)S(1)} %broadcast_in_dim.19), channel_id=1, replica_groups=mesh['kv_0'=8,'kv_1'=4,'tp_0'=4,'tp_1'=2] {'tp_0','tp_1'}, dimensions={0} | all-to-all | bytes 262144 | tf_op jit(solution)/shard_map/all_to_all | solution.py:26
  159.7 0.1 fusion.2
  159.8 0.2 multiply_reduce_fusion
  160.0 0.1 pad_maximum_fusion.2
  160.1 11.9 %all_to_all.59 = f32[32,1,128]{2,1,0:T(1,128)S(1)} all-to-all(f32[32,1,128]{2,1,0:T(1,128)S(1)} %broadcast_in_dim.20), channel_id=1, replica_groups=mesh['kv_0'=8,'kv_1'=4,'tp_0'=4,'tp_1'=2] {'kv_0','kv_1'}, dimensions={0} | all-to-all | bytes 32768 | tf_op jit(solution)/shard_map/all_to_all | solution.py:26
  172.1 0.1 multiply_reduce_fusion.2
  172.2 0.1 add_convert_fusion.1
  172.4 0.7 copy.41
  (58 shorter events, 0.6 us)
Async XLA Ops:
  0.6 47.4 %copy-start.7 = (bf16[128,512]{1,0:T(8,128)(2,1)S(1)}, bf16[128,512]{1,0:T(8,128)(2,1)}, u32[]{:S(2)}) copy-start(bf16[128,512]{1,0:T(8,128)(2,1)} %w3.1) | copy-start | bytes 393220
  0.6 47.4 %copy-start.8 = (bf16[128,512]{1,0:T(8,128)(2,1)S(1)}, bf16[128,512]{1,0:T(8,128)(2,1)}, u32[]{:S(2)}) copy-start(bf16[128,512]{1,0:T(8,128)(2,1)} %w2.1) | copy-start | bytes 393220
  0.7 47.4 %copy-start.9 = (bf16[128,512]{1,0:T(8,128)(2,1)S(1)}, bf16[128,512]{1,0:T(8,128)(2,1)}, u32[]{:S(2)}) copy-start(bf16[128,512]{1,0:T(8,128)(2,1)} %w1.1) | copy-start | bytes 393220
  0.7 47.3 %copy-start.10 = (bf16[128,512]{1,0:T(8,128)(2,1)S(1)}, bf16[128,512]{1,0:T(8,128)(2,1)}, u32[]{:S(2)}) copy-start(bf16[128,512]{1,0:T(8,128)(2,1)} %w0.1) | copy-start | bytes 393220
  0.8 0.8 copy-start.11
  1.6 0.7 copy-start.12
  2.2 0.7 copy-start.14
  42.5 1.1 copy-start
  43.6 1.1 copy-start.2
  44.7 1.1 copy-start.4
  47.5 2.8 %collective-permute-start = (bf16[32,32,128]{2,1,0:T(8,128)(2,1)S(1)}, bf16[32,32,128]{2,1,0:T(8,128)(2,1)S(1)}, u32[]{:S(2)}, u32[]{:S(2)}) collective-permute-start(bf16[32,32,128]{2,1,0:T(8,128)(2,1)S(1)} %get-tuple-element.138), channel_id=1, source_target_pairs={{0,1},{1,0},{2,3},{3,2},{4,5},{5,4},{6,7},{7,6},{8,9},{9,8},{10,11... | collective-permute-start | bytes 786440 | tf_op jit(solution)/shard_map/ppermute | solution.py:457
  50.3 45.0 %copy-start.6 = (f32[2,4,128,128]{3,2,1,0:T(8,128)S(1)}, f32[2,4,128,128]{3,2,1,0:T(8,128)}, u32[]{:S(2)}) copy-start(f32[2,4,128,128]{3,2,1,0:T(8,128)} %state_ref.1) | copy-start | bytes 1572868
  50.3 45.0 %copy-start.16 = (f32[512]{0:T(512)S(1)}, f32[512]{0:T(512)}, u32[]{:S(2)}) copy-start(f32[512]{0:T(512)} %param.24) | copy-start | bytes 6148
  50.3 44.9 %copy-start.17 = (f32[512]{0:T(512)S(1)}, f32[512]{0:T(512)}, u32[]{:S(2)}) copy-start(f32[512]{0:T(512)} %param.25) | copy-start | bytes 6148
  79.0 52.3 %copy-start.1 = (bf16[2,4096,44]{1,0,2:T(2,128)(2,1)S(1)}, bf16[2,4096,44]{1,0,2:T(2,128)(2,1)}, u32[]{:S(2)}) copy-start(bf16[2,4096,44]{1,0,2:T(2,128)(2,1)} %param.15) | copy-start | bytes 2162692
  79.0 52.3 %copy-start.3 = (bf16[2,4096,44]{1,0,2:T(2,128)(2,1)S(1)}, bf16[2,4096,44]{1,0,2:T(2,128)(2,1)}, u32[]{:S(2)}) copy-start(bf16[2,4096,44]{1,0,2:T(2,128)(2,1)} %param.16) | copy-start | bytes 2162692
  79.0 52.2 %copy-start.5 = (bf16[2,44,4096]{2,0,1:T(2,128)(2,1)S(1)}, bf16[2,44,4096]{2,0,1:T(2,128)(2,1)}, u32[]{:S(2)}) copy-start(bf16[2,44,4096]{2,0,1:T(2,128)(2,1)} %param.17) | copy-start | bytes 2162692
  97.7 74.5 %copy-start.13 = (bf16[3,16]{1,0:T(4,128)(2,1)S(1)}, bf16[3,16]{1,0:T(4,128)(2,1)}, u32[]{:S(2)}) copy-start(bf16[3,16]{1,0:T(4,128)(2,1)} %gain_ref.1) | copy-start | bytes 292
  97.7 74.5 %copy-start.15 = (bf16[3,16]{1,0:T(4,128)(2,1)S(1)}, bf16[3,16]{1,0:T(4,128)(2,1)}, u32[]{:S(2)}) copy-start(bf16[3,16]{1,0:T(4,128)(2,1)} %bias_ref.1) | copy-start | bytes 292
  133.4 1.6 collective-permute-start.1

commit v7 on v6

--- a/solution.py
+++ b/solution.py
@@ -48,7 +48,26 @@
 ANYWHERE = pl.BlockSpec(memory_space=pl.ANY)
 
 
-def place_kernel(at_ref, tokens_ref, gain_ref, bias_ref, result_ref, lines_ref):
+def off_chip(x):
+    return pltpu.with_memory_space_constraint(x, pltpu.HBM)
+
+
+def place_kernel(
+    at_ref,
+    tokens_hbm,
+    gain_hbm,
+    bias_hbm,
+    result_ref,
+    lines_ref,
+    tokens_ref,
+    gain_ref,
+    bias_ref,
+    sem,
+):
+    pairs = ((tokens_hbm, tokens_ref), (gain_hbm, gain_ref), (bias_hbm, bias_ref))
+    fetches = [pltpu.make_async_copy(*pair, sem.at[i]) for i, pair in enumerate(pairs)]
+    for fetch in fetches:
+        fetch.start()
     own_cols, batch = tokens_ref.shape
     half = batch // 2
     shape = (own_cols, LANES)
@@ -57,6 +76,8 @@
     row = lax.broadcasted_iota(jnp.int32, (batch, batch), 0)
     source = 2 * (row % half) + row // half
     order = (lax.broadcasted_iota(jnp.int32, (batch, batch), 1) == source).astype(f32)
+    for fetch in fetches:
+        fetch.wait()
     turned = lax.dot_general(
         order.astype(bf16), tokens_ref[...], (((1,), (1,)), ((), ())), preferred_element_type=f32
     ).astype(bf16)
@@ -73,50 +94,88 @@
     batch, own_cols = tokens.shape
     return pl.pallas_call(
         place_kernel,
-        in_specs=[SMEM, VMEM, VMEM, VMEM],
+        in_specs=[SMEM] + [ANYWHERE] * 3,
         out_specs=VMEM,
         out_shape=jax.ShapeDtypeStruct((count, batch + 8, LANES), bf16),
-        scratch_shapes=[pltpu.VMEM((batch + 8, LANES), f32)],
+        scratch_shapes=[
+            pltpu.VMEM((batch + 8, LANES), f32),
+            pltpu.VMEM((own_cols, batch), bf16),
+            pltpu.VMEM(gain.shape, bf16),
+            pltpu.VMEM(bias.shape, bf16),
+            pltpu.SemaphoreType.DMA((3,)),
+        ],
         compiler_params=small(),
         name="place",
-    )(at, tokens.T, gain, bias)
-
-
-def prepare_kernel(lines_ref, w0, w1, w2, w3, weight_hbm, bias_ref, weight_ref, weight_sem):
-    parts, _, step = weight_ref.shape
-    weight_copies = [
+    )(at, off_chip(tokens.T), off_chip(gain), off_chip(bias))
+
+
+def load_kernel(
+    lines_ref,
+    hbm_0,
+    hbm_1,
+    hbm_2,
+    hbm_3,
+    out_hbm,
+    gate_hbm,
+    up_hbm,
+    down_hbm,
+    bias_ref,
+    out_ref,
+    gate_ref,
+    up_ref,
+    down_ref,
+    project_ref,
+    project_sem,
+    part_sem,
+    sem,
+):
+    parts, _, step = out_ref.shape
+    pairs = ((gate_hbm, gate_ref), (up_hbm, up_ref), (down_hbm, down_ref))
+    projections = [
+        pltpu.make_async_copy(hbm, project_ref.at[i], project_sem.at[i])
+        for i, hbm in enumerate((hbm_0, hbm_1, hbm_2, hbm_3))
+    ]
+    fetches = [pltpu.make_async_copy(*pair, sem.at[i]) for i, pair in enumerate(pairs)]
+    fetches += [
         pltpu.make_async_copy(
-            weight_hbm.at[:, pl.ds(part * step, step)], weight_ref.at[part], weight_sem.at[part]
+            out_hbm.at[:, pl.ds(part * step, step)], out_ref.at[part], part_sem.at[part]
         )
         for part in range(parts)
     ]
-    for copy in weight_copies:
-        copy.start()
+    for fetch in projections + fetches:
+        fetch.start()
     lines = lines_ref[...]
-    for index, w_ref in enumerate((w0, w1, w2, w3)):
-        sums = jnp.dot(lines, w_ref[...], preferred_element_type=f32)
+    for index, projection in enumerate(projections):
+        projection.wait()
+        sums = jnp.dot(lines, project_ref[index], preferred_element_type=f32)
         heads = sums.shape[1] // LANES
         for head in range(heads):
             chunk = index * heads + head
             bias_ref[chunk : chunk + 1, :] = sums[3:4, head * LANES : (head + 1) * LANES]
-    for copy in weight_copies:
-        copy.wait()
-
-
-def prepare(lines, weights, weight, parts):
-    depth, width = weight.shape
+    for fetch in fetches:
+        fetch.wait()
+
+
+def load(lines, weights, out_weight, stored, parts):
+    depth, width = out_weight.shape
     return pl.pallas_call(
-        prepare_kernel,
-        in_specs=[VMEM] * 5 + [ANYWHERE],
-        out_specs=[VMEM, VMEM],
+        load_kernel,
+        in_specs=[VMEM] + [ANYWHERE] * 8,
+        out_specs=[VMEM] * 5,
         out_shape=[
             jax.ShapeDtypeStruct((4 * weights[0].shape[1] // LANES, LANES), f32),
             jax.ShapeDtypeStruct((parts, depth, width // parts), bf16),
-        ],
-        scratch_shapes=[pltpu.SemaphoreType.DMA((parts,))],
-        compiler_params=small(),
-        name="prepare",
-    )(lines, *weights, pltpu.with_memory_space_constraint(weight, pltpu.HBM))
+        ]
+        + [jax.ShapeDtypeStruct(w.shape, bf16) for w in stored],
+        scratch_shapes=[
+            pltpu.VMEM((4, *weights[0].shape), bf16),
+            pltpu.SemaphoreType.DMA((4,)),
+            pltpu.SemaphoreType.DMA((parts,)),
+            pltpu.SemaphoreType.DMA((3,)),
+        ],
+        compiler_params=small(12),
+        name="load",
+    )(lines, *[off_chip(w) for w in (*weights, out_weight, *stored)])
 
 
 def feed_forward(rows, core, layer, gate_ref, up_ref, down_ref):
@@ -173,7 +232,7 @@
     return gate.transpose(2, 0, 1), up.transpose(2, 0, 1), down.transpose(1, 0, 2)
 
 
-def first_block(at, rows, gate, up, down, half):
+def first_block(at, rows, stored, half):
     chunks = rows.shape[1]
     return pl.pallas_call(
         first_kernel,
@@ -188,7 +247,7 @@
         scratch_shapes=[pltpu.VMEM((2 * half, chunks * LANES), bf16)],
         compiler_params=small(12),
         name="first_block",
-    )(at, rows, *stored_order(gate, up, down))
+    )(at, rows, *stored)
 
 
 def blocks_kernel(kept_ref, came_ref, tail_ref, bias_ref, result_ref):
@@ -260,7 +319,7 @@
     write_halves(part, kept_ref, sent_ref)
 
 
-def second_block(at, arrived, params, gate, up, down):
+def second_block(at, arrived, params, stored):
     cores, kv_count, x_count, rows, lanes = arrived.shape
     chunks = cores * x_count * rows // 2
     return pl.pallas_call(
@@ -278,7 +337,7 @@
         ],
         compiler_params=small(12),
         name="second_block",
-    )(at, arrived, params, *stored_order(gate, up, down))
+    )(at, arrived, params, *stored)
 
 
 def mixer_kernel(
@@ -450,10 +509,11 @@
     weights = (query_weight, forget_weight, input_weight, outgate_weight)
     chunk_count = 4 * heads
     share = kv_count // chunk_count
-    bias_rows, mixer_weight = prepare(block[batch:], weights, out_weight, tp_count)
-    kept, sent, tail, token_sum = first_block(
-        at, both, gate_weights, up_weights, down_weights, half
-    )
+    stored = stored_order(gate_weights, up_weights, down_weights)
+    bias_rows, mixer_weight, *stored = load(
+        block[batch:], weights, out_weight, stored, tp_count
+    )
+    kept, sent, tail, token_sum = first_block(at, both, stored, half)
     blocks = first_blocks(kept, lax.ppermute(sent, CORE, SWAP), tail, bias_rows)
     arrived, at, kv, tp, norm_gain, norm_bias, block, params, token_sum = alone(
         blocks, KV, at, kv, tp, norm_gain, norm_bias, block, params, token_sum
@@ -508,9 +568,7 @@
     arrived = lax.all_gather(arrived, CORE, axis=0)
     arrived = arrived.reshape(2, kv_count, x_count, *stream_own.shape)
 
-    kept, sent, own_normed = second_block(
-        at, arrived, params, gate_weights, up_weights, down_weights
-    )
+    kept, sent, own_normed = second_block(at, arrived, params, stored)
     came = lax.ppermute(sent, CORE, SWAP)
     blocks = (kept.astype(f32) + came.astype(f32)).astype(bf16)
     arrived, tp, norm_gain, norm_bias, own_normed = alone(

time: 174 us -> 168 us (0.966)
  blocking collectives: 152 us -> 128 us
  starting transfers between devices: 0.92 us -> 12.1 us
  waiting for transfers between devices: 1.16 us -> 9.89 us
  local copies, waits for them, and re-layouts: 6.73 us -> 3.85 us
    all_to_all x10 -> x9, blocking collectives: 143 us -> 119 us  [exchange(): return lax.all_to_all(blocks, axes, split_axis=0, concat_axis=0, tiled=True)]
    all_to_all x0 -> x1, starting transfers between devices: none -> 11.2 us  [exchange(): return lax.all_to_all(blocks, axes, split_axis=0, concat_axis=0, tiled=True)]
    all_to_all x0 -> x1, waiting for transfers between devices: none -> 7.57 us  [exchange(): return lax.all_to_all(blocks, axes, split_axis=0, concat_axis=0, tiled=True)]
    unnamed x38 -> x24, local copies, waits for them, and re-layouts: 6.27 us -> 2.67 us
  transfers between devices with their start and end apart: 2 -> 3, of which waited for: 1 -> 3; matrix products, arithmetic and copies ran while one was open for 0% -> 0% of each run, Pallas kernels for 1% -> 2%
where the time goes in v7:
time: 168 us
  blocking collectives  128 us (76%)
  starting transfers between devices  12.1 us (7%)
  Pallas kernels  10.9 us (6%)
  waiting for transfers between devices  9.89 us (6%)
  local copies, waits for them, and re-layouts  3.85 us (2%)
    all_to_all x9, blocking collectives, exchange(): return lax.all_to_all(blocks, axes, split_axis=0, concat_axis=0, tiled=True)  119 us
    all_to_all x1, starting transfers between devices, exchange(): return lax.all_to_all(blocks, axes, split_axis=0, concat_axis=0, tiled=True)  11.2 us
    all_to_all x1, waiting for transfers between devices, exchange(): return lax.all_to_all(blocks, axes, split_axis=0, concat_axis=0, tiled=True)  7.57 us
    all_gather x1, blocking collectives, local(): arrived = lax.all_gather(arrived, CORE, axis=0)  4.59 us
    all_gather x1, blocking collectives, local(): both = lax.all_gather(arrived, CORE, axis=0)  4.07 us
  transfers between devices with their start and end apart: 3, of which 3 were waited for; matrix products, arithmetic and copies ran while one was open for 0% of the time, Pallas kernels for 2%

profile of v7, /device:TPU:1, one launch (start us, length us, event | category | flops | bytes accessed | tf_op | source)
XLA Modules:
  0.0 167.7 jit_solution(1447622487455257368)
XLA Ops:
  0.6 0.1 pad_add_fusion.at_ref
  0.7 1.5 place.1
  2.3 11.0 %all_to_all.50 = bf16[8,72,128]{2,1,0:T(8,128)(2,1)S(1)} all-to-all(bf16[8,72,128]{2,1,0:T(8,128)(2,1)S(1)} %place.1), channel_id=1, replica_groups=mesh['kv_0'=8,'kv_1'=4,'tp_0'=4,'tp_1'=2] {'tp_0','tp_1'}, dimensions={0} | all-to-all | bytes 294912 | tf_op jit(solution)/shard_map/all_to_all | solution.py:26
  13.3 0.8 broadcast_in_dim.14
  14.1 11.2 %all-to-all-start.1 = ((bf16[32,40,128]{2,1,0:T(8,128)(2,1)}), bf16[32,40,128]{2,1,0:T(8,128)(2,1)S(1)}, u32[]{:S(2)}, u32[]{:S(2)}) async-start(bf16[32,40,128]{2,1,0:T(8,128)(2,1)} %broadcast_in_dim.14), calls=%async_computation.1 | async-start | bytes 655360 | tf_op jit(solution)/shard_map/all_to_all | solution.py:26
  25.3 3.1 %load.1 = (f32[16,128]{1,0:T(8,128)S(1)}, bf16[8,512,512]{2,1,0:T(8,128)(2,1)S(1)}, bf16[44,2,4096]{2,1,0:T(2,128)(2,1)S(1)}, bf16[44,2,4096]{2,1,0:T(2,128)(2,1)S(1)}, bf16[44,2,4096]{2,1,0:T(2,128)(2,1)S(1)}) custom-call(bf16[8,128]{1,0:T(8,128)(2,1)S(1)} %slice.57.lines_ref, bf16[128,512]{1,0:T(8,128)(2,1)} %hbm_0.1, bf16[128,512]{1,0:T(8,128)(2,1)} %hbm_1.1, ...), custom_call_target="tpu_custom_call" | custom-call | tf_op jit(solution)/shard_map/load/pallas_call | solution.py:161
  28.4 1.9 %copy-done = bf16[8,512,512]{2,1,0:T(8,128)(2,1)} copy-done((bf16[8,512,512]{2,1,0:T(8,128)(2,1)}, bf16[8,512,512]{2,1,0:T(8,128)(2,1)S(1)}, u32[]{:S(2)}) %copy-start) | copy-done | bytes 4194328
  30.3 7.6 %all-to-all-done.1 = bf16[32,40,128]{2,1,0:T(8,128)(2,1)S(1)} async-done(((bf16[32,40,128]{2,1,0:T(8,128)(2,1)}), bf16[32,40,128]{2,1,0:T(8,128)(2,1)S(1)}, u32[]{:S(2)}, u32[]{:S(2)}) %all-to-all-start.1) | async-done | bytes 327712 | tf_op jit(solution)/shard_map/all_to_all | solution.py:26
  37.9 4.1 %all-gather = bf16[64,40,128]{2,1,0:T(8,128)(2,1)S(1)} all-gather(bf16[32,40,128]{2,1,0:T(8,128)(2,1)S(1)} %all-to-all-done.1), channel_id=2, replica_groups=mesh['kv_0'=8,'kv_1'=4,'tp_0'=4,'tp_1'=2] {'tp_1'}, dimensions={0}, use_global_device_ids=true | all-gather | bytes 983040 | tf_op jit(solution)/shard_map/all_gather | solution.py:502
  42.0 1.7 first_block.1
  43.7 0.5 collective-permute-start
  44.1 1.2 collective-permute-done.came_ref
  45.3 0.1 first_blocks.1
  45.4 16.6 %all_to_all.51 = bf16[32,40,128]{2,1,0:T(8,128)(2,1)S(1)} all-to-all(bf16[32,40,128]{2,1,0:T(8,128)(2,1)S(1)} %first_blocks.1), channel_id=1, replica_groups=mesh['kv_0'=8,'kv_1'=4,'tp_0'=4,'tp_1'=2] {'kv_0','kv_1'}, dimensions={0} | all-to-all | bytes 655360 | tf_op jit(solution)/shard_map/all_to_all | solution.py:26
  62.0 0.1 convert_reduce_fusion
  62.1 10.3 %all_to_all.52 = f32[8,40,128]{2,1,0:T(8,128)S(1)} all-to-all(f32[8,40,128]{2,1,0:T(8,128)S(1)} %broadcast_in_dim.15), channel_id=1, replica_groups=mesh['kv_0'=8,'kv_1'=4,'tp_0'=4,'tp_1'=2] {'tp_0','tp_1'}, dimensions={0} | all-to-all | bytes 327680 | tf_op jit(solution)/shard_map/all_to_all | solution.py:26
  72.4 0.1 multiply_reduce_fusion.1
  72.6 0.1 add_multiply_fusion
  72.6 0.1 multiply_convert_fusion
  72.7 0.0 copy-done.5
  72.7 0.1 convolution_convert_fusion
  72.9 0.1 convolution_convert_fusion.1
  73.1 0.1 convolution_convert_fusion.2
  73.2 0.1 convolution_convert_fusion.3
  73.5 0.3 copy.38
  73.8 0.1 pad_maximum_fusion
  73.8 16.1 %all_to_all.53.arrived_ref = bf16[32,40,128]{2,1,0:T(8,128)(2,1)S(1)} all-to-all(bf16[32,40,128]{2,1,0:T(8,128)(2,1)S(1)} %pad_maximum_fusion), channel_id=1, replica_groups=mesh['kv_0'=8,'kv_1'=4,'tp_0'=4,'tp_1'=2] {'kv_0','kv_1'}, dimensions={0} | all-to-all | bytes 655360 | tf_op jit(solution)/shard_map/all_to_all | solution.py:26
  89.9 0.0 copy-done.2
  89.9 2.4 %mixer.1 = (f32[8,8,128]{2,1,0:T(8,128)S(1)}, f32[8,128]{1,0:T(8,128)S(1)}, f32[2,4,128,128]{3,2,1,0:T(8,128)}) custom-call(s32[3]{0:T(128)S(1)} %pad_add_fusion.at_ref, bf16[32,40,128]{2,1,0:T(8,128)(2,1)S(1)} %all_to_all.53.arrived_ref, bf16[32,8,128]{2,1,0:T(8,128)(2,1)S(1)} %slice_bitcast_fusion.params_ref, f32[4,128]{1,0:T(4,128)S(1)} %bitcast.64, ...), custom_call_target="tpu_custom_call" | custom-call | tf_op jit(solution)/shard_map/mixer/pallas_call | solution.py:446
  92.4 0.0 copy-start.9
  92.4 0.0 copy-start.10
  92.4 9.3 %all_to_all.54 = f32[8,8,128]{2,1,0:T(8,128)S(1)} all-to-all(f32[8,8,128]{2,1,0:T(8,128)S(1)} %get-tuple-element.200), channel_id=1, replica_groups=mesh['kv_0'=8,'kv_1'=4,'tp_0'=4,'tp_1'=2] {'tp_0','tp_1'}, dimensions={0} | all-to-all | bytes 65536 | tf_op jit(solution)/shard_map/all_to_all | solution.py:26
  101.7 19.6 %all_to_all.55 = bf16[128,8,128]{2,1,0:T(8,128)(2,1)S(1)} all-to-all(bf16[128,8,128]{2,1,0:T(8,128)(2,1)S(1)} %broadcast_in_dim.18), channel_id=1, replica_groups=mesh['kv_0'=8,'kv_1'=4,'tp_0'=4,'tp_1'=2] {'kv_0','kv_1','tp_0'}, dimensions={0} | all-to-all | bytes 524288 | tf_op jit(solution)/shard_map/all_to_all | solution.py:26
  121.4 4.6 %all-gather.1 = bf16[256,8,128]{2,1,0:T(8,128)(2,1)S(1)} all-gather(bf16[128,8,128]{2,1,0:T(8,128)(2,1)S(1)} %all_to_all.55), channel_id=3, replica_groups=mesh['kv_0'=8,'kv_1'=4,'tp_0'=4,'tp_1'=2] {'tp_1'}, dimensions={0}, use_global_device_ids=true | all-gather | bytes 786432 | tf_op jit(solution)/shard_map/all_gather | solution.py:568
  125.9 2.2 %second_block.1 = (bf16[32,32,128]{2,1,0:T(8,128)(2,1)S(1)}, bf16[32,32,128]{2,1,0:T(8,128)(2,1)S(1)}, bf16[64,128]{1,0:T(8,128)(2,1)S(1)}) custom-call(s32[3]{0:T(128)S(1)} %pad_add_fusion.at_ref, bf16[2,32,4,8,128]{4,3,2,1,0:T(8,128)(2,1)S(1)} %bitcast.63, bf16[32,8,128]{2,1,0:T(8,128)(2,1)S(1)} %slice_bitcast_fusion.params_ref, ...), custom_call_target="tpu_custom_call" | custom-call | tf_op jit(solution)/shard_map/second_block/pallas_call | solution.py:325
  128.1 0.5 collective-permute-start.1
  128.6 1.2 collective-permute-done.1
  129.7 0.1 add_convert_fusion
  129.8 14.8 %all_to_all.56 = bf16[32,32,128]{2,1,0:T(8,128)(2,1)S(1)} all-to-all(bf16[32,32,128]{2,1,0:T(8,128)(2,1)S(1)} %add_convert_fusion), channel_id=1, replica_groups=mesh['kv_0'=8,'kv_1'=4,'tp_0'=4,'tp_1'=2] {'kv_0','kv_1'}, dimensions={0} | all-to-all | bytes 524288 | tf_op jit(solution)/shard_map/all_to_all | solution.py:26
  144.6 9.7 %all_to_all.57 = f32[8,32,128]{2,1,0:T(8,128)S(1)} all-to-all(f32[8,32,128]{2,1,0:T(8,128)S(1)} %broadcast_in_dim.19), channel_id=1, replica_groups=mesh['kv_0'=8,'kv_1'=4,'tp_0'=4,'tp_1'=2] {'tp_0','tp_1'}, dimensions={0} | all-to-all | bytes 262144 | tf_op jit(solution)/shard_map/all_to_all | solution.py:26
  154.4 0.1 fusion.2
  154.5 0.2 multiply_reduce_fusion
  154.7 0.1 pad_maximum_fusion.2
  154.8 11.9 %all_to_all.58 = f32[32,1,128]{2,1,0:T(1,128)S(1)} all-to-all(f32[32,1,128]{2,1,0:T(1,128)S(1)} %broadcast_in_dim.20), channel_id=1, replica_groups=mesh['kv_0'=8,'kv_1'=4,'tp_0'=4,'tp_1'=2] {'kv_0','kv_1'}, dimensions={0} | all-to-all | bytes 32768 | tf_op jit(solution)/shard_map/all_to_all | solution.py:26
  166.8 0.1 multiply_reduce_fusion.2
  166.9 0.0 copy-done.10
  166.9 0.1 add_convert_fusion.1
  167.0 0.7 copy.41
  (45 shorter events, 0.4 us)
Async XLA Ops:
  14.1 23.8 %all-to-all-start.1 = ((bf16[32,40,128]{2,1,0:T(8,128)(2,1)}), bf16[32,40,128]{2,1,0:T(8,128)(2,1)S(1)}, u32[]{:S(2)}, u32[]{:S(2)}) async-start(bf16[32,40,128]{2,1,0:T(8,128)(2,1)} %broadcast_in_dim.14), calls=%async_computation.1 | async-start | bytes 655360 | tf_op jit(solution)/shard_map/all_to_all | solution.py:26
  28.4 1.9 %copy-start = (bf16[8,512,512]{2,1,0:T(8,128)(2,1)}, bf16[8,512,512]{2,1,0:T(8,128)(2,1)S(1)}, u32[]{:S(2)}) copy-start(bf16[8,512,512]{2,1,0:T(8,128)(2,1)S(1)} %get-tuple-element.194.weight_ref) | copy-start | bytes 12582916
  30.3 42.4 %copy-start.5 = (bf16[128,512]{1,0:T(8,128)(2,1)S(1)}, bf16[128,512]{1,0:T(8,128)(2,1)}, u32[]{:S(2)}) copy-start(bf16[128,512]{1,0:T(8,128)(2,1)} %hbm_3.1) | copy-start | bytes 393220
  30.3 42.5 %copy-start.6 = (bf16[128,512]{1,0:T(8,128)(2,1)S(1)}, bf16[128,512]{1,0:T(8,128)(2,1)}, u32[]{:S(2)}) copy-start(bf16[128,512]{1,0:T(8,128)(2,1)} %hbm_2.1) | copy-start | bytes 393220
  30.3 42.7 %copy-start.7 = (bf16[128,512]{1,0:T(8,128)(2,1)S(1)}, bf16[128,512]{1,0:T(8,128)(2,1)}, u32[]{:S(2)}) copy-start(bf16[128,512]{1,0:T(8,128)(2,1)} %hbm_1.1) | copy-start | bytes 393220
  30.3 42.9 %copy-start.8 = (bf16[128,512]{1,0:T(8,128)(2,1)S(1)}, bf16[128,512]{1,0:T(8,128)(2,1)}, u32[]{:S(2)}) copy-start(bf16[128,512]{1,0:T(8,128)(2,1)} %hbm_0.1) | copy-start | bytes 393220
  42.0 47.9 %copy-start.1 = (bf16[8,512,512]{2,1,0:T(8,128)(2,1)S(1)}, bf16[8,512,512]{2,1,0:T(8,128)(2,1)}, u32[]{:S(2)}) copy-start(bf16[8,512,512]{2,1,0:T(8,128)(2,1)} %copy-done) | copy-start | bytes 12582916
  42.0 47.9 %copy-start.2 = (f32[2,4,128,128]{3,2,1,0:T(8,128)S(1)}, f32[2,4,128,128]{3,2,1,0:T(8,128)}, u32[]{:S(2)}) copy-start(f32[2,4,128,128]{3,2,1,0:T(8,128)} %state_ref.1) | copy-start | bytes 1572868
  42.0 47.9 %copy-start.3 = (f32[512]{0:T(512)S(1)}, f32[512]{0:T(512)}, u32[]{:S(2)}) copy-start(f32[512]{0:T(512)} %param.24) | copy-start | bytes 6148
  42.0 47.9 %copy-start.4 = (f32[512]{0:T(512)S(1)}, f32[512]{0:T(512)}, u32[]{:S(2)}) copy-start(f32[512]{0:T(512)} %param.25) | copy-start | bytes 6148
  43.7 1.6 collective-permute-start
  92.4 74.5 %copy-start.9 = (bf16[3,16]{1,0:T(4,128)(2,1)S(1)}, bf16[3,16]{1,0:T(4,128)(2,1)}, u32[]{:S(2)}) copy-start(bf16[3,16]{1,0:T(4,128)(2,1)} %gain_hbm.1) | copy-start | bytes 292
  92.4 74.5 %copy-start.10 = (bf16[3,16]{1,0:T(4,128)(2,1)S(1)}, bf16[3,16]{1,0:T(4,128)(2,1)}, u32[]{:S(2)}) copy-start(bf16[3,16]{1,0:T(4,128)(2,1)} %bias_hbm.1) | copy-start | bytes 292
  128.1 1.6 collective-permute-start.1

commit v8 on v7

--- a/solution.py
+++ b/solution.py
@@ -33,6 +33,10 @@
 def alone(blocks, axes, *held):
     blocks, *held = lax.optimization_barrier((blocks, *held))
     return lax.optimization_barrier((exchange(blocks, axes), *held))
+
+
+def wide_sum(blocks):
+    return lax.optimization_barrier(blocks.astype(f32).sum(axis=0))
 
 
 def copies(block, count):
@@ -256,9 +260,11 @@
     top = lax.broadcasted_iota(jnp.int32, (8, LANES), 0) == 0
     for chunk in range(chunks):
         both = kept_ref[chunk].astype(f32) + came_ref[chunk].astype(f32)
-        result_ref[chunk, :half, :] = both.astype(bf16)
         bias = bias_ref[chunk // share : chunk // share + 1, :]
-        result_ref[chunk, half:, :] = jnp.where(top, tail_ref[...], bias).astype(bf16)
+        tail = jnp.where(top, tail_ref[...], bias)
+        lines = jnp.concatenate([both, tail]).astype(bf16)
+        pairs = lines.reshape(lines.shape[0] // 2, 2, LANES)
+        result_ref[chunk] = pairs[: result_ref.shape[1]]
 
 
 def first_blocks(kept, came, tail, bias):
@@ -267,7 +273,7 @@
         blocks_kernel,
         in_specs=[VMEM] * 4,
         out_specs=VMEM,
-        out_shape=jax.ShapeDtypeStruct((chunks, half + 8, lanes), bf16),
+        out_shape=jax.ShapeDtypeStruct((chunks, half // 2 + 1, 2, lanes), bf16),
         compiler_params=small(),
         name="first_blocks",
     )(kept, came, tail, bias)
@@ -365,25 +371,28 @@
     share = kv_count // chunks
     parts = sent_ref.shape[0]
     piece_chunks = kv_count // parts
-    total = arrived_ref[0].astype(f32)
+    def block_rows(block):
+        lines = arrived_ref[block, :chunks]
+        return lines.reshape(seqs * chunks, LANES).astype(f32)
+
+    total = block_rows(0)
     for block in range(1, kv_count):
-        total = total + arrived_ref[block].astype(f32)
+        total = total + block_rows(block)
     tail = seqs * chunks
     width = kv_count * LANES
-    mean = jnp.sum(total[tail : tail + 8], axis=1, keepdims=True) / width
-    squares = jnp.zeros((8, LANES), f32)
-    for block in range(kv_count):
-        off = arrived_ref[block, tail : tail + 8, :].astype(f32) - mean
-        squares = squares + off * off
-    scale = lax.rsqrt(jnp.sum(squares, axis=1, keepdims=True) / width + norm_eps)
+    own = arrived_ref[:, chunks].astype(f32)
+    mean = jnp.sum(jnp.sum(own, axis=0), axis=1, keepdims=True) / width
+    off = own - mean
+    scale = jnp.sum(jnp.sum(off * off, axis=0), axis=1, keepdims=True) / width
+    scale = lax.rsqrt(scale + norm_eps)
     for chunk in range(chunks):
-        bias = arrived_ref[chunk * share, tail : tail + 8, :].astype(f32)
+        bias = arrived_ref[chunk * share, chunks + 1].astype(f32)
         for other in range(1, share):
-            bias = bias + arrived_ref[chunk * share + other, tail : tail + 8, :].astype(f32)
-        rows_ref[2 * chunk : 2 * chunk + 2, :] = jnp.broadcast_to(bias[2:3], (2, LANES))
+            bias = bias + arrived_ref[chunk * share + other, chunks + 1].astype(f32)
+        rows_ref[2 * chunk : 2 * chunk + 2, :] = bias
     odd = lax.broadcasted_iota(jnp.int32, (tail, LANES), 0) % 2 == 1
     row_scale = jnp.where(odd, scale[1:2], scale[0:1])
-    pre = (total[:tail] * row_scale + rows_ref[...]).astype(bf16).astype(f32)
+    pre = (total * row_scale + rows_ref[...]).astype(bf16).astype(f32)
     size = 2 * heads
     query_pre, forget_pre = pre[:size], pre[size : 2 * size]
     input_pre, outgate_pre = pre[2 * size : 3 * size], pre[3 * size :]
@@ -391,10 +400,10 @@
     tp = at_ref[1]
     for chunk in range(piece_chunks):
         at = tp * piece_chunks + chunk
-        rows = arrived_ref[at, tail : tail + 8, :].astype(f32)
+        rows = arrived_ref[at, chunks].astype(f32)
         params = params_ref[at].astype(f32)
         rows = ((rows - mean) * scale * params[0:1] + params[3:4]).astype(bf16).astype(f32)
-        piece_ref[2 * chunk : 2 * chunk + 2, :] = residual_scale * rows[0:2]
+        piece_ref[2 * chunk : 2 * chunk + 2, :] = residual_scale * rows
 
     for head in range(heads):
         at = slice(2 * head, 2 * head + 2)
@@ -518,11 +527,12 @@
     arrived, at, kv, tp, norm_gain, norm_bias, block, params, token_sum = alone(
         blocks, KV, at, kv, tp, norm_gain, norm_bias, block, params, token_sum
     )
-    arrived = arrived.astype(f32).sum(axis=0)
+    arrived = wide_sum(arrived).reshape(half + 2, LANES).astype(bf16)
     gathered, at, kv, tp, norm_gain, norm_bias, block, params, token_sum, arrived = over_tp(
         arrived, at, kv, tp, norm_gain, norm_bias, block, params, token_sum, arrived
     )
-    bias_own = (arrived[half + 1 : half + 2] / share).astype(bf16)
+    gathered = gathered.astype(f32)
+    bias_own = arrived[half + 1 : half + 2] / share
     gain_one = block[batch : batch + 1]
     total = gathered[:, :, :half].sum(axis=0).reshape(batch, LANES)
     total_row = gathered[:, :, half].sum(axis=(0, 1))
@@ -540,9 +550,9 @@
     projected = projected.reshape(2, half, chunk_count, LANES).transpose(1, 2, 0, 3)
     blocks = jnp.concatenate(
         [
-            projected.reshape(kv_count, 2 * chunk_count, LANES),
-            centred.astype(bf16).reshape(2, half, LANES).swapaxes(0, 1),
-            jnp.broadcast_to(bias_own[None], (kv_count, 6, LANES)),
+            projected,
+            centred.astype(bf16).reshape(2, half, LANES).swapaxes(0, 1)[:, None],
+            jnp.broadcast_to(bias_own.astype(bf16)[None, None], (kv_count, 1, 2, LANES)),
         ],
         axis=1,
     )
@@ -575,8 +585,9 @@
         blocks, KV, tp, norm_gain, norm_bias, own_normed
     )
     gathered, tp, norm_gain, norm_bias, own_normed = over_tp(
-        arrived.astype(f32).sum(axis=0), tp, norm_gain, norm_bias, own_normed
-    )
+        wide_sum(arrived).astype(bf16), tp, norm_gain, norm_bias, own_normed
+    )
+    gathered = gathered.astype(f32)
     total = gathered.sum(axis=0).reshape(batch, LANES)
     stream_three = residual_scale * own_normed.astype(f32) + 0.5 * total
     block_sum = stream_three.sum(axis=1)

time: 168 us -> 167 us (level)
  blocking collectives: 128 us -> 125 us
    all_to_all x9, blocking collectives: 119 us -> 117 us  [exchange(): return lax.all_to_all(blocks, axes, split_axis=0, concat_axis=0, tiled=True)]
where the time goes in v8:
time: 167 us; the launch traced here: 166 us
  blocking collectives  125 us (75%)
  starting transfers between devices  12.1 us (7%)
  Pallas kernels  11.1 us (7%)
  waiting for transfers between devices  9.89 us (6%)
  local copies, waits for them, and re-layouts  3.89 us (2%)
  other arithmetic  1.89 us (1%)
    all_to_all x9, blocking collectives, exchange(): return lax.all_to_all(blocks, axes, split_axis=0, concat_axis=0, tiled=True)  117 us
    all_to_all x1, starting transfers between devices, exchange(): return lax.all_to_all(blocks, axes, split_axis=0, concat_axis=0, tiled=True)  11.2 us
    all_to_all x1, waiting for transfers between devices, exchange(): return lax.all_to_all(blocks, axes, split_axis=0, concat_axis=0, tiled=True)  7.57 us
    all_gather x1, blocking collectives, local(): arrived = lax.all_gather(arrived, CORE, axis=0)  4.59 us
    all_gather x1, blocking collectives, local(): both = lax.all_gather(arrived, CORE, axis=0)  4.07 us
  transfers between devices with their start and end apart: 3, of which 3 were waited for; matrix products, arithmetic and copies ran while one was open for 0% of the time, Pallas kernels for 2%

profile of v8, /device:TPU:1, one launch (start us, length us, event | category | flops | bytes accessed | tf_op | source)
XLA Modules:
  0.0 166.0 jit_solution(13981165134710523139)
XLA Ops:
  0.6 0.1 pad_add_fusion.at_ref
  0.7 1.5 place.1
  2.3 11.0 %all_to_all.50 = bf16[8,72,128]{2,1,0:T(8,128)(2,1)S(1)} all-to-all(bf16[8,72,128]{2,1,0:T(8,128)(2,1)S(1)} %place.1), channel_id=1, replica_groups=mesh['kv_0'=8,'kv_1'=4,'tp_0'=4,'tp_1'=2] {'tp_0','tp_1'}, dimensions={0} | all-to-all | bytes 294912 | tf_op jit(solution)/shard_map/all_to_all | solution.py:26
  13.3 0.8 broadcast_in_dim.16
  14.1 11.2 %all-to-all-start.1 = ((bf16[32,40,128]{2,1,0:T(8,128)(2,1)}), bf16[32,40,128]{2,1,0:T(8,128)(2,1)S(1)}, u32[]{:S(2)}, u32[]{:S(2)}) async-start(bf16[32,40,128]{2,1,0:T(8,128)(2,1)} %broadcast_in_dim.16), calls=%async_computation.1 | async-start | bytes 655360 | tf_op jit(solution)/shard_map/all_to_all | solution.py:26
  25.3 3.1 %load.1 = (f32[16,128]{1,0:T(8,128)S(1)}, bf16[8,512,512]{2,1,0:T(8,128)(2,1)S(1)}, bf16[44,2,4096]{2,1,0:T(2,128)(2,1)S(1)}, bf16[44,2,4096]{2,1,0:T(2,128)(2,1)S(1)}, bf16[44,2,4096]{2,1,0:T(2,128)(2,1)S(1)}) custom-call(bf16[8,128]{1,0:T(8,128)(2,1)S(1)} %slice.57.lines_ref, bf16[128,512]{1,0:T(8,128)(2,1)} %hbm_0.1, bf16[128,512]{1,0:T(8,128)(2,1)} %hbm_1.1, ...), custom_call_target="tpu_custom_call" | custom-call | tf_op jit(solution)/shard_map/load/pallas_call | solution.py:165
  28.4 0.0 copy-start
  28.4 1.9 %copy-done = bf16[8,512,512]{2,1,0:T(8,128)(2,1)} copy-done((bf16[8,512,512]{2,1,0:T(8,128)(2,1)}, bf16[8,512,512]{2,1,0:T(8,128)(2,1)S(1)}, u32[]{:S(2)}) %copy-start) | copy-done | bytes 4194328
  30.3 7.6 %all-to-all-done.1 = bf16[32,40,128]{2,1,0:T(8,128)(2,1)S(1)} async-done(((bf16[32,40,128]{2,1,0:T(8,128)(2,1)}), bf16[32,40,128]{2,1,0:T(8,128)(2,1)S(1)}, u32[]{:S(2)}, u32[]{:S(2)}) %all-to-all-start.1) | async-done | bytes 327712 | tf_op jit(solution)/shard_map/all_to_all | solution.py:26
  37.9 4.1 %all-gather = bf16[64,40,128]{2,1,0:T(8,128)(2,1)S(1)} all-gather(bf16[32,40,128]{2,1,0:T(8,128)(2,1)S(1)} %all-to-all-done.1), channel_id=2, replica_groups=mesh['kv_0'=8,'kv_1'=4,'tp_0'=4,'tp_1'=2] {'tp_1'}, dimensions={0}, use_global_device_ids=true | all-gather | bytes 983040 | tf_op jit(solution)/shard_map/all_gather | solution.py:511
  42.0 1.7 %first_block.1 = (bf16[32,32,128]{2,1,0:T(8,128)(2,1)S(1)}, bf16[32,32,128]{2,1,0:T(8,128)(2,1)S(1)}, f32[8,128]{1,0:T(8,128)S(1)}, f32[64,128]{1,0:T(8,128)S(1)}) custom-call(s32[3]{0:T(128)S(1)} %pad_add_fusion.at_ref, bf16[2,32,40,128]{3,2,1,0:T(8,128)(2,1)S(1)} %bitcast.64, bf16[44,2,4096]{2,1,0:T(2,128)(2,1)S(1)} %get-tuple-element.140.gate_ref, ...), custom_call_target="tpu_custom_call" | custom-call | tf_op jit(solution)/shard_map/first_block/pallas_call | solution.py:241
  43.7 0.5 collective-permute-start
  44.1 1.2 collective-permute-done.came_ref
  45.3 0.2 first_blocks.1
  45.5 15.9 %all_to_all.51 = bf16[32,17,2,128]{3,2,1,0:T(2,128)(2,1)S(1)} all-to-all(bf16[32,17,2,128]{3,2,1,0:T(2,128)(2,1)S(1)} %first_blocks.1), channel_id=1, replica_groups=mesh['kv_0'=8,'kv_1'=4,'tp_0'=4,'tp_1'=2] {'kv_0','kv_1'}, dimensions={0} | all-to-all | bytes 557056 | tf_op jit(solution)/shard_map/all_to_all | solution.py:26
  61.4 0.2 convert_reduce_fusion
  61.7 9.7 %all_to_all.52 = bf16[8,34,128]{2,1,0:T(8,128)(2,1)S(1)} all-to-all(bf16[8,34,128]{2,1,0:T(8,128)(2,1)S(1)} %broadcast_in_dim.17), channel_id=1, replica_groups=mesh['kv_0'=8,'kv_1'=4,'tp_0'=4,'tp_1'=2] {'tp_0','tp_1'}, dimensions={0} | all-to-all | bytes 139264 | tf_op jit(solution)/shard_map/all_to_all | solution.py:26
  71.5 0.1 multiply_reduce_fusion.1
  71.6 0.1 add_multiply_fusion
  71.7 0.1 multiply_convert_fusion
  71.8 0.1 convolution_convert_fusion
  71.9 0.1 convolution_convert_fusion.1
  72.1 0.0 copy-done.7
  72.1 0.1 convolution_convert_fusion.2
  72.3 0.1 convolution_convert_fusion.3
  72.5 0.3 copy.52
  72.8 0.4 pad_maximum_fusion
  73.2 15.3 %all_to_all.53.arrived_ref = bf16[32,18,2,128]{3,2,1,0:T(2,128)(2,1)S(1)} all-to-all(bf16[32,18,2,128]{3,2,1,0:T(2,128)(2,1)S(1)} %pad_maximum_fusion), channel_id=1, replica_groups=mesh['kv_0'=8,'kv_1'=4,'tp_0'=4,'tp_1'=2] {'kv_0','kv_1'}, dimensions={0} | all-to-all | bytes 589824 | tf_op jit(solution)/shard_map/all_to_all | solution.py:26
  88.6 0.0 copy-done.4
  88.6 2.5 %mixer.1 = (f32[8,8,128]{2,1,0:T(8,128)S(1)}, f32[8,128]{1,0:T(8,128)S(1)}, f32[2,4,128,128]{3,2,1,0:T(8,128)}) custom-call(s32[3]{0:T(128)S(1)} %pad_add_fusion.at_ref, bf16[32,18,2,128]{3,2,1,0:T(2,128)(2,1)S(1)} %all_to_all.53.arrived_ref, bf16[32,8,128]{2,1,0:T(8,128)(2,1)S(1)} %slice_bitcast_fusion.params_ref, f32[4,128]{1,0:T(4,128)S(1)} %bitcast.67, ...), custom_call_target="tpu_custom_call" | custom-call | tf_op jit(solution)/shard_map/mixer/pallas_call | solution.py:455
  91.0 0.0 copy-start.9
  91.1 0.0 copy-start.10
  91.1 9.4 %all_to_all.54 = f32[8,8,128]{2,1,0:T(8,128)S(1)} all-to-all(f32[8,8,128]{2,1,0:T(8,128)S(1)} %get-tuple-element.200), channel_id=1, replica_groups=mesh['kv_0'=8,'kv_1'=4,'tp_0'=4,'tp_1'=2] {'tp_0','tp_1'}, dimensions={0} | all-to-all | bytes 65536 | tf_op jit(solution)/shard_map/all_to_all | solution.py:26
  100.5 19.5 %all_to_all.55 = bf16[128,8,128]{2,1,0:T(8,128)(2,1)S(1)} all-to-all(bf16[128,8,128]{2,1,0:T(8,128)(2,1)S(1)} %broadcast_in_dim.21), channel_id=1, replica_groups=mesh['kv_0'=8,'kv_1'=4,'tp_0'=4,'tp_1'=2] {'kv_0','kv_1','tp_0'}, dimensions={0} | all-to-all | bytes 524288 | tf_op jit(solution)/shard_map/all_to_all | solution.py:26
  120.0 4.6 %all-gather.1 = bf16[256,8,128]{2,1,0:T(8,128)(2,1)S(1)} all-gather(bf16[128,8,128]{2,1,0:T(8,128)(2,1)S(1)} %all_to_all.55), channel_id=3, replica_groups=mesh['kv_0'=8,'kv_1'=4,'tp_0'=4,'tp_1'=2] {'tp_1'}, dimensions={0}, use_global_device_ids=true | all-gather | bytes 786432 | tf_op jit(solution)/shard_map/all_gather | solution.py:578
  124.6 2.1 %second_block.1 = (bf16[32,32,128]{2,1,0:T(8,128)(2,1)S(1)}, bf16[32,32,128]{2,1,0:T(8,128)(2,1)S(1)}, bf16[64,128]{1,0:T(8,128)(2,1)S(1)}) custom-call(s32[3]{0:T(128)S(1)} %pad_add_fusion.at_ref, bf16[2,32,4,8,128]{4,3,2,1,0:T(8,128)(2,1)S(1)} %bitcast.66, bf16[32,8,128]{2,1,0:T(8,128)(2,1)S(1)} %slice_bitcast_fusion.params_ref, ...), custom_call_target="tpu_custom_call" | custom-call | tf_op jit(solution)/shard_map/second_block/pallas_call | solution.py:331
  126.8 0.5 collective-permute-start.1
  127.2 1.2 collective-permute-done.1
  128.4 0.1 add_convert_fusion
  128.5 14.8 %all_to_all.56 = bf16[32,32,128]{2,1,0:T(8,128)(2,1)S(1)} all-to-all(bf16[32,32,128]{2,1,0:T(8,128)(2,1)S(1)} %add_convert_fusion), channel_id=1, replica_groups=mesh['kv_0'=8,'kv_1'=4,'tp_0'=4,'tp_1'=2] {'kv_0','kv_1'}, dimensions={0} | all-to-all | bytes 524288 | tf_op jit(solution)/shard_map/all_to_all | solution.py:26
  143.3 9.3 %all_to_all.57 = bf16[8,32,128]{2,1,0:T(8,128)(2,1)S(1)} all-to-all(bf16[8,32,128]{2,1,0:T(8,128)(2,1)S(1)} %broadcast_in_dim.22), channel_id=1, replica_groups=mesh['kv_0'=8,'kv_1'=4,'tp_0'=4,'tp_1'=2] {'tp_0','tp_1'}, dimensions={0} | all-to-all | bytes 131072 | tf_op jit(solution)/shard_map/all_to_all | solution.py:26
  152.7 0.1 fusion.2
  152.8 0.2 multiply_reduce_fusion
  153.0 0.1 pad_maximum_fusion.2
  153.1 11.9 %all_to_all.58 = f32[32,1,128]{2,1,0:T(1,128)S(1)} all-to-all(f32[32,1,128]{2,1,0:T(1,128)S(1)} %broadcast_in_dim.23), channel_id=1, replica_groups=mesh['kv_0'=8,'kv_1'=4,'tp_0'=4,'tp_1'=2] {'kv_0','kv_1'}, dimensions={0} | all-to-all | bytes 32768 | tf_op jit(solution)/shard_map/all_to_all | solution.py:26
  165.0 0.1 multiply_reduce_fusion.2
  165.2 0.1 add_convert_fusion.1
  165.3 0.7 copy.43
  (47 shorter events, 0.5 us)
Async XLA Ops:
  14.1 23.8 %all-to-all-start.1 = ((bf16[32,40,128]{2,1,0:T(8,128)(2,1)}), bf16[32,40,128]{2,1,0:T(8,128)(2,1)S(1)}, u32[]{:S(2)}, u32[]{:S(2)}) async-start(bf16[32,40,128]{2,1,0:T(8,128)(2,1)} %broadcast_in_dim.16), calls=%async_computation.1 | async-start | bytes 655360 | tf_op jit(solution)/shard_map/all_to_all | solution.py:26
  28.4 1.9 %copy-start = (bf16[8,512,512]{2,1,0:T(8,128)(2,1)}, bf16[8,512,512]{2,1,0:T(8,128)(2,1)S(1)}, u32[]{:S(2)}) copy-start(bf16[8,512,512]{2,1,0:T(8,128)(2,1)S(1)} %get-tuple-element.194.weight_ref) | copy-start | bytes 12582916
  30.3 41.4 %copy-start.5 = (bf16[128,512]{1,0:T(8,128)(2,1)S(1)}, bf16[128,512]{1,0:T(8,128)(2,1)}, u32[]{:S(2)}) copy-start(bf16[128,512]{1,0:T(8,128)(2,1)} %hbm_3.1) | copy-start | bytes 393220
  30.3 41.6 %copy-start.6 = (bf16[128,512]{1,0:T(8,128)(2,1)S(1)}, bf16[128,512]{1,0:T(8,128)(2,1)}, u32[]{:S(2)}) copy-start(bf16[128,512]{1,0:T(8,128)(2,1)} %hbm_2.1) | copy-start | bytes 393220
  30.3 41.7 %copy-start.7 = (bf16[128,512]{1,0:T(8,128)(2,1)S(1)}, bf16[128,512]{1,0:T(8,128)(2,1)}, u32[]{:S(2)}) copy-start(bf16[128,512]{1,0:T(8,128)(2,1)} %hbm_1.1) | copy-start | bytes 393220
  30.3 41.9 %copy-start.8 = (bf16[128,512]{1,0:T(8,128)(2,1)S(1)}, bf16[128,512]{1,0:T(8,128)(2,1)}, u32[]{:S(2)}) copy-start(bf16[128,512]{1,0:T(8,128)(2,1)} %hbm_0.1) | copy-start | bytes 393220
  42.0 46.6 %copy-start.2 = (f32[2,4,128,128]{3,2,1,0:T(8,128)S(1)}, f32[2,4,128,128]{3,2,1,0:T(8,128)}, u32[]{:S(2)}) copy-start(f32[2,4,128,128]{3,2,1,0:T(8,128)} %state_ref.1) | copy-start | bytes 1572868
  42.0 46.6 %copy-start.3 = (f32[512]{0:T(512)S(1)}, f32[512]{0:T(512)}, u32[]{:S(2)}) copy-start(f32[512]{0:T(512)} %param.24) | copy-start | bytes 6148
  42.0 46.6 %copy-start.4 = (f32[512]{0:T(512)S(1)}, f32[512]{0:T(512)}, u32[]{:S(2)}) copy-start(f32[512]{0:T(512)} %param.25) | copy-start | bytes 6148
  43.7 1.6 collective-permute-start
  61.7 26.9 %copy-start.1 = (bf16[8,512,512]{2,1,0:T(8,128)(2,1)S(1)}, bf16[8,512,512]{2,1,0:T(8,128)(2,1)}, u32[]{:S(2)}) copy-start(bf16[8,512,512]{2,1,0:T(8,128)(2,1)} %copy-done) | copy-start | bytes 12582916
  91.0 74.1 %copy-start.9 = (bf16[3,16]{1,0:T(4,128)(2,1)S(1)}, bf16[3,16]{1,0:T(4,128)(2,1)}, u32[]{:S(2)}) copy-start(bf16[3,16]{1,0:T(4,128)(2,1)} %gain_hbm.1) | copy-start | bytes 292
  91.1 74.1 %copy-start.10 = (bf16[3,16]{1,0:T(4,128)(2,1)S(1)}, bf16[3,16]{1,0:T(4,128)(2,1)}, u32[]{:S(2)}) copy-start(bf16[3,16]{1,0:T(4,128)(2,1)} %bias_hbm.1) | copy-start | bytes 292
  126.8 1.6 collective-permute-start.1

commit v9 on v8

--- a/solution.py
+++ b/solution.py
@@ -74,22 +74,30 @@
         fetch.start()
     own_cols, batch = tokens_ref.shape
     half = batch // 2
-    shape = (own_cols, LANES)
-    spot = lax.broadcasted_iota(jnp.int32, shape, 0) + at_ref[1] * own_cols
-    place = (lax.broadcasted_iota(jnp.int32, shape, 1) == spot).astype(f32).astype(bf16)
-    row = lax.broadcasted_iota(jnp.int32, (batch, batch), 0)
-    source = 2 * (row % half) + row // half
-    order = (lax.broadcasted_iota(jnp.int32, (batch, batch), 1) == source).astype(f32)
+    lane = lax.broadcasted_iota(jnp.int32, (batch, LANES), 1)
+    row = lane % batch
+    taken = lax.broadcasted_iota(jnp.int32, (batch, LANES), 0) == 2 * (row % half) + row // half
+    first = jnp.where(taken & (lane < batch), 1.0, 0.0).astype(bf16)
+    second = jnp.where(taken & (lane >= batch), 1.0, 0.0).astype(bf16)
+    groups = LANES // own_cols
+    spot = lax.broadcasted_iota(jnp.int32, (own_cols, LANES), 0)
+    own_lane = lax.broadcasted_iota(jnp.int32, (own_cols, LANES), 1)
     for fetch in fetches:
         fetch.wait()
-    turned = lax.dot_general(
-        order.astype(bf16), tokens_ref[...], (((1,), (1,)), ((), ())), preferred_element_type=f32
-    ).astype(bf16)
-    lines_ref[batch:, :] = jnp.zeros((8, LANES), f32)
-    lines_ref[:batch, :] = jnp.dot(turned, place, preferred_element_type=f32)
-    lines_ref[batch : batch + 3, :] = jnp.dot(gain_ref[...], place, preferred_element_type=f32)
-    lines_ref[batch + 3 : batch + 6, :] = jnp.dot(bias_ref[...], place, preferred_element_type=f32)
-    lines = lines_ref[...].astype(bf16)
+    top = jnp.dot(tokens_ref[...], first, preferred_element_type=f32)
+    low = jnp.dot(tokens_ref[...], second, preferred_element_type=f32)
+    line = jnp.zeros((1, LANES), f32)
+    for index in range(6):
+        at = (index + at_ref[1]) % groups * own_cols
+        place = jnp.where(own_lane == spot + at, 1.0, 0.0).astype(bf16)
+        source = gain_ref if index < 3 else bias_ref
+        moved = jnp.dot(source[...], place, preferred_element_type=f32)
+        line = line + moved[index % 3 : index % 3 + 1]
+    count = own_cols // 2
+    lines_ref[...] = jnp.zeros(lines_ref.shape, f32)
+    lines_ref[:count, :] = top[:count] + low[count:]
+    lines_ref[count : count + 1, :] = line
+    lines = lines_ref[...].astype(bf16).reshape(count, 2, LANES)[: result_ref.shape[1]]
     for copy in range(result_ref.shape[0]):
         result_ref[copy] = lines
 
@@ -100,9 +108,9 @@
         place_kernel,
         in_specs=[SMEM] + [ANYWHERE] * 3,
         out_specs=VMEM,
-        out_shape=jax.ShapeDtypeStruct((count, batch + 8, LANES), bf16),
+        out_shape=jax.ShapeDtypeStruct((count, own_cols // 4 + 1, 2, LANES), bf16),
         scratch_shapes=[
-            pltpu.VMEM((batch + 8, LANES), f32),
+            pltpu.VMEM((own_cols, LANES), f32),
             pltpu.VMEM((own_cols, batch), bf16),
             pltpu.VMEM(gain.shape, bf16),
             pltpu.VMEM(bias.shape, bf16),
@@ -114,31 +122,10 @@
 
 
 def load_kernel(
-    lines_ref,
-    hbm_0,
-    hbm_1,
-    hbm_2,
-    hbm_3,
-    out_hbm,
-    gate_hbm,
-    up_hbm,
-    down_hbm,
-    bias_ref,
-    out_ref,
-    gate_ref,
-    up_ref,
-    down_ref,
-    project_ref,
-    project_sem,
-    part_sem,
-    sem,
+    out_hbm, gate_hbm, up_hbm, down_hbm, out_ref, gate_ref, up_ref, down_ref, part_sem, sem
 ):
     parts, _, step = out_ref.shape
     pairs = ((gate_hbm, gate_ref), (up_hbm, up_ref), (down_hbm, down_ref))
-    projections = [
-        pltpu.make_async_copy(hbm, project_ref.at[i], project_sem.at[i])
-        for i, hbm in enumerate((hbm_0, hbm_1, hbm_2, hbm_3))
-    ]
     fetches = [pltpu.make_async_copy(*pair, sem.at[i]) for i, pair in enumerate(pairs)]
     fetches += [
         pltpu.make_async_copy(
@@ -146,49 +133,73 @@
         )
         for part in range(parts)
     ]
-    for fetch in projections + fetches:
+    for fetch in fetches:
         fetch.start()
-    lines = lines_ref[...]
-    for index, projection in enumerate(projections):
-        projection.wait()
-        sums = jnp.dot(lines, project_ref[index], preferred_element_type=f32)
+    for fetch in fetches:
+        fetch.wait()
+
+
+def load(out_weight, stored, parts):
+    depth, width = out_weight.shape
+    return pl.pallas_call(
+        load_kernel,
+        in_specs=[ANYWHERE] * 4,
+        out_specs=[VMEM] * 4,
+        out_shape=[jax.ShapeDtypeStruct((parts, depth, width // parts), bf16)]
+        + [jax.ShapeDtypeStruct(w.shape, bf16) for w in stored],
+        scratch_shapes=[pltpu.SemaphoreType.DMA((parts,)), pltpu.SemaphoreType.DMA((3,))],
+        compiler_params=small(12),
+        name="load",
+    )(*[off_chip(w) for w in (out_weight, *stored)])
+
+
+def order_kernel(at_ref, rows_ref, w0, w1, w2, w3, params_ref, bias_ref):
+    cores, kv_count, x_count = rows_ref.shape[:3]
+    last = rows_ref.shape[3] - 1
+    groups = cores * x_count
+    own_cols = LANES // groups
+    lines = [
+        rows_ref[group % cores, :, group // cores, last].astype(f32)[:, 0, :]
+        for group in range(groups)
+    ]
+    place = lax.broadcasted_iota(jnp.int32, (kv_count, LANES), 1) // own_cols
+    params_ref[...] = jnp.zeros(params_ref.shape, f32)
+    for index in range(6):
+        total = jnp.zeros((kv_count, LANES), f32)
+        for group in range(groups):
+            total = jnp.where(place == (index + group) % groups, lines[group], total)
+        if index:
+            total = pltpu.roll(total, LANES - index * own_cols, 1)
+        params_ref[pl.ds(index, kv_count, stride=8), :] = total
+    own = params_ref[pl.ds(pl.multiple_of(at_ref[0] * 8, 8), 8), :].astype(bf16)
+    for index, w_ref in enumerate((w0, w1, w2, w3)):
+        sums = jnp.dot(own, w_ref[...], preferred_element_type=f32)
         heads = sums.shape[1] // LANES
         for head in range(heads):
             chunk = index * heads + head
             bias_ref[chunk : chunk + 1, :] = sums[3:4, head * LANES : (head + 1) * LANES]
-    for fetch in fetches:
-        fetch.wait()
-
-
-def load(lines, weights, out_weight, stored, parts):
-    depth, width = out_weight.shape
+
+
+def in_order(at, rows, weights):
+    kv_count = rows.shape[1]
     return pl.pallas_call(
-        load_kernel,
-        in_specs=[VMEM] + [ANYWHERE] * 8,
-        out_specs=[VMEM] * 5,
+        order_kernel,
+        in_specs=[SMEM] + [VMEM] * 5,
+        out_specs=[VMEM] * 2,
         out_shape=[
+            jax.ShapeDtypeStruct((kv_count * 8, LANES), f32),
             jax.ShapeDtypeStruct((4 * weights[0].shape[1] // LANES, LANES), f32),
-            jax.ShapeDtypeStruct((parts, depth, width // parts), bf16),
-        ]
-        + [jax.ShapeDtypeStruct(w.shape, bf16) for w in stored],
-        scratch_shapes=[
-            pltpu.VMEM((4, *weights[0].shape), bf16),
-            pltpu.SemaphoreType.DMA((4,)),
-            pltpu.SemaphoreType.DMA((parts,)),
-            pltpu.SemaphoreType.DMA((3,)),
-        ],
-        compiler_params=small(12),
-        name="load",
-    )(lines, *[off_chip(w) for w in (*weights, out_weight, *stored)])
-
-
-def feed_forward(rows, core, layer, gate_ref, up_ref, down_ref):
-    def stored(ref):
-        return ref[...].reshape(ref.shape[0] * ref.shape[1], ref.shape[2])
-
-    dims = (((1,), (1,)), ((), ()))
-    gate = lax.dot_general(rows, stored(gate_ref), dims, preferred_element_type=f32)
-    up = lax.dot_general(rows, stored(up_ref), dims, preferred_element_type=f32)
+        ],
+        compiler_params=small(),
+        name="in_order",
+    )(at, rows, *weights)
+
+
+def stored(ref):
+    return ref[...].reshape(ref.shape[0] * ref.shape[1], ref.shape[2])
+
+
+def feed_forward(gate, up, core, layer, down_ref):
     hidden = jax.nn.silu(gate) * up
     unit = lax.broadcasted_iota(jnp.int32, hidden.shape, 1)
     hidden = jnp.where(unit % 2 == layer, hidden, 0.0)
@@ -208,21 +219,42 @@
 
 
 def first_kernel(
-    at_ref, rows_ref, gate_ref, up_ref, down_ref, kept_ref, sent_ref, tail_ref, total_ref, x_ref
+    at_ref,
+    rows_ref,
+    gate_ref,
+    up_ref,
+    down_ref,
+    kept_ref,
+    sent_ref,
+    tail_ref,
+    total_ref,
+    block_ref,
+    x_ref,
 ):
-    chunks, half, _ = kept_ref.shape
+    half = kept_ref.shape[1]
+    batch = 2 * half
+    cores, kv_count, x_count = rows_ref.shape[:3]
+    pairs = rows_ref.shape[3] - 1
     core = at_ref[2]
-    for seq in range(2):
-        at = slice(seq * half, (seq + 1) * half)
-        total = jnp.zeros((half, LANES), f32)
-        for chunk in range(chunks):
-            lines = rows_ref[seq, chunk, :half, :]
-            x_ref[at, chunk * LANES : (chunk + 1) * LANES] = lines
-            total = total + lines.astype(f32)
-        total_ref[at, :] = jnp.broadcast_to(jnp.sum(total, axis=1, keepdims=True), (half, LANES))
-    part = feed_forward(x_ref[...], core, 0, gate_ref, up_ref, down_ref)
+    total = jnp.zeros((8, LANES), f32)
+    for index in range(cores):
+        for x in range(x_count):
+            lines = rows_ref[index, :, x, :pairs].reshape(kv_count * 8, LANES).astype(f32)
+            other = pltpu.roll(lines, LANES - batch, 1)
+            lines = lines.reshape(kv_count, 8, LANES)
+            total = total + lines.sum(axis=0)
+            lines = jnp.concatenate([lines, other.reshape(kv_count, 8, LANES)], axis=1)
+            x_ref[:, x * cores + index] = lines.astype(bf16)
+    total = jnp.sum(total, axis=0, keepdims=True)
+    total = total + pltpu.roll(total, LANES - batch, 1)
+    total_ref[...] = jnp.broadcast_to(total, total_ref.shape)
+    own = x_ref[at_ref[0]].reshape(LANES, LANES).astype(f32)
+    block_ref[...] = own.T[:batch]
+    rows = x_ref[...].reshape(kv_count * LANES, LANES)
+    gate = jnp.dot(stored(gate_ref), rows, preferred_element_type=f32).T[:batch]
+    up = jnp.dot(stored(up_ref), rows, preferred_element_type=f32).T[:batch]
+    part = feed_forward(gate, up, core, 0, down_ref)
     write_halves(part, kept_ref, sent_ref)
-    batch = 2 * half
     sums = jnp.broadcast_to(jnp.sum(part, axis=1, keepdims=True), (batch, LANES))
     row = (lax.broadcasted_iota(jnp.int32, (batch, LANES), 0) + core * half) % batch
     lane = lax.broadcasted_iota(jnp.int32, (batch, LANES), 1)
@@ -238,17 +270,19 @@
 
 def first_block(at, rows, stored, half):
     chunks = rows.shape[1]
+    groups = rows.shape[0] * rows.shape[2]
     return pl.pallas_call(
         first_kernel,
         in_specs=[SMEM] + [VMEM] * 4,
-        out_specs=[VMEM] * 4,
+        out_specs=[VMEM] * 5,
         out_shape=[
             jax.ShapeDtypeStruct((chunks, half, LANES), bf16),
             jax.ShapeDtypeStruct((chunks, half, LANES), bf16),
             jax.ShapeDtypeStruct((8, LANES), f32),
+            jax.ShapeDtypeStruct((8, LANES), f32),
             jax.ShapeDtypeStruct((2 * half, LANES), f32),
         ],
-        scratch_shapes=[pltpu.VMEM((2 * half, chunks * LANES), bf16)],
+        scratch_shapes=[pltpu.VMEM((chunks, groups, LANES // groups, LANES), bf16)],
         compiler_params=small(12),
         name="first_block",
     )(at, rows, *stored)
@@ -321,7 +355,11 @@
                 seq * kv_count : (seq + 1) * kv_count, chunk * LANES : (chunk + 1) * LANES
             ] = normed.astype(bf16)
     own_ref[...] = result_ref[:, pl.ds(pl.multiple_of(at_ref[0] * LANES, LANES), LANES)]
-    part = feed_forward(result_ref[...], at_ref[2], 1, gate_ref, up_ref, down_ref)
+    dims = (((1,), (1,)), ((), ()))
+    rows = result_ref[...]
+    gate = lax.dot_general(rows, stored(gate_ref), dims, preferred_element_type=f32)
+    up = lax.dot_general(rows, stored(up_ref), dims, preferred_element_type=f32)
+    part = feed_forward(gate, up, at_ref[2], 1, down_ref)
     write_halves(part, kept_ref, sent_ref)
 
 
@@ -501,15 +539,10 @@
     kv, tp, core = lax.axis_index(KV), lax.axis_index(TP), lax.axis_index(CORE)
 
     at = jnp.stack([kv, tp, core])
-    blocks = placed_copies(at, tokens, norm_gain, norm_bias, tp_count)
-    arrived, at, kv, tp, core, norm_gain, norm_bias = alone(
-        blocks, TP, at, kv, tp, core, norm_gain, norm_bias
-    )
-    block = arrived.astype(f32).sum(axis=0).astype(bf16)
-    own_half = lax.dynamic_slice_in_dim(block, core * half, half, 0)
-    arrived = to_everyone(jnp.concatenate([own_half, block[batch:]]), KV, kv_count)
-    both = lax.all_gather(arrived, CORE, axis=0)
-    params = both[0, :, half:]
+    blocks = placed_copies(at, tokens, norm_gain, norm_bias, chip_count)
+    arrived = exchange(blocks, CHIPS)
+    rows = lax.all_gather(arrived, CORE, axis=0)
+    rows = rows.reshape(2, kv_count, x_count, *rows.shape[2:])
 
     def over_tp(lines, *held):
         gathered, *held = alone(copies(lines, tp_count), TP, *held)
@@ -519,10 +552,10 @@
     chunk_count = 4 * heads
     share = kv_count // chunk_count
     stored = stored_order(gate_weights, up_weights, down_weights)
-    bias_rows, mixer_weight, *stored = load(
-        block[batch:], weights, out_weight, stored, tp_count
-    )
-    kept, sent, tail, token_sum = first_block(at, both, stored, half)
+    mixer_weight, *stored = load(out_weight, stored, tp_count)
+    kept, sent, tail, token_sum, block = first_block(at, rows, stored, half)
+    params, bias_rows = in_order(at, rows, weights)
+    params = params.reshape(kv_count, 8, LANES)
     blocks = first_blocks(kept, lax.ppermute(sent, CORE, SWAP), tail, bias_rows)
     arrived, at, kv, tp, norm_gain, norm_bias, block, params, token_sum = alone(
         blocks, KV, at, kv, tp, norm_gain, norm_bias, block, params, token_sum
@@ -533,12 +566,12 @@
     )
     gathered = gathered.astype(f32)
     bias_own = arrived[half + 1 : half + 2] / share
-    gain_one = block[batch : batch + 1]
+    gain_one = lax.dynamic_index_in_dim(params, kv, 0, keepdims=False)[:1]
     total = gathered[:, :, :half].sum(axis=0).reshape(batch, LANES)
     total_row = gathered[:, :, half].sum(axis=(0, 1))
-    stream_one = residual_scale * block[:batch].astype(f32) + 0.5 * total
+    stream_one = residual_scale * block + 0.5 * total
     row_mean = (
-        residual_scale * token_sum[:, 0]
+        residual_scale * token_sum[0, :batch]
         + 0.5 * (total_row[:batch] + total_row[batch:])
     ) / width
     centred = stream_one - row_mean[:, None]

time: 167 us -> 165 us (0.988)
  blocking collectives: 125 us -> 114 us
  starting transfers between devices: 12.1 us -> 17.3 us
  Pallas kernels: 11.1 us -> 13 us
    all_to_all x9 -> x8, blocking collectives: 117 us -> 105 us  [exchange(): return lax.all_to_all(blocks, axes, split_axis=0, concat_axis=0, tiled=True)]
    all_to_all x1, starting transfers between devices: 11.2 us -> 16.3 us  [exchange(): return lax.all_to_all(blocks, axes, split_axis=0, concat_axis=0, tiled=True)]
    all_to_all x1, waiting for transfers between devices: 7.57 us -> 9.8 us  [exchange(): return lax.all_to_all(blocks, axes, split_axis=0, concat_axis=0, tiled=True)]
    unnamed x24, local copies, waits for them, and re-layouts: 2.67 us -> 4.86 us
    pallas_call x1 -> x2, Pallas kernels: 3.11 us -> 3.94 us  [the longest x1 2.99 us: load(): pl.pallas_call(load_kernel, in_specs=[ANYWHERE] * 4, out_specs=[VMEM] * 4...]
where the time goes in v9:
time: 165 us; the launch traced here: 164 us
  blocking collectives  114 us (69%)
  starting transfers between devices  17.3 us (10%)
  Pallas kernels  13 us (8%)
  waiting for transfers between devices  11.2 us (7%)
  local copies, waits for them, and re-layouts  5.31 us (3%)
  other arithmetic  1.76 us (1%)
    all_to_all x8, blocking collectives, exchange(): return lax.all_to_all(blocks, axes, split_axis=0, concat_axis=0, tiled=True)  105 us
    all_to_all x1, starting transfers between devices, exchange(): return lax.all_to_all(blocks, axes, split_axis=0, concat_axis=0, tiled=True)  16.3 us
    all_to_all x1, waiting for transfers between devices, exchange(): return lax.all_to_all(blocks, axes, split_axis=0, concat_axis=0, tiled=True)  9.8 us
    unnamed x24, local copies, waits for them, and re-layouts  4.86 us
    all_gather x1, blocking collectives, local(): arrived = lax.all_gather(arrived, CORE, axis=0)  4.77 us
    all_gather x1, blocking collectives, local(): rows = lax.all_gather(arrived, CORE, axis=0)  4.61 us
  transfers between devices with their start and end apart: 3, of which 3 were waited for; matrix products, arithmetic and copies ran while one was open for 0% of the time, Pallas kernels for 2%

profile of v9, /device:TPU:1, one launch (start us, length us, event | category | flops | bytes accessed | tf_op | source)
XLA Modules:
  0.0 164.2 jit_solution(12454243237027642913)
XLA Ops:
  0.6 0.1 pad_add_fusion.at_ref
  0.7 2.4 %place.1 = bf16[128,5,2,128]{3,2,1,0:T(2,128)(2,1)} custom-call(s32[3]{0:T(128)S(1)} %pad_add_fusion.at_ref, bf16[16,64]{1,0:T(8,128)(2,1)} %bitcast.88, bf16[3,16]{1,0:T(4,128)(2,1)} %gain_hbm.1, bf16[3,16]{1,0:T(4,128)(2,1)} %bias_hbm.1), custom_call_target="tpu_custom_call" | custom-call | tf_op jit(solution)/shard_map/place/pallas_call | solution.py:107
  3.1 16.3 %all-to-all-start = ((bf16[128,5,2,128]{3,2,1,0:T(2,128)(2,1)}), bf16[128,5,2,128]{3,2,1,0:T(2,128)(2,1)S(1)}, u32[]{:S(2)}, u32[]{:S(2)}) async-start(bf16[128,5,2,128]{3,2,1,0:T(2,128)(2,1)} %place.1), calls=%async_computation | async-start | bytes 655360 | tf_op jit(solution)/shard_map/all_to_all | solution.py:26
  19.4 0.0 copy-start.3
  19.4 0.0 copy-start.4
  19.5 0.0 copy-start.6
  19.5 3.0 %load.1 = (bf16[8,512,512]{2,1,0:T(8,128)(2,1)S(1)}, bf16[44,2,4096]{2,1,0:T(2,128)(2,1)S(1)}, bf16[44,2,4096]{2,1,0:T(2,128)(2,1)S(1)}, bf16[44,2,4096]{2,1,0:T(2,128)(2,1)S(1)}) custom-call(bf16[512,4096]{1,0:T(8,128)(2,1)} %out_hbm.1, bf16[44,2,4096]{2,1,0:T(2,128)(2,1)} %bitcast.76, bf16[44,2,4096]{2,1,0:T(2,128)(2,1)} %bitcast.77, ...), custom_call_target="tpu_custom_call" | custom-call | tf_op jit(solution)/shard_map/load/pallas_call | solution.py:144
  22.5 1.9 %copy-done = bf16[8,512,512]{2,1,0:T(8,128)(2,1)} copy-done((bf16[8,512,512]{2,1,0:T(8,128)(2,1)}, bf16[8,512,512]{2,1,0:T(8,128)(2,1)S(1)}, u32[]{:S(2)}) %copy-start) | copy-done | bytes 4194328
  24.4 9.8 %all-to-all-done = bf16[128,5,2,128]{3,2,1,0:T(2,128)(2,1)S(1)} async-done(((bf16[128,5,2,128]{3,2,1,0:T(2,128)(2,1)}), bf16[128,5,2,128]{3,2,1,0:T(2,128)(2,1)S(1)}, u32[]{:S(2)}, u32[]{:S(2)}) %all-to-all-start) | async-done | bytes 327712 | tf_op jit(solution)/shard_map/all_to_all | solution.py:26
  34.2 4.6 %all-gather = bf16[256,5,2,128]{3,2,1,0:T(2,128)(2,1)S(1)} all-gather(bf16[128,5,2,128]{3,2,1,0:T(2,128)(2,1)S(1)} %all-to-all-done), channel_id=2, replica_groups=mesh['kv_0'=8,'kv_1'=4,'tp_0'=4,'tp_1'=2] {'tp_1'}, dimensions={0}, use_global_device_ids=true | all-gather | bytes 983040 | tf_op jit(solution)/shard_map/all_gather | solution.py:544
  38.8 2.0 %first_block.1 = (bf16[32,32,128]{2,1,0:T(8,128)(2,1)S(1)}, bf16[32,32,128]{2,1,0:T(8,128)(2,1)S(1)}, f32[8,128]{1,0:T(8,128)S(1)}, f32[8,128]{1,0:T(8,128)S(1)}, f32[64,128]{1,0:T(8,128)S(1)}) custom-call(s32[3]{0:T(128)S(1)} %pad_add_fusion.at_ref, bf16[2,32,4,5,2,128]{5,4,3,2,1,0:T(2,128)(2,1)S(1)} %bitcast.66, ...), custom_call_target="tpu_custom_call" | custom-call | tf_op jit(solution)/shard_map/first_block/pallas_call | solution.py:274
  40.8 0.0 copy-start.7
  40.8 0.0 copy-start.8
  40.8 0.5 collective-permute-start
  41.3 1.0 in_order.1
  42.2 0.2 collective-permute-done.came_ref
  42.4 0.2 first_blocks.1
  42.6 15.1 %all_to_all.45 = bf16[32,17,2,128]{3,2,1,0:T(2,128)(2,1)S(1)} all-to-all(bf16[32,17,2,128]{3,2,1,0:T(2,128)(2,1)S(1)} %first_blocks.1), channel_id=1, replica_groups=mesh['kv_0'=8,'kv_1'=4,'tp_0'=4,'tp_1'=2] {'kv_0','kv_1'}, dimensions={0} | all-to-all | bytes 557056 | tf_op jit(solution)/shard_map/all_to_all | solution.py:26
  57.7 0.2 convert_reduce_fusion
  58.0 9.4 %all_to_all.46 = bf16[8,34,128]{2,1,0:T(8,128)(2,1)S(1)} all-to-all(bf16[8,34,128]{2,1,0:T(8,128)(2,1)S(1)} %broadcast_in_dim.14), channel_id=1, replica_groups=mesh['kv_0'=8,'kv_1'=4,'tp_0'=4,'tp_1'=2] {'tp_0','tp_1'}, dimensions={0} | all-to-all | bytes 139264 | tf_op jit(solution)/shard_map/all_to_all | solution.py:26
  67.5 0.1 fusion.2
  67.6 0.1 multiply_convert_fusion
  67.7 0.1 convolution_convert_fusion
  67.8 0.1 convolution_convert_fusion.1
  68.0 0.1 convolution_convert_fusion.2
  68.1 0.1 convolution_convert_fusion.3
  68.4 0.3 copy.52
  68.7 0.4 pad_maximum_fusion
  69.1 15.3 %all_to_all.47.arrived_ref = bf16[32,18,2,128]{3,2,1,0:T(2,128)(2,1)S(1)} all-to-all(bf16[32,18,2,128]{3,2,1,0:T(2,128)(2,1)S(1)} %pad_maximum_fusion), channel_id=1, replica_groups=mesh['kv_0'=8,'kv_1'=4,'tp_0'=4,'tp_1'=2] {'kv_0','kv_1'}, dimensions={0} | all-to-all | bytes 589824 | tf_op jit(solution)/shard_map/all_to_all | solution.py:26
  84.4 2.2 %copy-done.1 = bf16[8,512,512]{2,1,0:T(8,128)(2,1)S(1)} copy-done((bf16[8,512,512]{2,1,0:T(8,128)(2,1)S(1)}, bf16[8,512,512]{2,1,0:T(8,128)(2,1)}, u32[]{:S(2)}) %copy-start.1) | copy-done | bytes 4194328
  86.6 2.5 %mixer.1 = (f32[8,8,128]{2,1,0:T(8,128)S(1)}, f32[8,128]{1,0:T(8,128)S(1)}, f32[2,4,128,128]{3,2,1,0:T(8,128)}) custom-call(s32[3]{0:T(128)S(1)} %pad_add_fusion.at_ref, bf16[32,18,2,128]{3,2,1,0:T(2,128)(2,1)S(1)} %all_to_all.47.arrived_ref, f32[32,8,128]{2,1,0:T(8,128)S(1)} %bitcast.70, f32[4,128]{1,0:T(4,128)S(1)} %bitcast.72, f32[4,128]{1,0:T(4,128)S(1)} %bitcast.73, ...), custom_call_target="tpu_custom_call" | custom-call | tf_op jit(solution)/shard_map/mixer/pallas_call | solution.py:493
  89.1 0.0 copy-start.9
  89.1 9.4 %all_to_all.48 = f32[8,8,128]{2,1,0:T(8,128)S(1)} all-to-all(f32[8,8,128]{2,1,0:T(8,128)S(1)} %get-tuple-element.188), channel_id=1, replica_groups=mesh['kv_0'=8,'kv_1'=4,'tp_0'=4,'tp_1'=2] {'tp_0','tp_1'}, dimensions={0} | all-to-all | bytes 65536 | tf_op jit(solution)/shard_map/all_to_all | solution.py:26
  98.6 19.5 %all_to_all.49 = bf16[128,8,128]{2,1,0:T(8,128)(2,1)S(1)} all-to-all(bf16[128,8,128]{2,1,0:T(8,128)(2,1)S(1)} %broadcast_in_dim.18), channel_id=1, replica_groups=mesh['kv_0'=8,'kv_1'=4,'tp_0'=4,'tp_1'=2] {'kv_0','kv_1','tp_0'}, dimensions={0} | all-to-all | bytes 524288 | tf_op jit(solution)/shard_map/all_to_all | solution.py:26
  118.1 4.8 %all-gather.1 = bf16[256,8,128]{2,1,0:T(8,128)(2,1)S(1)} all-gather(bf16[128,8,128]{2,1,0:T(8,128)(2,1)S(1)} %all_to_all.49), channel_id=3, replica_groups=mesh['kv_0'=8,'kv_1'=4,'tp_0'=4,'tp_1'=2] {'tp_1'}, dimensions={0}, use_global_device_ids=true | all-gather | bytes 786432 | tf_op jit(solution)/shard_map/all_gather | solution.py:611
  122.8 2.1 %second_block.1 = (bf16[32,32,128]{2,1,0:T(8,128)(2,1)S(1)}, bf16[32,32,128]{2,1,0:T(8,128)(2,1)S(1)}, bf16[64,128]{1,0:T(8,128)(2,1)S(1)}) custom-call(s32[3]{0:T(128)S(1)} %pad_add_fusion.at_ref, bf16[2,32,4,8,128]{4,3,2,1,0:T(8,128)(2,1)S(1)} %bitcast.68, f32[32,8,128]{2,1,0:T(8,128)S(1)} %bitcast.71, ...), custom_call_target="tpu_custom_call" | custom-call | tf_op jit(solution)/shard_map/second_block/pallas_call | solution.py:369
  125.0 0.5 collective-permute-start.1
  125.4 1.2 collective-permute-done.1
  126.6 0.1 add_convert_fusion
  126.7 14.8 %all_to_all.50 = bf16[32,32,128]{2,1,0:T(8,128)(2,1)S(1)} all-to-all(bf16[32,32,128]{2,1,0:T(8,128)(2,1)S(1)} %add_convert_fusion), channel_id=1, replica_groups=mesh['kv_0'=8,'kv_1'=4,'tp_0'=4,'tp_1'=2] {'kv_0','kv_1'}, dimensions={0} | all-to-all | bytes 524288 | tf_op jit(solution)/shard_map/all_to_all | solution.py:26
  141.5 9.3 %all_to_all.51 = bf16[8,32,128]{2,1,0:T(8,128)(2,1)S(1)} all-to-all(bf16[8,32,128]{2,1,0:T(8,128)(2,1)S(1)} %broadcast_in_dim.19), channel_id=1, replica_groups=mesh['kv_0'=8,'kv_1'=4,'tp_0'=4,'tp_1'=2] {'tp_0','tp_1'}, dimensions={0} | all-to-all | bytes 131072 | tf_op jit(solution)/shard_map/all_to_all | solution.py:26
  150.9 0.1 fusion.3
  151.0 0.2 multiply_reduce_fusion
  151.2 0.1 pad_maximum_fusion.1
  151.3 11.9 %all_to_all.52 = f32[32,1,128]{2,1,0:T(1,128)S(1)} all-to-all(f32[32,1,128]{2,1,0:T(1,128)S(1)} %broadcast_in_dim.20), channel_id=1, replica_groups=mesh['kv_0'=8,'kv_1'=4,'tp_0'=4,'tp_1'=2] {'kv_0','kv_1'}, dimensions={0} | all-to-all | bytes 32768 | tf_op jit(solution)/shard_map/all_to_all | solution.py:26
  163.2 0.1 multiply_reduce_fusion.1
  163.4 0.1 add_convert_fusion.1
  163.5 0.7 copy.43
  (41 shorter events, 0.5 us)
Async XLA Ops:
  3.1 31.1 %all-to-all-start = ((bf16[128,5,2,128]{3,2,1,0:T(2,128)(2,1)}), bf16[128,5,2,128]{3,2,1,0:T(2,128)(2,1)S(1)}, u32[]{:S(2)}, u32[]{:S(2)}) async-start(bf16[128,5,2,128]{3,2,1,0:T(2,128)(2,1)} %place.1), calls=%async_computation | async-start | bytes 655360 | tf_op jit(solution)/shard_map/all_to_all | solution.py:26
  19.4 21.8 %copy-start.3 = (bf16[128,512]{1,0:T(8,128)(2,1)S(1)}, bf16[128,512]{1,0:T(8,128)(2,1)}, u32[]{:S(2)}) copy-start(bf16[128,512]{1,0:T(8,128)(2,1)} %w3.1) | copy-start | bytes 393220
  19.4 21.8 %copy-start.4 = (bf16[128,512]{1,0:T(8,128)(2,1)S(1)}, bf16[128,512]{1,0:T(8,128)(2,1)}, u32[]{:S(2)}) copy-start(bf16[128,512]{1,0:T(8,128)(2,1)} %w2.1) | copy-start | bytes 393220
  19.5 21.8 %copy-start.5 = (bf16[128,512]{1,0:T(8,128)(2,1)S(1)}, bf16[128,512]{1,0:T(8,128)(2,1)}, u32[]{:S(2)}) copy-start(bf16[128,512]{1,0:T(8,128)(2,1)} %w1.1) | copy-start | bytes 393220
  19.5 21.8 %copy-start.6 = (bf16[128,512]{1,0:T(8,128)(2,1)S(1)}, bf16[128,512]{1,0:T(8,128)(2,1)}, u32[]{:S(2)}) copy-start(bf16[128,512]{1,0:T(8,128)(2,1)} %w0.1) | copy-start | bytes 393220
  22.5 1.9 %copy-start = (bf16[8,512,512]{2,1,0:T(8,128)(2,1)}, bf16[8,512,512]{2,1,0:T(8,128)(2,1)S(1)}, u32[]{:S(2)}) copy-start(bf16[8,512,512]{2,1,0:T(8,128)(2,1)S(1)} %get-tuple-element.182.weight_ref) | copy-start | bytes 12582916
  40.8 43.6 %copy-start.2 = (f32[2,4,128,128]{3,2,1,0:T(8,128)S(1)}, f32[2,4,128,128]{3,2,1,0:T(8,128)}, u32[]{:S(2)}) copy-start(f32[2,4,128,128]{3,2,1,0:T(8,128)} %state_ref.1) | copy-start | bytes 1572868
  40.8 43.6 %copy-start.7 = (f32[512]{0:T(512)S(1)}, f32[512]{0:T(512)}, u32[]{:S(2)}) copy-start(f32[512]{0:T(512)} %param.24) | copy-start | bytes 6148
  40.8 43.6 %copy-start.8 = (f32[512]{0:T(512)S(1)}, f32[512]{0:T(512)}, u32[]{:S(2)}) copy-start(f32[512]{0:T(512)} %param.25) | copy-start | bytes 6148
  40.8 1.6 collective-permute-start
  84.4 2.2 %copy-start.1 = (bf16[8,512,512]{2,1,0:T(8,128)(2,1)S(1)}, bf16[8,512,512]{2,1,0:T(8,128)(2,1)}, u32[]{:S(2)}) copy-start(bf16[8,512,512]{2,1,0:T(8,128)(2,1)} %copy-done) | copy-start | bytes 12582916
  89.1 74.3 %copy-start.9 = (bf16[3,16]{1,0:T(4,128)(2,1)S(1)}, bf16[3,16]{1,0:T(4,128)(2,1)}, u32[]{:S(2)}) copy-start(bf16[3,16]{1,0:T(4,128)(2,1)} %gain_hbm.1) | copy-start | bytes 292
  89.1 74.2 %copy-start.10 = (bf16[3,16]{1,0:T(4,128)(2,1)S(1)}, bf16[3,16]{1,0:T(4,128)(2,1)}, u32[]{:S(2)}) copy-start(bf16[3,16]{1,0:T(4,128)(2,1)} %bias_hbm.1) | copy-start | bytes 292
  125.0 1.6 collective-permute-start.1

commit v10 on v9

--- a/solution.py
+++ b/solution.py
@@ -121,36 +121,25 @@
     )(at, off_chip(tokens.T), off_chip(gain), off_chip(bias))
 
 
-def load_kernel(
-    out_hbm, gate_hbm, up_hbm, down_hbm, out_ref, gate_ref, up_ref, down_ref, part_sem, sem
-):
-    parts, _, step = out_ref.shape
+def load_kernel(gate_hbm, up_hbm, down_hbm, gate_ref, up_ref, down_ref, sem):
     pairs = ((gate_hbm, gate_ref), (up_hbm, up_ref), (down_hbm, down_ref))
     fetches = [pltpu.make_async_copy(*pair, sem.at[i]) for i, pair in enumerate(pairs)]
-    fetches += [
-        pltpu.make_async_copy(
-            out_hbm.at[:, pl.ds(part * step, step)], out_ref.at[part], part_sem.at[part]
-        )
-        for part in range(parts)
-    ]
     for fetch in fetches:
         fetch.start()
     for fetch in fetches:
         fetch.wait()
 
 
-def load(out_weight, stored, parts):
-    depth, width = out_weight.shape
+def load(stored):
     return pl.pallas_call(
         load_kernel,
-        in_specs=[ANYWHERE] * 4,
-        out_specs=[VMEM] * 4,
-        out_shape=[jax.ShapeDtypeStruct((parts, depth, width // parts), bf16)]
-        + [jax.ShapeDtypeStruct(w.shape, bf16) for w in stored],
-        scratch_shapes=[pltpu.SemaphoreType.DMA((parts,)), pltpu.SemaphoreType.DMA((3,))],
-        compiler_params=small(12),
+        in_specs=[ANYWHERE] * 3,
+        out_specs=[VMEM] * 3,
+        out_shape=[jax.ShapeDtypeStruct(w.shape, bf16) for w in stored],
+        scratch_shapes=[pltpu.SemaphoreType.DMA((3,))],
+        compiler_params=small(),
         name="load",
-    )(*[off_chip(w) for w in (out_weight, *stored)])
+    )(*[off_chip(w) for w in stored])
 
 
 def order_kernel(at_ref, rows_ref, w0, w1, w2, w3, params_ref, bias_ref):
@@ -391,17 +380,19 @@
     low_ref,
     head_gain_ref,
     state_ref,
-    weight_ref,
+    weight_hbm,
     sent_ref,
     piece_ref,
     updated_hbm,
     updated_ref,
+    weight_ref,
     rows_ref,
     low_rows_ref,
     gain_rows_ref,
     readout_ref,
     gated_ref,
     updated_sem,
+    weight_sem,
 ):
     seqs, heads = state_ref.shape[:2]
     kv_count = arrived_ref.shape[0]
@@ -409,6 +400,16 @@
     share = kv_count // chunks
     parts = sent_ref.shape[0]
     piece_chunks = kv_count // parts
+    step = weight_ref.shape[2]
+    fetches = [
+        pltpu.make_async_copy(
+            weight_hbm.at[:, pl.ds(part * step, step)], weight_ref.at[part], weight_sem.at[part]
+        )
+        for part in range(parts)
+    ]
+    for fetch in fetches:
+        fetch.start()
+
     def block_rows(block):
         lines = arrived_ref[block, :chunks]
         return lines.reshape(seqs * chunks, LANES).astype(f32)
@@ -477,6 +478,7 @@
         gated_ref[0:2, head * HEAD : (head + 1) * HEAD] = gated[2 * head : 2 * head + 2]
     lhs = gated_ref[...].astype(bf16)
     for part in range(parts):
+        fetches[part].wait()
         mixed = jnp.dot(lhs, weight_ref[part], preferred_element_type=f32)
         for chunk in range(piece_chunks):
             sent_ref[part, 2 * chunk : 2 * chunk + 2, :] = mixed[
@@ -486,13 +488,13 @@
         copy.wait()
 
 
-def mixer(at, arrived, params, lower_bound, head_gain, state, weight):
+def mixer(at, arrived, params, lower_bound, head_gain, state, weight, parts):
     seqs, heads = state.shape[:2]
-    parts, _, step = weight.shape
-    rows = 2 * step // LANES
+    depth, width = weight.shape
+    rows = 2 * width // parts // LANES
     return pl.pallas_call(
         mixer_kernel,
-        in_specs=[SMEM] + [VMEM] * 6,
+        in_specs=[SMEM] + [VMEM] * 5 + [ANYWHERE],
         out_specs=[VMEM, VMEM, ANYWHERE],
         out_shape=[
             jax.ShapeDtypeStruct((parts, rows, LANES), f32),
@@ -501,16 +503,18 @@
         ],
         scratch_shapes=[
             pltpu.VMEM(state.shape, f32),
+            pltpu.VMEM((parts, depth, width // parts), bf16),
             pltpu.VMEM((seqs * 4 * heads, LANES), f32),
             pltpu.VMEM((2 * heads, LANES), f32),
             pltpu.VMEM((2 * heads, LANES), f32),
             pltpu.VMEM((2 * heads, LANES), f32),
             pltpu.VMEM((8, heads * HEAD), f32),
             pltpu.SemaphoreType.DMA((seqs * heads,)),
+            pltpu.SemaphoreType.DMA((parts,)),
         ],
         compiler_params=small(),
         name="mixer",
-    )(at, arrived, params, lower_bound, head_gain, state, weight)
+    )(at, arrived, params, lower_bound, head_gain, state, off_chip(weight))
 
 
 def local(
@@ -552,7 +556,7 @@
     chunk_count = 4 * heads
     share = kv_count // chunk_count
     stored = stored_order(gate_weights, up_weights, down_weights)
-    mixer_weight, *stored = load(out_weight, stored, tp_count)
+    stored = load(stored)
     kept, sent, tail, token_sum, block = first_block(at, rows, stored, half)
     params, bias_rows = in_order(at, rows, weights)
     params = params.reshape(kv_count, 8, LANES)
@@ -599,7 +603,8 @@
         lower_bound.reshape(heads, HEAD),
         head_gain.reshape(heads, HEAD),
         state,
-        mixer_weight,
+        out_weight,
+        tp_count,
     )
     arrived, at, tp, norm_gain, norm_bias, params, piece = alone(
         mixer_part, TP, at, tp, norm_gain, norm_bias, params, piece

time: 165 us -> 164 us (level)
  local copies, waits for them, and re-layouts: 5.31 us -> 1.2 us
  waiting for transfers between devices: 11.2 us -> 14.6 us
    unnamed x24 -> x20, local copies, waits for them, and re-layouts: 4.86 us -> 0.76 us
    all_to_all x1, waiting for transfers between devices: 9.8 us -> 13.2 us  [exchange(): return lax.all_to_all(blocks, axes, split_axis=0, concat_axis=0, tiled=True)]
where the time goes in v10:
time: 164 us
  blocking collectives  114 us (70%)
  starting transfers between devices  17.3 us (11%)
  waiting for transfers between devices  14.6 us (9%)
  Pallas kernels  13.3 us (8%)
  other arithmetic  1.76 us (1%)
    all_to_all x8, blocking collectives, exchange(): return lax.all_to_all(blocks, axes, split_axis=0, concat_axis=0, tiled=True)  105 us
    all_to_all x1, starting transfers between devices, exchange(): return lax.all_to_all(blocks, axes, split_axis=0, concat_axis=0, tiled=True)  16.3 us
    all_to_all x1, waiting for transfers between devices, exchange(): return lax.all_to_all(blocks, axes, split_axis=0, concat_axis=0, tiled=True)  13.2 us
    all_gather x1, blocking collectives, local(): arrived = lax.all_gather(arrived, CORE, axis=0)  4.77 us
    all_gather x1, blocking collectives, local(): rows = lax.all_gather(arrived, CORE, axis=0)  4.61 us
    pallas_call x1, Pallas kernels, mixer(): pl.pallas_call(mixer_kernel, in_specs=[SMEM] + [VMEM] * 5 + [ANYWHERE], o...  4.19 us
  transfers between devices with their start and end apart: 3, of which 3 were waited for; matrix products, arithmetic and copies ran while one was open for 0% of the time, Pallas kernels for 2%

profile of v10, /device:TPU:1, one launch (start us, length us, event | category | flops | bytes accessed | tf_op | source)
XLA Modules:
  0.0 163.7 jit_solution(6586213707800937334)
XLA Ops:
  0.6 0.0 copy-start.1
  0.6 0.0 copy-start.2
  0.7 0.1 pad_add_fusion.at_ref
  0.8 2.4 %place.1 = bf16[128,5,2,128]{3,2,1,0:T(2,128)(2,1)} custom-call(s32[3]{0:T(128)S(1)} %pad_add_fusion.at_ref, bf16[16,64]{1,0:T(8,128)(2,1)} %bitcast.88, bf16[3,16]{1,0:T(4,128)(2,1)} %gain_hbm.1, bf16[3,16]{1,0:T(4,128)(2,1)} %bias_hbm.1), custom_call_target="tpu_custom_call" | custom-call | tf_op jit(solution)/shard_map/place/pallas_call | solution.py:107
  3.1 16.3 %all-to-all-start = ((bf16[128,5,2,128]{3,2,1,0:T(2,128)(2,1)}), bf16[128,5,2,128]{3,2,1,0:T(2,128)(2,1)S(1)}, u32[]{:S(2)}, u32[]{:S(2)}) async-start(bf16[128,5,2,128]{3,2,1,0:T(2,128)(2,1)} %place.1), calls=%async_computation | async-start | bytes 655360 | tf_op jit(solution)/shard_map/all_to_all | solution.py:26
  19.5 1.6 load.1
  21.1 13.2 %all-to-all-done = bf16[128,5,2,128]{3,2,1,0:T(2,128)(2,1)S(1)} async-done(((bf16[128,5,2,128]{3,2,1,0:T(2,128)(2,1)}), bf16[128,5,2,128]{3,2,1,0:T(2,128)(2,1)S(1)}, u32[]{:S(2)}, u32[]{:S(2)}) %all-to-all-start) | async-done | bytes 327712 | tf_op jit(solution)/shard_map/all_to_all | solution.py:26
  34.2 4.6 %all-gather = bf16[256,5,2,128]{3,2,1,0:T(2,128)(2,1)S(1)} all-gather(bf16[128,5,2,128]{3,2,1,0:T(2,128)(2,1)S(1)} %all-to-all-done), channel_id=2, replica_groups=mesh['kv_0'=8,'kv_1'=4,'tp_0'=4,'tp_1'=2] {'tp_1'}, dimensions={0}, use_global_device_ids=true | all-gather | bytes 983040 | tf_op jit(solution)/shard_map/all_gather | solution.py:548
  38.9 2.0 %first_block.1 = (bf16[32,32,128]{2,1,0:T(8,128)(2,1)S(1)}, bf16[32,32,128]{2,1,0:T(8,128)(2,1)S(1)}, f32[8,128]{1,0:T(8,128)S(1)}, f32[8,128]{1,0:T(8,128)S(1)}, f32[64,128]{1,0:T(8,128)S(1)}) custom-call(s32[3]{0:T(128)S(1)} %pad_add_fusion.at_ref, bf16[2,32,4,5,2,128]{5,4,3,2,1,0:T(2,128)(2,1)S(1)} %bitcast.66, ...), custom_call_target="tpu_custom_call" | custom-call | tf_op jit(solution)/shard_map/first_block/pallas_call | solution.py:263
  40.8 0.0 copy-start
  40.8 0.0 copy-start.5
  40.8 0.0 copy-start.6
  40.8 0.5 collective-permute-start
  41.3 1.0 in_order.1
  42.3 0.2 collective-permute-done.came_ref
  42.5 0.2 first_blocks.1
  42.7 15.1 %all_to_all.45 = bf16[32,17,2,128]{3,2,1,0:T(2,128)(2,1)S(1)} all-to-all(bf16[32,17,2,128]{3,2,1,0:T(2,128)(2,1)S(1)} %first_blocks.1), channel_id=1, replica_groups=mesh['kv_0'=8,'kv_1'=4,'tp_0'=4,'tp_1'=2] {'kv_0','kv_1'}, dimensions={0} | all-to-all | bytes 557056 | tf_op jit(solution)/shard_map/all_to_all | solution.py:26
  57.7 0.2 convert_reduce_fusion
  58.0 9.4 %all_to_all.46 = bf16[8,34,128]{2,1,0:T(8,128)(2,1)S(1)} all-to-all(bf16[8,34,128]{2,1,0:T(8,128)(2,1)S(1)} %broadcast_in_dim.14), channel_id=1, replica_groups=mesh['kv_0'=8,'kv_1'=4,'tp_0'=4,'tp_1'=2] {'tp_0','tp_1'}, dimensions={0} | all-to-all | bytes 139264 | tf_op jit(solution)/shard_map/all_to_all | solution.py:26
  67.6 0.1 fusion.2
  67.6 0.1 multiply_convert_fusion
  67.7 0.1 convolution_convert_fusion
  67.9 0.1 convolution_convert_fusion.1
  68.0 0.1 convolution_convert_fusion.2
  68.2 0.1 convolution_convert_fusion.3
  68.4 0.3 copy.52
  68.7 0.4 pad_maximum_fusion
  69.2 15.3 %all_to_all.47.arrived_ref = bf16[32,18,2,128]{3,2,1,0:T(2,128)(2,1)S(1)} all-to-all(bf16[32,18,2,128]{3,2,1,0:T(2,128)(2,1)S(1)} %pad_maximum_fusion), channel_id=1, replica_groups=mesh['kv_0'=8,'kv_1'=4,'tp_0'=4,'tp_1'=2] {'kv_0','kv_1'}, dimensions={0} | all-to-all | bytes 589824 | tf_op jit(solution)/shard_map/all_to_all | solution.py:26
  84.5 0.0 copy-done.6
  84.5 4.2 %mixer.1 = (f32[8,8,128]{2,1,0:T(8,128)S(1)}, f32[8,128]{1,0:T(8,128)S(1)}, f32[2,4,128,128]{3,2,1,0:T(8,128)}) custom-call(s32[3]{0:T(128)S(1)} %pad_add_fusion.at_ref, bf16[32,18,2,128]{3,2,1,0:T(2,128)(2,1)S(1)} %all_to_all.47.arrived_ref, f32[32,8,128]{2,1,0:T(8,128)S(1)} %bitcast.70, f32[4,128]{1,0:T(4,128)S(1)} %bitcast.72, f32[4,128]{1,0:T(4,128)S(1)} %bitcast.73, ...), custom_call_target="tpu_custom_call" | custom-call | tf_op jit(solution)/shard_map/mixer/pallas_call | solution.py:495
  88.7 0.0 copy-start.7
  88.7 0.0 copy-start.8
  88.7 9.4 %all_to_all.48 = f32[8,8,128]{2,1,0:T(8,128)S(1)} all-to-all(f32[8,8,128]{2,1,0:T(8,128)S(1)} %get-tuple-element.186), channel_id=1, replica_groups=mesh['kv_0'=8,'kv_1'=4,'tp_0'=4,'tp_1'=2] {'tp_0','tp_1'}, dimensions={0} | all-to-all | bytes 65536 | tf_op jit(solution)/shard_map/all_to_all | solution.py:26
  98.1 19.5 %all_to_all.49 = bf16[128,8,128]{2,1,0:T(8,128)(2,1)S(1)} all-to-all(bf16[128,8,128]{2,1,0:T(8,128)(2,1)S(1)} %broadcast_in_dim.18), channel_id=1, replica_groups=mesh['kv_0'=8,'kv_1'=4,'tp_0'=4,'tp_1'=2] {'kv_0','kv_1','tp_0'}, dimensions={0} | all-to-all | bytes 524288 | tf_op jit(solution)/shard_map/all_to_all | solution.py:26
  117.6 4.8 %all-gather.1 = bf16[256,8,128]{2,1,0:T(8,128)(2,1)S(1)} all-gather(bf16[128,8,128]{2,1,0:T(8,128)(2,1)S(1)} %all_to_all.49), channel_id=3, replica_groups=mesh['kv_0'=8,'kv_1'=4,'tp_0'=4,'tp_1'=2] {'tp_1'}, dimensions={0}, use_global_device_ids=true | all-gather | bytes 786432 | tf_op jit(solution)/shard_map/all_gather | solution.py:616
  122.4 2.1 %second_block.1 = (bf16[32,32,128]{2,1,0:T(8,128)(2,1)S(1)}, bf16[32,32,128]{2,1,0:T(8,128)(2,1)S(1)}, bf16[64,128]{1,0:T(8,128)(2,1)S(1)}) custom-call(s32[3]{0:T(128)S(1)} %pad_add_fusion.at_ref, bf16[2,32,4,8,128]{4,3,2,1,0:T(8,128)(2,1)S(1)} %bitcast.68, f32[32,8,128]{2,1,0:T(8,128)S(1)} %bitcast.71, ...), custom_call_target="tpu_custom_call" | custom-call | tf_op jit(solution)/shard_map/second_block/pallas_call | solution.py:358
  124.5 0.5 collective-permute-start.1
  125.0 1.2 collective-permute-done.1
  126.2 0.1 add_convert_fusion
  126.2 14.8 %all_to_all.50 = bf16[32,32,128]{2,1,0:T(8,128)(2,1)S(1)} all-to-all(bf16[32,32,128]{2,1,0:T(8,128)(2,1)S(1)} %add_convert_fusion), channel_id=1, replica_groups=mesh['kv_0'=8,'kv_1'=4,'tp_0'=4,'tp_1'=2] {'kv_0','kv_1'}, dimensions={0} | all-to-all | bytes 524288 | tf_op jit(solution)/shard_map/all_to_all | solution.py:26
  141.1 9.3 %all_to_all.51 = bf16[8,32,128]{2,1,0:T(8,128)(2,1)S(1)} all-to-all(bf16[8,32,128]{2,1,0:T(8,128)(2,1)S(1)} %broadcast_in_dim.19), channel_id=1, replica_groups=mesh['kv_0'=8,'kv_1'=4,'tp_0'=4,'tp_1'=2] {'tp_0','tp_1'}, dimensions={0} | all-to-all | bytes 131072 | tf_op jit(solution)/shard_map/all_to_all | solution.py:26
  150.4 0.1 fusion.3
  150.5 0.2 multiply_reduce_fusion
  150.7 0.1 pad_maximum_fusion.1
  150.8 11.9 %all_to_all.52 = f32[32,1,128]{2,1,0:T(1,128)S(1)} all-to-all(f32[32,1,128]{2,1,0:T(1,128)S(1)} %broadcast_in_dim.20), channel_id=1, replica_groups=mesh['kv_0'=8,'kv_1'=4,'tp_0'=4,'tp_1'=2] {'kv_0','kv_1'}, dimensions={0} | all-to-all | bytes 32768 | tf_op jit(solution)/shard_map/all_to_all | solution.py:26
  162.8 0.1 multiply_reduce_fusion.1
  162.9 0.1 add_convert_fusion.1
  163.1 0.7 copy.43
  (37 shorter events, 0.5 us)
Async XLA Ops:
  0.6 40.7 %copy-start.1 = (bf16[128,512]{1,0:T(8,128)(2,1)S(1)}, bf16[128,512]{1,0:T(8,128)(2,1)}, u32[]{:S(2)}) copy-start(bf16[128,512]{1,0:T(8,128)(2,1)} %w3.1) | copy-start | bytes 393220
  0.6 40.7 %copy-start.2 = (bf16[128,512]{1,0:T(8,128)(2,1)S(1)}, bf16[128,512]{1,0:T(8,128)(2,1)}, u32[]{:S(2)}) copy-start(bf16[128,512]{1,0:T(8,128)(2,1)} %w2.1) | copy-start | bytes 393220
  0.7 40.7 %copy-start.3 = (bf16[128,512]{1,0:T(8,128)(2,1)S(1)}, bf16[128,512]{1,0:T(8,128)(2,1)}, u32[]{:S(2)}) copy-start(bf16[128,512]{1,0:T(8,128)(2,1)} %w1.1) | copy-start | bytes 393220
  0.7 40.7 %copy-start.4 = (bf16[128,512]{1,0:T(8,128)(2,1)S(1)}, bf16[128,512]{1,0:T(8,128)(2,1)}, u32[]{:S(2)}) copy-start(bf16[128,512]{1,0:T(8,128)(2,1)} %w0.1) | copy-start | bytes 393220
  3.1 31.1 %all-to-all-start = ((bf16[128,5,2,128]{3,2,1,0:T(2,128)(2,1)}), bf16[128,5,2,128]{3,2,1,0:T(2,128)(2,1)S(1)}, u32[]{:S(2)}, u32[]{:S(2)}) async-start(bf16[128,5,2,128]{3,2,1,0:T(2,128)(2,1)} %place.1), calls=%async_computation | async-start | bytes 655360 | tf_op jit(solution)/shard_map/all_to_all | solution.py:26
  40.8 43.6 %copy-start = (f32[2,4,128,128]{3,2,1,0:T(8,128)S(1)}, f32[2,4,128,128]{3,2,1,0:T(8,128)}, u32[]{:S(2)}) copy-start(f32[2,4,128,128]{3,2,1,0:T(8,128)} %state_ref.1) | copy-start | bytes 1572868
  40.8 43.6 %copy-start.5 = (f32[512]{0:T(512)S(1)}, f32[512]{0:T(512)}, u32[]{:S(2)}) copy-start(f32[512]{0:T(512)} %param.24) | copy-start | bytes 6148
  40.8 43.6 %copy-start.6 = (f32[512]{0:T(512)S(1)}, f32[512]{0:T(512)}, u32[]{:S(2)}) copy-start(f32[512]{0:T(512)} %param.25) | copy-start | bytes 6148
  40.8 1.6 collective-permute-start
  88.7 74.3 %copy-start.7 = (bf16[3,16]{1,0:T(4,128)(2,1)S(1)}, bf16[3,16]{1,0:T(4,128)(2,1)}, u32[]{:S(2)}) copy-start(bf16[3,16]{1,0:T(4,128)(2,1)} %gain_hbm.1) | copy-start | bytes 292
  88.7 74.2 %copy-start.8 = (bf16[3,16]{1,0:T(4,128)(2,1)S(1)}, bf16[3,16]{1,0:T(4,128)(2,1)}, u32[]{:S(2)}) copy-start(bf16[3,16]{1,0:T(4,128)(2,1)} %bias_hbm.1) | copy-start | bytes 292
  124.5 1.6 collective-permute-start.1

commit v11 on v10

--- a/solution.py
+++ b/solution.py
@@ -277,6 +277,60 @@
     )(at, rows, *stored)
 
 
+def project_kernel(
+    at_ref, parts_ref, block_ref, total_ref, params_ref, own_ref, w0, w1, w2, w3, result_ref, line_ref
+):
+    members, lines, _ = parts_ref.shape
+    half = lines - 2
+    batch = 2 * half
+    kv_count = params_ref.shape[0]
+    width = kv_count * LANES
+    stride = line_ref.shape[0] // half
+    sums = jnp.zeros((2, LANES), f32)
+    halves = [jnp.zeros((half, LANES), f32) for _ in range(2)]
+    for member in range(members):
+        part = parts_ref[member].astype(f32)
+        halves[member % 2] = halves[member % 2] + part[:half]
+        sums = sums + part[half:]
+    row = lax.broadcasted_iota(jnp.int32, (batch, LANES), 0)
+    lane = lax.broadcasted_iota(jnp.int32, (batch, LANES), 1)
+    tokens = jnp.where(lane[:1] < batch, total_ref[0:1, :], 0.0)
+    line = (residual_scale * tokens + 0.5 * sums[0:1]) / width
+    mean = jnp.sum(jnp.where(lane % batch == row, line, 0.0), axis=1, keepdims=True)
+    centred = residual_scale * block_ref[...] + 0.5 * jnp.concatenate(halves) - mean
+    scaled = (centred * params_ref[at_ref[0], 0:1, :]).astype(bf16)
+
+    def put(pair, rows):
+        for seq in range(2):
+            at = slice(seq * half, (seq + 1) * half)
+            line_ref[pl.ds(2 * pair + seq, half, stride=stride), :] = rows[at]
+
+    pair = 0
+    for w_ref in (w0, w1, w2, w3):
+        projected = jnp.dot(scaled, w_ref[...], preferred_element_type=f32)
+        for head in range(projected.shape[1] // LANES):
+            put(pair, projected[:, head * LANES : (head + 1) * LANES])
+            pair += 1
+    put(pair, centred)
+    own = own_ref[...].astype(f32)[half + 1 : half + 2] * (pair / kv_count)
+    put(pair + 1, jnp.broadcast_to(own, (batch, LANES)))
+    result_ref[...] = line_ref[...].astype(bf16).reshape(result_ref.shape)
+
+
+def project(at, parts, block, total, params, own, weights):
+    half = parts.shape[1] - 2
+    stride = 2 * (4 * weights[0].shape[1] // LANES + 2)
+    return pl.pallas_call(
+        project_kernel,
+        in_specs=[SMEM] + [VMEM] * 9,
+        out_specs=VMEM,
+        out_shape=jax.ShapeDtypeStruct((half * stride // 2, 2, LANES), bf16),
+        scratch_shapes=[pltpu.VMEM((half * stride, LANES), f32)],
+        compiler_params=small(),
+        name="project",
+    )(at, parts, block, total, params, own, *weights)
+
+
 def blocks_kernel(kept_ref, came_ref, tail_ref, bias_ref, result_ref):
     chunks, half, _ = kept_ref.shape
     share = chunks // bias_ref.shape[0]
@@ -407,7 +461,7 @@
         )
         for part in range(parts)
     ]
-    for fetch in fetches:
+    for fetch in fetches[: parts // 2]:
         fetch.start()
 
     def block_rows(block):
@@ -452,6 +506,8 @@
     forget = (low + (1.0 - low) * jax.nn.sigmoid(forget_pre)).T
     key = ((1.0 - low) * jax.nn.sigmoid(-forget_pre)).T
     query = jax.nn.silu(query_pre).T
+    for fetch in fetches[parts // 2 :]:
+        fetch.start()
     updated_copies = []
     for head in range(heads):
         for seq in range(seqs):
@@ -553,8 +609,6 @@
         return gathered.reshape(x_count, 2, *lines.shape), *held
 
     weights = (query_weight, forget_weight, input_weight, outgate_weight)
-    chunk_count = 4 * heads
-    share = kv_count // chunk_count
     stored = stored_order(gate_weights, up_weights, down_weights)
     stored = load(stored)
     kept, sent, tail, token_sum, block = first_block(at, rows, stored, half)
@@ -565,34 +619,22 @@
         blocks, KV, at, kv, tp, norm_gain, norm_bias, block, params, token_sum
     )
     arrived = wide_sum(arrived).reshape(half + 2, LANES).astype(bf16)
-    gathered, at, kv, tp, norm_gain, norm_bias, block, params, token_sum, arrived = over_tp(
-        arrived, at, kv, tp, norm_gain, norm_bias, block, params, token_sum, arrived
-    )
-    gathered = gathered.astype(f32)
-    bias_own = arrived[half + 1 : half + 2] / share
-    gain_one = lax.dynamic_index_in_dim(params, kv, 0, keepdims=False)[:1]
-    total = gathered[:, :, :half].sum(axis=0).reshape(batch, LANES)
-    total_row = gathered[:, :, half].sum(axis=(0, 1))
-    stream_one = residual_scale * block + 0.5 * total
-    row_mean = (
-        residual_scale * token_sum[0, :batch]
-        + 0.5 * (total_row[:batch] + total_row[batch:])
-    ) / width
-    centred = stream_one - row_mean[:, None]
-
-    scaled = (centred * gain_one.astype(f32)).astype(bf16)
-    projected = jnp.concatenate(
-        [jnp.dot(scaled, w, preferred_element_type=f32) for w in weights], axis=1
-    ).astype(bf16)
-    projected = projected.reshape(2, half, chunk_count, LANES).transpose(1, 2, 0, 3)
-    blocks = jnp.concatenate(
-        [
-            projected,
-            centred.astype(bf16).reshape(2, half, LANES).swapaxes(0, 1)[:, None],
-            jnp.broadcast_to(bias_own.astype(bf16)[None, None], (kv_count, 1, 2, LANES)),
-        ],
-        axis=1,
-    )
+    gathered, at, kv, tp, norm_gain, norm_bias, block, params, token_sum, arrived = alone(
+        copies(arrived, tp_count),
+        TP,
+        at,
+        kv,
+        tp,
+        norm_gain,
+        norm_bias,
+        block,
+        params,
+        token_sum,
+        arrived,
+    )
+
+    blocks = project(at, gathered, block, token_sum, params, arrived, weights)
+    blocks = blocks.reshape(kv_count, -1, 2, LANES)
     arrived, at, kv, tp, norm_gain, norm_bias, params = alone(
         blocks, KV, at, kv, tp, norm_gain, norm_bias, params
     )

time: 164 us -> 164 us (level)
  no operation moved by 1% of the time
where the time goes in v11:
time: 164 us; the launch traced here: 163 us
  blocking collectives  114 us (70%)
  starting transfers between devices  17.7 us (11%)
  Pallas kernels  14.3 us (9%)
  waiting for transfers between devices  14.2 us (9%)
    all_to_all x8, blocking collectives, exchange(): return lax.all_to_all(blocks, axes, split_axis=0, concat_axis=0, tiled=True)  105 us
    all_to_all x1, starting transfers between devices, exchange(): return lax.all_to_all(blocks, axes, split_axis=0, concat_axis=0, tiled=True)  16.8 us
    all_to_all x1, waiting for transfers between devices, exchange(): return lax.all_to_all(blocks, axes, split_axis=0, concat_axis=0, tiled=True)  12.8 us
    all_gather x1, blocking collectives, local(): rows = lax.all_gather(arrived, CORE, axis=0)  4.83 us
    all_gather x1, blocking collectives, local(): arrived = lax.all_gather(arrived, CORE, axis=0)  4.59 us
    pallas_call x1, Pallas kernels, mixer(): pl.pallas_call(mixer_kernel, in_specs=[SMEM] + [VMEM] * 5 + [ANYWHERE], o...  4.19 us
  transfers between devices with their start and end apart: 3, of which 3 were waited for; matrix products, arithmetic and copies ran while one was open for 0% of the time, Pallas kernels for 2%

profile of v11, /device:TPU:1, one launch (start us, length us, event | category | flops | bytes accessed | tf_op | source)
XLA Modules:
  0.0 163.1 jit_solution(9496071236623564904)
XLA Ops:
  0.6 0.0 copy-start.4
  0.6 0.0 copy-start.3
  0.7 0.0 copy-start.2
  0.7 0.0 copy-start.1
  0.7 0.1 pad_add_fusion.at_ref
  0.8 2.4 %place.1 = bf16[128,5,2,128]{3,2,1,0:T(2,128)(2,1)} custom-call(s32[3]{0:T(128)S(1)} %pad_add_fusion.at_ref, bf16[16,64]{1,0:T(8,128)(2,1)} %bitcast.46, bf16[3,16]{1,0:T(4,128)(2,1)} %gain_hbm.1, bf16[3,16]{1,0:T(4,128)(2,1)} %bias_hbm.1), custom_call_target="tpu_custom_call" | custom-call | tf_op jit(solution)/shard_map/place/pallas_call | solution.py:107
  3.1 16.8 %all-to-all-start = ((bf16[128,5,2,128]{3,2,1,0:T(2,128)(2,1)}), bf16[128,5,2,128]{3,2,1,0:T(2,128)(2,1)}, u32[]{:S(2)}, u32[]{:S(2)}) async-start(bf16[128,5,2,128]{3,2,1,0:T(2,128)(2,1)} %place.1), calls=%async_computation | async-start | bytes 655360 | tf_op jit(solution)/shard_map/all_to_all | solution.py:26
  19.9 1.6 load.1
  21.5 0.0 copy-start
  21.5 0.0 copy-start.5
  21.5 0.0 copy-start.6
  21.6 12.8 %all-to-all-done = bf16[128,5,2,128]{3,2,1,0:T(2,128)(2,1)} async-done(((bf16[128,5,2,128]{3,2,1,0:T(2,128)(2,1)}), bf16[128,5,2,128]{3,2,1,0:T(2,128)(2,1)}, u32[]{:S(2)}, u32[]{:S(2)}) %all-to-all-start) | async-done | bytes 327712 | tf_op jit(solution)/shard_map/all_to_all | solution.py:26
  34.3 4.8 %all-gather = bf16[256,5,2,128]{3,2,1,0:T(2,128)(2,1)S(1)} all-gather(bf16[128,5,2,128]{3,2,1,0:T(2,128)(2,1)} %all-to-all-done), channel_id=2, replica_groups=mesh['kv_0'=8,'kv_1'=4,'tp_0'=4,'tp_1'=2] {'tp_1'}, dimensions={0}, use_global_device_ids=true | all-gather | bytes 983040 | tf_op jit(solution)/shard_map/all_gather | solution.py:604
  39.2 2.0 %first_block.1 = (bf16[32,32,128]{2,1,0:T(8,128)(2,1)S(1)}, bf16[32,32,128]{2,1,0:T(8,128)(2,1)S(1)}, f32[8,128]{1,0:T(8,128)S(1)}, f32[8,128]{1,0:T(8,128)S(1)}, f32[64,128]{1,0:T(8,128)S(1)}) custom-call(s32[3]{0:T(128)S(1)} %pad_add_fusion.at_ref, bf16[2,32,4,5,2,128]{5,4,3,2,1,0:T(2,128)(2,1)S(1)} %bitcast.29, ...), custom_call_target="tpu_custom_call" | custom-call | tf_op jit(solution)/shard_map/first_block/pallas_call | solution.py:263
  41.1 0.5 collective-permute-start
  41.6 0.0 copy-done.4
  41.6 0.0 copy-done.3
  41.6 0.0 copy-done.2
  41.6 0.0 copy-done.1
  41.6 1.0 in_order.1
  42.6 0.2 collective-permute-done.came_ref
  42.8 0.2 first_blocks.1
  42.9 15.1 %all_to_all.45 = bf16[32,17,2,128]{3,2,1,0:T(2,128)(2,1)S(1)} all-to-all(bf16[32,17,2,128]{3,2,1,0:T(2,128)(2,1)S(1)} %first_blocks.1), channel_id=1, replica_groups=mesh['kv_0'=8,'kv_1'=4,'tp_0'=4,'tp_1'=2] {'kv_0','kv_1'}, dimensions={0} | all-to-all | bytes 557056 | tf_op jit(solution)/shard_map/all_to_all | solution.py:26
  58.0 0.2 convert_reduce_fusion
  58.3 9.4 %all_to_all.46.parts_ref = bf16[8,34,128]{2,1,0:T(8,128)(2,1)S(1)} all-to-all(bf16[8,34,128]{2,1,0:T(8,128)(2,1)S(1)} %broadcast_in_dim.8), channel_id=1, replica_groups=mesh['kv_0'=8,'kv_1'=4,'tp_0'=4,'tp_1'=2] {'tp_0','tp_1'}, dimensions={0} | all-to-all | bytes 139264 | tf_op jit(solution)/shard_map/all_to_all | solution.py:26
  67.7 1.0 project.1
  68.7 15.3 %all_to_all.47.arrived_ref = bf16[32,18,2,128]{3,2,1,0:T(2,128)(2,1)S(1)} all-to-all(bf16[32,18,2,128]{3,2,1,0:T(2,128)(2,1)S(1)} %bitcast.32), channel_id=1, replica_groups=mesh['kv_0'=8,'kv_1'=4,'tp_0'=4,'tp_1'=2] {'kv_0','kv_1'}, dimensions={0} | all-to-all | bytes 589824 | tf_op jit(solution)/shard_map/all_to_all | solution.py:26
  84.0 0.0 copy-done
  84.0 0.0 copy-done.5
  84.0 4.2 %mixer.1 = (f32[8,8,128]{2,1,0:T(8,128)S(1)}, f32[8,128]{1,0:T(8,128)S(1)}, f32[2,4,128,128]{3,2,1,0:T(8,128)}) custom-call(s32[3]{0:T(128)S(1)} %pad_add_fusion.at_ref, bf16[32,18,2,128]{3,2,1,0:T(2,128)(2,1)S(1)} %all_to_all.47.arrived_ref, f32[32,8,128]{2,1,0:T(8,128)S(1)} %bitcast.34, f32[4,128]{1,0:T(4,128)S(1)} %bitcast.36, f32[4,128]{1,0:T(4,128)S(1)} %bitcast.37, ...), custom_call_target="tpu_custom_call" | custom-call | tf_op jit(solution)/shard_map/mixer/pallas_call | solution.py:551
  88.2 0.0 copy-start.7
  88.2 0.0 copy-start.8
  88.2 9.4 %all_to_all.48 = f32[8,8,128]{2,1,0:T(8,128)S(1)} all-to-all(f32[8,8,128]{2,1,0:T(8,128)S(1)} %get-tuple-element.178), channel_id=1, replica_groups=mesh['kv_0'=8,'kv_1'=4,'tp_0'=4,'tp_1'=2] {'tp_0','tp_1'}, dimensions={0} | all-to-all | bytes 65536 | tf_op jit(solution)/shard_map/all_to_all | solution.py:26
  97.7 19.5 %all_to_all.49 = bf16[128,8,128]{2,1,0:T(8,128)(2,1)S(1)} all-to-all(bf16[128,8,128]{2,1,0:T(8,128)(2,1)S(1)} %broadcast_in_dim.9), channel_id=1, replica_groups=mesh['kv_0'=8,'kv_1'=4,'tp_0'=4,'tp_1'=2] {'kv_0','kv_1','tp_0'}, dimensions={0} | all-to-all | bytes 524288 | tf_op jit(solution)/shard_map/all_to_all | solution.py:26
  117.1 4.6 %all-gather.1 = bf16[256,8,128]{2,1,0:T(8,128)(2,1)S(1)} all-gather(bf16[128,8,128]{2,1,0:T(8,128)(2,1)S(1)} %all_to_all.49), channel_id=3, replica_groups=mesh['kv_0'=8,'kv_1'=4,'tp_0'=4,'tp_1'=2] {'tp_1'}, dimensions={0}, use_global_device_ids=true | all-gather | bytes 786432 | tf_op jit(solution)/shard_map/all_gather | solution.py:658
  121.7 2.1 %second_block.1 = (bf16[32,32,128]{2,1,0:T(8,128)(2,1)S(1)}, bf16[32,32,128]{2,1,0:T(8,128)(2,1)S(1)}, bf16[64,128]{1,0:T(8,128)(2,1)S(1)}) custom-call(s32[3]{0:T(128)S(1)} %pad_add_fusion.at_ref, bf16[2,32,4,8,128]{4,3,2,1,0:T(8,128)(2,1)S(1)} %bitcast.31, f32[32,8,128]{2,1,0:T(8,128)S(1)} %bitcast.35, ...), custom_call_target="tpu_custom_call" | custom-call | tf_op jit(solution)/shard_map/second_block/pallas_call | solution.py:412
  123.9 0.5 collective-permute-start.1
  124.3 1.2 collective-permute-done.1
  125.5 0.1 add_convert_fusion
  125.6 14.8 %all_to_all.50 = bf16[32,32,128]{2,1,0:T(8,128)(2,1)S(1)} all-to-all(bf16[32,32,128]{2,1,0:T(8,128)(2,1)S(1)} %add_convert_fusion), channel_id=1, replica_groups=mesh['kv_0'=8,'kv_1'=4,'tp_0'=4,'tp_1'=2] {'kv_0','kv_1'}, dimensions={0} | all-to-all | bytes 524288 | tf_op jit(solution)/shard_map/all_to_all | solution.py:26
  140.4 9.3 %all_to_all.51 = bf16[8,32,128]{2,1,0:T(8,128)(2,1)S(1)} all-to-all(bf16[8,32,128]{2,1,0:T(8,128)(2,1)S(1)} %broadcast_in_dim.10), channel_id=1, replica_groups=mesh['kv_0'=8,'kv_1'=4,'tp_0'=4,'tp_1'=2] {'tp_0','tp_1'}, dimensions={0} | all-to-all | bytes 131072 | tf_op jit(solution)/shard_map/all_to_all | solution.py:26
  149.8 0.1 fusion
  149.9 0.2 multiply_reduce_fusion
  150.1 0.1 pad_maximum_fusion
  150.2 11.9 %all_to_all.52 = f32[32,1,128]{2,1,0:T(1,128)S(1)} all-to-all(f32[32,1,128]{2,1,0:T(1,128)S(1)} %broadcast_in_dim.11), channel_id=1, replica_groups=mesh['kv_0'=8,'kv_1'=4,'tp_0'=4,'tp_1'=2] {'kv_0','kv_1'}, dimensions={0} | all-to-all | bytes 32768 | tf_op jit(solution)/shard_map/all_to_all | solution.py:26
  162.2 0.1 multiply_reduce_fusion.1
  162.3 0.1 add_convert_fusion.1
  162.4 0.7 copy.24
  (19 shorter events, 0.3 us)
Async XLA Ops:
  0.6 41.0 %copy-start.4 = (bf16[128,512]{1,0:T(8,128)(2,1)S(1)}, bf16[128,512]{1,0:T(8,128)(2,1)}, u32[]{:S(2)}) copy-start(bf16[128,512]{1,0:T(8,128)(2,1)} %w3.3) | copy-start | bytes 393220
  0.6 41.0 %copy-start.3 = (bf16[128,512]{1,0:T(8,128)(2,1)S(1)}, bf16[128,512]{1,0:T(8,128)(2,1)}, u32[]{:S(2)}) copy-start(bf16[128,512]{1,0:T(8,128)(2,1)} %w2.3) | copy-start | bytes 393220
  0.7 40.9 %copy-start.2 = (bf16[128,512]{1,0:T(8,128)(2,1)S(1)}, bf16[128,512]{1,0:T(8,128)(2,1)}, u32[]{:S(2)}) copy-start(bf16[128,512]{1,0:T(8,128)(2,1)} %w1.3) | copy-start | bytes 393220
  0.7 40.9 %copy-start.1 = (bf16[128,512]{1,0:T(8,128)(2,1)S(1)}, bf16[128,512]{1,0:T(8,128)(2,1)}, u32[]{:S(2)}) copy-start(bf16[128,512]{1,0:T(8,128)(2,1)} %w0.3) | copy-start | bytes 393220
  3.1 31.2 %all-to-all-start = ((bf16[128,5,2,128]{3,2,1,0:T(2,128)(2,1)}), bf16[128,5,2,128]{3,2,1,0:T(2,128)(2,1)}, u32[]{:S(2)}, u32[]{:S(2)}) async-start(bf16[128,5,2,128]{3,2,1,0:T(2,128)(2,1)} %place.1), calls=%async_computation | async-start | bytes 655360 | tf_op jit(solution)/shard_map/all_to_all | solution.py:26
  21.5 62.5 %copy-start = (f32[2,4,128,128]{3,2,1,0:T(8,128)S(1)}, f32[2,4,128,128]{3,2,1,0:T(8,128)}, u32[]{:S(2)}) copy-start(f32[2,4,128,128]{3,2,1,0:T(8,128)} %state_ref.1) | copy-start | bytes 1572868
  21.5 62.4 %copy-start.5 = (f32[512]{0:T(512)S(1)}, f32[512]{0:T(512)}, u32[]{:S(2)}) copy-start(f32[512]{0:T(512)} %param.24) | copy-start | bytes 6148
  21.5 62.4 %copy-start.6 = (f32[512]{0:T(512)S(1)}, f32[512]{0:T(512)}, u32[]{:S(2)}) copy-start(f32[512]{0:T(512)} %param.25) | copy-start | bytes 6148
  41.1 1.6 collective-permute-start
  88.2 74.1 %copy-start.7 = (bf16[3,16]{1,0:T(4,128)(2,1)S(1)}, bf16[3,16]{1,0:T(4,128)(2,1)}, u32[]{:S(2)}) copy-start(bf16[3,16]{1,0:T(4,128)(2,1)} %gain_hbm.1) | copy-start | bytes 292
  88.2 74.1 %copy-start.8 = (bf16[3,16]{1,0:T(4,128)(2,1)S(1)}, bf16[3,16]{1,0:T(4,128)(2,1)}, u32[]{:S(2)}) copy-start(bf16[3,16]{1,0:T(4,128)(2,1)} %bias_hbm.1) | copy-start | bytes 292
  123.9 1.6 %collective-permute-start.1 = (bf16[32,32,128]{2,1,0:T(8,128)(2,1)S(1)}, bf16[32,32,128]{2,1,0:T(8,128)(2,1)S(1)}, u32[]{:S(2)}, u32[]{:S(2)}) collective-permute-start(bf16[32,32,128]{2,1,0:T(8,128)(2,1)S(1)} %get-tuple-element.202), channel_id=1, source_target_pairs={{0,1},{1,0},{2,3},{3,2},{4,5},{5,4},{6,7},{7,6},{8,9},{9,8},{10,11... | collective-permute-start | bytes 786440 | tf_op jit(solution)/shard_map/ppermute | solution.py:662

commit v12 on v11

--- a/solution.py
+++ b/solution.py
@@ -534,7 +534,9 @@
         gated_ref[0:2, head * HEAD : (head + 1) * HEAD] = gated[2 * head : 2 * head + 2]
     lhs = gated_ref[...].astype(bf16)
     for part in range(parts):
-        fetches[part].wait()
+        if part % (parts // 2) == 0:
+            for fetch in fetches[part : part + parts // 2]:
+                fetch.wait()
         mixed = jnp.dot(lhs, weight_ref[part], preferred_element_type=f32)
         for chunk in range(piece_chunks):
             sent_ref[part, 2 * chunk : 2 * chunk + 2, :] = mixed[

time: 164 us -> 164 us (level)
  no operation moved by 1% of the time
where the time goes in v12:
time: 164 us; the launch traced here: 163 us
  blocking collectives  114 us (70%)
  starting transfers between devices  17.7 us (11%)
  Pallas kernels  14.4 us (9%)
  waiting for transfers between devices  14.2 us (9%)
    all_to_all x8, blocking collectives, exchange(): return lax.all_to_all(blocks, axes, split_axis=0, concat_axis=0, tiled=True)  105 us
    all_to_all x1, starting transfers between devices, exchange(): return lax.all_to_all(blocks, axes, split_axis=0, concat_axis=0, tiled=True)  16.8 us
    all_to_all x1, waiting for transfers between devices, exchange(): return lax.all_to_all(blocks, axes, split_axis=0, concat_axis=0, tiled=True)  12.8 us
    all_gather x1, blocking collectives, local(): rows = lax.all_gather(arrived, CORE, axis=0)  4.83 us
    all_gather x1, blocking collectives, local(): arrived = lax.all_gather(arrived, CORE, axis=0)  4.59 us
    pallas_call x1, Pallas kernels, mixer(): pl.pallas_call(mixer_kernel, in_specs=[SMEM] + [VMEM] * 5 + [ANYWHERE], o...  4.23 us
  transfers between devices with their start and end apart: 3, of which 3 were waited for; matrix products, arithmetic and copies ran while one was open for 0% of the time, Pallas kernels for 2%

profile of v12, /device:TPU:1, one launch (start us, length us, event | category | flops | bytes accessed | tf_op | source)
XLA Modules:
  0.0 163.1 jit_solution(4274816768855855497)
XLA Ops:
  0.6 0.0 copy-start.4
  0.6 0.0 copy-start.3
  0.7 0.0 copy-start.2
  0.7 0.0 copy-start.1
  0.7 0.1 pad_add_fusion.at_ref
  0.8 2.4 %place.1 = bf16[128,5,2,128]{3,2,1,0:T(2,128)(2,1)} custom-call(s32[3]{0:T(128)S(1)} %pad_add_fusion.at_ref, bf16[16,64]{1,0:T(8,128)(2,1)} %bitcast.46, bf16[3,16]{1,0:T(4,128)(2,1)} %gain_hbm.1, bf16[3,16]{1,0:T(4,128)(2,1)} %bias_hbm.1), custom_call_target="tpu_custom_call" | custom-call | tf_op jit(solution)/shard_map/place/pallas_call | solution.py:107
  3.1 16.8 %all-to-all-start = ((bf16[128,5,2,128]{3,2,1,0:T(2,128)(2,1)}), bf16[128,5,2,128]{3,2,1,0:T(2,128)(2,1)}, u32[]{:S(2)}, u32[]{:S(2)}) async-start(bf16[128,5,2,128]{3,2,1,0:T(2,128)(2,1)} %place.1), calls=%async_computation | async-start | bytes 655360 | tf_op jit(solution)/shard_map/all_to_all | solution.py:26
  19.9 1.6 load.1
  21.5 0.0 copy-start
  21.5 0.0 copy-start.5
  21.5 0.0 copy-start.6
  21.6 12.8 %all-to-all-done = bf16[128,5,2,128]{3,2,1,0:T(2,128)(2,1)} async-done(((bf16[128,5,2,128]{3,2,1,0:T(2,128)(2,1)}), bf16[128,5,2,128]{3,2,1,0:T(2,128)(2,1)}, u32[]{:S(2)}, u32[]{:S(2)}) %all-to-all-start) | async-done | bytes 327712 | tf_op jit(solution)/shard_map/all_to_all | solution.py:26
  34.3 4.8 %all-gather = bf16[256,5,2,128]{3,2,1,0:T(2,128)(2,1)S(1)} all-gather(bf16[128,5,2,128]{3,2,1,0:T(2,128)(2,1)} %all-to-all-done), channel_id=2, replica_groups=mesh['kv_0'=8,'kv_1'=4,'tp_0'=4,'tp_1'=2] {'tp_1'}, dimensions={0}, use_global_device_ids=true | all-gather | bytes 983040 | tf_op jit(solution)/shard_map/all_gather | solution.py:606
  39.2 2.0 %first_block.1 = (bf16[32,32,128]{2,1,0:T(8,128)(2,1)S(1)}, bf16[32,32,128]{2,1,0:T(8,128)(2,1)S(1)}, f32[8,128]{1,0:T(8,128)S(1)}, f32[8,128]{1,0:T(8,128)S(1)}, f32[64,128]{1,0:T(8,128)S(1)}) custom-call(s32[3]{0:T(128)S(1)} %pad_add_fusion.at_ref, bf16[2,32,4,5,2,128]{5,4,3,2,1,0:T(2,128)(2,1)S(1)} %bitcast.29, ...), custom_call_target="tpu_custom_call" | custom-call | tf_op jit(solution)/shard_map/first_block/pallas_call | solution.py:263
  41.1 0.5 collective-permute-start
  41.6 0.0 copy-done.4
  41.6 0.0 copy-done.3
  41.6 0.0 copy-done.2
  41.6 0.0 copy-done.1
  41.6 1.0 in_order.1
  42.6 0.2 collective-permute-done.came_ref
  42.8 0.2 first_blocks.1
  42.9 15.1 %all_to_all.45 = bf16[32,17,2,128]{3,2,1,0:T(2,128)(2,1)S(1)} all-to-all(bf16[32,17,2,128]{3,2,1,0:T(2,128)(2,1)S(1)} %first_blocks.1), channel_id=1, replica_groups=mesh['kv_0'=8,'kv_1'=4,'tp_0'=4,'tp_1'=2] {'kv_0','kv_1'}, dimensions={0} | all-to-all | bytes 557056 | tf_op jit(solution)/shard_map/all_to_all | solution.py:26
  58.0 0.2 convert_reduce_fusion
  58.3 9.4 %all_to_all.46.parts_ref = bf16[8,34,128]{2,1,0:T(8,128)(2,1)S(1)} all-to-all(bf16[8,34,128]{2,1,0:T(8,128)(2,1)S(1)} %broadcast_in_dim.8), channel_id=1, replica_groups=mesh['kv_0'=8,'kv_1'=4,'tp_0'=4,'tp_1'=2] {'tp_0','tp_1'}, dimensions={0} | all-to-all | bytes 139264 | tf_op jit(solution)/shard_map/all_to_all | solution.py:26
  67.7 1.0 project.1
  68.7 15.3 %all_to_all.47.arrived_ref = bf16[32,18,2,128]{3,2,1,0:T(2,128)(2,1)S(1)} all-to-all(bf16[32,18,2,128]{3,2,1,0:T(2,128)(2,1)S(1)} %bitcast.32), channel_id=1, replica_groups=mesh['kv_0'=8,'kv_1'=4,'tp_0'=4,'tp_1'=2] {'kv_0','kv_1'}, dimensions={0} | all-to-all | bytes 589824 | tf_op jit(solution)/shard_map/all_to_all | solution.py:26
  84.0 0.0 copy-done.5
  84.0 4.2 %mixer.1 = (f32[8,8,128]{2,1,0:T(8,128)S(1)}, f32[8,128]{1,0:T(8,128)S(1)}, f32[2,4,128,128]{3,2,1,0:T(8,128)}) custom-call(s32[3]{0:T(128)S(1)} %pad_add_fusion.at_ref, bf16[32,18,2,128]{3,2,1,0:T(2,128)(2,1)S(1)} %all_to_all.47.arrived_ref, f32[32,8,128]{2,1,0:T(8,128)S(1)} %bitcast.34, f32[4,128]{1,0:T(4,128)S(1)} %bitcast.36, f32[4,128]{1,0:T(4,128)S(1)} %bitcast.37, ...), custom_call_target="tpu_custom_call" | custom-call | tf_op jit(solution)/shard_map/mixer/pallas_call | solution.py:553
  88.2 0.0 copy-start.7
  88.2 0.0 copy-start.8
  88.2 9.4 %all_to_all.48 = f32[8,8,128]{2,1,0:T(8,128)S(1)} all-to-all(f32[8,8,128]{2,1,0:T(8,128)S(1)} %get-tuple-element.178), channel_id=1, replica_groups=mesh['kv_0'=8,'kv_1'=4,'tp_0'=4,'tp_1'=2] {'tp_0','tp_1'}, dimensions={0} | all-to-all | bytes 65536 | tf_op jit(solution)/shard_map/all_to_all | solution.py:26
  97.7 19.5 %all_to_all.49 = bf16[128,8,128]{2,1,0:T(8,128)(2,1)S(1)} all-to-all(bf16[128,8,128]{2,1,0:T(8,128)(2,1)S(1)} %broadcast_in_dim.9), channel_id=1, replica_groups=mesh['kv_0'=8,'kv_1'=4,'tp_0'=4,'tp_1'=2] {'kv_0','kv_1','tp_0'}, dimensions={0} | all-to-all | bytes 524288 | tf_op jit(solution)/shard_map/all_to_all | solution.py:26
  117.2 4.6 %all-gather.1 = bf16[256,8,128]{2,1,0:T(8,128)(2,1)S(1)} all-gather(bf16[128,8,128]{2,1,0:T(8,128)(2,1)S(1)} %all_to_all.49), channel_id=3, replica_groups=mesh['kv_0'=8,'kv_1'=4,'tp_0'=4,'tp_1'=2] {'tp_1'}, dimensions={0}, use_global_device_ids=true | all-gather | bytes 786432 | tf_op jit(solution)/shard_map/all_gather | solution.py:660
  121.8 2.1 %second_block.1 = (bf16[32,32,128]{2,1,0:T(8,128)(2,1)S(1)}, bf16[32,32,128]{2,1,0:T(8,128)(2,1)S(1)}, bf16[64,128]{1,0:T(8,128)(2,1)S(1)}) custom-call(s32[3]{0:T(128)S(1)} %pad_add_fusion.at_ref, bf16[2,32,4,8,128]{4,3,2,1,0:T(8,128)(2,1)S(1)} %bitcast.31, f32[32,8,128]{2,1,0:T(8,128)S(1)} %bitcast.35, ...), custom_call_target="tpu_custom_call" | custom-call | tf_op jit(solution)/shard_map/second_block/pallas_call | solution.py:412
  123.9 0.4 collective-permute-start.1
  124.4 1.2 collective-permute-done.1
  125.5 0.1 add_convert_fusion
  125.6 14.8 %all_to_all.50 = bf16[32,32,128]{2,1,0:T(8,128)(2,1)S(1)} all-to-all(bf16[32,32,128]{2,1,0:T(8,128)(2,1)S(1)} %add_convert_fusion), channel_id=1, replica_groups=mesh['kv_0'=8,'kv_1'=4,'tp_0'=4,'tp_1'=2] {'kv_0','kv_1'}, dimensions={0} | all-to-all | bytes 524288 | tf_op jit(solution)/shard_map/all_to_all | solution.py:26
  140.5 9.3 %all_to_all.51 = bf16[8,32,128]{2,1,0:T(8,128)(2,1)S(1)} all-to-all(bf16[8,32,128]{2,1,0:T(8,128)(2,1)S(1)} %broadcast_in_dim.10), channel_id=1, replica_groups=mesh['kv_0'=8,'kv_1'=4,'tp_0'=4,'tp_1'=2] {'tp_0','tp_1'}, dimensions={0} | all-to-all | bytes 131072 | tf_op jit(solution)/shard_map/all_to_all | solution.py:26
  149.8 0.1 fusion
  149.9 0.2 multiply_reduce_fusion
  150.1 0.1 pad_maximum_fusion
  150.2 11.9 %all_to_all.52 = f32[32,1,128]{2,1,0:T(1,128)S(1)} all-to-all(f32[32,1,128]{2,1,0:T(1,128)S(1)} %broadcast_in_dim.11), channel_id=1, replica_groups=mesh['kv_0'=8,'kv_1'=4,'tp_0'=4,'tp_1'=2] {'kv_0','kv_1'}, dimensions={0} | all-to-all | bytes 32768 | tf_op jit(solution)/shard_map/all_to_all | solution.py:26
  162.2 0.1 multiply_reduce_fusion.1
  162.3 0.0 copy-done.8
  162.3 0.1 add_convert_fusion.1
  162.5 0.7 copy.24
  (19 shorter events, 0.3 us)
Async XLA Ops:
  0.6 41.0 %copy-start.4 = (bf16[128,512]{1,0:T(8,128)(2,1)S(1)}, bf16[128,512]{1,0:T(8,128)(2,1)}, u32[]{:S(2)}) copy-start(bf16[128,512]{1,0:T(8,128)(2,1)} %w3.3) | copy-start | bytes 393220
  0.6 41.0 %copy-start.3 = (bf16[128,512]{1,0:T(8,128)(2,1)S(1)}, bf16[128,512]{1,0:T(8,128)(2,1)}, u32[]{:S(2)}) copy-start(bf16[128,512]{1,0:T(8,128)(2,1)} %w2.3) | copy-start | bytes 393220
  0.7 40.9 %copy-start.2 = (bf16[128,512]{1,0:T(8,128)(2,1)S(1)}, bf16[128,512]{1,0:T(8,128)(2,1)}, u32[]{:S(2)}) copy-start(bf16[128,512]{1,0:T(8,128)(2,1)} %w1.3) | copy-start | bytes 393220
  0.7 40.9 %copy-start.1 = (bf16[128,512]{1,0:T(8,128)(2,1)S(1)}, bf16[128,512]{1,0:T(8,128)(2,1)}, u32[]{:S(2)}) copy-start(bf16[128,512]{1,0:T(8,128)(2,1)} %w0.3) | copy-start | bytes 393220
  3.1 31.2 %all-to-all-start = ((bf16[128,5,2,128]{3,2,1,0:T(2,128)(2,1)}), bf16[128,5,2,128]{3,2,1,0:T(2,128)(2,1)}, u32[]{:S(2)}, u32[]{:S(2)}) async-start(bf16[128,5,2,128]{3,2,1,0:T(2,128)(2,1)} %place.1), calls=%async_computation | async-start | bytes 655360 | tf_op jit(solution)/shard_map/all_to_all | solution.py:26
  21.5 62.5 %copy-start = (f32[2,4,128,128]{3,2,1,0:T(8,128)S(1)}, f32[2,4,128,128]{3,2,1,0:T(8,128)}, u32[]{:S(2)}) copy-start(f32[2,4,128,128]{3,2,1,0:T(8,128)} %state_ref.1) | copy-start | bytes 1572868
  21.5 62.4 %copy-start.5 = (f32[512]{0:T(512)S(1)}, f32[512]{0:T(512)}, u32[]{:S(2)}) copy-start(f32[512]{0:T(512)} %param.24) | copy-start | bytes 6148
  21.5 62.4 %copy-start.6 = (f32[512]{0:T(512)S(1)}, f32[512]{0:T(512)}, u32[]{:S(2)}) copy-start(f32[512]{0:T(512)} %param.25) | copy-start | bytes 6148
  41.1 1.6 collective-permute-start
  88.2 74.1 %copy-start.7 = (bf16[3,16]{1,0:T(4,128)(2,1)S(1)}, bf16[3,16]{1,0:T(4,128)(2,1)}, u32[]{:S(2)}) copy-start(bf16[3,16]{1,0:T(4,128)(2,1)} %gain_hbm.1) | copy-start | bytes 292
  88.2 74.1 %copy-start.8 = (bf16[3,16]{1,0:T(4,128)(2,1)S(1)}, bf16[3,16]{1,0:T(4,128)(2,1)}, u32[]{:S(2)}) copy-start(bf16[3,16]{1,0:T(4,128)(2,1)} %bias_hbm.1) | copy-start | bytes 292
  123.9 1.6 collective-permute-start.1

commit v13 on v11

--- a/solution.py
+++ b/solution.py
@@ -454,15 +454,15 @@
     share = kv_count // chunks
     parts = sent_ref.shape[0]
     piece_chunks = kv_count // parts
-    step = weight_ref.shape[2]
-    fetches = [
-        pltpu.make_async_copy(
-            weight_hbm.at[:, pl.ds(part * step, step)], weight_ref.at[part], weight_sem.at[part]
+    step = weight_ref.shape[1] // parts
+    lines = weight_ref.shape[0] // parts
+    fetches = []
+    for part in range(parts):
+        own = pl.ds(part * lines, lines)
+        fetches.append(
+            pltpu.make_async_copy(weight_hbm.at[own], weight_ref.at[own], weight_sem.at[part])
         )
-        for part in range(parts)
-    ]
-    for fetch in fetches[: parts // 2]:
-        fetch.start()
+        fetches[-1].start()
 
     def block_rows(block):
         lines = arrived_ref[block, :chunks]
@@ -506,8 +506,6 @@
     forget = (low + (1.0 - low) * jax.nn.sigmoid(forget_pre)).T
     key = ((1.0 - low) * jax.nn.sigmoid(-forget_pre)).T
     query = jax.nn.silu(query_pre).T
-    for fetch in fetches[parts // 2 :]:
-        fetch.start()
     updated_copies = []
     for head in range(heads):
         for seq in range(seqs):
@@ -533,9 +531,11 @@
     for head in range(heads):
         gated_ref[0:2, head * HEAD : (head + 1) * HEAD] = gated[2 * head : 2 * head + 2]
     lhs = gated_ref[...].astype(bf16)
+    for fetch in fetches:
+        fetch.wait()
     for part in range(parts):
-        fetches[part].wait()
-        mixed = jnp.dot(lhs, weight_ref[part], preferred_element_type=f32)
+        weight = weight_ref[:, part * step : (part + 1) * step]
+        mixed = jnp.dot(lhs, weight, preferred_element_type=f32)
         for chunk in range(piece_chunks):
             sent_ref[part, 2 * chunk : 2 * chunk + 2, :] = mixed[
                 0:2, chunk * LANES : (chunk + 1) * LANES
@@ -559,7 +559,7 @@
         ],
         scratch_shapes=[
             pltpu.VMEM(state.shape, f32),
-            pltpu.VMEM((parts, depth, width // parts), bf16),
+            pltpu.VMEM((depth, width), bf16),
             pltpu.VMEM((seqs * 4 * heads, LANES), f32),
             pltpu.VMEM((2 * heads, LANES), f32),
             pltpu.VMEM((2 * heads, LANES), f32),

time: 164 us -> 164 us (level)
  no operation moved by 1% of the time
where the time goes in v13:
time: 164 us; the launch traced here: 163 us
  blocking collectives  114 us (70%)
  starting transfers between devices  17.7 us (11%)
  Pallas kernels  14.6 us (9%)
  waiting for transfers between devices  14.2 us (9%)
    all_to_all x8, blocking collectives, exchange(): return lax.all_to_all(blocks, axes, split_axis=0, concat_axis=0, tiled=True)  105 us
    all_to_all x1, starting transfers between devices, exchange(): return lax.all_to_all(blocks, axes, split_axis=0, concat_axis=0, tiled=True)  16.8 us
    all_to_all x1, waiting for transfers between devices, exchange(): return lax.all_to_all(blocks, axes, split_axis=0, concat_axis=0, tiled=True)  12.8 us
    all_gather x1, blocking collectives, local(): rows = lax.all_gather(arrived, CORE, axis=0)  4.83 us
    all_gather x1, blocking collectives, local(): arrived = lax.all_gather(arrived, CORE, axis=0)  4.59 us
    pallas_call x1, Pallas kernels, mixer(): pl.pallas_call(mixer_kernel, in_specs=[SMEM] + [VMEM] * 5 + [ANYWHERE], o...  4.48 us
  transfers between devices with their start and end apart: 3, of which 3 were waited for; matrix products, arithmetic and copies ran while one was open for 0% of the time, Pallas kernels for 2%

profile of v13, /device:TPU:1, one launch (start us, length us, event | category | flops | bytes accessed | tf_op | source)
XLA Modules:
  0.0 163.4 jit_solution(2314242366592340945)
XLA Ops:
  0.6 0.0 copy-start.4
  0.6 0.0 copy-start.3
  0.7 0.0 copy-start.2
  0.7 0.0 copy-start.1
  0.7 0.1 pad_add_fusion.at_ref
  0.8 2.4 %place.1 = bf16[128,5,2,128]{3,2,1,0:T(2,128)(2,1)} custom-call(s32[3]{0:T(128)S(1)} %pad_add_fusion.at_ref, bf16[16,64]{1,0:T(8,128)(2,1)} %bitcast.46, bf16[3,16]{1,0:T(4,128)(2,1)} %gain_hbm.1, bf16[3,16]{1,0:T(4,128)(2,1)} %bias_hbm.1), custom_call_target="tpu_custom_call" | custom-call | tf_op jit(solution)/shard_map/place/pallas_call | solution.py:107
  3.1 16.8 %all-to-all-start = ((bf16[128,5,2,128]{3,2,1,0:T(2,128)(2,1)}), bf16[128,5,2,128]{3,2,1,0:T(2,128)(2,1)}, u32[]{:S(2)}, u32[]{:S(2)}) async-start(bf16[128,5,2,128]{3,2,1,0:T(2,128)(2,1)} %place.1), calls=%async_computation | async-start | bytes 655360 | tf_op jit(solution)/shard_map/all_to_all | solution.py:26
  19.9 1.6 load.1
  21.5 0.0 copy-start
  21.5 0.0 copy-start.5
  21.5 0.0 copy-start.6
  21.6 12.8 %all-to-all-done = bf16[128,5,2,128]{3,2,1,0:T(2,128)(2,1)} async-done(((bf16[128,5,2,128]{3,2,1,0:T(2,128)(2,1)}), bf16[128,5,2,128]{3,2,1,0:T(2,128)(2,1)}, u32[]{:S(2)}, u32[]{:S(2)}) %all-to-all-start) | async-done | bytes 327712 | tf_op jit(solution)/shard_map/all_to_all | solution.py:26
  34.3 4.8 %all-gather = bf16[256,5,2,128]{3,2,1,0:T(2,128)(2,1)S(1)} all-gather(bf16[128,5,2,128]{3,2,1,0:T(2,128)(2,1)} %all-to-all-done), channel_id=2, replica_groups=mesh['kv_0'=8,'kv_1'=4,'tp_0'=4,'tp_1'=2] {'tp_1'}, dimensions={0}, use_global_device_ids=true | all-gather | bytes 983040 | tf_op jit(solution)/shard_map/all_gather | solution.py:604
  39.2 2.0 %first_block.1 = (bf16[32,32,128]{2,1,0:T(8,128)(2,1)S(1)}, bf16[32,32,128]{2,1,0:T(8,128)(2,1)S(1)}, f32[8,128]{1,0:T(8,128)S(1)}, f32[8,128]{1,0:T(8,128)S(1)}, f32[64,128]{1,0:T(8,128)S(1)}) custom-call(s32[3]{0:T(128)S(1)} %pad_add_fusion.at_ref, bf16[2,32,4,5,2,128]{5,4,3,2,1,0:T(2,128)(2,1)S(1)} %bitcast.29, ...), custom_call_target="tpu_custom_call" | custom-call | tf_op jit(solution)/shard_map/first_block/pallas_call | solution.py:263
  41.1 0.5 collective-permute-start
  41.6 0.0 copy-done.4
  41.6 0.0 copy-done.3
  41.6 0.0 copy-done.2
  41.6 0.0 copy-done.1
  41.6 1.0 in_order.1
  42.6 0.2 collective-permute-done.came_ref
  42.8 0.2 first_blocks.1
  42.9 15.1 %all_to_all.45 = bf16[32,17,2,128]{3,2,1,0:T(2,128)(2,1)S(1)} all-to-all(bf16[32,17,2,128]{3,2,1,0:T(2,128)(2,1)S(1)} %first_blocks.1), channel_id=1, replica_groups=mesh['kv_0'=8,'kv_1'=4,'tp_0'=4,'tp_1'=2] {'kv_0','kv_1'}, dimensions={0} | all-to-all | bytes 557056 | tf_op jit(solution)/shard_map/all_to_all | solution.py:26
  58.0 0.2 convert_reduce_fusion
  58.3 9.4 %all_to_all.46.parts_ref = bf16[8,34,128]{2,1,0:T(8,128)(2,1)S(1)} all-to-all(bf16[8,34,128]{2,1,0:T(8,128)(2,1)S(1)} %broadcast_in_dim.8), channel_id=1, replica_groups=mesh['kv_0'=8,'kv_1'=4,'tp_0'=4,'tp_1'=2] {'tp_0','tp_1'}, dimensions={0} | all-to-all | bytes 139264 | tf_op jit(solution)/shard_map/all_to_all | solution.py:26
  67.7 1.0 project.1
  68.7 15.3 %all_to_all.47.arrived_ref = bf16[32,18,2,128]{3,2,1,0:T(2,128)(2,1)S(1)} all-to-all(bf16[32,18,2,128]{3,2,1,0:T(2,128)(2,1)S(1)} %bitcast.32), channel_id=1, replica_groups=mesh['kv_0'=8,'kv_1'=4,'tp_0'=4,'tp_1'=2] {'kv_0','kv_1'}, dimensions={0} | all-to-all | bytes 589824 | tf_op jit(solution)/shard_map/all_to_all | solution.py:26
  84.0 0.0 copy-done.5
  84.0 4.5 %mixer.1 = (f32[8,8,128]{2,1,0:T(8,128)S(1)}, f32[8,128]{1,0:T(8,128)S(1)}, f32[2,4,128,128]{3,2,1,0:T(8,128)}) custom-call(s32[3]{0:T(128)S(1)} %pad_add_fusion.at_ref, bf16[32,18,2,128]{3,2,1,0:T(2,128)(2,1)S(1)} %all_to_all.47.arrived_ref, f32[32,8,128]{2,1,0:T(8,128)S(1)} %bitcast.34, f32[4,128]{1,0:T(4,128)S(1)} %bitcast.36, f32[4,128]{1,0:T(4,128)S(1)} %bitcast.37, ...), custom_call_target="tpu_custom_call" | custom-call | tf_op jit(solution)/shard_map/mixer/pallas_call | solution.py:551
  88.5 0.0 copy-start.7
  88.5 0.0 copy-start.8
  88.5 9.4 %all_to_all.48 = f32[8,8,128]{2,1,0:T(8,128)S(1)} all-to-all(f32[8,8,128]{2,1,0:T(8,128)S(1)} %get-tuple-element.178), channel_id=1, replica_groups=mesh['kv_0'=8,'kv_1'=4,'tp_0'=4,'tp_1'=2] {'tp_0','tp_1'}, dimensions={0} | all-to-all | bytes 65536 | tf_op jit(solution)/shard_map/all_to_all | solution.py:26
  98.0 19.5 %all_to_all.49 = bf16[128,8,128]{2,1,0:T(8,128)(2,1)S(1)} all-to-all(bf16[128,8,128]{2,1,0:T(8,128)(2,1)S(1)} %broadcast_in_dim.9), channel_id=1, replica_groups=mesh['kv_0'=8,'kv_1'=4,'tp_0'=4,'tp_1'=2] {'kv_0','kv_1','tp_0'}, dimensions={0} | all-to-all | bytes 524288 | tf_op jit(solution)/shard_map/all_to_all | solution.py:26
  117.4 4.6 %all-gather.1 = bf16[256,8,128]{2,1,0:T(8,128)(2,1)S(1)} all-gather(bf16[128,8,128]{2,1,0:T(8,128)(2,1)S(1)} %all_to_all.49), channel_id=3, replica_groups=mesh['kv_0'=8,'kv_1'=4,'tp_0'=4,'tp_1'=2] {'tp_1'}, dimensions={0}, use_global_device_ids=true | all-gather | bytes 786432 | tf_op jit(solution)/shard_map/all_gather | solution.py:658
  122.0 2.1 %second_block.1 = (bf16[32,32,128]{2,1,0:T(8,128)(2,1)S(1)}, bf16[32,32,128]{2,1,0:T(8,128)(2,1)S(1)}, bf16[64,128]{1,0:T(8,128)(2,1)S(1)}) custom-call(s32[3]{0:T(128)S(1)} %pad_add_fusion.at_ref, bf16[2,32,4,8,128]{4,3,2,1,0:T(8,128)(2,1)S(1)} %bitcast.31, f32[32,8,128]{2,1,0:T(8,128)S(1)} %bitcast.35, ...), custom_call_target="tpu_custom_call" | custom-call | tf_op jit(solution)/shard_map/second_block/pallas_call | solution.py:412
  124.2 0.4 collective-permute-start.1
  124.6 1.2 collective-permute-done.1
  125.8 0.1 add_convert_fusion
  125.9 14.8 %all_to_all.50 = bf16[32,32,128]{2,1,0:T(8,128)(2,1)S(1)} all-to-all(bf16[32,32,128]{2,1,0:T(8,128)(2,1)S(1)} %add_convert_fusion), channel_id=1, replica_groups=mesh['kv_0'=8,'kv_1'=4,'tp_0'=4,'tp_1'=2] {'kv_0','kv_1'}, dimensions={0} | all-to-all | bytes 524288 | tf_op jit(solution)/shard_map/all_to_all | solution.py:26
  140.7 9.3 %all_to_all.51 = bf16[8,32,128]{2,1,0:T(8,128)(2,1)S(1)} all-to-all(bf16[8,32,128]{2,1,0:T(8,128)(2,1)S(1)} %broadcast_in_dim.10), channel_id=1, replica_groups=mesh['kv_0'=8,'kv_1'=4,'tp_0'=4,'tp_1'=2] {'tp_0','tp_1'}, dimensions={0} | all-to-all | bytes 131072 | tf_op jit(solution)/shard_map/all_to_all | solution.py:26
  150.1 0.1 fusion
  150.2 0.2 multiply_reduce_fusion
  150.4 0.1 pad_maximum_fusion
  150.5 11.9 %all_to_all.52 = f32[32,1,128]{2,1,0:T(1,128)S(1)} all-to-all(f32[32,1,128]{2,1,0:T(1,128)S(1)} %broadcast_in_dim.11), channel_id=1, replica_groups=mesh['kv_0'=8,'kv_1'=4,'tp_0'=4,'tp_1'=2] {'kv_0','kv_1'}, dimensions={0} | all-to-all | bytes 32768 | tf_op jit(solution)/shard_map/all_to_all | solution.py:26
  162.4 0.1 multiply_reduce_fusion.1
  162.6 0.0 copy-done.7
  162.6 0.1 add_convert_fusion.1
  162.7 0.7 copy.24
  (19 shorter events, 0.3 us)
Async XLA Ops:
  0.6 41.0 %copy-start.4 = (bf16[128,512]{1,0:T(8,128)(2,1)S(1)}, bf16[128,512]{1,0:T(8,128)(2,1)}, u32[]{:S(2)}) copy-start(bf16[128,512]{1,0:T(8,128)(2,1)} %w3.3) | copy-start | bytes 393220
  0.6 41.0 %copy-start.3 = (bf16[128,512]{1,0:T(8,128)(2,1)S(1)}, bf16[128,512]{1,0:T(8,128)(2,1)}, u32[]{:S(2)}) copy-start(bf16[128,512]{1,0:T(8,128)(2,1)} %w2.3) | copy-start | bytes 393220
  0.7 40.9 %copy-start.2 = (bf16[128,512]{1,0:T(8,128)(2,1)S(1)}, bf16[128,512]{1,0:T(8,128)(2,1)}, u32[]{:S(2)}) copy-start(bf16[128,512]{1,0:T(8,128)(2,1)} %w1.3) | copy-start | bytes 393220
  0.7 40.9 %copy-start.1 = (bf16[128,512]{1,0:T(8,128)(2,1)S(1)}, bf16[128,512]{1,0:T(8,128)(2,1)}, u32[]{:S(2)}) copy-start(bf16[128,512]{1,0:T(8,128)(2,1)} %w0.3) | copy-start | bytes 393220
  3.1 31.2 %all-to-all-start = ((bf16[128,5,2,128]{3,2,1,0:T(2,128)(2,1)}), bf16[128,5,2,128]{3,2,1,0:T(2,128)(2,1)}, u32[]{:S(2)}, u32[]{:S(2)}) async-start(bf16[128,5,2,128]{3,2,1,0:T(2,128)(2,1)} %place.1), calls=%async_computation | async-start | bytes 655360 | tf_op jit(solution)/shard_map/all_to_all | solution.py:26
  21.5 62.5 %copy-start = (f32[2,4,128,128]{3,2,1,0:T(8,128)S(1)}, f32[2,4,128,128]{3,2,1,0:T(8,128)}, u32[]{:S(2)}) copy-start(f32[2,4,128,128]{3,2,1,0:T(8,128)} %state_ref.1) | copy-start | bytes 1572868
  21.5 62.4 %copy-start.5 = (f32[512]{0:T(512)S(1)}, f32[512]{0:T(512)}, u32[]{:S(2)}) copy-start(f32[512]{0:T(512)} %param.24) | copy-start | bytes 6148
  21.5 62.4 %copy-start.6 = (f32[512]{0:T(512)S(1)}, f32[512]{0:T(512)}, u32[]{:S(2)}) copy-start(f32[512]{0:T(512)} %param.25) | copy-start | bytes 6148
  41.1 1.6 collective-permute-start
  88.5 74.1 %copy-start.7 = (bf16[3,16]{1,0:T(4,128)(2,1)S(1)}, bf16[3,16]{1,0:T(4,128)(2,1)}, u32[]{:S(2)}) copy-start(bf16[3,16]{1,0:T(4,128)(2,1)} %gain_hbm.1) | copy-start | bytes 292
  88.5 74.1 %copy-start.8 = (bf16[3,16]{1,0:T(4,128)(2,1)S(1)}, bf16[3,16]{1,0:T(4,128)(2,1)}, u32[]{:S(2)}) copy-start(bf16[3,16]{1,0:T(4,128)(2,1)} %bias_hbm.1) | copy-start | bytes 292
  124.2 1.6 collective-permute-start.1
